TPU v7x, 512 devices: a whole 4x8x8 slice. The times are simulated.
512 devices in a mesh: fs: 64 (over z, y), tp: 8 (over x, core).
Axes of the slice: x: 4, y: 8, z: 8, core: 2. Of those that a mesh axis runs over, the one named last changes fastest.
Arguments:
- later_input: bfloat16 [12288, 2048], P(('fs', 'tp')), may hold values from -6 to 6
- earlier_input: bfloat16 [12288, 2048], P(('fs', 'tp')), may hold values from -6 to 6
- cotangent: bfloat16 [12288, 2048], P(('fs', 'tp')), may hold values from -24 to 24
- gate_weight: bfloat16 [2048, 3072], P('fs', 'tp'), may hold values from -0.125 to 0.125
- up_weight: bfloat16 [2048, 3072], P('fs', 'tp'), may hold values from -0.125 to 0.125
- down_weight: bfloat16 [2048, 3072], P('fs', 'tp'), may hold values from -0.109375 to 0.109375
- down_grad_sum: float32 [2048, 3072], P('fs', 'tp'), may hold values from -6 to 6
Outputs:
- later_output: bfloat16 [12288, 2048], P(('fs', 'tp'))
- earlier_grad_input: bfloat16 [12288, 2048], P(('fs', 'tp'))
- new_down_grad_sum: float32 [2048, 3072], P('fs', 'tp')
All inputs are finite; a program needn't handle non-finite values.
Results may differ from a plain program's by a relative error of at most 0.0057.
Values may be sent and summed in bfloat16 or wider, within the bound.
No kernel may reach another device: no remote copies, remote signals or barrier semaphores. Data moves between devices by JAX's collectives and lax.ppermute only.
A program may use at most 64 MiB of HBM per device.

v0:
```python
import jax
import jax.numpy as jnp
from jax import lax
from jax.sharding import Mesh
from jax.sharding import PartitionSpec as P


AXES = ("z", "y", "x", "c")
FS = ("z", "y")
STEPS = (0, 1, -1, 2)
BF, F32 = jnp.bfloat16, jnp.float32


def shift(value, axis, step):
    count = lax.axis_size(axis)
    if step == 0:
        return value
    return lax.ppermute(value, axis, [(i, (i + step) % count) for i in range(count)])


def spread(value, axis):
    count = lax.axis_size(axis)
    return lax.all_to_all(jnp.broadcast_to(value, (count, *value.shape)), axis, 0, 0)


def after(value, *others):
    return lax.optimization_barrier((value, *others))[0]


def gather_down(down):
    line = spread(down, "z")
    count = lax.axis_size("y")
    half = line.shape[0] // 2
    mine = lax.axis_index("y")
    whole = jnp.zeros((line.shape[0], count, *down.shape), down.dtype)

    def put(whole, chunk, offset, lead):
        at = (lead, (mine + offset) & (count - 1), 0, 0)
        return lax.dynamic_update_slice(whole, chunk[:, None], at)

    whole = put(whole, line, 0, 0)
    ahead = behind = line
    for hop in range(1, count // 2):
        ahead, behind = shift(ahead, "y", 1), shift(behind, "y", -1)
        whole = put(put(whole, ahead, -hop, 0), behind, hop, 0)
    whole = put(whole, shift(ahead[:half], "y", 1), count // 2, 0)
    whole = put(whole, shift(behind[half:], "y", -1), count // 2, half)
    return whole.reshape(-1, down.shape[1])


def collect_tokens(own):
    line = jnp.concatenate([shift(own, "x", step) for step in STEPS], axis=0)
    return jnp.concatenate([line, shift(line, "c", 1)], axis=0)


def give_rows(partial, rows):
    own, other = jnp.split(partial, 2, axis=0)
    both = (own + shift(other.astype(BF), "c", 1).astype(F32)).astype(BF)
    total = jnp.zeros((rows, partial.shape[1]), F32)
    for at, step in enumerate(STEPS):
        total += shift(both[at * rows : (at + 1) * rows], "x", -step).astype(F32)
    return total.astype(BF)


def contract_last(leading, trailing):
    return lax.dot_general(
        leading, trailing, (((1,), (1,)), ((), ())), preferred_element_type=F32
    )


def shards(later, early, cotangent, gate_w, up_w, down_w, down_grad_sum):
    rows, _ = later.shape
    line = spread(jnp.concatenate([gate_w, up_w], axis=1), "y")
    line = line.reshape(-1, line.shape[-1])
    whole = lax.all_gather(line, "z", axis=0, tiled=True)
    gate_whole, up_whole = jnp.split(whole, 2, axis=1)
    tokens = collect_tokens(jnp.concatenate([later, early, cotangent], axis=1))
    later_rows, early_rows, grad_rows = jnp.split(tokens, 3, axis=1)
    down_whole = gather_down(after(down_w, line))

    gate_early = jnp.dot(early_rows, gate_whole, preferred_element_type=F32)
    up_early = jnp.dot(early_rows, up_whole, preferred_element_type=F32)
    sig = jax.nn.sigmoid(gate_early)
    activated = gate_early * sig
    hidden_early = (activated * up_early).astype(BF)
    down_grad = lax.dot_general(
        grad_rows, hidden_early, (((0,), (0,)), ((), ())), preferred_element_type=F32
    ).astype(BF)
    received = lax.all_to_all(down_grad.reshape(-1, *gate_w.shape), FS, 0, 0)

    grad_hidden = jnp.dot(grad_rows, down_whole, preferred_element_type=F32)
    grad_gate = grad_hidden * up_early * sig * (1.0 + gate_early * (1.0 - sig))
    grad_up = grad_hidden * activated
    input_partial = contract_last(grad_gate.astype(BF), gate_whole)
    input_partial += contract_last(grad_up.astype(BF), up_whole)

    gate_later = jnp.dot(later_rows, gate_whole, preferred_element_type=F32)
    up_later = jnp.dot(later_rows, up_whole, preferred_element_type=F32)
    hidden_later = (jax.nn.silu(gate_later) * up_later).astype(BF)
    output_partial = contract_last(hidden_later, down_whole)

    both = give_rows(jnp.concatenate([output_partial, input_partial], axis=1), rows)
    later_output, earlier_grad_input = jnp.split(both, 2, axis=1)

    summed = jnp.sum(received.astype(F32), axis=0)
    factor = (rows * lax.axis_size(AXES)) ** (-0.5)
    return later_output, earlier_grad_input, down_grad_sum + summed * factor


def solution(mesh):
    split = Mesh(mesh.devices.reshape(8, 8, 4, 2), AXES)
    tokens, weights = P(AXES, None), P(FS, ("x", "c"))
    return jax.shard_map(
        shards,
        mesh=split,
        in_specs=(tokens,) * 3 + (weights,) * 4,
        out_specs=(tokens, tokens, weights),
        check_vma=False,
    )
```

profile of v0, /device:TPU:2, one launch (start us, length us, event | category | flops | bytes accessed | tf_op | source)
XLA Modules:
  0.0 182.4 jit_solution(680765771638284149)
XLA Ops:
  8.8 7.1 %all-to-all-start = ((bf16[8,32,768]{2,1,0:T(8,128)(2,1)}), bf16[8,32,768]{2,1,0:T(8,128)(2,1)S(1)}, u32[]{:S(2)}, u32[]{:S(2)}) async-start(bf16[8,32,768]{2,1,0:T(8,128)(2,1)} %broadcast_in_dim.36), calls=%async_computation | async-start | bytes 786432 | tf_op jit(solution)/shard_map/all_to_all | solution.py:23
  18.8 3.4 %collective-permute-start = (bf16[24,6144]{1,0:T(8,128)(2,1)S(1)}, bf16[24,6144]{1,0:T(8,128)(2,1)S(1)}, u32[]{:S(2)}, u32[]{:S(2)}) collective-permute-start(bf16[24,6144]{1,0:T(8,128)(2,1)S(1)} %get-tuple-element.10), channel_id=1, source_target_pairs={{0,2},{2,4},{4,6},{6,0},{1,3},{3,5},{5,7},{7,1},{8,10},{10,12},{12... | collective-permute-start | bytes 884744 | tf_op jit(solution)/shard_map/ppermute | solution.py:18
  22.2 2.7 %collective-permute-start.1 = (bf16[24,6144]{1,0:T(8,128)(2,1)S(1)}, bf16[24,6144]{1,0:T(8,128)(2,1)S(1)}, u32[]{:S(2)}, u32[]{:S(2)}) collective-permute-start(bf16[24,6144]{1,0:T(8,128)(2,1)S(1)} %get-tuple-element.10), channel_id=1, source_target_pairs={{0,6},{2,0},{4,2},{6,4},{1,7},{3,1},{5,3},{7,5},{8,14},{10,8},{12,... | collective-permute-start | bytes 884744 | tf_op jit(solution)/shard_map/ppermute | solution.py:18
  24.8 4.0 %collective-permute-start.2 = (bf16[24,6144]{1,0:T(8,128)(2,1)S(1)}, bf16[24,6144]{1,0:T(8,128)(2,1)S(1)}, u32[]{:S(2)}, u32[]{:S(2)}) collective-permute-start(bf16[24,6144]{1,0:T(8,128)(2,1)S(1)} %get-tuple-element.10), channel_id=1, source_target_pairs={{0,4},{2,6},{4,0},{6,2},{1,5},{3,7},{5,1},{7,3},{8,12},{10,14},{12... | collective-permute-start | bytes 884744 | tf_op jit(solution)/shard_map/ppermute | solution.py:18
  28.8 1.7 all-to-all-done
  31.3 2.1 %collective-permute-done.1 = bf16[24,6144]{1,0:T(8,128)(2,1)S(1)} collective-permute-done((bf16[24,6144]{1,0:T(8,128)(2,1)S(1)}, bf16[24,6144]{1,0:T(8,128)(2,1)S(1)}, u32[]{:S(2)}, u32[]{:S(2)}) %collective-permute-start.1) | collective-permute-done | bytes 294944 | tf_op jit(solution)/shard_map/ppermute | solution.py:18
  33.5 5.7 %collective-permute-done.2 = bf16[24,6144]{1,0:T(8,128)(2,1)S(1)} collective-permute-done((bf16[24,6144]{1,0:T(8,128)(2,1)S(1)}, bf16[24,6144]{1,0:T(8,128)(2,1)S(1)}, u32[]{:S(2)}, u32[]{:S(2)}) %collective-permute-start.2) | collective-permute-done | bytes 294944 | tf_op jit(solution)/shard_map/ppermute | solution.py:18
  39.3 1.9 %collective-permute-start.3 = (bf16[96,6144]{1,0:T(8,128)(2,1)S(1)}, bf16[96,6144]{1,0:T(8,128)(2,1)}, u32[]{:S(2)}, u32[]{:S(2)}) collective-permute-start(bf16[96,6144]{1,0:T(8,128)(2,1)S(1)} %pad_maximum_fusion.1), channel_id=1, source_target_pairs={{0,1},{1,0},{2,3},{3,2},{4,5},{5,4},{6,7},{7,6},{8,9},{9,8},{10,11... | collective-permute-start | bytes 3538952 | tf_op jit(solution)/shard_map/ppermute | solution.py:18
  43.4 10.3 %all-to-all-start.1 = ((bf16[8,32,384]{2,1,0:T(8,128)(2,1)}), bf16[8,32,384]{2,1,0:T(8,128)(2,1)S(1)}, u32[]{:S(2)}, u32[]{:S(2)}) async-start(bf16[8,32,384]{2,1,0:T(8,128)(2,1)} %broadcast_in_dim.38), calls=%async_computation.1 | async-start | bytes 393216 | tf_op jit(solution)/shard_map/all_to_all | solution.py:23
  54.4 12.8 %all-to-all-done.1 = bf16[8,32,384]{2,1,0:T(8,128)(2,1)S(1)} async-done(((bf16[8,32,384]{2,1,0:T(8,128)(2,1)}), bf16[8,32,384]{2,1,0:T(8,128)(2,1)S(1)}, u32[]{:S(2)}, u32[]{:S(2)}) %all-to-all-start.1) | async-done | bytes 196640 | tf_op jit(solution)/shard_map/all_to_all | solution.py:23
  67.2 3.8 %collective-permute-start.4 = (bf16[8,32,384]{2,1,0:T(8,128)(2,1)S(1)}, bf16[8,32,384]{2,1,0:T(8,128)(2,1)S(1)}, u32[]{:S(2)}, u32[]{:S(2)}) collective-permute-start(bf16[8,32,384]{2,1,0:T(8,128)(2,1)S(1)} %all-to-all-done.1), channel_id=1, source_target_pairs={{0,8},{8,16},{16,24},{24,32},{32,40},{40,48},{48,56},{56,0},{1,9},... | collective-permute-start | bytes 589832 | tf_op jit(solution)/shard_map/ppermute | solution.py:18
  71.0 3.4 %collective-permute-start.5 = (bf16[8,32,384]{2,1,0:T(8,128)(2,1)S(1)}, bf16[8,32,384]{2,1,0:T(8,128)(2,1)S(1)}, u32[]{:S(2)}, u32[]{:S(2)}) collective-permute-start(bf16[8,32,384]{2,1,0:T(8,128)(2,1)S(1)} %all-to-all-done.1), channel_id=1, source_target_pairs={{0,56},{8,0},{16,8},{24,16},{32,24},{40,32},{48,40},{56,48},{1,57}... | collective-permute-start | bytes 589832 | tf_op jit(solution)/shard_map/ppermute | solution.py:18
  74.6 2.4 %collective-permute-done.4 = bf16[8,32,384]{2,1,0:T(8,128)(2,1)S(1)} collective-permute-done((bf16[8,32,384]{2,1,0:T(8,128)(2,1)S(1)}, bf16[8,32,384]{2,1,0:T(8,128)(2,1)S(1)}, u32[]{:S(2)}, u32[]{:S(2)}) %collective-permute-start.4) | collective-permute-done | bytes 196640 | tf_op jit(solution)/shard_map/ppermute | solution.py:18
  77.1 2.3 %collective-permute-start.6 = (bf16[8,32,384]{2,1,0:T(8,128)(2,1)S(1)}, bf16[8,32,384]{2,1,0:T(8,128)(2,1)S(1)}, u32[]{:S(2)}, u32[]{:S(2)}) collective-permute-start(bf16[8,32,384]{2,1,0:T(8,128)(2,1)S(1)} %collective-permute-done.4), channel_id=1, source_target_pairs={{0,8},{8,16},{16,24},{24,32},{32,40},{40,48},{48,56},{56,0},{1,9},... | collective-permute-start | bytes 589832 | tf_op jit(solution)/shard_map/ppermute | solution.py:18
  79.4 4.7 %collective-permute-start.7 = (bf16[8,32,384]{2,1,0:T(8,128)(2,1)S(1)}, bf16[8,32,384]{2,1,0:T(8,128)(2,1)S(1)}, u32[]{:S(2)}, u32[]{:S(2)}) collective-permute-start(bf16[8,32,384]{2,1,0:T(8,128)(2,1)S(1)} %collective-permute-done.5), channel_id=1, source_target_pairs={{0,56},{8,0},{16,8},{24,16},{32,24},{40,32},{48,40},{56,48},{1,57}... | collective-permute-start | bytes 589832 | tf_op jit(solution)/shard_map/ppermute | solution.py:18
  84.2 1.8 collective-permute-done.6
  86.0 1.9 %collective-permute-start.8 = (bf16[8,32,384]{2,1,0:T(8,128)(2,1)S(1)}, bf16[8,32,384]{2,1,0:T(8,128)(2,1)S(1)}, u32[]{:S(2)}, u32[]{:S(2)}) collective-permute-start(bf16[8,32,384]{2,1,0:T(8,128)(2,1)S(1)} %collective-permute-done.6), channel_id=1, source_target_pairs={{0,8},{8,16},{16,24},{24,32},{32,40},{40,48},{48,56},{56,0},{1,9},... | collective-permute-start | bytes 589832 | tf_op jit(solution)/shard_map/ppermute | solution.py:18
  87.9 5.1 %collective-permute-start.9 = (bf16[8,32,384]{2,1,0:T(8,128)(2,1)S(1)}, bf16[8,32,384]{2,1,0:T(8,128)(2,1)S(1)}, u32[]{:S(2)}, u32[]{:S(2)}) collective-permute-start(bf16[8,32,384]{2,1,0:T(8,128)(2,1)S(1)} %collective-permute-done.7), channel_id=1, source_target_pairs={{0,56},{8,0},{16,8},{24,16},{32,24},{40,32},{48,40},{56,48},{1,57}... | collective-permute-start | bytes 589832 | tf_op jit(solution)/shard_map/ppermute | solution.py:18
  94.8 1.9 %collective-permute-start.10 = (bf16[4,32,384]{2,1,0:T(8,128)(2,1)S(1)}, bf16[4,32,384]{2,1,0:T(8,128)(2,1)S(1)}, u32[]{:S(2)}, u32[]{:S(2)}) collective-permute-start(bf16[4,32,384]{2,1,0:T(8,128)(2,1)S(1)} %slice.24), channel_id=1, source_target_pairs={{0,8},{8,16},{16,24},{24,32},{32,40},{40,48},{48,56},{56,0},{1,9},... | collective-permute-start | bytes 294920 | tf_op jit(solution)/shard_map/ppermute | solution.py:18
  96.7 5.1 %collective-permute-start.11 = (bf16[4,32,384]{2,1,0:T(8,128)(2,1)S(1)}, bf16[4,32,384]{2,1,0:T(8,128)(2,1)S(1)}, u32[]{:S(2)}, u32[]{:S(2)}) collective-permute-start(bf16[4,32,384]{2,1,0:T(8,128)(2,1)S(1)} %slice.25), channel_id=1, source_target_pairs={{0,56},{8,0},{16,8},{24,16},{32,24},{40,32},{48,40},{56,48},{1,57}... | collective-permute-start | bytes 294920 | tf_op jit(solution)/shard_map/ppermute | solution.py:18
  105.9 2.4 %fusion.11 = f32[192,384]{1,0:T(8,128)S(1)} fusion(bf16[2048,768]{1,0:T(8,128)(2,1)} %all-gather.2.cloned.1.call-done, bf16[192,6144]{1,0:T(8,128)(2,1)} %copy-done.11), kind=kOutput, calls=%fused_computation.17 | convolution fusion | flops 301989888 | bytes 2654208 | tf_op jit(solution)/shard_map/dot_general | solution.py:81
  110.2 2.5 %fusion.7 = f32[192,384]{1,0:T(8,128)} fusion(bf16[2048,768]{1,0:T(8,128)(2,1)S(1)} %copy-done.1, bf16[192,6144]{1,0:T(8,128)(2,1)} %copy-done.11), kind=kOutput, calls=%fused_computation.13 | convolution fusion | flops 301989888 | bytes 2654208 | tf_op jit(solution)/shard_map/dot_general | solution.py:98
  114.2 3.4 %fusion.23 = f32[192,2048]{1,0:T(8,128)S(1)} fusion(bf16[2048,384]{1,0:T(8,128)(2,1)} %bitcast.41, f32[192,384]{1,0:T(8,128)} %fusion.7, bf16[2048,768]{1,0:T(8,128)(2,1)} %all-gather.2.cloned.1.call-done, bf16[192,6144]{1,0:T(8,128)(2,1)} %copy-done.11), kind=kOutput, calls=%fused_computation.43 | convolution fusion | flops 604422144 | bytes 5799936 | tf_op jit(solution)/shard_map/dot_general | solution.py:66
  119.1 1.9 %collective-permute-start.12 = (bf16[96,4096]{1,0:T(8,128)(2,1)}, bf16[96,4096]{1,0:T(8,128)(2,1)}, u32[]{:S(2)}, u32[]{:S(2)}) collective-permute-start(bf16[96,4096]{1,0:T(8,128)(2,1)} %fusion.3), channel_id=1, source_target_pairs={{0,1},{1,0},{2,3},{3,2},{4,5},{5,4},{6,7},{7,6},{8,9},{9,8},{10,11... | collective-permute-start | bytes 2359304 | tf_op jit(solution)/shard_map/ppermute | solution.py:18
  121.0 3.1 %convolution_convert_fusion = bf16[2048,384]{1,0:T(8,128)(2,1)} fusion(bf16[192,6144]{1,0:T(8,128)(2,1)} %copy-done.11, f32[192,384]{1,0:T(8,128)S(1)} %copy-done.5, f32[192,384]{1,0:T(8,128)S(1)} %fusion.11), kind=kOutput, calls=%fused_computation.3 | convolution fusion | flops 303218688 | bytes 2949120 | tf_op jit(solution)/shard_map/dot_general | solution.py:86
  124.1 8.7 %all-to-all-start.2 = ((bf16[64,32,384]{2,1,0:T(8,128)(2,1)}), bf16[64,32,384]{2,1,0:T(8,128)(2,1)S(1)}, u32[]{:S(2)}, u32[]{:S(2)}) async-start(bf16[64,32,384]{2,1,0:T(8,128)(2,1)} %bitcast.39), calls=%async_computation.2 | async-start | bytes 3145728 | tf_op jit(solution)/shard_map/all_to_all | solution.py:89
  134.4 2.1 %collective-permute-start.13 = (bf16[24,4096]{1,0:T(8,128)(2,1)S(1)}, bf16[24,4096]{1,0:T(8,128)(2,1)S(1)}, u32[]{:S(2)}, u32[]{:S(2)}) collective-permute-start(bf16[24,4096]{1,0:T(8,128)(2,1)S(1)} %get-tuple-element.5), channel_id=1, source_target_pairs={{0,6},{2,0},{4,2},{6,4},{1,7},{3,1},{5,3},{7,5},{8,14},{10,8},{12,... | collective-permute-start | bytes 589832 | tf_op jit(solution)/shard_map/ppermute | solution.py:18
  136.5 3.9 %collective-permute-start.14 = (bf16[24,4096]{1,0:T(8,128)(2,1)S(1)}, bf16[24,4096]{1,0:T(8,128)(2,1)S(1)}, u32[]{:S(2)}, u32[]{:S(2)}) collective-permute-start(bf16[24,4096]{1,0:T(8,128)(2,1)S(1)} %get-tuple-element.7), channel_id=1, source_target_pairs={{0,2},{2,4},{4,6},{6,0},{1,3},{3,5},{5,7},{7,1},{8,10},{10,12},{12... | collective-permute-start | bytes 589832 | tf_op jit(solution)/shard_map/ppermute | solution.py:18
  140.4 4.9 %collective-permute-start.15 = (bf16[24,4096]{1,0:T(8,128)(2,1)S(1)}, bf16[24,4096]{1,0:T(8,128)(2,1)S(1)}, u32[]{:S(2)}, u32[]{:S(2)}) collective-permute-start(bf16[24,4096]{1,0:T(8,128)(2,1)S(1)} %get-tuple-element.6), channel_id=1, source_target_pairs={{0,4},{2,6},{4,0},{6,2},{1,5},{3,7},{5,1},{7,3},{8,12},{10,14},{12... | collective-permute-start | bytes 589832 | tf_op jit(solution)/shard_map/ppermute | solution.py:18
  145.3 1.7 collective-permute-done.14
  147.1 3.2 %collective-permute-done.15 = bf16[24,4096]{1,0:T(8,128)(2,1)S(1)} collective-permute-done((bf16[24,4096]{1,0:T(8,128)(2,1)S(1)}, bf16[24,4096]{1,0:T(8,128)(2,1)S(1)}, u32[]{:S(2)}, u32[]{:S(2)}) %collective-permute-start.15) | collective-permute-done | bytes 196640 | tf_op jit(solution)/shard_map/ppermute | solution.py:18
  151.1 23.6 %all-to-all-done.2 = bf16[64,32,384]{2,1,0:T(8,128)(2,1)S(1)} async-done(((bf16[64,32,384]{2,1,0:T(8,128)(2,1)}), bf16[64,32,384]{2,1,0:T(8,128)(2,1)S(1)}, u32[]{:S(2)}, u32[]{:S(2)}) %all-to-all-start.2) | async-done | bytes 1572896 | tf_op jit(solution)/shard_map/all_to_all | solution.py:89
  (71 shorter events, 22.2 us)
Async XLA Ops:
  7.2 10.3 %copy-start.6 = (bf16[24,2048]{1,0:T(8,128)(2,1)S(1)}, bf16[24,2048]{1,0:T(8,128)(2,1)}, u32[]{:S(2)}) copy-start(bf16[24,2048]{1,0:T(8,128)(2,1)} %param.8) | copy-start | bytes 294916
  7.2 10.9 %copy-start.7 = (bf16[24,2048]{1,0:T(8,128)(2,1)S(1)}, bf16[24,2048]{1,0:T(8,128)(2,1)}, u32[]{:S(2)}) copy-start(bf16[24,2048]{1,0:T(8,128)(2,1)} %param.9) | copy-start | bytes 294916
  8.8 21.8 %all-to-all-start = ((bf16[8,32,768]{2,1,0:T(8,128)(2,1)}), bf16[8,32,768]{2,1,0:T(8,128)(2,1)S(1)}, u32[]{:S(2)}, u32[]{:S(2)}) async-start(bf16[8,32,768]{2,1,0:T(8,128)(2,1)} %broadcast_in_dim.36), calls=%async_computation | async-start | bytes 786432 | tf_op jit(solution)/shard_map/all_to_all | solution.py:23
  15.9 90.0 %all-gather.2.cloned.1.call-start = ((), (), s32[]{:S(2)}) async-start(), calls=%async_computation.3 | async-start | bytes 3538944 | tf_op jit(solution)/shard_map/all_gather | solution.py:75
  18.8 12.6 %collective-permute-start = (bf16[24,6144]{1,0:T(8,128)(2,1)S(1)}, bf16[24,6144]{1,0:T(8,128)(2,1)S(1)}, u32[]{:S(2)}, u32[]{:S(2)}) collective-permute-start(bf16[24,6144]{1,0:T(8,128)(2,1)S(1)} %get-tuple-element.10), channel_id=1, source_target_pairs={{0,2},{2,4},{4,6},{6,0},{1,3},{3,5},{5,7},{7,1},{8,10},{10,12},{12... | collective-permute-start | bytes 884744 | tf_op jit(solution)/shard_map/ppermute | solution.py:18
  22.2 11.3 %collective-permute-start.1 = (bf16[24,6144]{1,0:T(8,128)(2,1)S(1)}, bf16[24,6144]{1,0:T(8,128)(2,1)S(1)}, u32[]{:S(2)}, u32[]{:S(2)}) collective-permute-start(bf16[24,6144]{1,0:T(8,128)(2,1)S(1)} %get-tuple-element.10), channel_id=1, source_target_pairs={{0,6},{2,0},{4,2},{6,4},{1,7},{3,1},{5,3},{7,5},{8,14},{10,8},{12,... | collective-permute-start | bytes 884744 | tf_op jit(solution)/shard_map/ppermute | solution.py:18
  24.8 14.4 %collective-permute-start.2 = (bf16[24,6144]{1,0:T(8,128)(2,1)S(1)}, bf16[24,6144]{1,0:T(8,128)(2,1)S(1)}, u32[]{:S(2)}, u32[]{:S(2)}) collective-permute-start(bf16[24,6144]{1,0:T(8,128)(2,1)S(1)} %get-tuple-element.10), channel_id=1, source_target_pairs={{0,4},{2,6},{4,0},{6,2},{1,5},{3,7},{5,1},{7,3},{8,12},{10,14},{12... | collective-permute-start | bytes 884744 | tf_op jit(solution)/shard_map/ppermute | solution.py:18
  30.6 0.7 copy-start.3
  31.3 11.3 %copy-start.9 = (bf16[32,384]{1,0:T(8,128)(2,1)S(1)}, bf16[32,384]{1,0:T(8,128)(2,1)}, u32[]{:S(2)}) copy-start(bf16[32,384]{1,0:T(8,128)(2,1)} %param.12) | copy-start | bytes 73732
  39.3 53.9 %collective-permute-start.3 = (bf16[96,6144]{1,0:T(8,128)(2,1)S(1)}, bf16[96,6144]{1,0:T(8,128)(2,1)}, u32[]{:S(2)}, u32[]{:S(2)}) collective-permute-start(bf16[96,6144]{1,0:T(8,128)(2,1)S(1)} %pad_maximum_fusion.1), channel_id=1, source_target_pairs={{0,1},{1,0},{2,3},{3,2},{4,5},{5,4},{6,7},{7,6},{8,9},{9,8},{10,11... | collective-permute-start | bytes 3538952 | tf_op jit(solution)/shard_map/ppermute | solution.py:18
  43.4 23.9 %all-to-all-start.1 = ((bf16[8,32,384]{2,1,0:T(8,128)(2,1)}), bf16[8,32,384]{2,1,0:T(8,128)(2,1)S(1)}, u32[]{:S(2)}, u32[]{:S(2)}) async-start(bf16[8,32,384]{2,1,0:T(8,128)(2,1)} %broadcast_in_dim.38), calls=%async_computation.1 | async-start | bytes 393216 | tf_op jit(solution)/shard_map/all_to_all | solution.py:23
  67.2 25.9 %copy-start.10 = (bf16[192,6144]{1,0:T(8,128)(2,1)S(1)}, bf16[192,6144]{1,0:T(8,128)(2,1)}, u32[]{:S(2)}) copy-start(bf16[192,6144]{1,0:T(8,128)(2,1)} %constant_dynamic-update-slice_fusion.4) | copy-start | bytes 7077892
  67.2 9.8 %collective-permute-start.4 = (bf16[8,32,384]{2,1,0:T(8,128)(2,1)S(1)}, bf16[8,32,384]{2,1,0:T(8,128)(2,1)S(1)}, u32[]{:S(2)}, u32[]{:S(2)}) collective-permute-start(bf16[8,32,384]{2,1,0:T(8,128)(2,1)S(1)} %all-to-all-done.1), channel_id=1, source_target_pairs={{0,8},{8,16},{16,24},{24,32},{32,40},{40,48},{48,56},{56,0},{1,9},... | collective-permute-start | bytes 589832 | tf_op jit(solution)/shard_map/ppermute | solution.py:18
  71.0 8.4 %collective-permute-start.5 = (bf16[8,32,384]{2,1,0:T(8,128)(2,1)S(1)}, bf16[8,32,384]{2,1,0:T(8,128)(2,1)S(1)}, u32[]{:S(2)}, u32[]{:S(2)}) collective-permute-start(bf16[8,32,384]{2,1,0:T(8,128)(2,1)S(1)} %all-to-all-done.1), channel_id=1, source_target_pairs={{0,56},{8,0},{16,8},{24,16},{32,24},{40,32},{48,40},{56,48},{1,57}... | collective-permute-start | bytes 589832 | tf_op jit(solution)/shard_map/ppermute | solution.py:18
  77.1 8.9 %collective-permute-start.6 = (bf16[8,32,384]{2,1,0:T(8,128)(2,1)S(1)}, bf16[8,32,384]{2,1,0:T(8,128)(2,1)S(1)}, u32[]{:S(2)}, u32[]{:S(2)}) collective-permute-start(bf16[8,32,384]{2,1,0:T(8,128)(2,1)S(1)} %collective-permute-done.4), channel_id=1, source_target_pairs={{0,8},{8,16},{16,24},{24,32},{32,40},{40,48},{48,56},{56,0},{1,9},... | collective-permute-start | bytes 589832 | tf_op jit(solution)/shard_map/ppermute | solution.py:18
  79.4 8.5 %collective-permute-start.7 = (bf16[8,32,384]{2,1,0:T(8,128)(2,1)S(1)}, bf16[8,32,384]{2,1,0:T(8,128)(2,1)S(1)}, u32[]{:S(2)}, u32[]{:S(2)}) collective-permute-start(bf16[8,32,384]{2,1,0:T(8,128)(2,1)S(1)} %collective-permute-done.5), channel_id=1, source_target_pairs={{0,56},{8,0},{16,8},{24,16},{32,24},{40,32},{48,40},{56,48},{1,57}... | collective-permute-start | bytes 589832 | tf_op jit(solution)/shard_map/ppermute | solution.py:18
  86.0 8.8 %collective-permute-start.8 = (bf16[8,32,384]{2,1,0:T(8,128)(2,1)S(1)}, bf16[8,32,384]{2,1,0:T(8,128)(2,1)S(1)}, u32[]{:S(2)}, u32[]{:S(2)}) collective-permute-start(bf16[8,32,384]{2,1,0:T(8,128)(2,1)S(1)} %collective-permute-done.6), channel_id=1, source_target_pairs={{0,8},{8,16},{16,24},{24,32},{32,40},{40,48},{48,56},{56,0},{1,9},... | collective-permute-start | bytes 589832 | tf_op jit(solution)/shard_map/ppermute | solution.py:18
  87.9 8.8 %collective-permute-start.9 = (bf16[8,32,384]{2,1,0:T(8,128)(2,1)S(1)}, bf16[8,32,384]{2,1,0:T(8,128)(2,1)S(1)}, u32[]{:S(2)}, u32[]{:S(2)}) collective-permute-start(bf16[8,32,384]{2,1,0:T(8,128)(2,1)S(1)} %collective-permute-done.7), channel_id=1, source_target_pairs={{0,56},{8,0},{16,8},{24,16},{32,24},{40,32},{48,40},{56,48},{1,57}... | collective-permute-start | bytes 589832 | tf_op jit(solution)/shard_map/ppermute | solution.py:18
  94.5 9.6 %copy-start.11 = (bf16[192,6144]{1,0:T(8,128)(2,1)}, bf16[192,6144]{1,0:T(8,128)(2,1)S(1)}, u32[]{:S(2)}) copy-start(bf16[192,6144]{1,0:T(8,128)(2,1)S(1)} %constant_dynamic-update-slice_fusion.3) | copy-start | bytes 7077892
  94.8 7.7 %collective-permute-start.10 = (bf16[4,32,384]{2,1,0:T(8,128)(2,1)S(1)}, bf16[4,32,384]{2,1,0:T(8,128)(2,1)S(1)}, u32[]{:S(2)}, u32[]{:S(2)}) collective-permute-start(bf16[4,32,384]{2,1,0:T(8,128)(2,1)S(1)} %slice.24), channel_id=1, source_target_pairs={{0,8},{8,16},{16,24},{24,32},{32,40},{40,48},{48,56},{56,0},{1,9},... | collective-permute-start | bytes 294920 | tf_op jit(solution)/shard_map/ppermute | solution.py:18
  96.7 7.3 %collective-permute-start.11 = (bf16[4,32,384]{2,1,0:T(8,128)(2,1)S(1)}, bf16[4,32,384]{2,1,0:T(8,128)(2,1)S(1)}, u32[]{:S(2)}, u32[]{:S(2)}) collective-permute-start(bf16[4,32,384]{2,1,0:T(8,128)(2,1)S(1)} %slice.25), channel_id=1, source_target_pairs={{0,56},{8,0},{16,8},{24,16},{32,24},{40,32},{48,40},{56,48},{1,57}... | collective-permute-start | bytes 294920 | tf_op jit(solution)/shard_map/ppermute | solution.py:18
  104.1 1.2 copy-start.2
  105.8 2.6 %copy-start.1 = (bf16[2048,768]{1,0:T(8,128)(2,1)S(1)}, bf16[2048,768]{1,0:T(8,128)(2,1)}, u32[]{:S(2)}) copy-start(bf16[2048,768]{1,0:T(8,128)(2,1)} %all-gather.2.cloned.1.call-done) | copy-start | bytes 9437188
  110.1 2.5 %copy-start.4 = (f32[192,384]{1,0:T(8,128)}, f32[192,384]{1,0:T(8,128)S(1)}, u32[]{:S(2)}) copy-start(f32[192,384]{1,0:T(8,128)S(1)} %fusion.5) | copy-start | bytes 884740
  117.6 1.5 copy-start
  117.6 3.4 %copy-start.5 = (f32[192,384]{1,0:T(8,128)S(1)}, f32[192,384]{1,0:T(8,128)}, u32[]{:S(2)}) copy-start(f32[192,384]{1,0:T(8,128)} %copy-done.4) | copy-start | bytes 884740
  119.1 13.8 %collective-permute-start.12 = (bf16[96,4096]{1,0:T(8,128)(2,1)}, bf16[96,4096]{1,0:T(8,128)(2,1)}, u32[]{:S(2)}, u32[]{:S(2)}) collective-permute-start(bf16[96,4096]{1,0:T(8,128)(2,1)} %fusion.3), channel_id=1, source_target_pairs={{0,1},{1,0},{2,3},{3,2},{4,5},{5,4},{6,7},{7,6},{8,9},{9,8},{10,11... | collective-permute-start | bytes 2359304 | tf_op jit(solution)/shard_map/ppermute | solution.py:18
  124.1 50.6 %all-to-all-start.2 = ((bf16[64,32,384]{2,1,0:T(8,128)(2,1)}), bf16[64,32,384]{2,1,0:T(8,128)(2,1)S(1)}, u32[]{:S(2)}, u32[]{:S(2)}) async-start(bf16[64,32,384]{2,1,0:T(8,128)(2,1)} %bitcast.39), calls=%async_computation.2 | async-start | bytes 3145728 | tf_op jit(solution)/shard_map/all_to_all | solution.py:89
  134.4 40.5 %copy-start.8 = (f32[32,384]{1,0:T(8,128)S(1)}, f32[32,384]{1,0:T(8,128)}, u32[]{:S(2)}) copy-start(f32[32,384]{1,0:T(8,128)} %param.13) | copy-start | bytes 147460
  134.4 10.9 %collective-permute-start.13 = (bf16[24,4096]{1,0:T(8,128)(2,1)S(1)}, bf16[24,4096]{1,0:T(8,128)(2,1)S(1)}, u32[]{:S(2)}, u32[]{:S(2)}) collective-permute-start(bf16[24,4096]{1,0:T(8,128)(2,1)S(1)} %get-tuple-element.5), channel_id=1, source_target_pairs={{0,6},{2,0},{4,2},{6,4},{1,7},{3,1},{5,3},{7,5},{8,14},{10,8},{12,... | collective-permute-start | bytes 589832 | tf_op jit(solution)/shard_map/ppermute | solution.py:18
  136.5 10.6 %collective-permute-start.14 = (bf16[24,4096]{1,0:T(8,128)(2,1)S(1)}, bf16[24,4096]{1,0:T(8,128)(2,1)S(1)}, u32[]{:S(2)}, u32[]{:S(2)}) collective-permute-start(bf16[24,4096]{1,0:T(8,128)(2,1)S(1)} %get-tuple-element.7), channel_id=1, source_target_pairs={{0,2},{2,4},{4,6},{6,0},{1,3},{3,5},{5,7},{7,1},{8,10},{10,12},{12... | collective-permute-start | bytes 589832 | tf_op jit(solution)/shard_map/ppermute | solution.py:18
  140.4 9.9 %collective-permute-start.15 = (bf16[24,4096]{1,0:T(8,128)(2,1)S(1)}, bf16[24,4096]{1,0:T(8,128)(2,1)S(1)}, u32[]{:S(2)}, u32[]{:S(2)}) collective-permute-start(bf16[24,4096]{1,0:T(8,128)(2,1)S(1)} %get-tuple-element.6), channel_id=1, source_target_pairs={{0,4},{2,6},{4,0},{6,2},{1,5},{3,7},{5,1},{7,3},{8,12},{10,14},{12... | collective-permute-start | bytes 589832 | tf_op jit(solution)/shard_map/ppermute | solution.py:18
Sparse Core Ops, SparseCore 0:
  31.4 54.9 all-gather.1
where the time goes:
time: 184 us; the launch traced here: 182 us
  starting transfers between devices  79.2 us (43%)
  waiting for transfers between devices  57.5 us (31%)
  matrix products  15.2 us (8%)
  between operations  14.5 us (8%)
  local copies, waits for them, and re-layouts  11.7 us (6%)
  other arithmetic  4.33 us (2%)
    ppermute x16, starting transfers between devices, shift(): lax.ppermute(value, axis, [(i, (i + step) % count) for i in range(count)])  53 us
    all_to_all x1, waiting for transfers between devices, shards(): received = lax.all_to_all(down_grad.reshape(-1, *gate_w.shape), FS, 0, 0)  23.6 us
    ppermute x16, waiting for transfers between devices, shift(): lax.ppermute(value, axis, [(i, (i + step) % count) for i in range(count)])  19.3 us
    all_to_all x2, starting transfers between devices, spread(): lax.all_to_all(jnp.broadcast_to(value, (count, *value.shape)), axis, 0, 0)  17.4 us
    all_to_all x2, waiting for transfers between devices, spread(): lax.all_to_all(jnp.broadcast_to(value, (count, *value.shape)), axis, 0, 0)  14.5 us
    all_to_all x1, starting transfers between devices, shards(): received = lax.all_to_all(down_grad.reshape(-1, *gate_w.shape), FS, 0, 0)  8.75 us
    unnamed x29, local copies, waits for them, and re-layouts  7 us
    dot_general x3, matrix products, contract_last(): lax.dot_general(leading, trailing, (((1,), (1,)), ((), ())), preferred_el...  4.93 us
  transfers between devices with their start and end apart: 20, of which 12 were waited for; matrix products, arithmetic and copies ran while one was open for 7% of the time, Pallas kernels for 0%

commit v1 on v0

--- a/solution.py
+++ b/solution.py
@@ -23,16 +23,21 @@
     return lax.all_to_all(jnp.broadcast_to(value, (count, *value.shape)), axis, 0, 0)
 
 
-def after(value, *others):
-    return lax.optimization_barrier((value, *others))[0]
+def line_of(value, axis):
+    count = lax.axis_size(axis)
+    mine = lax.axis_index(axis)
+    whole = jnp.zeros((count, *value.shape), value.dtype)
+    for step in range(count):
+        at = ((mine + step) & (count - 1), 0, 0)
+        whole = lax.dynamic_update_slice(whole, shift(value, axis, -step)[None], at)
+    return whole
 
 
-def gather_down(down):
-    line = spread(down, "z")
+def ring_gather(line):
     count = lax.axis_size("y")
     half = line.shape[0] // 2
     mine = lax.axis_index("y")
-    whole = jnp.zeros((line.shape[0], count, *down.shape), down.dtype)
+    whole = jnp.zeros((line.shape[0], count, *line.shape[1:]), line.dtype)
 
     def put(whole, chunk, offset, lead):
         at = (lead, (mine + offset) & (count - 1), 0, 0)
@@ -45,7 +50,7 @@
         whole = put(put(whole, ahead, -hop, 0), behind, hop, 0)
     whole = put(whole, shift(ahead[:half], "y", 1), count // 2, 0)
     whole = put(whole, shift(behind[half:], "y", -1), count // 2, half)
-    return whole.reshape(-1, down.shape[1])
+    return whole.reshape(-1, line.shape[-1])
 
 
 def collect_tokens(own):
@@ -74,9 +79,11 @@
     line = line.reshape(-1, line.shape[-1])
     whole = lax.all_gather(line, "z", axis=0, tiled=True)
     gate_whole, up_whole = jnp.split(whole, 2, axis=1)
-    tokens = collect_tokens(jnp.concatenate([later, early, cotangent], axis=1))
+    down_line = line_of(down_w, "z")
+    down_whole = ring_gather(down_line)
+    tokens = jnp.concatenate([later, early, cotangent], axis=1)
+    tokens = collect_tokens(tokens)
     later_rows, early_rows, grad_rows = jnp.split(tokens, 3, axis=1)
-    down_whole = gather_down(after(down_w, line))
 
     gate_early = jnp.dot(early_rows, gate_whole, preferred_element_type=F32)
     up_early = jnp.dot(early_rows, up_whole, preferred_element_type=F32)

time: 184 us -> 213 us (1.16)
  starting transfers between devices: 79.2 us -> 103 us
  waiting for transfers between devices: 57.5 us -> 61.1 us
    ppermute x16 -> x23, starting transfers between devices: 53 us -> 86.1 us  [shift(): lax.ppermute(value, axis, [(i, (i + step) % count) for i in range(count)])]
    all_gather x1, waiting for transfers between devices: 0.02 us -> 19.3 us  [shards(): whole = lax.all_gather(line, 'z', axis=0, tiled=True)]
    all_to_all x2 -> x1, waiting for transfers between devices: 14.5 us -> 0.01 us  [spread(): lax.all_to_all(jnp.broadcast_to(value, (count, *value.shape)), axis, 0, 0)]
    all_to_all x2 -> x1, starting transfers between devices: 17.4 us -> 7.1 us  [spread(): lax.all_to_all(jnp.broadcast_to(value, (count, *value.shape)), axis, 0, 0)]
    ppermute x16 -> x23, waiting for transfers between devices: 19.3 us -> 18.2 us  [shift(): lax.ppermute(value, axis, [(i, (i + step) % count) for i in range(count)])]
    unnamed x29 -> x27, local copies, waits for them, and re-layouts: 7 us -> 6.09 us
  transfers between devices with their start and end apart: 20 -> 26, of which waited for: 12 -> 12; matrix products, arithmetic and copies ran while one was open for 7% -> 5% of each run, Pallas kernels for 0% -> 0%
where the time goes in v1:
time: 213 us; the launch traced here: 211 us
  starting transfers between devices  103 us (48%)
  waiting for transfers between devices  61.1 us (29%)
  matrix products  16.1 us (8%)
  between operations  14.7 us (7%)
  local copies, waits for them, and re-layouts  11.8 us (6%)
  other arithmetic  4.31 us (2%)
    ppermute x23, starting transfers between devices, shift(): lax.ppermute(value, axis, [(i, (i + step) % count) for i in range(count)])  86.1 us
    all_to_all x1, waiting for transfers between devices, shards(): received = lax.all_to_all(down_grad.reshape(-1, *gate_w.shape), FS, 0, 0)  23.6 us
    all_gather x1, waiting for transfers between devices, shards(): whole = lax.all_gather(line, 'z', axis=0, tiled=True)  19.3 us
    ppermute x23, waiting for transfers between devices, shift(): lax.ppermute(value, axis, [(i, (i + step) % count) for i in range(count)])  18.2 us
    all_to_all x1, starting transfers between devices, shards(): received = lax.all_to_all(down_grad.reshape(-1, *gate_w.shape), FS, 0, 0)  10 us
    all_to_all x1, starting transfers between devices, spread(): lax.all_to_all(jnp.broadcast_to(value, (count, *value.shape)), axis, 0, 0)  7.1 us
    unnamed x27, local copies, waits for them, and re-layouts  6.09 us
    dot_general x3, matrix products, contract_last(): lax.dot_general(leading, trailing, (((1,), (1,)), ((), ())), preferred_el...  5.87 us
  transfers between devices with their start and end apart: 26, of which 12 were waited for; matrix products, arithmetic and copies ran while one was open for 5% of the time, Pallas kernels for 0%

profile of v1, /device:TPU:2, one launch (start us, length us, event | category | flops | bytes accessed | tf_op | source)
XLA Modules:
  0.0 211.3 jit_solution(14580116958410451449)
XLA Ops:
  11.8 3.4 %collective-permute-start = (bf16[24,6144]{1,0:T(8,128)(2,1)S(1)}, bf16[24,6144]{1,0:T(8,128)(2,1)S(1)}, u32[]{:S(2)}, u32[]{:S(2)}) collective-permute-start(bf16[24,6144]{1,0:T(8,128)(2,1)S(1)} %get-tuple-element.8), channel_id=1, source_target_pairs={{0,2},{2,4},{4,6},{6,0},{1,3},{3,5},{5,7},{7,1},{8,10},{10,12},{12... | collective-permute-start | bytes 884744 | tf_op jit(solution)/shard_map/ppermute | solution.py:18
  15.2 6.3 %collective-permute-start.1 = (bf16[24,6144]{1,0:T(8,128)(2,1)S(1)}, bf16[24,6144]{1,0:T(8,128)(2,1)S(1)}, u32[]{:S(2)}, u32[]{:S(2)}) collective-permute-start(bf16[24,6144]{1,0:T(8,128)(2,1)S(1)} %get-tuple-element.8), channel_id=1, source_target_pairs={{0,6},{2,0},{4,2},{6,4},{1,7},{3,1},{5,3},{7,5},{8,14},{10,8},{12,... | collective-permute-start | bytes 884744 | tf_op jit(solution)/shard_map/ppermute | solution.py:18
  21.5 4.0 %collective-permute-start.2 = (bf16[24,6144]{1,0:T(8,128)(2,1)S(1)}, bf16[24,6144]{1,0:T(8,128)(2,1)S(1)}, u32[]{:S(2)}, u32[]{:S(2)}) collective-permute-start(bf16[24,6144]{1,0:T(8,128)(2,1)S(1)} %get-tuple-element.8), channel_id=1, source_target_pairs={{0,4},{2,6},{4,0},{6,2},{1,5},{3,7},{5,1},{7,3},{8,12},{10,14},{12... | collective-permute-start | bytes 884744 | tf_op jit(solution)/shard_map/ppermute | solution.py:18
  25.5 7.1 %collective-permute-start.4 = (bf16[32,384]{1,0:T(8,128)(2,1)}, bf16[32,384]{1,0:T(8,128)(2,1)S(1)}, u32[]{:S(2)}, u32[]{:S(2)}) collective-permute-start(bf16[32,384]{1,0:T(8,128)(2,1)} %param.12), channel_id=1, source_target_pairs={{0,448},{64,0},{128,64},{192,128},{256,192},{320,256},{384,320},{4... | collective-permute-start | bytes 73736 | tf_op jit(solution)/shard_map/ppermute | solution.py:18
  32.7 2.5 %collective-permute-start.5 = (bf16[32,384]{1,0:T(8,128)(2,1)}, bf16[32,384]{1,0:T(8,128)(2,1)S(1)}, u32[]{:S(2)}, u32[]{:S(2)}) collective-permute-start(bf16[32,384]{1,0:T(8,128)(2,1)} %param.12), channel_id=1, source_target_pairs={{0,384},{64,448},{128,0},{192,64},{256,128},{320,192},{384,256},{4... | collective-permute-start | bytes 73736 | tf_op jit(solution)/shard_map/ppermute | solution.py:18
  36.6 7.1 %all-to-all-start = ((bf16[8,32,768]{2,1,0:T(8,128)(2,1)}), bf16[8,32,768]{2,1,0:T(8,128)(2,1)S(1)}, u32[]{:S(2)}, u32[]{:S(2)}) async-start(bf16[8,32,768]{2,1,0:T(8,128)(2,1)} %broadcast_in_dim.60), calls=%async_computation | async-start | bytes 786432 | tf_op jit(solution)/shard_map/all_to_all | solution.py:23
  43.9 1.9 collective-permute-start.6
  45.9 7.8 %collective-permute-start.7 = (bf16[32,384]{1,0:T(8,128)(2,1)S(1)}, bf16[32,384]{1,0:T(8,128)(2,1)S(1)}, u32[]{:S(2)}, u32[]{:S(2)}) collective-permute-start(bf16[32,384]{1,0:T(8,128)(2,1)S(1)} %copy-done.8), channel_id=1, source_target_pairs={{0,256},{64,320},{128,384},{192,448},{256,0},{320,64},{384,128},{4... | collective-permute-start | bytes 73736 | tf_op jit(solution)/shard_map/ppermute | solution.py:18
  55.7 4.6 %collective-permute-start.9 = (bf16[32,384]{1,0:T(8,128)(2,1)S(1)}, bf16[32,384]{1,0:T(8,128)(2,1)S(1)}, u32[]{:S(2)}, u32[]{:S(2)}) collective-permute-start(bf16[32,384]{1,0:T(8,128)(2,1)S(1)} %copy-done.8), channel_id=1, source_target_pairs={{0,128},{64,192},{128,256},{192,320},{256,384},{320,448},{384,0},{... | collective-permute-start | bytes 73736 | tf_op jit(solution)/shard_map/ppermute | solution.py:18
  60.3 2.4 %collective-permute-done.8 = bf16[32,384]{1,0:T(8,128)(2,1)S(1)} collective-permute-done((bf16[32,384]{1,0:T(8,128)(2,1)S(1)}, bf16[32,384]{1,0:T(8,128)(2,1)S(1)}, u32[]{:S(2)}, u32[]{:S(2)}) %collective-permute-start.8) | collective-permute-done | bytes 24608 | tf_op jit(solution)/shard_map/ppermute | solution.py:18
  62.7 3.1 %collective-permute-start.10 = (bf16[32,384]{1,0:T(8,128)(2,1)S(1)}, bf16[32,384]{1,0:T(8,128)(2,1)S(1)}, u32[]{:S(2)}, u32[]{:S(2)}) collective-permute-start(bf16[32,384]{1,0:T(8,128)(2,1)S(1)} %copy-done.8), channel_id=1, source_target_pairs={{0,64},{64,128},{128,192},{192,256},{256,320},{320,384},{384,448},... | collective-permute-start | bytes 73736 | tf_op jit(solution)/shard_map/ppermute | solution.py:18
  65.9 3.7 %collective-permute-done.10 = bf16[32,384]{1,0:T(8,128)(2,1)S(1)} collective-permute-done((bf16[32,384]{1,0:T(8,128)(2,1)S(1)}, bf16[32,384]{1,0:T(8,128)(2,1)S(1)}, u32[]{:S(2)}, u32[]{:S(2)}) %collective-permute-start.10) | collective-permute-done | bytes 24608 | tf_op jit(solution)/shard_map/ppermute | solution.py:18
  69.7 4.1 %collective-permute-start.11 = (bf16[8,32,384]{2,1,0:T(8,128)(2,1)S(1)}, bf16[8,32,384]{2,1,0:T(8,128)(2,1)}, u32[]{:S(2)}, u32[]{:S(2)}) collective-permute-start(bf16[8,32,384]{2,1,0:T(8,128)(2,1)S(1)} %bitcast_dynamic-update-slice_fusion.9), channel_id=1, source_target_pairs={{0,8},{8,16},{16,24},{24,32},{32,40},{40,48},{48,56},{56,0},{1,9},... | collective-permute-start | bytes 589832 | tf_op jit(solution)/shard_map/ppermute | solution.py:18
  73.8 3.1 %collective-permute-start.12 = (bf16[8,32,384]{2,1,0:T(8,128)(2,1)S(1)}, bf16[8,32,384]{2,1,0:T(8,128)(2,1)}, u32[]{:S(2)}, u32[]{:S(2)}) collective-permute-start(bf16[8,32,384]{2,1,0:T(8,128)(2,1)S(1)} %bitcast_dynamic-update-slice_fusion.9), channel_id=1, source_target_pairs={{0,56},{8,0},{16,8},{24,16},{32,24},{40,32},{48,40},{56,48},{1,57}... | collective-permute-start | bytes 589832 | tf_op jit(solution)/shard_map/ppermute | solution.py:18
  78.8 4.2 %collective-permute-start.13 = (bf16[8,32,384]{2,1,0:T(8,128)(2,1)}, bf16[8,32,384]{2,1,0:T(8,128)(2,1)S(1)}, u32[]{:S(2)}, u32[]{:S(2)}) collective-permute-start(bf16[8,32,384]{2,1,0:T(8,128)(2,1)} %collective-permute-done.11), channel_id=1, source_target_pairs={{0,8},{8,16},{16,24},{24,32},{32,40},{40,48},{48,56},{56,0},{1,9},... | collective-permute-start | bytes 589832 | tf_op jit(solution)/shard_map/ppermute | solution.py:18
  83.3 2.9 %collective-permute-start.14 = (bf16[8,32,384]{2,1,0:T(8,128)(2,1)}, bf16[8,32,384]{2,1,0:T(8,128)(2,1)S(1)}, u32[]{:S(2)}, u32[]{:S(2)}) collective-permute-start(bf16[8,32,384]{2,1,0:T(8,128)(2,1)} %collective-permute-done.12), channel_id=1, source_target_pairs={{0,56},{8,0},{16,8},{24,16},{32,24},{40,32},{48,40},{56,48},{1,57}... | collective-permute-start | bytes 589832 | tf_op jit(solution)/shard_map/ppermute | solution.py:18
  89.2 1.9 collective-permute-start.3
  91.2 3.0 %collective-permute-start.15 = (bf16[8,32,384]{2,1,0:T(8,128)(2,1)S(1)}, bf16[8,32,384]{2,1,0:T(8,128)(2,1)S(1)}, u32[]{:S(2)}, u32[]{:S(2)}) collective-permute-start(bf16[8,32,384]{2,1,0:T(8,128)(2,1)S(1)} %collective-permute-done.13), channel_id=1, source_target_pairs={{0,8},{8,16},{16,24},{24,32},{32,40},{40,48},{48,56},{56,0},{1,9},... | collective-permute-start | bytes 589832 | tf_op jit(solution)/shard_map/ppermute | solution.py:18
  94.2 4.1 %collective-permute-start.16 = (bf16[8,32,384]{2,1,0:T(8,128)(2,1)S(1)}, bf16[8,32,384]{2,1,0:T(8,128)(2,1)S(1)}, u32[]{:S(2)}, u32[]{:S(2)}) collective-permute-start(bf16[8,32,384]{2,1,0:T(8,128)(2,1)S(1)} %collective-permute-done.14), channel_id=1, source_target_pairs={{0,56},{8,0},{16,8},{24,16},{32,24},{40,32},{48,40},{56,48},{1,57}... | collective-permute-start | bytes 589832 | tf_op jit(solution)/shard_map/ppermute | solution.py:18
  98.4 3.2 %collective-permute-done.15 = bf16[8,32,384]{2,1,0:T(8,128)(2,1)S(1)} collective-permute-done((bf16[8,32,384]{2,1,0:T(8,128)(2,1)S(1)}, bf16[8,32,384]{2,1,0:T(8,128)(2,1)S(1)}, u32[]{:S(2)}, u32[]{:S(2)}) %collective-permute-start.15) | collective-permute-done | bytes 196640 | tf_op jit(solution)/shard_map/ppermute | solution.py:18
  103.6 5.1 %collective-permute-start.18 = (bf16[4,32,384]{2,1,0:T(8,128)(2,1)S(1)}, bf16[4,32,384]{2,1,0:T(8,128)(2,1)S(1)}, u32[]{:S(2)}, u32[]{:S(2)}) collective-permute-start(bf16[4,32,384]{2,1,0:T(8,128)(2,1)S(1)} %slice.25), channel_id=1, source_target_pairs={{0,56},{8,0},{16,8},{24,16},{32,24},{40,32},{48,40},{56,48},{1,57}... | collective-permute-start | bytes 294920 | tf_op jit(solution)/shard_map/ppermute | solution.py:18
  113.2 19.3 %all-gather.2.cloned.1.call-done = bf16[2048,768]{1,0:T(8,128)(2,1)} async-done(((bf16[256,768]{1,0:T(8,128)(2,1)}), bf16[2048,768]{1,0:T(8,128)(2,1)}) %all-gather.2.cloned.1.call-update) | async-done | bytes 3145744 | tf_op jit(solution)/shard_map/all_gather | solution.py:80
  132.4 2.4 %fusion.11 = f32[192,384]{1,0:T(8,128)S(1)} fusion(bf16[2048,768]{1,0:T(8,128)(2,1)} %all-gather.2.cloned.1.call-done, bf16[192,6144]{1,0:T(8,128)(2,1)} %copy-done.10), kind=kOutput, calls=%fused_computation.17 | convolution fusion | flops 301989888 | bytes 2654208 | tf_op jit(solution)/shard_map/dot_general | solution.py:88
  136.8 2.5 %fusion.7 = f32[192,384]{1,0:T(8,128)} fusion(bf16[2048,768]{1,0:T(8,128)(2,1)S(1)} %copy-done.1, bf16[192,6144]{1,0:T(8,128)(2,1)} %copy-done.10), kind=kOutput, calls=%fused_computation.13 | convolution fusion | flops 301989888 | bytes 2654208 | tf_op jit(solution)/shard_map/dot_general | solution.py:105
  141.7 3.4 %fusion.23 = f32[192,2048]{1,0:T(8,128)S(1)} fusion(bf16[2048,384]{1,0:T(8,128)(2,1)} %bitcast.57, f32[192,384]{1,0:T(8,128)} %fusion.7, bf16[2048,768]{1,0:T(8,128)(2,1)} %all-gather.2.cloned.1.call-done, bf16[192,6144]{1,0:T(8,128)(2,1)} %copy-done.10), kind=kOutput, calls=%fused_computation.43 | convolution fusion | flops 604422144 | bytes 5799936 | tf_op jit(solution)/shard_map/dot_general | solution.py:71
  148.5 3.1 %convolution_convert_fusion = bf16[2048,384]{1,0:T(8,128)(2,1)} fusion(bf16[192,6144]{1,0:T(8,128)(2,1)} %copy-done.10, f32[192,384]{1,0:T(8,128)S(1)} %copy-done.6, f32[192,384]{1,0:T(8,128)S(1)} %fusion.11), kind=kOutput, calls=%fused_computation.3 | convolution fusion | flops 303218688 | bytes 2949120 | tf_op jit(solution)/shard_map/dot_general | solution.py:93
  151.6 10.0 %all-to-all-start.1 = ((bf16[64,32,384]{2,1,0:T(8,128)(2,1)}), bf16[64,32,384]{2,1,0:T(8,128)(2,1)S(1)}, u32[]{:S(2)}, u32[]{:S(2)}) async-start(bf16[64,32,384]{2,1,0:T(8,128)(2,1)} %bitcast.55), calls=%async_computation.1 | async-start | bytes 3145728 | tf_op jit(solution)/shard_map/all_to_all | solution.py:96
  163.3 2.6 %collective-permute-start.20 = (bf16[24,4096]{1,0:T(8,128)(2,1)S(1)}, bf16[24,4096]{1,0:T(8,128)(2,1)S(1)}, u32[]{:S(2)}, u32[]{:S(2)}) collective-permute-start(bf16[24,4096]{1,0:T(8,128)(2,1)S(1)} %get-tuple-element.3), channel_id=1, source_target_pairs={{0,6},{2,0},{4,2},{6,4},{1,7},{3,1},{5,3},{7,5},{8,14},{10,8},{12,... | collective-permute-start | bytes 589832 | tf_op jit(solution)/shard_map/ppermute | solution.py:18
  165.9 3.4 %collective-permute-start.21 = (bf16[24,4096]{1,0:T(8,128)(2,1)S(1)}, bf16[24,4096]{1,0:T(8,128)(2,1)S(1)}, u32[]{:S(2)}, u32[]{:S(2)}) collective-permute-start(bf16[24,4096]{1,0:T(8,128)(2,1)S(1)} %get-tuple-element.5), channel_id=1, source_target_pairs={{0,2},{2,4},{4,6},{6,0},{1,3},{3,5},{5,7},{7,1},{8,10},{10,12},{12... | collective-permute-start | bytes 589832 | tf_op jit(solution)/shard_map/ppermute | solution.py:18
  169.3 5.2 %collective-permute-start.22 = (bf16[24,4096]{1,0:T(8,128)(2,1)S(1)}, bf16[24,4096]{1,0:T(8,128)(2,1)S(1)}, u32[]{:S(2)}, u32[]{:S(2)}) collective-permute-start(bf16[24,4096]{1,0:T(8,128)(2,1)S(1)} %get-tuple-element.4), channel_id=1, source_target_pairs={{0,4},{2,6},{4,0},{6,2},{1,5},{3,7},{5,1},{7,3},{8,12},{10,14},{12... | collective-permute-start | bytes 589832 | tf_op jit(solution)/shard_map/ppermute | solution.py:18
  176.0 3.1 %collective-permute-done.22 = bf16[24,4096]{1,0:T(8,128)(2,1)S(1)} collective-permute-done((bf16[24,4096]{1,0:T(8,128)(2,1)S(1)}, bf16[24,4096]{1,0:T(8,128)(2,1)S(1)}, u32[]{:S(2)}, u32[]{:S(2)}) %collective-permute-start.22) | collective-permute-done | bytes 196640 | tf_op jit(solution)/shard_map/ppermute | solution.py:18
  180.0 23.6 %all-to-all-done.1 = bf16[64,32,384]{2,1,0:T(8,128)(2,1)S(1)} async-done(((bf16[64,32,384]{2,1,0:T(8,128)(2,1)}), bf16[64,32,384]{2,1,0:T(8,128)(2,1)S(1)}, u32[]{:S(2)}, u32[]{:S(2)}) %all-to-all-start.1) | async-done | bytes 1572896 | tf_op jit(solution)/shard_map/all_to_all | solution.py:96
  (89 shorter events, 32.3 us)
Async XLA Ops:
  7.2 36.7 %copy-start.8 = (bf16[32,384]{1,0:T(8,128)(2,1)S(1)}, bf16[32,384]{1,0:T(8,128)(2,1)}, u32[]{:S(2)}) copy-start(bf16[32,384]{1,0:T(8,128)(2,1)} %param.12) | copy-start | bytes 73732
  11.8 77.2 %collective-permute-start = (bf16[24,6144]{1,0:T(8,128)(2,1)S(1)}, bf16[24,6144]{1,0:T(8,128)(2,1)S(1)}, u32[]{:S(2)}, u32[]{:S(2)}) collective-permute-start(bf16[24,6144]{1,0:T(8,128)(2,1)S(1)} %get-tuple-element.8), channel_id=1, source_target_pairs={{0,2},{2,4},{4,6},{6,0},{1,3},{3,5},{5,7},{7,1},{8,10},{10,12},{12... | collective-permute-start | bytes 884744 | tf_op jit(solution)/shard_map/ppermute | solution.py:18
  15.2 73.9 %collective-permute-start.1 = (bf16[24,6144]{1,0:T(8,128)(2,1)S(1)}, bf16[24,6144]{1,0:T(8,128)(2,1)S(1)}, u32[]{:S(2)}, u32[]{:S(2)}) collective-permute-start(bf16[24,6144]{1,0:T(8,128)(2,1)S(1)} %get-tuple-element.8), channel_id=1, source_target_pairs={{0,6},{2,0},{4,2},{6,4},{1,7},{3,1},{5,3},{7,5},{8,14},{10,8},{12,... | collective-permute-start | bytes 884744 | tf_op jit(solution)/shard_map/ppermute | solution.py:18
  21.5 67.5 %collective-permute-start.2 = (bf16[24,6144]{1,0:T(8,128)(2,1)S(1)}, bf16[24,6144]{1,0:T(8,128)(2,1)S(1)}, u32[]{:S(2)}, u32[]{:S(2)}) collective-permute-start(bf16[24,6144]{1,0:T(8,128)(2,1)S(1)} %get-tuple-element.8), channel_id=1, source_target_pairs={{0,4},{2,6},{4,0},{6,2},{1,5},{3,7},{5,1},{7,3},{8,12},{10,14},{12... | collective-permute-start | bytes 884744 | tf_op jit(solution)/shard_map/ppermute | solution.py:18
  25.5 18.4 %collective-permute-start.4 = (bf16[32,384]{1,0:T(8,128)(2,1)}, bf16[32,384]{1,0:T(8,128)(2,1)S(1)}, u32[]{:S(2)}, u32[]{:S(2)}) collective-permute-start(bf16[32,384]{1,0:T(8,128)(2,1)} %param.12), channel_id=1, source_target_pairs={{0,448},{64,0},{128,64},{192,128},{256,192},{320,256},{384,320},{4... | collective-permute-start | bytes 73736 | tf_op jit(solution)/shard_map/ppermute | solution.py:18
  32.7 13.2 %collective-permute-start.5 = (bf16[32,384]{1,0:T(8,128)(2,1)}, bf16[32,384]{1,0:T(8,128)(2,1)S(1)}, u32[]{:S(2)}, u32[]{:S(2)}) collective-permute-start(bf16[32,384]{1,0:T(8,128)(2,1)} %param.12), channel_id=1, source_target_pairs={{0,384},{64,448},{128,0},{192,64},{256,128},{320,192},{384,256},{4... | collective-permute-start | bytes 73736 | tf_op jit(solution)/shard_map/ppermute | solution.py:18
  36.6 49.5 %all-to-all-start = ((bf16[8,32,768]{2,1,0:T(8,128)(2,1)}), bf16[8,32,768]{2,1,0:T(8,128)(2,1)S(1)}, u32[]{:S(2)}, u32[]{:S(2)}) async-start(bf16[8,32,768]{2,1,0:T(8,128)(2,1)} %broadcast_in_dim.60), calls=%async_computation | async-start | bytes 786432 | tf_op jit(solution)/shard_map/all_to_all | solution.py:23
  43.7 88.7 %all-gather.2.cloned.1.call-start = ((), (), s32[]{:S(2)}) async-start(), calls=%async_computation.2 | async-start | bytes 3538944 | tf_op jit(solution)/shard_map/all_gather | solution.py:80
  43.9 9.8 %collective-permute-start.6 = (bf16[32,384]{1,0:T(8,128)(2,1)S(1)}, bf16[32,384]{1,0:T(8,128)(2,1)S(1)}, u32[]{:S(2)}, u32[]{:S(2)}) collective-permute-start(bf16[32,384]{1,0:T(8,128)(2,1)S(1)} %copy-done.8), channel_id=1, source_target_pairs={{0,320},{64,384},{128,448},{192,0},{256,64},{320,128},{384,192},{4... | collective-permute-start | bytes 73736 | tf_op jit(solution)/shard_map/ppermute | solution.py:18
  45.9 9.9 %collective-permute-start.7 = (bf16[32,384]{1,0:T(8,128)(2,1)S(1)}, bf16[32,384]{1,0:T(8,128)(2,1)S(1)}, u32[]{:S(2)}, u32[]{:S(2)}) collective-permute-start(bf16[32,384]{1,0:T(8,128)(2,1)S(1)} %copy-done.8), channel_id=1, source_target_pairs={{0,256},{64,320},{128,384},{192,448},{256,0},{320,64},{384,128},{4... | collective-permute-start | bytes 73736 | tf_op jit(solution)/shard_map/ppermute | solution.py:18
  53.7 9.0 %collective-permute-start.8 = (bf16[32,384]{1,0:T(8,128)(2,1)S(1)}, bf16[32,384]{1,0:T(8,128)(2,1)S(1)}, u32[]{:S(2)}, u32[]{:S(2)}) collective-permute-start(bf16[32,384]{1,0:T(8,128)(2,1)S(1)} %copy-done.8), channel_id=1, source_target_pairs={{0,192},{64,256},{128,320},{192,384},{256,448},{320,0},{384,64},{4... | collective-permute-start | bytes 73736 | tf_op jit(solution)/shard_map/ppermute | solution.py:18
  55.7 10.2 %collective-permute-start.9 = (bf16[32,384]{1,0:T(8,128)(2,1)S(1)}, bf16[32,384]{1,0:T(8,128)(2,1)S(1)}, u32[]{:S(2)}, u32[]{:S(2)}) collective-permute-start(bf16[32,384]{1,0:T(8,128)(2,1)S(1)} %copy-done.8), channel_id=1, source_target_pairs={{0,128},{64,192},{128,256},{192,320},{256,384},{320,448},{384,0},{... | collective-permute-start | bytes 73736 | tf_op jit(solution)/shard_map/ppermute | solution.py:18
  62.7 6.9 %collective-permute-start.10 = (bf16[32,384]{1,0:T(8,128)(2,1)S(1)}, bf16[32,384]{1,0:T(8,128)(2,1)S(1)}, u32[]{:S(2)}, u32[]{:S(2)}) collective-permute-start(bf16[32,384]{1,0:T(8,128)(2,1)S(1)} %copy-done.8), channel_id=1, source_target_pairs={{0,64},{64,128},{128,192},{192,256},{256,320},{320,384},{384,448},... | collective-permute-start | bytes 73736 | tf_op jit(solution)/shard_map/ppermute | solution.py:18
  69.7 9.1 %collective-permute-start.11 = (bf16[8,32,384]{2,1,0:T(8,128)(2,1)S(1)}, bf16[8,32,384]{2,1,0:T(8,128)(2,1)}, u32[]{:S(2)}, u32[]{:S(2)}) collective-permute-start(bf16[8,32,384]{2,1,0:T(8,128)(2,1)S(1)} %bitcast_dynamic-update-slice_fusion.9), channel_id=1, source_target_pairs={{0,8},{8,16},{16,24},{24,32},{32,40},{40,48},{48,56},{56,0},{1,9},... | collective-permute-start | bytes 589832 | tf_op jit(solution)/shard_map/ppermute | solution.py:18
  73.8 9.5 %collective-permute-start.12 = (bf16[8,32,384]{2,1,0:T(8,128)(2,1)S(1)}, bf16[8,32,384]{2,1,0:T(8,128)(2,1)}, u32[]{:S(2)}, u32[]{:S(2)}) collective-permute-start(bf16[8,32,384]{2,1,0:T(8,128)(2,1)S(1)} %bitcast_dynamic-update-slice_fusion.9), channel_id=1, source_target_pairs={{0,56},{8,0},{16,8},{24,16},{32,24},{40,32},{48,40},{56,48},{1,57}... | collective-permute-start | bytes 589832 | tf_op jit(solution)/shard_map/ppermute | solution.py:18
  78.8 12.4 %collective-permute-start.13 = (bf16[8,32,384]{2,1,0:T(8,128)(2,1)}, bf16[8,32,384]{2,1,0:T(8,128)(2,1)S(1)}, u32[]{:S(2)}, u32[]{:S(2)}) collective-permute-start(bf16[8,32,384]{2,1,0:T(8,128)(2,1)} %collective-permute-done.11), channel_id=1, source_target_pairs={{0,8},{8,16},{16,24},{24,32},{32,40},{40,48},{48,56},{56,0},{1,9},... | collective-permute-start | bytes 589832 | tf_op jit(solution)/shard_map/ppermute | solution.py:18
  83.3 10.9 %collective-permute-start.14 = (bf16[8,32,384]{2,1,0:T(8,128)(2,1)}, bf16[8,32,384]{2,1,0:T(8,128)(2,1)S(1)}, u32[]{:S(2)}, u32[]{:S(2)}) collective-permute-start(bf16[8,32,384]{2,1,0:T(8,128)(2,1)} %collective-permute-done.12), channel_id=1, source_target_pairs={{0,56},{8,0},{16,8},{24,16},{32,24},{40,32},{48,40},{56,48},{1,57}... | collective-permute-start | bytes 589832 | tf_op jit(solution)/shard_map/ppermute | solution.py:18
  86.9 4.2 %copy-start.9 = (bf16[192,6144]{1,0:T(8,128)(2,1)S(1)}, bf16[192,6144]{1,0:T(8,128)(2,1)}, u32[]{:S(2)}) copy-start(bf16[192,6144]{1,0:T(8,128)(2,1)} %get-tuple-element.9) | copy-start | bytes 7077892
  89.2 21.8 %collective-permute-start.3 = (bf16[96,6144]{1,0:T(8,128)(2,1)S(1)}, bf16[96,6144]{1,0:T(8,128)(2,1)S(1)}, u32[]{:S(2)}, u32[]{:S(2)}) collective-permute-start(bf16[96,6144]{1,0:T(8,128)(2,1)S(1)} %pad_maximum_fusion.1), channel_id=1, source_target_pairs={{0,1},{1,0},{2,3},{3,2},{4,5},{5,4},{6,7},{7,6},{8,9},{9,8},{10,11... | collective-permute-start | bytes 3538952 | tf_op jit(solution)/shard_map/ppermute | solution.py:18
  91.2 10.4 %collective-permute-start.15 = (bf16[8,32,384]{2,1,0:T(8,128)(2,1)S(1)}, bf16[8,32,384]{2,1,0:T(8,128)(2,1)S(1)}, u32[]{:S(2)}, u32[]{:S(2)}) collective-permute-start(bf16[8,32,384]{2,1,0:T(8,128)(2,1)S(1)} %collective-permute-done.13), channel_id=1, source_target_pairs={{0,8},{8,16},{16,24},{24,32},{32,40},{40,48},{48,56},{56,0},{1,9},... | collective-permute-start | bytes 589832 | tf_op jit(solution)/shard_map/ppermute | solution.py:18
  94.2 9.4 %collective-permute-start.16 = (bf16[8,32,384]{2,1,0:T(8,128)(2,1)S(1)}, bf16[8,32,384]{2,1,0:T(8,128)(2,1)S(1)}, u32[]{:S(2)}, u32[]{:S(2)}) collective-permute-start(bf16[8,32,384]{2,1,0:T(8,128)(2,1)S(1)} %collective-permute-done.14), channel_id=1, source_target_pairs={{0,56},{8,0},{16,8},{24,16},{32,24},{40,32},{48,40},{56,48},{1,57}... | collective-permute-start | bytes 589832 | tf_op jit(solution)/shard_map/ppermute | solution.py:18
  101.6 7.7 %collective-permute-start.17 = (bf16[4,32,384]{2,1,0:T(8,128)(2,1)S(1)}, bf16[4,32,384]{2,1,0:T(8,128)(2,1)S(1)}, u32[]{:S(2)}, u32[]{:S(2)}) collective-permute-start(bf16[4,32,384]{2,1,0:T(8,128)(2,1)S(1)} %slice.24), channel_id=1, source_target_pairs={{0,8},{8,16},{16,24},{24,32},{32,40},{40,48},{48,56},{56,0},{1,9},... | collective-permute-start | bytes 294920 | tf_op jit(solution)/shard_map/ppermute | solution.py:18
  103.6 7.3 %collective-permute-start.18 = (bf16[4,32,384]{2,1,0:T(8,128)(2,1)S(1)}, bf16[4,32,384]{2,1,0:T(8,128)(2,1)S(1)}, u32[]{:S(2)}, u32[]{:S(2)}) collective-permute-start(bf16[4,32,384]{2,1,0:T(8,128)(2,1)S(1)} %slice.25), channel_id=1, source_target_pairs={{0,56},{8,0},{16,8},{24,16},{32,24},{40,32},{48,40},{56,48},{1,57}... | collective-permute-start | bytes 294920 | tf_op jit(solution)/shard_map/ppermute | solution.py:18
  113.1 26.1 %copy-start.4 = (f32[192,384]{1,0:T(8,128)}, f32[192,384]{1,0:T(8,128)S(1)}, u32[]{:S(2)}) copy-start(f32[192,384]{1,0:T(8,128)S(1)} %fusion.18) | copy-start | bytes 884740
  132.4 2.6 %copy-start.1 = (bf16[2048,768]{1,0:T(8,128)(2,1)S(1)}, bf16[2048,768]{1,0:T(8,128)(2,1)}, u32[]{:S(2)}) copy-start(bf16[2048,768]{1,0:T(8,128)(2,1)} %all-gather.2.cloned.1.call-done) | copy-start | bytes 9437188
  145.2 3.3 %copy-start.6 = (f32[192,384]{1,0:T(8,128)S(1)}, f32[192,384]{1,0:T(8,128)}, u32[]{:S(2)}) copy-start(f32[192,384]{1,0:T(8,128)} %copy-done.5) | copy-start | bytes 884740
  146.6 15.1 %collective-permute-start.19 = (bf16[96,4096]{1,0:T(8,128)(2,1)}, bf16[96,4096]{1,0:T(8,128)(2,1)}, u32[]{:S(2)}, u32[]{:S(2)}) collective-permute-start(bf16[96,4096]{1,0:T(8,128)(2,1)} %fusion.3), channel_id=1, source_target_pairs={{0,1},{1,0},{2,3},{3,2},{4,5},{5,4},{6,7},{7,6},{8,9},{9,8},{10,11... | collective-permute-start | bytes 2359304 | tf_op jit(solution)/shard_map/ppermute | solution.py:18
  151.6 51.9 %all-to-all-start.1 = ((bf16[64,32,384]{2,1,0:T(8,128)(2,1)}), bf16[64,32,384]{2,1,0:T(8,128)(2,1)S(1)}, u32[]{:S(2)}, u32[]{:S(2)}) async-start(bf16[64,32,384]{2,1,0:T(8,128)(2,1)} %bitcast.55), calls=%async_computation.1 | async-start | bytes 3145728 | tf_op jit(solution)/shard_map/all_to_all | solution.py:96
  163.3 40.5 %copy-start.7 = (f32[32,384]{1,0:T(8,128)S(1)}, f32[32,384]{1,0:T(8,128)}, u32[]{:S(2)}) copy-start(f32[32,384]{1,0:T(8,128)} %param.13) | copy-start | bytes 147460
  163.3 11.2 %collective-permute-start.20 = (bf16[24,4096]{1,0:T(8,128)(2,1)S(1)}, bf16[24,4096]{1,0:T(8,128)(2,1)S(1)}, u32[]{:S(2)}, u32[]{:S(2)}) collective-permute-start(bf16[24,4096]{1,0:T(8,128)(2,1)S(1)} %get-tuple-element.3), channel_id=1, source_target_pairs={{0,6},{2,0},{4,2},{6,4},{1,7},{3,1},{5,3},{7,5},{8,14},{10,8},{12,... | collective-permute-start | bytes 589832 | tf_op jit(solution)/shard_map/ppermute | solution.py:18
  165.9 10.2 %collective-permute-start.21 = (bf16[24,4096]{1,0:T(8,128)(2,1)S(1)}, bf16[24,4096]{1,0:T(8,128)(2,1)S(1)}, u32[]{:S(2)}, u32[]{:S(2)}) collective-permute-start(bf16[24,4096]{1,0:T(8,128)(2,1)S(1)} %get-tuple-element.5), channel_id=1, source_target_pairs={{0,2},{2,4},{4,6},{6,0},{1,3},{3,5},{5,7},{7,1},{8,10},{10,12},{12... | collective-permute-start | bytes 589832 | tf_op jit(solution)/shard_map/ppermute | solution.py:18
  169.3 9.9 %collective-permute-start.22 = (bf16[24,4096]{1,0:T(8,128)(2,1)S(1)}, bf16[24,4096]{1,0:T(8,128)(2,1)S(1)}, u32[]{:S(2)}, u32[]{:S(2)}) collective-permute-start(bf16[24,4096]{1,0:T(8,128)(2,1)S(1)} %get-tuple-element.4), channel_id=1, source_target_pairs={{0,4},{2,6},{4,0},{6,2},{1,5},{3,7},{5,1},{7,3},{8,12},{10,14},{12... | collective-permute-start | bytes 589832 | tf_op jit(solution)/shard_map/ppermute | solution.py:18
  (5 other events, 8.4 us)
Sparse Core Ops, SparseCore 0:
  87.1 45.3 all-gather.1

commit v2 on v1

--- a/solution.py
+++ b/solution.py
@@ -23,39 +23,34 @@
     return lax.all_to_all(jnp.broadcast_to(value, (count, *value.shape)), axis, 0, 0)
 
 
-def line_of(value, axis):
+def ring_gather(line, axis):
     count = lax.axis_size(axis)
+    half = line.shape[0] // 2
     mine = lax.axis_index(axis)
-    whole = jnp.zeros((count, *value.shape), value.dtype)
-    for step in range(count):
-        at = ((mine + step) & (count - 1), 0, 0)
-        whole = lax.dynamic_update_slice(whole, shift(value, axis, -step)[None], at)
-    return whole
-
-
-def ring_gather(line):
-    count = lax.axis_size("y")
-    half = line.shape[0] // 2
-    mine = lax.axis_index("y")
-    whole = jnp.zeros((line.shape[0], count, *line.shape[1:]), line.dtype)
+    at_dim = FS.index(axis)
+    shape = list(line.shape)
+    shape.insert(at_dim, count)
+    whole = jnp.zeros(shape, line.dtype)
 
     def put(whole, chunk, offset, lead):
-        at = (lead, (mine + offset) & (count - 1), 0, 0)
-        return lax.dynamic_update_slice(whole, chunk[:, None], at)
+        at = [lead, 0, 0]
+        at.insert(at_dim, (mine + offset) & (count - 1))
+        return lax.dynamic_update_slice(whole, jnp.expand_dims(chunk, at_dim), at)
 
     whole = put(whole, line, 0, 0)
     ahead = behind = line
     for hop in range(1, count // 2):
-        ahead, behind = shift(ahead, "y", 1), shift(behind, "y", -1)
+        ahead, behind = shift(ahead, axis, 1), shift(behind, axis, -1)
         whole = put(put(whole, ahead, -hop, 0), behind, hop, 0)
-    whole = put(whole, shift(ahead[:half], "y", 1), count // 2, 0)
-    whole = put(whole, shift(behind[half:], "y", -1), count // 2, half)
+    whole = put(whole, shift(ahead[:half], axis, 1), count // 2, 0)
+    whole = put(whole, shift(behind[half:], axis, -1), count // 2, half)
     return whole.reshape(-1, line.shape[-1])
 
 
 def collect_tokens(own):
     line = jnp.concatenate([shift(own, "x", step) for step in STEPS], axis=0)
-    return jnp.concatenate([line, shift(line, "c", 1)], axis=0)
+    other = shift(line, "c", 1)
+    return jnp.concatenate([line, other], axis=0)
 
 
 def give_rows(partial, rows):
@@ -75,14 +70,13 @@
 
 def shards(later, early, cotangent, gate_w, up_w, down_w, down_grad_sum):
     rows, _ = later.shape
-    line = spread(jnp.concatenate([gate_w, up_w], axis=1), "y")
-    line = line.reshape(-1, line.shape[-1])
-    whole = lax.all_gather(line, "z", axis=0, tiled=True)
-    gate_whole, up_whole = jnp.split(whole, 2, axis=1)
-    down_line = line_of(down_w, "z")
-    down_whole = ring_gather(down_line)
+    down_whole = lax.all_gather(down_w, FS, axis=0, tiled=True)
+    gate_line = spread(gate_w, "y")
+    up_line = spread(up_w, "z")
     tokens = jnp.concatenate([later, early, cotangent], axis=1)
     tokens = collect_tokens(tokens)
+    gate_whole = ring_gather(gate_line, "z")
+    up_whole = ring_gather(up_line, "y")
     later_rows, early_rows, grad_rows = jnp.split(tokens, 3, axis=1)
 
     gate_early = jnp.dot(early_rows, gate_whole, preferred_element_type=F32)

time: 213 us -> 203 us (0.953)
  the two profiles are of different devices: /device:TPU:2 before, /device:TPU:8 now
where the time goes in v2:
time: 203 us; the launch traced here: 201 us
  starting transfers between devices  109 us (54%)
  waiting for transfers between devices  37.4 us (18%)
  matrix products  17.5 us (9%)
  local copies, waits for them, and re-layouts  15.2 us (7%)
  between operations  14.6 us (7%)
  other arithmetic  6.94 us (3%)
    ppermute x24, starting transfers between devices, shift(): lax.ppermute(value, axis, [(i, (i + step) % count) for i in range(count)])  80.1 us
    all_to_all x1, waiting for transfers between devices, shards(): received = lax.all_to_all(down_grad.reshape(-1, *gate_w.shape), FS, 0, 0)  24.8 us
    all_to_all x2, starting transfers between devices, spread(): lax.all_to_all(jnp.broadcast_to(value, (count, *value.shape)), axis, 0, 0)  17.9 us
    all_to_all x1, starting transfers between devices, shards(): received = lax.all_to_all(down_grad.reshape(-1, *gate_w.shape), FS, 0, 0)  11.2 us
    all_to_all x2, waiting for transfers between devices, spread(): lax.all_to_all(jnp.broadcast_to(value, (count, *value.shape)), axis, 0, 0)  6.87 us
    ppermute x24, waiting for transfers between devices, shift(): lax.ppermute(value, axis, [(i, (i + step) % count) for i in range(count)])  5.64 us
    dot_general x3, matrix products, contract_last(): lax.dot_general(leading, trailing, (((1,), (1,)), ((), ())), preferred_el...  5.63 us
    unnamed x15, local copies, waits for them, and re-layouts  5.59 us
  transfers between devices with their start and end apart: 28, of which 7 were waited for; matrix products, arithmetic and copies ran while one was open for 11% of the time, Pallas kernels for 0%

profile of v2, /device:TPU:8, one launch (start us, length us, event | category | flops | bytes accessed | tf_op | source)
XLA Modules:
  0.0 200.8 jit_solution(3713810763384548738)
XLA Ops:
  11.9 3.4 %collective-permute-start = (bf16[24,6144]{1,0:T(8,128)(2,1)S(1)}, bf16[24,6144]{1,0:T(8,128)(2,1)S(1)}, u32[]{:S(2)}, u32[]{:S(2)}) collective-permute-start(bf16[24,6144]{1,0:T(8,128)(2,1)S(1)} %get-tuple-element.8), channel_id=1, source_target_pairs={{0,2},{2,4},{4,6},{6,0},{1,3},{3,5},{5,7},{7,1},{8,10},{10,12},{12... | collective-permute-start | bytes 884744 | tf_op jit(solution)/shard_map/ppermute | solution.py:18
  15.3 3.7 %collective-permute-start.1 = (bf16[24,6144]{1,0:T(8,128)(2,1)S(1)}, bf16[24,6144]{1,0:T(8,128)(2,1)S(1)}, u32[]{:S(2)}, u32[]{:S(2)}) collective-permute-start(bf16[24,6144]{1,0:T(8,128)(2,1)S(1)} %get-tuple-element.8), channel_id=1, source_target_pairs={{0,6},{2,0},{4,2},{6,4},{1,7},{3,1},{5,3},{7,5},{8,14},{10,8},{12,... | collective-permute-start | bytes 884744 | tf_op jit(solution)/shard_map/ppermute | solution.py:18
  18.9 3.7 %collective-permute-start.2 = (bf16[24,6144]{1,0:T(8,128)(2,1)S(1)}, bf16[24,6144]{1,0:T(8,128)(2,1)S(1)}, u32[]{:S(2)}, u32[]{:S(2)}) collective-permute-start(bf16[24,6144]{1,0:T(8,128)(2,1)S(1)} %get-tuple-element.8), channel_id=1, source_target_pairs={{0,4},{2,6},{4,0},{6,2},{1,5},{3,7},{5,1},{7,3},{8,12},{10,14},{12... | collective-permute-start | bytes 884744 | tf_op jit(solution)/shard_map/ppermute | solution.py:18
  24.1 10.3 %all-to-all-start.1 = ((bf16[8,32,384]{2,1,0:T(8,128)(2,1)}), bf16[8,32,384]{2,1,0:T(8,128)(2,1)S(1)}, u32[]{:S(2)}, u32[]{:S(2)}) async-start(bf16[8,32,384]{2,1,0:T(8,128)(2,1)} %broadcast_in_dim.70), calls=%async_computation.1 | async-start | bytes 393216 | tf_op jit(solution)/shard_map/all_to_all | solution.py:23
  39.0 5.2 %all-to-all-done.1 = bf16[8,32,384]{2,1,0:T(8,128)(2,1)S(1)} async-done(((bf16[8,32,384]{2,1,0:T(8,128)(2,1)}), bf16[8,32,384]{2,1,0:T(8,128)(2,1)S(1)}, u32[]{:S(2)}, u32[]{:S(2)}) %all-to-all-start.1) | async-done | bytes 196640 | tf_op jit(solution)/shard_map/all_to_all | solution.py:23
  44.9 7.5 %all-to-all-start = ((bf16[8,32,384]{2,1,0:T(8,128)(2,1)}), bf16[8,32,384]{2,1,0:T(8,128)(2,1)S(1)}, u32[]{:S(2)}, u32[]{:S(2)}) async-start(bf16[8,32,384]{2,1,0:T(8,128)(2,1)} %broadcast_in_dim.60), calls=%async_computation | async-start | bytes 393216 | tf_op jit(solution)/shard_map/all_to_all | solution.py:23
  53.2 3.4 %collective-permute-start.12 = (bf16[8,32,384]{2,1,0:T(8,128)(2,1)S(1)}, bf16[8,32,384]{2,1,0:T(8,128)(2,1)}, u32[]{:S(2)}, u32[]{:S(2)}) collective-permute-start(bf16[8,32,384]{2,1,0:T(8,128)(2,1)S(1)} %all-to-all-done.1), channel_id=1, source_target_pairs={{0,8},{8,16},{16,24},{24,32},{32,40},{40,48},{48,56},{56,0},{1,9},... | collective-permute-start | bytes 589832 | tf_op jit(solution)/shard_map/ppermute | solution.py:18
  56.6 2.5 %collective-permute-start.13 = (bf16[8,32,384]{2,1,0:T(8,128)(2,1)S(1)}, bf16[8,32,384]{2,1,0:T(8,128)(2,1)}, u32[]{:S(2)}, u32[]{:S(2)}) collective-permute-start(bf16[8,32,384]{2,1,0:T(8,128)(2,1)S(1)} %all-to-all-done.1), channel_id=1, source_target_pairs={{0,56},{8,0},{16,8},{24,16},{32,24},{40,32},{48,40},{56,48},{1,57}... | collective-permute-start | bytes 589832 | tf_op jit(solution)/shard_map/ppermute | solution.py:18
  60.7 2.7 %collective-permute-start.4 = (bf16[8,32,384]{2,1,0:T(8,128)(2,1)S(1)}, bf16[8,32,384]{2,1,0:T(8,128)(2,1)S(1)}, u32[]{:S(2)}, u32[]{:S(2)}) collective-permute-start(bf16[8,32,384]{2,1,0:T(8,128)(2,1)S(1)} %all-to-all-done), channel_id=1, source_target_pairs={{0,64},{64,128},{128,192},{192,256},{256,320},{320,384},{384,448},... | collective-permute-start | bytes 589832 | tf_op jit(solution)/shard_map/ppermute | solution.py:18
  63.5 4.3 %collective-permute-start.5 = (bf16[8,32,384]{2,1,0:T(8,128)(2,1)S(1)}, bf16[8,32,384]{2,1,0:T(8,128)(2,1)S(1)}, u32[]{:S(2)}, u32[]{:S(2)}) collective-permute-start(bf16[8,32,384]{2,1,0:T(8,128)(2,1)S(1)} %all-to-all-done), channel_id=1, source_target_pairs={{0,448},{64,0},{128,64},{192,128},{256,192},{320,256},{384,320},{4... | collective-permute-start | bytes 589832 | tf_op jit(solution)/shard_map/ppermute | solution.py:18
  68.2 3.7 %collective-permute-start.14 = (bf16[8,32,384]{2,1,0:T(8,128)(2,1)}, bf16[8,32,384]{2,1,0:T(8,128)(2,1)S(1)}, u32[]{:S(2)}, u32[]{:S(2)}) collective-permute-start(bf16[8,32,384]{2,1,0:T(8,128)(2,1)} %collective-permute-done.12), channel_id=1, source_target_pairs={{0,8},{8,16},{16,24},{24,32},{32,40},{40,48},{48,56},{56,0},{1,9},... | collective-permute-start | bytes 589832 | tf_op jit(solution)/shard_map/ppermute | solution.py:18
  71.9 2.9 %collective-permute-start.15 = (bf16[8,32,384]{2,1,0:T(8,128)(2,1)}, bf16[8,32,384]{2,1,0:T(8,128)(2,1)S(1)}, u32[]{:S(2)}, u32[]{:S(2)}) collective-permute-start(bf16[8,32,384]{2,1,0:T(8,128)(2,1)} %collective-permute-done.13), channel_id=1, source_target_pairs={{0,56},{8,0},{16,8},{24,16},{32,24},{40,32},{48,40},{56,48},{1,57}... | collective-permute-start | bytes 589832 | tf_op jit(solution)/shard_map/ppermute | solution.py:18
  74.8 1.9 collective-permute-start.6
  76.8 5.1 %collective-permute-start.7 = (bf16[8,32,384]{2,1,0:T(8,128)(2,1)S(1)}, bf16[8,32,384]{2,1,0:T(8,128)(2,1)S(1)}, u32[]{:S(2)}, u32[]{:S(2)}) collective-permute-start(bf16[8,32,384]{2,1,0:T(8,128)(2,1)S(1)} %collective-permute-done.5), channel_id=1, source_target_pairs={{0,448},{64,0},{128,64},{192,128},{256,192},{320,256},{384,320},{4... | collective-permute-start | bytes 589832 | tf_op jit(solution)/shard_map/ppermute | solution.py:18
  83.9 3.0 %collective-permute-start.16 = (bf16[8,32,384]{2,1,0:T(8,128)(2,1)S(1)}, bf16[8,32,384]{2,1,0:T(8,128)(2,1)S(1)}, u32[]{:S(2)}, u32[]{:S(2)}) collective-permute-start(bf16[8,32,384]{2,1,0:T(8,128)(2,1)S(1)} %collective-permute-done.14), channel_id=1, source_target_pairs={{0,8},{8,16},{16,24},{24,32},{32,40},{40,48},{48,56},{56,0},{1,9},... | collective-permute-start | bytes 589832 | tf_op jit(solution)/shard_map/ppermute | solution.py:18
  86.9 4.1 %collective-permute-start.17 = (bf16[8,32,384]{2,1,0:T(8,128)(2,1)S(1)}, bf16[8,32,384]{2,1,0:T(8,128)(2,1)S(1)}, u32[]{:S(2)}, u32[]{:S(2)}) collective-permute-start(bf16[8,32,384]{2,1,0:T(8,128)(2,1)S(1)} %collective-permute-done.15), channel_id=1, source_target_pairs={{0,56},{8,0},{16,8},{24,16},{32,24},{40,32},{48,40},{56,48},{1,57}... | collective-permute-start | bytes 589832 | tf_op jit(solution)/shard_map/ppermute | solution.py:18
  93.0 5.1 %collective-permute-start.9 = (bf16[8,32,384]{2,1,0:T(8,128)(2,1)S(1)}, bf16[8,32,384]{2,1,0:T(8,128)(2,1)S(1)}, u32[]{:S(2)}, u32[]{:S(2)}) collective-permute-start(bf16[8,32,384]{2,1,0:T(8,128)(2,1)S(1)} %collective-permute-done.7), channel_id=1, source_target_pairs={{0,448},{64,0},{128,64},{192,128},{256,192},{320,256},{384,320},{4... | collective-permute-start | bytes 589832 | tf_op jit(solution)/shard_map/ppermute | solution.py:18
  100.3 5.1 %collective-permute-start.19 = (bf16[4,32,384]{2,1,0:T(8,128)(2,1)S(1)}, bf16[4,32,384]{2,1,0:T(8,128)(2,1)S(1)}, u32[]{:S(2)}, u32[]{:S(2)}) collective-permute-start(bf16[4,32,384]{2,1,0:T(8,128)(2,1)S(1)} %slice.35), channel_id=1, source_target_pairs={{0,56},{8,0},{16,8},{24,16},{32,24},{40,32},{48,40},{56,48},{1,57}... | collective-permute-start | bytes 294920 | tf_op jit(solution)/shard_map/ppermute | solution.py:18
  107.4 5.1 %collective-permute-start.11 = (bf16[4,32,384]{2,1,0:T(8,128)(2,1)S(1)}, bf16[4,32,384]{2,1,0:T(8,128)(2,1)S(1)}, u32[]{:S(2)}, u32[]{:S(2)}) collective-permute-start(bf16[4,32,384]{2,1,0:T(8,128)(2,1)S(1)} %slice.33), channel_id=1, source_target_pairs={{0,448},{64,0},{128,64},{192,128},{256,192},{320,256},{384,320},{4... | collective-permute-start | bytes 294920 | tf_op jit(solution)/shard_map/ppermute | solution.py:18
  114.8 2.4 %constant_dynamic-update-slice_fusion.3 = bf16[192,6144]{1,0:T(8,128)(2,1)} fusion(bf16[192,6144]{1,0:T(8,128)(2,1)} %constant_dynamic-update-slice_fusion.4, bf16[96,6144]{1,0:T(8,128)(2,1)} %collective-permute-done.3), kind=kLoop, calls=%fused_computation.55 | loop fusion | bytes 2359296 | tf_op jit(solution)/shard_map/concatenate | solution.py:53
  117.1 2.4 %fusion.11 = f32[192,384]{1,0:T(8,128)} fusion(bf16[2048,384]{1,0:T(8,128)(2,1)S(1)} %bitcast.66, bf16[192,6144]{1,0:T(8,128)(2,1)} %constant_dynamic-update-slice_fusion.3), kind=kOutput, calls=%fused_computation.18 | convolution fusion | flops 301989888 | bytes 2654208 | tf_op jit(solution)/shard_map/dot_general | solution.py:99
  119.6 2.4 %fusion.6 = f32[192,384]{1,0:T(8,128)} fusion(bf16[2048,384]{1,0:T(8,128)(2,1)S(1)} %bitcast.67, bf16[192,6144]{1,0:T(8,128)(2,1)} %constant_dynamic-update-slice_fusion.3), kind=kOutput, calls=%fused_computation.13 | convolution fusion | flops 301989888 | bytes 2654208 | tf_op jit(solution)/shard_map/dot_general | solution.py:83
  123.7 2.2 %fusion.9 = f32[192,384]{1,0:T(8,128)S(1)} fusion(bf16[2048,384]{1,0:T(8,128)(2,1)} %all-gather.2.cloned.1.call-done, bf16[192,6144]{1,0:T(8,128)(2,1)} %constant_dynamic-update-slice_fusion.3), kind=kOutput, calls=%fused_computation.16 | convolution fusion | flops 301989888 | bytes 2654208 | tf_op jit(solution)/shard_map/dot_general | solution.py:92
  127.7 4.2 %fusion.16 = f32[192,2048]{1,0:T(8,128)} fusion(bf16[2048,384]{1,0:T(8,128)(2,1)} %all-gather.2.cloned.1.call-done, f32[192,384]{1,0:T(8,128)} %fusion.11, bf16[2048,384]{1,0:T(8,128)(2,1)S(1)} %bitcast.65, bf16[192,6144]{1,0:T(8,128)(2,1)} %constant_dynamic-update-slice_fusion.3), kind=kOutput, calls=%fused_computation.43 | convolution fusion | flops 604422144 | bytes 5799936 | tf_op jit(solution)/shard_map/dot_general | solution.py:66
  131.8 2.1 %fusion.3 = bf16[96,4096]{1,0:T(8,128)(2,1)} fusion(f32[192,2048]{1,0:T(8,128)S(1)} %convolution_add_fusion, f32[192,2048]{1,0:T(8,128)} %fusion.16), kind=kLoop, calls=%fused_computation.9 | loop fusion | flops 1572864 | bytes 3932160 | tf_op jit(solution)/shard_map/convert
  135.9 3.1 %convolution_convert_fusion = bf16[2048,384]{1,0:T(8,128)(2,1)} fusion(bf16[192,6144]{1,0:T(8,128)(2,1)} %constant_dynamic-update-slice_fusion.3, f32[192,384]{1,0:T(8,128)S(1)} %copy-done.2, f32[192,384]{1,0:T(8,128)S(1)} %fusion.4), kind=kOutput, calls=%fused_computation.3 | convolution fusion | flops 303218688 | bytes 2949120 | tf_op jit(solution)/shard_map/dot_general | solution.py:87
  139.0 11.2 %all-to-all-start.2 = ((bf16[64,32,384]{2,1,0:T(8,128)(2,1)}), bf16[64,32,384]{2,1,0:T(8,128)(2,1)}, u32[]{:S(2)}, u32[]{:S(2)}) async-start(bf16[64,32,384]{2,1,0:T(8,128)(2,1)} %bitcast.69), calls=%async_computation.2 | async-start | bytes 3145728 | tf_op jit(solution)/shard_map/all_to_all | solution.py:90
  151.5 3.8 %collective-permute-start.23 = (bf16[24,4096]{1,0:T(8,128)(2,1)S(1)}, bf16[24,4096]{1,0:T(8,128)(2,1)S(1)}, u32[]{:S(2)}, u32[]{:S(2)}) collective-permute-start(bf16[24,4096]{1,0:T(8,128)(2,1)S(1)} %get-tuple-element.4), channel_id=1, source_target_pairs={{0,4},{2,6},{4,0},{6,2},{1,5},{3,7},{5,1},{7,3},{8,12},{10,14},{12... | collective-permute-start | bytes 589832 | tf_op jit(solution)/shard_map/ppermute | solution.py:18
  155.3 2.6 %collective-permute-start.22 = (bf16[24,4096]{1,0:T(8,128)(2,1)S(1)}, bf16[24,4096]{1,0:T(8,128)(2,1)S(1)}, u32[]{:S(2)}, u32[]{:S(2)}) collective-permute-start(bf16[24,4096]{1,0:T(8,128)(2,1)S(1)} %get-tuple-element.5), channel_id=1, source_target_pairs={{0,2},{2,4},{4,6},{6,0},{1,3},{3,5},{5,7},{7,1},{8,10},{10,12},{12... | collective-permute-start | bytes 589832 | tf_op jit(solution)/shard_map/ppermute | solution.py:18
  157.9 4.5 %collective-permute-start.21 = (bf16[24,4096]{1,0:T(8,128)(2,1)S(1)}, bf16[24,4096]{1,0:T(8,128)(2,1)S(1)}, u32[]{:S(2)}, u32[]{:S(2)}) collective-permute-start(bf16[24,4096]{1,0:T(8,128)(2,1)S(1)} %get-tuple-element.3), channel_id=1, source_target_pairs={{0,6},{2,0},{4,2},{6,4},{1,7},{3,1},{5,3},{7,5},{8,14},{10,8},{12,... | collective-permute-start | bytes 589832 | tf_op jit(solution)/shard_map/ppermute | solution.py:18
  162.9 3.2 %collective-permute-done.22 = bf16[24,4096]{1,0:T(8,128)(2,1)S(1)} collective-permute-done((bf16[24,4096]{1,0:T(8,128)(2,1)S(1)}, bf16[24,4096]{1,0:T(8,128)(2,1)S(1)}, u32[]{:S(2)}, u32[]{:S(2)}) %collective-permute-start.22) | collective-permute-done | bytes 196640 | tf_op jit(solution)/shard_map/ppermute | solution.py:18
  166.9 24.8 %all-to-all-done.2 = bf16[64,32,384]{2,1,0:T(8,128)(2,1)} async-done(((bf16[64,32,384]{2,1,0:T(8,128)(2,1)}), bf16[64,32,384]{2,1,0:T(8,128)(2,1)}, u32[]{:S(2)}, u32[]{:S(2)}) %all-to-all-start.2) | async-done | bytes 1572896 | tf_op jit(solution)/shard_map/all_to_all | solution.py:90
  (84 shorter events, 34.6 us)
Async XLA Ops:
  7.2 116.5 %all-gather.2.cloned.1.call-start = ((), (), s32[]{:S(2)}) async-start(), calls=%async_computation.3 | async-start | bytes 1597440 | tf_op jit(solution)/shard_map/all_gather | solution.py:73
  11.9 22.6 %collective-permute-start = (bf16[24,6144]{1,0:T(8,128)(2,1)S(1)}, bf16[24,6144]{1,0:T(8,128)(2,1)S(1)}, u32[]{:S(2)}, u32[]{:S(2)}) collective-permute-start(bf16[24,6144]{1,0:T(8,128)(2,1)S(1)} %get-tuple-element.8), channel_id=1, source_target_pairs={{0,2},{2,4},{4,6},{6,0},{1,3},{3,5},{5,7},{7,1},{8,10},{10,12},{12... | collective-permute-start | bytes 884744 | tf_op jit(solution)/shard_map/ppermute | solution.py:18
  15.3 19.2 %collective-permute-start.1 = (bf16[24,6144]{1,0:T(8,128)(2,1)S(1)}, bf16[24,6144]{1,0:T(8,128)(2,1)S(1)}, u32[]{:S(2)}, u32[]{:S(2)}) collective-permute-start(bf16[24,6144]{1,0:T(8,128)(2,1)S(1)} %get-tuple-element.8), channel_id=1, source_target_pairs={{0,6},{2,0},{4,2},{6,4},{1,7},{3,1},{5,3},{7,5},{8,14},{10,8},{12,... | collective-permute-start | bytes 884744 | tf_op jit(solution)/shard_map/ppermute | solution.py:18
  18.9 15.5 %collective-permute-start.2 = (bf16[24,6144]{1,0:T(8,128)(2,1)S(1)}, bf16[24,6144]{1,0:T(8,128)(2,1)S(1)}, u32[]{:S(2)}, u32[]{:S(2)}) collective-permute-start(bf16[24,6144]{1,0:T(8,128)(2,1)S(1)} %get-tuple-element.8), channel_id=1, source_target_pairs={{0,4},{2,6},{4,0},{6,2},{1,5},{3,7},{5,1},{7,3},{8,12},{10,14},{12... | collective-permute-start | bytes 884744 | tf_op jit(solution)/shard_map/ppermute | solution.py:18
  24.1 20.1 %all-to-all-start.1 = ((bf16[8,32,384]{2,1,0:T(8,128)(2,1)}), bf16[8,32,384]{2,1,0:T(8,128)(2,1)S(1)}, u32[]{:S(2)}, u32[]{:S(2)}) async-start(bf16[8,32,384]{2,1,0:T(8,128)(2,1)} %broadcast_in_dim.70), calls=%async_computation.1 | async-start | bytes 393216 | tf_op jit(solution)/shard_map/all_to_all | solution.py:23
  34.5 9.8 %copy-start.4 = (bf16[32,384]{1,0:T(8,128)(2,1)S(1)}, bf16[32,384]{1,0:T(8,128)(2,1)}, u32[]{:S(2)}) copy-start(bf16[32,384]{1,0:T(8,128)(2,1)} %param.10) | copy-start | bytes 73732
  35.6 79.2 %collective-permute-start.3 = (bf16[96,6144]{1,0:T(8,128)(2,1)}, bf16[96,6144]{1,0:T(8,128)(2,1)}, u32[]{:S(2)}, u32[]{:S(2)}) collective-permute-start(bf16[96,6144]{1,0:T(8,128)(2,1)} %pad_maximum_fusion.1), channel_id=1, source_target_pairs={{0,1},{1,0},{2,3},{3,2},{4,5},{5,4},{6,7},{7,6},{8,9},{9,8},{10,11... | collective-permute-start | bytes 3538952 | tf_op jit(solution)/shard_map/ppermute | solution.py:18
  44.9 15.8 %all-to-all-start = ((bf16[8,32,384]{2,1,0:T(8,128)(2,1)}), bf16[8,32,384]{2,1,0:T(8,128)(2,1)S(1)}, u32[]{:S(2)}, u32[]{:S(2)}) async-start(bf16[8,32,384]{2,1,0:T(8,128)(2,1)} %broadcast_in_dim.60), calls=%async_computation | async-start | bytes 393216 | tf_op jit(solution)/shard_map/all_to_all | solution.py:23
  53.2 15.0 %collective-permute-start.12 = (bf16[8,32,384]{2,1,0:T(8,128)(2,1)S(1)}, bf16[8,32,384]{2,1,0:T(8,128)(2,1)}, u32[]{:S(2)}, u32[]{:S(2)}) collective-permute-start(bf16[8,32,384]{2,1,0:T(8,128)(2,1)S(1)} %all-to-all-done.1), channel_id=1, source_target_pairs={{0,8},{8,16},{16,24},{24,32},{32,40},{40,48},{48,56},{56,0},{1,9},... | collective-permute-start | bytes 589832 | tf_op jit(solution)/shard_map/ppermute | solution.py:18
  56.6 15.3 %collective-permute-start.13 = (bf16[8,32,384]{2,1,0:T(8,128)(2,1)S(1)}, bf16[8,32,384]{2,1,0:T(8,128)(2,1)}, u32[]{:S(2)}, u32[]{:S(2)}) collective-permute-start(bf16[8,32,384]{2,1,0:T(8,128)(2,1)S(1)} %all-to-all-done.1), channel_id=1, source_target_pairs={{0,56},{8,0},{16,8},{24,16},{32,24},{40,32},{48,40},{56,48},{1,57}... | collective-permute-start | bytes 589832 | tf_op jit(solution)/shard_map/ppermute | solution.py:18
  60.7 14.1 %collective-permute-start.4 = (bf16[8,32,384]{2,1,0:T(8,128)(2,1)S(1)}, bf16[8,32,384]{2,1,0:T(8,128)(2,1)S(1)}, u32[]{:S(2)}, u32[]{:S(2)}) collective-permute-start(bf16[8,32,384]{2,1,0:T(8,128)(2,1)S(1)} %all-to-all-done), channel_id=1, source_target_pairs={{0,64},{64,128},{128,192},{192,256},{256,320},{320,384},{384,448},... | collective-permute-start | bytes 589832 | tf_op jit(solution)/shard_map/ppermute | solution.py:18
  63.5 13.3 %collective-permute-start.5 = (bf16[8,32,384]{2,1,0:T(8,128)(2,1)S(1)}, bf16[8,32,384]{2,1,0:T(8,128)(2,1)S(1)}, u32[]{:S(2)}, u32[]{:S(2)}) collective-permute-start(bf16[8,32,384]{2,1,0:T(8,128)(2,1)S(1)} %all-to-all-done), channel_id=1, source_target_pairs={{0,448},{64,0},{128,64},{192,128},{256,192},{320,256},{384,320},{4... | collective-permute-start | bytes 589832 | tf_op jit(solution)/shard_map/ppermute | solution.py:18
  68.2 15.7 %collective-permute-start.14 = (bf16[8,32,384]{2,1,0:T(8,128)(2,1)}, bf16[8,32,384]{2,1,0:T(8,128)(2,1)S(1)}, u32[]{:S(2)}, u32[]{:S(2)}) collective-permute-start(bf16[8,32,384]{2,1,0:T(8,128)(2,1)} %collective-permute-done.12), channel_id=1, source_target_pairs={{0,8},{8,16},{16,24},{24,32},{32,40},{40,48},{48,56},{56,0},{1,9},... | collective-permute-start | bytes 589832 | tf_op jit(solution)/shard_map/ppermute | solution.py:18
  71.9 15.0 %collective-permute-start.15 = (bf16[8,32,384]{2,1,0:T(8,128)(2,1)}, bf16[8,32,384]{2,1,0:T(8,128)(2,1)S(1)}, u32[]{:S(2)}, u32[]{:S(2)}) collective-permute-start(bf16[8,32,384]{2,1,0:T(8,128)(2,1)} %collective-permute-done.13), channel_id=1, source_target_pairs={{0,56},{8,0},{16,8},{24,16},{32,24},{40,32},{48,40},{56,48},{1,57}... | collective-permute-start | bytes 589832 | tf_op jit(solution)/shard_map/ppermute | solution.py:18
  74.8 16.2 %collective-permute-start.6 = (bf16[8,32,384]{2,1,0:T(8,128)(2,1)S(1)}, bf16[8,32,384]{2,1,0:T(8,128)(2,1)S(1)}, u32[]{:S(2)}, u32[]{:S(2)}) collective-permute-start(bf16[8,32,384]{2,1,0:T(8,128)(2,1)S(1)} %collective-permute-done.4), channel_id=1, source_target_pairs={{0,64},{64,128},{128,192},{192,256},{256,320},{320,384},{384,448},... | collective-permute-start | bytes 589832 | tf_op jit(solution)/shard_map/ppermute | solution.py:18
  76.8 16.2 %collective-permute-start.7 = (bf16[8,32,384]{2,1,0:T(8,128)(2,1)S(1)}, bf16[8,32,384]{2,1,0:T(8,128)(2,1)S(1)}, u32[]{:S(2)}, u32[]{:S(2)}) collective-permute-start(bf16[8,32,384]{2,1,0:T(8,128)(2,1)S(1)} %collective-permute-done.5), channel_id=1, source_target_pairs={{0,448},{64,0},{128,64},{192,128},{256,192},{320,256},{384,320},{4... | collective-permute-start | bytes 589832 | tf_op jit(solution)/shard_map/ppermute | solution.py:18
  83.9 14.4 %collective-permute-start.16 = (bf16[8,32,384]{2,1,0:T(8,128)(2,1)S(1)}, bf16[8,32,384]{2,1,0:T(8,128)(2,1)S(1)}, u32[]{:S(2)}, u32[]{:S(2)}) collective-permute-start(bf16[8,32,384]{2,1,0:T(8,128)(2,1)S(1)} %collective-permute-done.14), channel_id=1, source_target_pairs={{0,8},{8,16},{16,24},{24,32},{32,40},{40,48},{48,56},{56,0},{1,9},... | collective-permute-start | bytes 589832 | tf_op jit(solution)/shard_map/ppermute | solution.py:18
  86.9 13.3 %collective-permute-start.17 = (bf16[8,32,384]{2,1,0:T(8,128)(2,1)S(1)}, bf16[8,32,384]{2,1,0:T(8,128)(2,1)S(1)}, u32[]{:S(2)}, u32[]{:S(2)}) collective-permute-start(bf16[8,32,384]{2,1,0:T(8,128)(2,1)S(1)} %collective-permute-done.15), channel_id=1, source_target_pairs={{0,56},{8,0},{16,8},{24,16},{32,24},{40,32},{48,40},{56,48},{1,57}... | collective-permute-start | bytes 589832 | tf_op jit(solution)/shard_map/ppermute | solution.py:18
  91.0 14.4 %collective-permute-start.8 = (bf16[8,32,384]{2,1,0:T(8,128)(2,1)S(1)}, bf16[8,32,384]{2,1,0:T(8,128)(2,1)S(1)}, u32[]{:S(2)}, u32[]{:S(2)}) collective-permute-start(bf16[8,32,384]{2,1,0:T(8,128)(2,1)S(1)} %collective-permute-done.6), channel_id=1, source_target_pairs={{0,64},{64,128},{128,192},{192,256},{256,320},{320,384},{384,448},... | collective-permute-start | bytes 589832 | tf_op jit(solution)/shard_map/ppermute | solution.py:18
  93.0 14.4 %collective-permute-start.9 = (bf16[8,32,384]{2,1,0:T(8,128)(2,1)S(1)}, bf16[8,32,384]{2,1,0:T(8,128)(2,1)S(1)}, u32[]{:S(2)}, u32[]{:S(2)}) collective-permute-start(bf16[8,32,384]{2,1,0:T(8,128)(2,1)S(1)} %collective-permute-done.7), channel_id=1, source_target_pairs={{0,448},{64,0},{128,64},{192,128},{256,192},{320,256},{384,320},{4... | collective-permute-start | bytes 589832 | tf_op jit(solution)/shard_map/ppermute | solution.py:18
  98.3 14.4 %collective-permute-start.18 = (bf16[4,32,384]{2,1,0:T(8,128)(2,1)S(1)}, bf16[4,32,384]{2,1,0:T(8,128)(2,1)S(1)}, u32[]{:S(2)}, u32[]{:S(2)}) collective-permute-start(bf16[4,32,384]{2,1,0:T(8,128)(2,1)S(1)} %slice.34), channel_id=1, source_target_pairs={{0,8},{8,16},{16,24},{24,32},{32,40},{40,48},{48,56},{56,0},{1,9},... | collective-permute-start | bytes 294920 | tf_op jit(solution)/shard_map/ppermute | solution.py:18
  100.3 12.5 %collective-permute-start.19 = (bf16[4,32,384]{2,1,0:T(8,128)(2,1)S(1)}, bf16[4,32,384]{2,1,0:T(8,128)(2,1)S(1)}, u32[]{:S(2)}, u32[]{:S(2)}) collective-permute-start(bf16[4,32,384]{2,1,0:T(8,128)(2,1)S(1)} %slice.35), channel_id=1, source_target_pairs={{0,56},{8,0},{16,8},{24,16},{32,24},{40,32},{48,40},{56,48},{1,57}... | collective-permute-start | bytes 294920 | tf_op jit(solution)/shard_map/ppermute | solution.py:18
  105.5 7.7 %collective-permute-start.10 = (bf16[4,32,384]{2,1,0:T(8,128)(2,1)S(1)}, bf16[4,32,384]{2,1,0:T(8,128)(2,1)S(1)}, u32[]{:S(2)}, u32[]{:S(2)}) collective-permute-start(bf16[4,32,384]{2,1,0:T(8,128)(2,1)S(1)} %slice.32), channel_id=1, source_target_pairs={{0,64},{64,128},{128,192},{192,256},{256,320},{320,384},{384,448},... | collective-permute-start | bytes 294920 | tf_op jit(solution)/shard_map/ppermute | solution.py:18
  107.4 7.3 %collective-permute-start.11 = (bf16[4,32,384]{2,1,0:T(8,128)(2,1)S(1)}, bf16[4,32,384]{2,1,0:T(8,128)(2,1)S(1)}, u32[]{:S(2)}, u32[]{:S(2)}) collective-permute-start(bf16[4,32,384]{2,1,0:T(8,128)(2,1)S(1)} %slice.33), channel_id=1, source_target_pairs={{0,448},{64,0},{128,64},{192,128},{256,192},{320,256},{384,320},{4... | collective-permute-start | bytes 294920 | tf_op jit(solution)/shard_map/ppermute | solution.py:18
  131.8 4.1 %copy-start.2 = (f32[192,384]{1,0:T(8,128)S(1)}, f32[192,384]{1,0:T(8,128)}, u32[]{:S(2)}) copy-start(f32[192,384]{1,0:T(8,128)} %fusion.6) | copy-start | bytes 884740
  134.0 16.2 %collective-permute-start.20 = (bf16[96,4096]{1,0:T(8,128)(2,1)}, bf16[96,4096]{1,0:T(8,128)(2,1)}, u32[]{:S(2)}, u32[]{:S(2)}) collective-permute-start(bf16[96,4096]{1,0:T(8,128)(2,1)} %fusion.3), channel_id=1, source_target_pairs={{0,1},{1,0},{2,3},{3,2},{4,5},{5,4},{6,7},{7,6},{8,9},{9,8},{10,11... | collective-permute-start | bytes 2359304 | tf_op jit(solution)/shard_map/ppermute | solution.py:18
  139.0 11.2 %copy-start = (f32[192,2048]{1,0:T(8,128)S(1)}, f32[192,2048]{1,0:T(8,128)}, u32[]{:S(2)}) copy-start(f32[192,2048]{1,0:T(8,128)} %fusion.16) | copy-start | bytes 4718596
  139.0 52.7 %all-to-all-start.2 = ((bf16[64,32,384]{2,1,0:T(8,128)(2,1)}), bf16[64,32,384]{2,1,0:T(8,128)(2,1)}, u32[]{:S(2)}, u32[]{:S(2)}) async-start(bf16[64,32,384]{2,1,0:T(8,128)(2,1)} %bitcast.69), calls=%async_computation.2 | async-start | bytes 3145728 | tf_op jit(solution)/shard_map/all_to_all | solution.py:90
  151.5 41.8 %copy-start.3 = (f32[32,384]{1,0:T(8,128)S(1)}, f32[32,384]{1,0:T(8,128)}, u32[]{:S(2)}) copy-start(f32[32,384]{1,0:T(8,128)} %param.13) | copy-start | bytes 147460
  151.5 11.3 %collective-permute-start.23 = (bf16[24,4096]{1,0:T(8,128)(2,1)S(1)}, bf16[24,4096]{1,0:T(8,128)(2,1)S(1)}, u32[]{:S(2)}, u32[]{:S(2)}) collective-permute-start(bf16[24,4096]{1,0:T(8,128)(2,1)S(1)} %get-tuple-element.4), channel_id=1, source_target_pairs={{0,4},{2,6},{4,0},{6,2},{1,5},{3,7},{5,1},{7,3},{8,12},{10,14},{12... | collective-permute-start | bytes 589832 | tf_op jit(solution)/shard_map/ppermute | solution.py:18
  155.3 10.7 %collective-permute-start.22 = (bf16[24,4096]{1,0:T(8,128)(2,1)S(1)}, bf16[24,4096]{1,0:T(8,128)(2,1)S(1)}, u32[]{:S(2)}, u32[]{:S(2)}) collective-permute-start(bf16[24,4096]{1,0:T(8,128)(2,1)S(1)} %get-tuple-element.5), channel_id=1, source_target_pairs={{0,2},{2,4},{4,6},{6,0},{1,3},{3,5},{5,7},{7,1},{8,10},{10,12},{12... | collective-permute-start | bytes 589832 | tf_op jit(solution)/shard_map/ppermute | solution.py:18
  157.9 8.1 %collective-permute-start.21 = (bf16[24,4096]{1,0:T(8,128)(2,1)S(1)}, bf16[24,4096]{1,0:T(8,128)(2,1)S(1)}, u32[]{:S(2)}, u32[]{:S(2)}) collective-permute-start(bf16[24,4096]{1,0:T(8,128)(2,1)S(1)} %get-tuple-element.3), channel_id=1, source_target_pairs={{0,6},{2,0},{4,2},{6,4},{1,7},{3,1},{5,3},{7,5},{8,14},{10,8},{12,... | collective-permute-start | bytes 589832 | tf_op jit(solution)/shard_map/ppermute | solution.py:18
  (1 other events, 1.0 us)
Sparse Core Ops, SparseCore 0:
  22.8 86.5 all-gather.1

commit v3 on v0

--- a/solution.py
+++ b/solution.py
@@ -23,10 +23,6 @@
     return lax.all_to_all(jnp.broadcast_to(value, (count, *value.shape)), axis, 0, 0)
 
 
-def after(value, *others):
-    return lax.optimization_barrier((value, *others))[0]
-
-
 def gather_down(down):
     line = spread(down, "z")
     count = lax.axis_size("y")
@@ -50,7 +46,8 @@
 
 def collect_tokens(own):
     line = jnp.concatenate([shift(own, "x", step) for step in STEPS], axis=0)
-    return jnp.concatenate([line, shift(line, "c", 1)], axis=0)
+    other = shift(line, "c", 1)
+    return jnp.concatenate([line, other], axis=0)
 
 
 def give_rows(partial, rows):
@@ -74,9 +71,10 @@
     line = line.reshape(-1, line.shape[-1])
     whole = lax.all_gather(line, "z", axis=0, tiled=True)
     gate_whole, up_whole = jnp.split(whole, 2, axis=1)
-    tokens = collect_tokens(jnp.concatenate([later, early, cotangent], axis=1))
+    tokens = jnp.concatenate([later, early, cotangent], axis=1)
+    tokens = collect_tokens(tokens)
     later_rows, early_rows, grad_rows = jnp.split(tokens, 3, axis=1)
-    down_whole = gather_down(after(down_w, line))
+    down_whole = gather_down(down_w)
 
     gate_early = jnp.dot(early_rows, gate_whole, preferred_element_type=F32)
     up_early = jnp.dot(early_rows, up_whole, preferred_element_type=F32)

time: 184 us -> 173 us (0.940)
  waiting for transfers between devices: 57.5 us -> 43.2 us
  starting transfers between devices: 79.2 us -> 81.8 us
    all_to_all x2, waiting for transfers between devices: 14.5 us -> 6.58 us  [spread(): lax.all_to_all(jnp.broadcast_to(value, (count, *value.shape)), axis, 0, 0)]
    ppermute x16, waiting for transfers between devices: 19.3 us -> 11.8 us  [shift(): lax.ppermute(value, axis, [(i, (i + step) % count) for i in range(count)])]
    all_to_all x1, starting transfers between devices: 8.75 us -> 11.5 us  [shards(): received = lax.all_to_all(down_grad.reshape(-1, *gate_w.shape), FS, 0, 0)]
    unnamed x29 -> x25, local copies, waits for them, and re-layouts: 7 us -> 5.09 us
  transfers between devices with their start and end apart: 20 -> 20, of which waited for: 12 -> 11; matrix products, arithmetic and copies ran while one was open for 7% -> 10% of each run, Pallas kernels for 0% -> 0%
where the time goes in v3:
time: 173 us; the launch traced here: 172 us
  starting transfers between devices  81.8 us (47%)
  waiting for transfers between devices  43.2 us (25%)
  matrix products  16.3 us (9%)
  between operations  14.5 us (8%)
  local copies, waits for them, and re-layouts  11.4 us (7%)
  other arithmetic  4.35 us (3%)
    ppermute x16, starting transfers between devices, shift(): lax.ppermute(value, axis, [(i, (i + step) % count) for i in range(count)])  52.8 us
    all_to_all x1, waiting for transfers between devices, shards(): received = lax.all_to_all(down_grad.reshape(-1, *gate_w.shape), FS, 0, 0)  23.6 us
    all_to_all x2, starting transfers between devices, spread(): lax.all_to_all(jnp.broadcast_to(value, (count, *value.shape)), axis, 0, 0)  17.4 us
    ppermute x16, waiting for transfers between devices, shift(): lax.ppermute(value, axis, [(i, (i + step) % count) for i in range(count)])  11.8 us
    all_to_all x1, starting transfers between devices, shards(): received = lax.all_to_all(down_grad.reshape(-1, *gate_w.shape), FS, 0, 0)  11.5 us
    all_to_all x2, waiting for transfers between devices, spread(): lax.all_to_all(jnp.broadcast_to(value, (count, *value.shape)), axis, 0, 0)  6.58 us
    unnamed x25, local copies, waits for them, and re-layouts  5.09 us
    dot_general x3, matrix products, contract_last(): lax.dot_general(leading, trailing, (((1,), (1,)), ((), ())), preferred_el...  4.91 us
  transfers between devices with their start and end apart: 20, of which 11 were waited for; matrix products, arithmetic and copies ran while one was open for 10% of the time, Pallas kernels for 0%

profile of v3, /device:TPU:2, one launch (start us, length us, event | category | flops | bytes accessed | tf_op | source)
XLA Modules:
  0.0 171.5 jit_solution(4027197504188091380)
XLA Ops:
  8.8 7.1 %all-to-all-start = ((bf16[8,32,768]{2,1,0:T(8,128)(2,1)}), bf16[8,32,768]{2,1,0:T(8,128)(2,1)S(1)}, u32[]{:S(2)}, u32[]{:S(2)}) async-start(bf16[8,32,768]{2,1,0:T(8,128)(2,1)} %broadcast_in_dim.36), calls=%async_computation | async-start | bytes 786432 | tf_op jit(solution)/shard_map/all_to_all | solution.py:23
  18.7 3.4 %collective-permute-start = (bf16[24,6144]{1,0:T(8,128)(2,1)S(1)}, bf16[24,6144]{1,0:T(8,128)(2,1)S(1)}, u32[]{:S(2)}, u32[]{:S(2)}) collective-permute-start(bf16[24,6144]{1,0:T(8,128)(2,1)S(1)} %get-tuple-element.8), channel_id=1, source_target_pairs={{0,2},{2,4},{4,6},{6,0},{1,3},{3,5},{5,7},{7,1},{8,10},{10,12},{12... | collective-permute-start | bytes 884744 | tf_op jit(solution)/shard_map/ppermute | solution.py:18
  22.1 2.7 %collective-permute-start.1 = (bf16[24,6144]{1,0:T(8,128)(2,1)S(1)}, bf16[24,6144]{1,0:T(8,128)(2,1)S(1)}, u32[]{:S(2)}, u32[]{:S(2)}) collective-permute-start(bf16[24,6144]{1,0:T(8,128)(2,1)S(1)} %get-tuple-element.8), channel_id=1, source_target_pairs={{0,6},{2,0},{4,2},{6,4},{1,7},{3,1},{5,3},{7,5},{8,14},{10,8},{12,... | collective-permute-start | bytes 884744 | tf_op jit(solution)/shard_map/ppermute | solution.py:18
  24.8 4.0 %collective-permute-start.2 = (bf16[24,6144]{1,0:T(8,128)(2,1)S(1)}, bf16[24,6144]{1,0:T(8,128)(2,1)S(1)}, u32[]{:S(2)}, u32[]{:S(2)}) collective-permute-start(bf16[24,6144]{1,0:T(8,128)(2,1)S(1)} %get-tuple-element.8), channel_id=1, source_target_pairs={{0,4},{2,6},{4,0},{6,2},{1,5},{3,7},{5,1},{7,3},{8,12},{10,14},{12... | collective-permute-start | bytes 884744 | tf_op jit(solution)/shard_map/ppermute | solution.py:18
  28.8 1.8 %all-to-all-done = bf16[8,32,768]{2,1,0:T(8,128)(2,1)S(1)} async-done(((bf16[8,32,768]{2,1,0:T(8,128)(2,1)}), bf16[8,32,768]{2,1,0:T(8,128)(2,1)S(1)}, u32[]{:S(2)}, u32[]{:S(2)}) %all-to-all-start) | async-done | bytes 393248 | tf_op jit(solution)/shard_map/all_to_all | solution.py:23
  31.3 10.3 %all-to-all-start.1 = ((bf16[8,32,384]{2,1,0:T(8,128)(2,1)}), bf16[8,32,384]{2,1,0:T(8,128)(2,1)S(1)}, u32[]{:S(2)}, u32[]{:S(2)}) async-start(bf16[8,32,384]{2,1,0:T(8,128)(2,1)} %broadcast_in_dim.38), calls=%async_computation.1 | async-start | bytes 393216 | tf_op jit(solution)/shard_map/all_to_all | solution.py:23
  42.5 1.9 %collective-permute-start.3 = (bf16[96,6144]{1,0:T(8,128)(2,1)S(1)}, bf16[96,6144]{1,0:T(8,128)(2,1)}, u32[]{:S(2)}, u32[]{:S(2)}) collective-permute-start(bf16[96,6144]{1,0:T(8,128)(2,1)S(1)} %pad_maximum_fusion.1), channel_id=1, source_target_pairs={{0,1},{1,0},{2,3},{3,2},{4,5},{5,4},{6,7},{7,6},{8,9},{9,8},{10,11... | collective-permute-start | bytes 3538952 | tf_op jit(solution)/shard_map/ppermute | solution.py:18
  46.6 4.8 %all-to-all-done.1 = bf16[8,32,384]{2,1,0:T(8,128)(2,1)S(1)} async-done(((bf16[8,32,384]{2,1,0:T(8,128)(2,1)}), bf16[8,32,384]{2,1,0:T(8,128)(2,1)S(1)}, u32[]{:S(2)}, u32[]{:S(2)}) %all-to-all-start.1) | async-done | bytes 196640 | tf_op jit(solution)/shard_map/all_to_all | solution.py:23
  51.4 2.5 %collective-permute-start.4 = (bf16[8,32,384]{2,1,0:T(8,128)(2,1)S(1)}, bf16[8,32,384]{2,1,0:T(8,128)(2,1)S(1)}, u32[]{:S(2)}, u32[]{:S(2)}) collective-permute-start(bf16[8,32,384]{2,1,0:T(8,128)(2,1)S(1)} %all-to-all-done.1), channel_id=1, source_target_pairs={{0,8},{8,16},{16,24},{24,32},{32,40},{40,48},{48,56},{56,0},{1,9},... | collective-permute-start | bytes 589832 | tf_op jit(solution)/shard_map/ppermute | solution.py:18
  53.9 4.6 %collective-permute-start.5 = (bf16[8,32,384]{2,1,0:T(8,128)(2,1)S(1)}, bf16[8,32,384]{2,1,0:T(8,128)(2,1)S(1)}, u32[]{:S(2)}, u32[]{:S(2)}) collective-permute-start(bf16[8,32,384]{2,1,0:T(8,128)(2,1)S(1)} %all-to-all-done.1), channel_id=1, source_target_pairs={{0,56},{8,0},{16,8},{24,16},{32,24},{40,32},{48,40},{56,48},{1,57}... | collective-permute-start | bytes 589832 | tf_op jit(solution)/shard_map/ppermute | solution.py:18
  60.2 1.9 %collective-permute-start.6 = (bf16[8,32,384]{2,1,0:T(8,128)(2,1)S(1)}, bf16[8,32,384]{2,1,0:T(8,128)(2,1)S(1)}, u32[]{:S(2)}, u32[]{:S(2)}) collective-permute-start(bf16[8,32,384]{2,1,0:T(8,128)(2,1)S(1)} %collective-permute-done.4), channel_id=1, source_target_pairs={{0,8},{8,16},{16,24},{24,32},{32,40},{40,48},{48,56},{56,0},{1,9},... | collective-permute-start | bytes 589832 | tf_op jit(solution)/shard_map/ppermute | solution.py:18
  62.1 5.1 %collective-permute-start.7 = (bf16[8,32,384]{2,1,0:T(8,128)(2,1)S(1)}, bf16[8,32,384]{2,1,0:T(8,128)(2,1)S(1)}, u32[]{:S(2)}, u32[]{:S(2)}) collective-permute-start(bf16[8,32,384]{2,1,0:T(8,128)(2,1)S(1)} %collective-permute-done.5), channel_id=1, source_target_pairs={{0,56},{8,0},{16,8},{24,16},{32,24},{40,32},{48,40},{56,48},{1,57}... | collective-permute-start | bytes 589832 | tf_op jit(solution)/shard_map/ppermute | solution.py:18
  67.3 1.6 collective-permute-done.6
  68.9 1.9 %collective-permute-start.8 = (bf16[8,32,384]{2,1,0:T(8,128)(2,1)S(1)}, bf16[8,32,384]{2,1,0:T(8,128)(2,1)S(1)}, u32[]{:S(2)}, u32[]{:S(2)}) collective-permute-start(bf16[8,32,384]{2,1,0:T(8,128)(2,1)S(1)} %collective-permute-done.6), channel_id=1, source_target_pairs={{0,8},{8,16},{16,24},{24,32},{32,40},{40,48},{48,56},{56,0},{1,9},... | collective-permute-start | bytes 589832 | tf_op jit(solution)/shard_map/ppermute | solution.py:18
  70.9 5.1 %collective-permute-start.9 = (bf16[8,32,384]{2,1,0:T(8,128)(2,1)S(1)}, bf16[8,32,384]{2,1,0:T(8,128)(2,1)S(1)}, u32[]{:S(2)}, u32[]{:S(2)}) collective-permute-start(bf16[8,32,384]{2,1,0:T(8,128)(2,1)S(1)} %collective-permute-done.7), channel_id=1, source_target_pairs={{0,56},{8,0},{16,8},{24,16},{32,24},{40,32},{48,40},{56,48},{1,57}... | collective-permute-start | bytes 589832 | tf_op jit(solution)/shard_map/ppermute | solution.py:18
  77.7 1.9 %collective-permute-start.10 = (bf16[4,32,384]{2,1,0:T(8,128)(2,1)S(1)}, bf16[4,32,384]{2,1,0:T(8,128)(2,1)S(1)}, u32[]{:S(2)}, u32[]{:S(2)}) collective-permute-start(bf16[4,32,384]{2,1,0:T(8,128)(2,1)S(1)} %slice.24), channel_id=1, source_target_pairs={{0,8},{8,16},{16,24},{24,32},{32,40},{40,48},{48,56},{56,0},{1,9},... | collective-permute-start | bytes 294920 | tf_op jit(solution)/shard_map/ppermute | solution.py:18
  79.7 5.1 %collective-permute-start.11 = (bf16[4,32,384]{2,1,0:T(8,128)(2,1)S(1)}, bf16[4,32,384]{2,1,0:T(8,128)(2,1)S(1)}, u32[]{:S(2)}, u32[]{:S(2)}) collective-permute-start(bf16[4,32,384]{2,1,0:T(8,128)(2,1)S(1)} %slice.25), channel_id=1, source_target_pairs={{0,56},{8,0},{16,8},{24,16},{32,24},{40,32},{48,40},{56,48},{1,57}... | collective-permute-start | bytes 294920 | tf_op jit(solution)/shard_map/ppermute | solution.py:18
  87.0 3.0 %constant_dynamic-update-slice_fusion.3 = bf16[192,6144]{1,0:T(8,128)(2,1)} fusion(bf16[192,6144]{1,0:T(8,128)(2,1)} %constant_dynamic-update-slice_fusion.4, bf16[96,6144]{1,0:T(8,128)(2,1)} %collective-permute-done.3), kind=kLoop, calls=%fused_computation.53 | loop fusion | bytes 2359296 | tf_op jit(solution)/shard_map/concatenate | solution.py:50
  90.0 1.7 %fusion.18 = f32[192,384]{1,0:T(8,128)S(1)} fusion(bf16[2048,384]{1,0:T(8,128)(2,1)S(1)} %bitcast.40, bf16[192,6144]{1,0:T(8,128)(2,1)} %constant_dynamic-update-slice_fusion.3), kind=kOutput, calls=%fused_computation.25 | convolution fusion | flops 301989888 | bytes 2654208 | tf_op jit(solution)/shard_map/dot_general | solution.py:89
  92.2 2.4 %fusion.11 = f32[192,384]{1,0:T(8,128)S(1)} fusion(bf16[2048,768]{1,0:T(8,128)(2,1)} %all-gather.2.cloned.1.call-done, bf16[192,6144]{1,0:T(8,128)(2,1)} %constant_dynamic-update-slice_fusion.3), kind=kOutput, calls=%fused_computation.17 | convolution fusion | flops 301989888 | bytes 2654208 | tf_op jit(solution)/shard_map/dot_general | solution.py:79
  94.8 1.7 fusion.5
  96.5 2.5 %fusion.7 = f32[192,384]{1,0:T(8,128)} fusion(bf16[2048,768]{1,0:T(8,128)(2,1)S(1)} %copy-done.1, bf16[192,6144]{1,0:T(8,128)(2,1)} %constant_dynamic-update-slice_fusion.3), kind=kOutput, calls=%fused_computation.13 | convolution fusion | flops 301989888 | bytes 2654208 | tf_op jit(solution)/shard_map/dot_general | solution.py:96
  100.5 3.5 %fusion.23 = f32[192,2048]{1,0:T(8,128)S(1)} fusion(bf16[2048,384]{1,0:T(8,128)(2,1)} %bitcast.41, f32[192,384]{1,0:T(8,128)} %fusion.7, bf16[2048,768]{1,0:T(8,128)(2,1)} %all-gather.2.cloned.1.call-done, bf16[192,6144]{1,0:T(8,128)(2,1)} %constant_dynamic-update-slice_fusion.3), kind=kOutput, calls=%fused_computation.43 | convolution fusion | flops 604422144 | bytes 5799936 | tf_op jit(solution)/shard_map/dot_general | solution.py:63
  105.4 1.9 %collective-permute-start.12 = (bf16[96,4096]{1,0:T(8,128)(2,1)}, bf16[96,4096]{1,0:T(8,128)(2,1)}, u32[]{:S(2)}, u32[]{:S(2)}) collective-permute-start(bf16[96,4096]{1,0:T(8,128)(2,1)} %fusion.3), channel_id=1, source_target_pairs={{0,1},{1,0},{2,3},{3,2},{4,5},{5,4},{6,7},{7,6},{8,9},{9,8},{10,11... | collective-permute-start | bytes 2359304 | tf_op jit(solution)/shard_map/ppermute | solution.py:18
  107.3 3.1 %convolution_convert_fusion = bf16[2048,384]{1,0:T(8,128)(2,1)} fusion(bf16[192,6144]{1,0:T(8,128)(2,1)} %constant_dynamic-update-slice_fusion.3, f32[192,384]{1,0:T(8,128)S(1)} %copy-done.5, f32[192,384]{1,0:T(8,128)S(1)} %fusion.11), kind=kOutput, calls=%fused_computation.3 | convolution fusion | flops 303218688 | bytes 2949120 | tf_op jit(solution)/shard_map/dot_general | solution.py:84
  110.4 11.5 %all-to-all-start.2 = ((bf16[64,32,384]{2,1,0:T(8,128)(2,1)}), bf16[64,32,384]{2,1,0:T(8,128)(2,1)S(1)}, u32[]{:S(2)}, u32[]{:S(2)}) async-start(bf16[64,32,384]{2,1,0:T(8,128)(2,1)} %bitcast.39), calls=%async_computation.2 | async-start | bytes 3145728 | tf_op jit(solution)/shard_map/all_to_all | solution.py:87
  123.5 2.1 %collective-permute-start.13 = (bf16[24,4096]{1,0:T(8,128)(2,1)S(1)}, bf16[24,4096]{1,0:T(8,128)(2,1)S(1)}, u32[]{:S(2)}, u32[]{:S(2)}) collective-permute-start(bf16[24,4096]{1,0:T(8,128)(2,1)S(1)} %get-tuple-element.3), channel_id=1, source_target_pairs={{0,6},{2,0},{4,2},{6,4},{1,7},{3,1},{5,3},{7,5},{8,14},{10,8},{12,... | collective-permute-start | bytes 589832 | tf_op jit(solution)/shard_map/ppermute | solution.py:18
  125.6 3.9 %collective-permute-start.14 = (bf16[24,4096]{1,0:T(8,128)(2,1)S(1)}, bf16[24,4096]{1,0:T(8,128)(2,1)S(1)}, u32[]{:S(2)}, u32[]{:S(2)}) collective-permute-start(bf16[24,4096]{1,0:T(8,128)(2,1)S(1)} %get-tuple-element.5), channel_id=1, source_target_pairs={{0,2},{2,4},{4,6},{6,0},{1,3},{3,5},{5,7},{7,1},{8,10},{10,12},{12... | collective-permute-start | bytes 589832 | tf_op jit(solution)/shard_map/ppermute | solution.py:18
  129.5 4.8 %collective-permute-start.15 = (bf16[24,4096]{1,0:T(8,128)(2,1)S(1)}, bf16[24,4096]{1,0:T(8,128)(2,1)S(1)}, u32[]{:S(2)}, u32[]{:S(2)}) collective-permute-start(bf16[24,4096]{1,0:T(8,128)(2,1)S(1)} %get-tuple-element.4), channel_id=1, source_target_pairs={{0,4},{2,6},{4,0},{6,2},{1,5},{3,7},{5,1},{7,3},{8,12},{10,14},{12... | collective-permute-start | bytes 589832 | tf_op jit(solution)/shard_map/ppermute | solution.py:18
  134.3 1.7 %collective-permute-done.14 = bf16[24,4096]{1,0:T(8,128)(2,1)S(1)} collective-permute-done((bf16[24,4096]{1,0:T(8,128)(2,1)S(1)}, bf16[24,4096]{1,0:T(8,128)(2,1)S(1)}, u32[]{:S(2)}, u32[]{:S(2)}) %collective-permute-start.14) | collective-permute-done | bytes 196640 | tf_op jit(solution)/shard_map/ppermute | solution.py:18
  136.1 3.3 %collective-permute-done.15 = bf16[24,4096]{1,0:T(8,128)(2,1)S(1)} collective-permute-done((bf16[24,4096]{1,0:T(8,128)(2,1)S(1)}, bf16[24,4096]{1,0:T(8,128)(2,1)S(1)}, u32[]{:S(2)}, u32[]{:S(2)}) %collective-permute-start.15) | collective-permute-done | bytes 196640 | tf_op jit(solution)/shard_map/ppermute | solution.py:18
  140.2 23.6 %all-to-all-done.2 = bf16[64,32,384]{2,1,0:T(8,128)(2,1)S(1)} async-done(((bf16[64,32,384]{2,1,0:T(8,128)(2,1)}), bf16[64,32,384]{2,1,0:T(8,128)(2,1)S(1)}, u32[]{:S(2)}, u32[]{:S(2)}) %all-to-all-start.2) | async-done | bytes 1572896 | tf_op jit(solution)/shard_map/all_to_all | solution.py:87
  (67 shorter events, 20.6 us)
Async XLA Ops:
  7.2 10.3 %copy-start.6 = (bf16[24,2048]{1,0:T(8,128)(2,1)S(1)}, bf16[24,2048]{1,0:T(8,128)(2,1)}, u32[]{:S(2)}) copy-start(bf16[24,2048]{1,0:T(8,128)(2,1)} %param.8) | copy-start | bytes 294916
  7.2 10.9 %copy-start.7 = (bf16[24,2048]{1,0:T(8,128)(2,1)S(1)}, bf16[24,2048]{1,0:T(8,128)(2,1)}, u32[]{:S(2)}) copy-start(bf16[24,2048]{1,0:T(8,128)(2,1)} %param.9) | copy-start | bytes 294916
  7.2 23.4 %copy-start.9 = (bf16[32,384]{1,0:T(8,128)(2,1)S(1)}, bf16[32,384]{1,0:T(8,128)(2,1)}, u32[]{:S(2)}) copy-start(bf16[32,384]{1,0:T(8,128)(2,1)} %param.12) | copy-start | bytes 73732
  8.8 21.8 %all-to-all-start = ((bf16[8,32,768]{2,1,0:T(8,128)(2,1)}), bf16[8,32,768]{2,1,0:T(8,128)(2,1)S(1)}, u32[]{:S(2)}, u32[]{:S(2)}) async-start(bf16[8,32,768]{2,1,0:T(8,128)(2,1)} %broadcast_in_dim.36), calls=%async_computation | async-start | bytes 786432 | tf_op jit(solution)/shard_map/all_to_all | solution.py:23
  18.7 23.6 %collective-permute-start = (bf16[24,6144]{1,0:T(8,128)(2,1)S(1)}, bf16[24,6144]{1,0:T(8,128)(2,1)S(1)}, u32[]{:S(2)}, u32[]{:S(2)}) collective-permute-start(bf16[24,6144]{1,0:T(8,128)(2,1)S(1)} %get-tuple-element.8), channel_id=1, source_target_pairs={{0,2},{2,4},{4,6},{6,0},{1,3},{3,5},{5,7},{7,1},{8,10},{10,12},{12... | collective-permute-start | bytes 884744 | tf_op jit(solution)/shard_map/ppermute | solution.py:18
  22.1 20.3 %collective-permute-start.1 = (bf16[24,6144]{1,0:T(8,128)(2,1)S(1)}, bf16[24,6144]{1,0:T(8,128)(2,1)S(1)}, u32[]{:S(2)}, u32[]{:S(2)}) collective-permute-start(bf16[24,6144]{1,0:T(8,128)(2,1)S(1)} %get-tuple-element.8), channel_id=1, source_target_pairs={{0,6},{2,0},{4,2},{6,4},{1,7},{3,1},{5,3},{7,5},{8,14},{10,8},{12,... | collective-permute-start | bytes 884744 | tf_op jit(solution)/shard_map/ppermute | solution.py:18
  24.8 17.6 %collective-permute-start.2 = (bf16[24,6144]{1,0:T(8,128)(2,1)S(1)}, bf16[24,6144]{1,0:T(8,128)(2,1)S(1)}, u32[]{:S(2)}, u32[]{:S(2)}) collective-permute-start(bf16[24,6144]{1,0:T(8,128)(2,1)S(1)} %get-tuple-element.8), channel_id=1, source_target_pairs={{0,4},{2,6},{4,0},{6,2},{1,5},{3,7},{5,1},{7,3},{8,12},{10,14},{12... | collective-permute-start | bytes 884744 | tf_op jit(solution)/shard_map/ppermute | solution.py:18
  30.6 11.1 %copy-start.3 = (bf16[8,32,768]{2,1,0:T(8,128)(2,1)}, bf16[8,32,768]{2,1,0:T(8,128)(2,1)S(1)}, u32[]{:S(2)}) copy-start(bf16[8,32,768]{2,1,0:T(8,128)(2,1)S(1)} %all-to-all-done) | copy-start | bytes 1179652
  31.3 20.1 %all-to-all-start.1 = ((bf16[8,32,384]{2,1,0:T(8,128)(2,1)}), bf16[8,32,384]{2,1,0:T(8,128)(2,1)S(1)}, u32[]{:S(2)}, u32[]{:S(2)}) async-start(bf16[8,32,384]{2,1,0:T(8,128)(2,1)} %broadcast_in_dim.38), calls=%async_computation.1 | async-start | bytes 393216 | tf_op jit(solution)/shard_map/all_to_all | solution.py:23
  41.6 50.6 %all-gather.2.cloned.1.call-start = ((), (), s32[]{:S(2)}) async-start(), calls=%async_computation.3 | async-start | bytes 3538944 | tf_op jit(solution)/shard_map/all_gather | solution.py:72
  42.5 44.6 %collective-permute-start.3 = (bf16[96,6144]{1,0:T(8,128)(2,1)S(1)}, bf16[96,6144]{1,0:T(8,128)(2,1)}, u32[]{:S(2)}, u32[]{:S(2)}) collective-permute-start(bf16[96,6144]{1,0:T(8,128)(2,1)S(1)} %pad_maximum_fusion.1), channel_id=1, source_target_pairs={{0,1},{1,0},{2,3},{3,2},{4,5},{5,4},{6,7},{7,6},{8,9},{9,8},{10,11... | collective-permute-start | bytes 3538952 | tf_op jit(solution)/shard_map/ppermute | solution.py:18
  51.4 8.8 %collective-permute-start.4 = (bf16[8,32,384]{2,1,0:T(8,128)(2,1)S(1)}, bf16[8,32,384]{2,1,0:T(8,128)(2,1)S(1)}, u32[]{:S(2)}, u32[]{:S(2)}) collective-permute-start(bf16[8,32,384]{2,1,0:T(8,128)(2,1)S(1)} %all-to-all-done.1), channel_id=1, source_target_pairs={{0,8},{8,16},{16,24},{24,32},{32,40},{40,48},{48,56},{56,0},{1,9},... | collective-permute-start | bytes 589832 | tf_op jit(solution)/shard_map/ppermute | solution.py:18
  53.9 8.2 %collective-permute-start.5 = (bf16[8,32,384]{2,1,0:T(8,128)(2,1)S(1)}, bf16[8,32,384]{2,1,0:T(8,128)(2,1)S(1)}, u32[]{:S(2)}, u32[]{:S(2)}) collective-permute-start(bf16[8,32,384]{2,1,0:T(8,128)(2,1)S(1)} %all-to-all-done.1), channel_id=1, source_target_pairs={{0,56},{8,0},{16,8},{24,16},{32,24},{40,32},{48,40},{56,48},{1,57}... | collective-permute-start | bytes 589832 | tf_op jit(solution)/shard_map/ppermute | solution.py:18
  60.2 8.8 %collective-permute-start.6 = (bf16[8,32,384]{2,1,0:T(8,128)(2,1)S(1)}, bf16[8,32,384]{2,1,0:T(8,128)(2,1)S(1)}, u32[]{:S(2)}, u32[]{:S(2)}) collective-permute-start(bf16[8,32,384]{2,1,0:T(8,128)(2,1)S(1)} %collective-permute-done.4), channel_id=1, source_target_pairs={{0,8},{8,16},{16,24},{24,32},{32,40},{40,48},{48,56},{56,0},{1,9},... | collective-permute-start | bytes 589832 | tf_op jit(solution)/shard_map/ppermute | solution.py:18
  62.1 8.8 %collective-permute-start.7 = (bf16[8,32,384]{2,1,0:T(8,128)(2,1)S(1)}, bf16[8,32,384]{2,1,0:T(8,128)(2,1)S(1)}, u32[]{:S(2)}, u32[]{:S(2)}) collective-permute-start(bf16[8,32,384]{2,1,0:T(8,128)(2,1)S(1)} %collective-permute-done.5), channel_id=1, source_target_pairs={{0,56},{8,0},{16,8},{24,16},{32,24},{40,32},{48,40},{56,48},{1,57}... | collective-permute-start | bytes 589832 | tf_op jit(solution)/shard_map/ppermute | solution.py:18
  68.9 8.8 %collective-permute-start.8 = (bf16[8,32,384]{2,1,0:T(8,128)(2,1)S(1)}, bf16[8,32,384]{2,1,0:T(8,128)(2,1)S(1)}, u32[]{:S(2)}, u32[]{:S(2)}) collective-permute-start(bf16[8,32,384]{2,1,0:T(8,128)(2,1)S(1)} %collective-permute-done.6), channel_id=1, source_target_pairs={{0,8},{8,16},{16,24},{24,32},{32,40},{40,48},{48,56},{56,0},{1,9},... | collective-permute-start | bytes 589832 | tf_op jit(solution)/shard_map/ppermute | solution.py:18
  70.9 8.8 %collective-permute-start.9 = (bf16[8,32,384]{2,1,0:T(8,128)(2,1)S(1)}, bf16[8,32,384]{2,1,0:T(8,128)(2,1)S(1)}, u32[]{:S(2)}, u32[]{:S(2)}) collective-permute-start(bf16[8,32,384]{2,1,0:T(8,128)(2,1)S(1)} %collective-permute-done.7), channel_id=1, source_target_pairs={{0,56},{8,0},{16,8},{24,16},{32,24},{40,32},{48,40},{56,48},{1,57}... | collective-permute-start | bytes 589832 | tf_op jit(solution)/shard_map/ppermute | solution.py:18
  77.7 7.7 %collective-permute-start.10 = (bf16[4,32,384]{2,1,0:T(8,128)(2,1)S(1)}, bf16[4,32,384]{2,1,0:T(8,128)(2,1)S(1)}, u32[]{:S(2)}, u32[]{:S(2)}) collective-permute-start(bf16[4,32,384]{2,1,0:T(8,128)(2,1)S(1)} %slice.24), channel_id=1, source_target_pairs={{0,8},{8,16},{16,24},{24,32},{32,40},{40,48},{48,56},{56,0},{1,9},... | collective-permute-start | bytes 294920 | tf_op jit(solution)/shard_map/ppermute | solution.py:18
  79.7 7.3 %collective-permute-start.11 = (bf16[4,32,384]{2,1,0:T(8,128)(2,1)S(1)}, bf16[4,32,384]{2,1,0:T(8,128)(2,1)S(1)}, u32[]{:S(2)}, u32[]{:S(2)}) collective-permute-start(bf16[4,32,384]{2,1,0:T(8,128)(2,1)S(1)} %slice.25), channel_id=1, source_target_pairs={{0,56},{8,0},{16,8},{24,16},{32,24},{40,32},{48,40},{56,48},{1,57}... | collective-permute-start | bytes 294920 | tf_op jit(solution)/shard_map/ppermute | solution.py:18
  87.0 3.0 %copy-start.2 = (bf16[8,8,32,384]{3,2,1,0:T(8,128)(2,1)}, bf16[8,8,32,384]{3,2,1,0:T(8,128)(2,1)S(1)}, u32[]{:S(2)}) copy-start(bf16[8,8,32,384]{3,2,1,0:T(8,128)(2,1)S(1)} %bitcast_dynamic-update-slice_fusion.8) | copy-start | bytes 4718596
  92.2 2.6 %copy-start.1 = (bf16[2048,768]{1,0:T(8,128)(2,1)S(1)}, bf16[2048,768]{1,0:T(8,128)(2,1)}, u32[]{:S(2)}) copy-start(bf16[2048,768]{1,0:T(8,128)(2,1)} %all-gather.2.cloned.1.call-done) | copy-start | bytes 9437188
  96.5 2.5 %copy-start.4 = (f32[192,384]{1,0:T(8,128)}, f32[192,384]{1,0:T(8,128)S(1)}, u32[]{:S(2)}) copy-start(f32[192,384]{1,0:T(8,128)S(1)} %fusion.5) | copy-start | bytes 884740
  104.0 1.4 copy-start
  104.0 3.4 %copy-start.5 = (f32[192,384]{1,0:T(8,128)S(1)}, f32[192,384]{1,0:T(8,128)}, u32[]{:S(2)}) copy-start(f32[192,384]{1,0:T(8,128)} %copy-done.4) | copy-start | bytes 884740
  105.4 16.5 %collective-permute-start.12 = (bf16[96,4096]{1,0:T(8,128)(2,1)}, bf16[96,4096]{1,0:T(8,128)(2,1)}, u32[]{:S(2)}, u32[]{:S(2)}) collective-permute-start(bf16[96,4096]{1,0:T(8,128)(2,1)} %fusion.3), channel_id=1, source_target_pairs={{0,1},{1,0},{2,3},{3,2},{4,5},{5,4},{6,7},{7,6},{8,9},{9,8},{10,11... | collective-permute-start | bytes 2359304 | tf_op jit(solution)/shard_map/ppermute | solution.py:18
  110.4 53.4 %all-to-all-start.2 = ((bf16[64,32,384]{2,1,0:T(8,128)(2,1)}), bf16[64,32,384]{2,1,0:T(8,128)(2,1)S(1)}, u32[]{:S(2)}, u32[]{:S(2)}) async-start(bf16[64,32,384]{2,1,0:T(8,128)(2,1)} %bitcast.39), calls=%async_computation.2 | async-start | bytes 3145728 | tf_op jit(solution)/shard_map/all_to_all | solution.py:87
  123.5 40.5 %copy-start.8 = (f32[32,384]{1,0:T(8,128)S(1)}, f32[32,384]{1,0:T(8,128)}, u32[]{:S(2)}) copy-start(f32[32,384]{1,0:T(8,128)} %param.13) | copy-start | bytes 147460
  123.5 10.8 %collective-permute-start.13 = (bf16[24,4096]{1,0:T(8,128)(2,1)S(1)}, bf16[24,4096]{1,0:T(8,128)(2,1)S(1)}, u32[]{:S(2)}, u32[]{:S(2)}) collective-permute-start(bf16[24,4096]{1,0:T(8,128)(2,1)S(1)} %get-tuple-element.3), channel_id=1, source_target_pairs={{0,6},{2,0},{4,2},{6,4},{1,7},{3,1},{5,3},{7,5},{8,14},{10,8},{12,... | collective-permute-start | bytes 589832 | tf_op jit(solution)/shard_map/ppermute | solution.py:18
  125.6 10.5 %collective-permute-start.14 = (bf16[24,4096]{1,0:T(8,128)(2,1)S(1)}, bf16[24,4096]{1,0:T(8,128)(2,1)S(1)}, u32[]{:S(2)}, u32[]{:S(2)}) collective-permute-start(bf16[24,4096]{1,0:T(8,128)(2,1)S(1)} %get-tuple-element.5), channel_id=1, source_target_pairs={{0,2},{2,4},{4,6},{6,0},{1,3},{3,5},{5,7},{7,1},{8,10},{10,12},{12... | collective-permute-start | bytes 589832 | tf_op jit(solution)/shard_map/ppermute | solution.py:18
  129.5 9.9 %collective-permute-start.15 = (bf16[24,4096]{1,0:T(8,128)(2,1)S(1)}, bf16[24,4096]{1,0:T(8,128)(2,1)S(1)}, u32[]{:S(2)}, u32[]{:S(2)}) collective-permute-start(bf16[24,4096]{1,0:T(8,128)(2,1)S(1)} %get-tuple-element.4), channel_id=1, source_target_pairs={{0,4},{2,6},{4,0},{6,2},{1,5},{3,7},{5,1},{7,3},{8,12},{10,14},{12... | collective-permute-start | bytes 589832 | tf_op jit(solution)/shard_map/ppermute | solution.py:18
Sparse Core Ops, SparseCore 0:
  44.5 47.6 all-gather.1

commit v4 on v3

v4 whole, which is shorter than its diff:
```python
import jax
import jax.numpy as jnp
from jax import lax
from jax.experimental import pallas as pl
from jax.experimental.pallas import tpu as pltpu
from jax.sharding import Mesh
from jax.sharding import PartitionSpec as P


AXES = ("z", "y", "x", "c")
FS = ("z", "y")
STEPS = (0, 1, -1, 2)
BLOCKS = 4
OFFSETS = (0, -1, 1, -2, 2, -3, 3, 4)
BF, F32 = jnp.bfloat16, jnp.float32


def shift(value, axis, step):
    count = lax.axis_size(axis)
    if step == 0:
        return value
    return lax.ppermute(value, axis, [(i, (i + step) % count) for i in range(count)])


def spread(value, axis):
    count = lax.axis_size(axis)
    return lax.all_to_all(jnp.broadcast_to(value, (count, *value.shape)), axis, 0, 0)


def gather_down(down):
    line = spread(down, "z")
    chunks, ahead, behind = [line], line, line
    for _ in range(3):
        ahead, behind = shift(ahead, "y", 1), shift(behind, "y", -1)
        chunks += [ahead, behind]
    return [*chunks, shift(ahead, "y", 1)]


def collect_tokens(own):
    pieces = [shift(own, "x", step) for step in STEPS]
    line = jnp.concatenate(pieces, axis=0)
    other = shift(line, "c", 1)
    return jnp.concatenate([line, other], axis=0)


def give_rows(own, other, rows):
    both = (own + shift(other, "c", 1).astype(F32)).astype(BF)
    total = 0.0
    for at, step in enumerate(STEPS):
        total += shift(both[:, at * rows : (at + 1) * rows], "x", -step).astype(F32)
    return total.astype(BF)


def dot_nt(leading, trailing):
    return lax.dot_general(
        leading, trailing, (((1,), (1,)), ((), ())), preferred_element_type=F32
    )


def early_kernel(token_ref, weight_ref, cot_ref, gate_ref, up_ref, grad_ref, sum_ref, hidden_ref):
    step = pl.program_id(0)
    half = gate_ref.shape[1]

    @pl.when(step == 0)
    def _():
        sum_ref[...] = jnp.zeros_like(sum_ref)

    @pl.when(step < BLOCKS)
    def _():
        sum_ref[...] += jnp.dot(token_ref[...], weight_ref[...], preferred_element_type=F32)

    @pl.when(step == BLOCKS - 1)
    def _():
        gate, up = sum_ref[:, :half], sum_ref[:, half:]
        gate_ref[...] = gate
        up_ref[...] = up
        hidden_ref[...] = (gate / (1.0 + jnp.exp(-gate)) * up).astype(BF)

    @pl.when(step >= BLOCKS)
    def _():
        grad_ref[...] = lax.dot_general(
            cot_ref[...], hidden_ref[...], (((0,), (0,)), ((), ())), preferred_element_type=F32
        ).astype(BF)


def early_part(tokens, whole):
    rows, width = tokens.shape[0], whole.shape[0]
    both, block = whole.shape[1], width // BLOCKS
    half = both // 2
    first = lambda k: jnp.minimum(k, BLOCKS - 1)
    then = lambda k: jnp.maximum(k - BLOCKS, 0)
    return pl.pallas_call(
        early_kernel,
        grid=(2 * BLOCKS,),
        in_specs=[
            pl.BlockSpec((rows, block), lambda k: (0, BLOCKS + first(k))),
            pl.BlockSpec((block, both), lambda k: (first(k), 0)),
            pl.BlockSpec((rows, block), lambda k: (0, 2 * BLOCKS + then(k))),
        ],
        out_specs=[
            pl.BlockSpec((rows, half), lambda k: (0, 0)),
            pl.BlockSpec((rows, half), lambda k: (0, 0)),
            pl.BlockSpec((block, half), lambda k: (then(k), 0)),
        ],
        out_shape=[
            jax.ShapeDtypeStruct((rows, half), F32),
            jax.ShapeDtypeStruct((rows, half), F32),
            jax.ShapeDtypeStruct((width, half), BF),
        ],
        scratch_shapes=[pltpu.VMEM((rows, both), F32), pltpu.VMEM((rows, half), BF)],
        compiler_params=pltpu.CompilerParams(
            dimension_semantics=("arbitrary",), vmem_limit_bytes=12 << 20
        ),
        cost_estimate=pl.CostEstimate(
            flops=6 * rows * width * half, transcendentals=rows * half, bytes_accessed=8 << 20
        ),
    )(tokens, whole, tokens)


def rest_kernel(
    row_ref, later_ref, cot_ref, weight_ref, gate_ref, up_ref, *others
):
    chunk_refs, (own_ref, other_ref) = others[:8], others[8:10]
    down_ref, sum_ref, grad_ref, hidden_ref, to_gate_ref, to_up_ref = others[10:]
    step = pl.program_id(0)
    half, lines = gate_ref.shape[1], down_ref.shape[0] // BLOCKS
    mine = own_ref.shape[1]

    @pl.when(step == 0)
    def _():
        sum_ref[...] = jnp.zeros_like(sum_ref)
        grad_ref[...] = jnp.zeros_like(grad_ref)
        for offset, chunk_ref in zip(OFFSETS, chunk_refs):
            at = (row_ref[0] + offset) & (len(OFFSETS) - 1)
            down_ref[:, pl.ds(at, 1)] = chunk_ref[...][:, None]

    @pl.when(step < BLOCKS)
    def _():
        down = down_ref[pl.ds(step * lines, lines)].reshape(-1, half)
        sum_ref[...] += jnp.dot(later_ref[...], weight_ref[...], preferred_element_type=F32)
        grad_ref[...] += jnp.dot(cot_ref[...], down, preferred_element_type=F32)

    @pl.when(step == BLOCKS - 1)
    def _():
        gate, up = sum_ref[:, :half], sum_ref[:, half:]
        hidden_ref[...] = (gate / (1.0 + jnp.exp(-gate)) * up).astype(BF)
        gate, grad = gate_ref[...], grad_ref[...]
        sig = 1.0 / (1.0 + jnp.exp(-gate))
        to_gate_ref[...] = (grad * up_ref[...] * sig * (1.0 + gate * (1.0 - sig))).astype(BF)
        to_up_ref[...] = (grad * (gate * sig)).astype(BF)

    @pl.when(step >= BLOCKS)
    def _():
        down = down_ref[pl.ds((step - BLOCKS) * lines, lines)].reshape(-1, half)
        out = dot_nt(hidden_ref[...], down)
        back = dot_nt(to_gate_ref[...], weight_ref[:, :half])
        back += dot_nt(to_up_ref[...], weight_ref[:, half:])
        own_ref[0], own_ref[1] = out[:mine], back[:mine]
        other_ref[0], other_ref[1] = out[mine:].astype(BF), back[mine:].astype(BF)


def rest_part(tokens, whole, gate_early, up_early, chunks):
    rows, (width, both) = tokens.shape[0], whole.shape
    block, half = width // BLOCKS, both // 2
    lines = chunks[0].shape[0]
    first = lambda k: jnp.minimum(k, BLOCKS - 1)
    then = lambda k: jnp.maximum(k - BLOCKS, 0)
    whole_of = lambda array: pl.BlockSpec(array.shape, lambda k: (0,) * array.ndim)
    out_block = pl.BlockSpec((2, rows // 2, block), lambda k: (0, 0, then(k)))
    return pl.pallas_call(
        rest_kernel,
        grid=(2 * BLOCKS,),
        in_specs=[
            pl.BlockSpec(memory_space=pltpu.SMEM),
            pl.BlockSpec((rows, block), lambda k: (0, first(k))),
            pl.BlockSpec((rows, block), lambda k: (0, 2 * BLOCKS + first(k))),
            pl.BlockSpec((block, both), lambda k: (k % BLOCKS, 0)),
            whole_of(gate_early),
            whole_of(up_early),
            *map(whole_of, chunks),
        ],
        out_specs=[out_block, out_block],
        out_shape=[
            jax.ShapeDtypeStruct((2, rows // 2, width), F32),
            jax.ShapeDtypeStruct((2, rows // 2, width), BF),
        ],
        scratch_shapes=[
            pltpu.VMEM((lines, len(chunks), *chunks[0].shape[1:]), BF),
            pltpu.VMEM((rows, both), F32),
            pltpu.VMEM((rows, half), F32),
            pltpu.VMEM((rows, half), BF),
            pltpu.VMEM((rows, half), BF),
            pltpu.VMEM((rows, half), BF),
        ],
        compiler_params=pltpu.CompilerParams(
            dimension_semantics=("arbitrary",), vmem_limit_bytes=16 << 20
        ),
        cost_estimate=pl.CostEstimate(
            flops=12 * rows * width * half, transcendentals=2 * rows * half, bytes_accessed=16 << 20
        ),
    )(
        lax.axis_index("y").astype(jnp.int32)[None],
        tokens,
        tokens,
        whole,
        gate_early,
        up_early,
        *chunks,
    )


def shards(later, early, cotangent, gate_w, up_w, down_w, down_grad_sum):
    rows, _ = later.shape
    line = spread(jnp.concatenate([gate_w, up_w], axis=1), "y")
    line = line.reshape(-1, line.shape[-1])
    whole = lax.all_gather(line, "z", axis=0, tiled=True)
    tokens = jnp.concatenate([later, early, cotangent], axis=1)
    tokens = collect_tokens(tokens)
    chunks = gather_down(down_w)

    gate_early, up_early, down_grad = early_part(tokens, whole)
    received = lax.all_to_all(down_grad.reshape(-1, *gate_w.shape), FS, 0, 0)

    own, other = rest_part(tokens, whole, gate_early, up_early, chunks)
    later_output, earlier_grad_input = give_rows(own, other, rows)

    summed = jnp.sum(received.astype(F32), axis=0)
    factor = (rows * lax.axis_size(AXES)) ** (-0.5)
    return later_output, earlier_grad_input, down_grad_sum + summed * factor


def solution(mesh):
    split = Mesh(mesh.devices.reshape(8, 8, 4, 2), AXES)
    tokens, weights = P(AXES, None), P(FS, ("x", "c"))
    return jax.shard_map(
        shards,
        mesh=split,
        in_specs=(tokens,) * 3 + (weights,) * 4,
        out_specs=(tokens, tokens, weights),
        check_vma=False,
    )
```

time: 173 us -> 155 us (0.90)
  the two profiles are of different devices: /device:TPU:2 before, /device:TPU:1 now
where the time goes in v4:
time: 155 us; the launch traced here: 154 us
  starting transfers between devices  73.4 us (47%)
  blocking collectives  19.1 us (12%)
  waiting for transfers between devices  18.8 us (12%)
  between operations  14.4 us (9%)
  local copies, waits for them, and re-layouts  13.5 us (9%)
  Pallas kernels  9.64 us (6%)
  other arithmetic  5.52 us (4%)
    ppermute x15, starting transfers between devices, shift(): lax.ppermute(value, axis, [(i, (i + step) % count) for i in range(count)])  56.9 us
    all_to_all x1, blocking collectives, spread(): lax.all_to_all(jnp.broadcast_to(value, (count, *value.shape)), axis, 0, 0)  19.1 us
    ppermute x15, waiting for transfers between devices, shift(): lax.ppermute(value, axis, [(i, (i + step) % count) for i in range(count)])  14.6 us
    all_to_all x1, starting transfers between devices, spread(): lax.all_to_all(jnp.broadcast_to(value, (count, *value.shape)), axis, 0, 0)  10 us
    unnamed x23, local copies, waits for them, and re-layouts  10 us
    all_to_all x1, starting transfers between devices, shards(): received = lax.all_to_all(down_grad.reshape(-1, *gate_w.shape), FS, 0, 0)  6.48 us
    pallas_call x1, Pallas kernels, rest_part(): pl.pallas_call(rest_kernel, grid=(2 * BLOCKS,), in_specs=[pl.BlockSpec(me...  6.43 us
    all_to_all x1, waiting for transfers between devices, spread(): lax.all_to_all(jnp.broadcast_to(value, (count, *value.shape)), axis, 0, 0)  4.08 us
  transfers between devices with their start and end apart: 18, of which 8 were waited for; matrix products, arithmetic and copies ran while one was open for 6% of the time, Pallas kernels for 6%

profile of v4, /device:TPU:1, one launch (start us, length us, event | category | flops | bytes accessed | tf_op | source)
XLA Modules:
  0.0 154.3 jit_solution(18398492215465039915)
XLA Ops:
  8.0 19.1 %all_to_all.15 = bf16[8,32,768]{2,1,0:T(8,128)(2,1)} all-to-all(bf16[8,32,768]{2,1,0:T(8,128)(2,1)S(1)} %broadcast_in_dim.10), channel_id=1, replica_groups=mesh['z'=8,'y'=8,'x'=4,'c'=2] {'y'}, dimensions={0} | all-to-all | bytes 786432 | tf_op jit(solution)/shard_map/all_to_all | solution.py:27
  27.2 1.5 constant_dynamic-update-slice_fusion.2
  28.7 1.5 constant_dynamic-update-slice_fusion.1
  30.9 6.6 %collective-permute-start.2 = (bf16[24,6144]{1,0:T(8,128)(2,1)}, bf16[24,6144]{1,0:T(8,128)(2,1)S(1)}, u32[]{:S(2)}, u32[]{:S(2)}) collective-permute-start(bf16[24,6144]{1,0:T(8,128)(2,1)} %get-tuple-element.18), channel_id=1, source_target_pairs={{0,4},{2,6},{4,0},{6,2},{1,5},{3,7},{5,1},{7,3},{8,12},{10,14},{12... | collective-permute-start | bytes 884744 | tf_op jit(solution)/shard_map/ppermute | solution.py:22
  37.6 2.8 %collective-permute-start.1 = (bf16[24,6144]{1,0:T(8,128)(2,1)}, bf16[24,6144]{1,0:T(8,128)(2,1)S(1)}, u32[]{:S(2)}, u32[]{:S(2)}) collective-permute-start(bf16[24,6144]{1,0:T(8,128)(2,1)} %get-tuple-element.18), channel_id=1, source_target_pairs={{0,6},{2,0},{4,2},{6,4},{1,7},{3,1},{5,3},{7,5},{8,14},{10,8},{12,... | collective-permute-start | bytes 884744 | tf_op jit(solution)/shard_map/ppermute | solution.py:22
  40.3 2.5 %collective-permute-start = (bf16[24,6144]{1,0:T(8,128)(2,1)}, bf16[24,6144]{1,0:T(8,128)(2,1)S(1)}, u32[]{:S(2)}, u32[]{:S(2)}) collective-permute-start(bf16[24,6144]{1,0:T(8,128)(2,1)} %get-tuple-element.18), channel_id=1, source_target_pairs={{0,2},{2,4},{4,6},{6,0},{1,3},{3,5},{5,7},{7,1},{8,10},{10,12},{12... | collective-permute-start | bytes 884744 | tf_op jit(solution)/shard_map/ppermute | solution.py:22
  43.6 10.0 %all-to-all-start.1 = ((bf16[8,32,384]{2,1,0:T(8,128)(2,1)}), bf16[8,32,384]{2,1,0:T(8,128)(2,1)S(1)}, u32[]{:S(2)}, u32[]{:S(2)}) async-start(bf16[8,32,384]{2,1,0:T(8,128)(2,1)} %broadcast_in_dim.11), calls=%async_computation.1 | async-start | bytes 393216 | tf_op jit(solution)/shard_map/all_to_all | solution.py:27
  53.6 2.2 %pad_maximum_fusion = bf16[96,6144]{1,0:T(8,128)(2,1)} fusion(bf16[24,6144]{1,0:T(8,128)(2,1)S(1)} %collective-permute-done.2, bf16[24,6144]{1,0:T(8,128)(2,1)S(1)} %collective-permute-done.1, bf16[24,6144]{1,0:T(8,128)(2,1)S(1)} %collective-permute-done, bf16[24,6144]{1,0:T(8,128)(2,1)} %get-tuple-element.18), kind=kLoop, calls=%fused_computation.2 | loop fusion | flops 4718592 | bytes 2359296 | tf_op jit(solution)/shard_map/concatenate | solution.py:41
  55.8 5.1 %collective-permute-start.3 = (bf16[96,6144]{1,0:T(8,128)(2,1)}, bf16[96,6144]{1,0:T(8,128)(2,1)}, u32[]{:S(2)}, u32[]{:S(2)}) collective-permute-start(bf16[96,6144]{1,0:T(8,128)(2,1)} %pad_maximum_fusion), channel_id=1, source_target_pairs={{0,1},{1,0},{2,3},{3,2},{4,5},{5,4},{6,7},{7,6},{8,9},{9,8},{10,11... | collective-permute-start | bytes 3538952 | tf_op jit(solution)/shard_map/ppermute | solution.py:22
  60.9 4.1 %all-to-all-done.1.others_0_ = bf16[8,32,384]{2,1,0:T(8,128)(2,1)S(1)} async-done(((bf16[8,32,384]{2,1,0:T(8,128)(2,1)}), bf16[8,32,384]{2,1,0:T(8,128)(2,1)S(1)}, u32[]{:S(2)}, u32[]{:S(2)}) %all-to-all-start.1) | async-done | bytes 196640 | tf_op jit(solution)/shard_map/all_to_all | solution.py:27
  65.0 2.2 %collective-permute-start.4 = (bf16[8,32,384]{2,1,0:T(8,128)(2,1)S(1)}, bf16[8,32,384]{2,1,0:T(8,128)(2,1)S(1)}, u32[]{:S(2)}, u32[]{:S(2)}) collective-permute-start(bf16[8,32,384]{2,1,0:T(8,128)(2,1)S(1)} %all-to-all-done.1.others_0_), channel_id=1, source_target_pairs={{0,8},{8,16},{16,24},{24,32},{32,40},{40,48},{48,56},{56,0},{1,9},... | collective-permute-start | bytes 589832 | tf_op jit(solution)/shard_map/ppermute | solution.py:22
  67.2 4.3 %collective-permute-start.5 = (bf16[8,32,384]{2,1,0:T(8,128)(2,1)S(1)}, bf16[8,32,384]{2,1,0:T(8,128)(2,1)S(1)}, u32[]{:S(2)}, u32[]{:S(2)}) collective-permute-start(bf16[8,32,384]{2,1,0:T(8,128)(2,1)S(1)} %all-to-all-done.1.others_0_), channel_id=1, source_target_pairs={{0,56},{8,0},{16,8},{24,16},{32,24},{40,32},{48,40},{56,48},{1,57}... | collective-permute-start | bytes 589832 | tf_op jit(solution)/shard_map/ppermute | solution.py:22
  71.5 1.5 collective-permute-done.4.others_1_
  73.0 1.9 %collective-permute-start.6 = (bf16[8,32,384]{2,1,0:T(8,128)(2,1)S(1)}, bf16[8,32,384]{2,1,0:T(8,128)(2,1)S(1)}, u32[]{:S(2)}, u32[]{:S(2)}) collective-permute-start(bf16[8,32,384]{2,1,0:T(8,128)(2,1)S(1)} %collective-permute-done.4.others_1_), channel_id=1, source_target_pairs={{0,8},{8,16},{16,24},{24,32},{32,40},{40,48},{48,56},{56,0},{1,9},... | collective-permute-start | bytes 589832 | tf_op jit(solution)/shard_map/ppermute | solution.py:22
  75.9 4.6 %collective-permute-start.7 = (bf16[8,32,384]{2,1,0:T(8,128)(2,1)S(1)}, bf16[8,32,384]{2,1,0:T(8,128)(2,1)}, u32[]{:S(2)}, u32[]{:S(2)}) collective-permute-start(bf16[8,32,384]{2,1,0:T(8,128)(2,1)S(1)} %collective-permute-done.5.others_2_), channel_id=1, source_target_pairs={{0,56},{8,0},{16,8},{24,16},{32,24},{40,32},{48,40},{56,48},{1,57}... | collective-permute-start | bytes 589832 | tf_op jit(solution)/shard_map/ppermute | solution.py:22
  81.0 1.9 %collective-permute-start.8 = (bf16[8,32,384]{2,1,0:T(8,128)(2,1)S(1)}, bf16[8,32,384]{2,1,0:T(8,128)(2,1)}, u32[]{:S(2)}, u32[]{:S(2)}) collective-permute-start(bf16[8,32,384]{2,1,0:T(8,128)(2,1)S(1)} %collective-permute-done.6.others_3_), channel_id=1, source_target_pairs={{0,8},{8,16},{16,24},{24,32},{32,40},{40,48},{48,56},{56,0},{1,9},... | collective-permute-start | bytes 589832 | tf_op jit(solution)/shard_map/ppermute | solution.py:22
  83.1 5.1 %collective-permute-start.9 = (bf16[8,32,384]{2,1,0:T(8,128)(2,1)}, bf16[8,32,384]{2,1,0:T(8,128)(2,1)}, u32[]{:S(2)}, u32[]{:S(2)}) collective-permute-start(bf16[8,32,384]{2,1,0:T(8,128)(2,1)} %collective-permute-done.7.others_4_), channel_id=1, source_target_pairs={{0,56},{8,0},{16,8},{24,16},{32,24},{40,32},{48,40},{56,48},{1,57}... | collective-permute-start | bytes 589832 | tf_op jit(solution)/shard_map/ppermute | solution.py:22
  88.7 1.9 %collective-permute-start.10 = (bf16[8,32,384]{2,1,0:T(8,128)(2,1)}, bf16[8,32,384]{2,1,0:T(8,128)(2,1)}, u32[]{:S(2)}, u32[]{:S(2)}) collective-permute-start(bf16[8,32,384]{2,1,0:T(8,128)(2,1)} %collective-permute-done.8.others_5_), channel_id=1, source_target_pairs={{0,8},{8,16},{16,24},{24,32},{32,40},{40,48},{48,56},{56,0},{1,9},... | collective-permute-start | bytes 589832 | tf_op jit(solution)/shard_map/ppermute | solution.py:22
  90.7 1.3 constant_dynamic-update-slice_fusion.3.token_ref.cot_ref.later_ref
  92.1 1.9 %copy-done = bf16[2048,768]{1,0:T(8,128)(2,1)S(1)} copy-done((bf16[2048,768]{1,0:T(8,128)(2,1)S(1)}, bf16[2048,768]{1,0:T(8,128)(2,1)}, u32[]{:S(2)}) %copy-start) | copy-done | bytes 3145752
  93.9 3.2 %shard_map.94 = (f32[192,384]{1,0:T(8,128)S(1)}, f32[192,384]{1,0:T(8,128)S(1)}, bf16[2048,384]{1,0:T(8,128)(2,1)S(1)}) custom-call(bf16[192,6144]{1,0:T(8,128)(2,1)S(1)} %constant_dynamic-update-slice_fusion.3.token_ref.cot_ref.later_ref, bf16[2048,768]{1,0:T(8,128)(2,1)S(1)} %copy-done, ...), custom_call_target="tpu_custom_call" | custom-call | flops 905969664 | bytes 8388608 | tf_op jit(solution)/shard_map/pallas_call | solution.py:92
  98.4 6.5 %all-to-all-start.2 = ((bf16[64,32,384]{2,1,0:T(8,128)(2,1)}), bf16[64,32,384]{2,1,0:T(8,128)(2,1)}, u32[]{:S(2)}, u32[]{:S(2)}) async-start(bf16[64,32,384]{2,1,0:T(8,128)(2,1)} %bitcast.7), calls=%async_computation.2 | async-start | bytes 3145728 | tf_op jit(solution)/shard_map/all_to_all | solution.py:222
  104.9 1.9 %copy-done.1 = bf16[2048,768]{1,0:T(8,128)(2,1)S(1)} copy-done((bf16[2048,768]{1,0:T(8,128)(2,1)S(1)}, bf16[2048,768]{1,0:T(8,128)(2,1)}, u32[]{:S(2)}) %copy-start.1) | copy-done | bytes 3145752
  107.7 6.4 %shard_map.95 = (f32[2,96,2048]{2,1,0:T(8,128)S(1)}, bf16[2,96,2048]{2,1,0:T(8,128)(2,1)S(1)}) custom-call(s32[1]{0:T(128)} %bitcast.row_ref, bf16[192,6144]{1,0:T(8,128)(2,1)S(1)} %constant_dynamic-update-slice_fusion.3.token_ref.cot_ref.later_ref, bf16[192,6144]{1,0:T(8,128)(2,1)S(1)} %constant_dynamic-update-slice_fusion.3.token_ref.cot_ref.later_ref, ...), custom_call_target="tpu_custom_call" | custom-call | flops 1811939328 | bytes 16777216 | tf_op jit(solution)/shard_map/pallas_call | solution.py:170
  114.1 9.6 %collective-permute-start.11 = (bf16[2,96,2048]{2,1,0:T(8,128)(2,1)S(1)}, bf16[2,96,2048]{2,1,0:T(8,128)(2,1)S(1)}, u32[]{:S(2)}, u32[]{:S(2)}) collective-permute-start(bf16[2,96,2048]{2,1,0:T(8,128)(2,1)S(1)} %get-tuple-element.11), channel_id=1, source_target_pairs={{0,1},{1,0},{2,3},{3,2},{4,5},{5,4},{6,7},{7,6},{8,9},{9,8},{10,11... | collective-permute-start | bytes 2359304 | tf_op jit(solution)/shard_map/ppermute | solution.py:22
  123.8 1.9 %collective-permute-done.11 = bf16[2,96,2048]{2,1,0:T(8,128)(2,1)S(1)} collective-permute-done((bf16[2,96,2048]{2,1,0:T(8,128)(2,1)S(1)}, bf16[2,96,2048]{2,1,0:T(8,128)(2,1)S(1)}, u32[]{:S(2)}, u32[]{:S(2)}) %collective-permute-start.11) | collective-permute-done | bytes 786464 | tf_op jit(solution)/shard_map/ppermute | solution.py:22
  125.9 4.0 %collective-permute-start.12 = (bf16[2,24,2048]{2,1,0:T(8,128)(2,1)S(1)}, bf16[2,24,2048]{2,1,0:T(8,128)(2,1)S(1)}, u32[]{:S(2)}, u32[]{:S(2)}) collective-permute-start(bf16[2,24,2048]{2,1,0:T(8,128)(2,1)S(1)} %get-tuple-element.13), channel_id=1, source_target_pairs={{0,6},{2,0},{4,2},{6,4},{1,7},{3,1},{5,3},{7,5},{8,14},{10,8},{12,... | collective-permute-start | bytes 589832 | tf_op jit(solution)/shard_map/ppermute | solution.py:22
  129.9 2.2 %collective-permute-start.14 = (bf16[2,24,2048]{2,1,0:T(8,128)(2,1)S(1)}, bf16[2,24,2048]{2,1,0:T(8,128)(2,1)S(1)}, u32[]{:S(2)}, u32[]{:S(2)}) collective-permute-start(bf16[2,24,2048]{2,1,0:T(8,128)(2,1)S(1)} %get-tuple-element.14), channel_id=1, source_target_pairs={{0,4},{2,6},{4,0},{6,2},{1,5},{3,7},{5,1},{7,3},{8,12},{10,14},{12... | collective-permute-start | bytes 589832 | tf_op jit(solution)/shard_map/ppermute | solution.py:22
  132.2 2.2 %collective-permute-start.13 = (bf16[2,24,2048]{2,1,0:T(8,128)(2,1)S(1)}, bf16[2,24,2048]{2,1,0:T(8,128)(2,1)S(1)}, u32[]{:S(2)}, u32[]{:S(2)}) collective-permute-start(bf16[2,24,2048]{2,1,0:T(8,128)(2,1)S(1)} %get-tuple-element.15), channel_id=1, source_target_pairs={{0,2},{2,4},{4,6},{6,0},{1,3},{3,5},{5,7},{7,1},{8,10},{10,12},{12... | collective-permute-start | bytes 589832 | tf_op jit(solution)/shard_map/ppermute | solution.py:22
  134.3 4.9 %collective-permute-done.14 = bf16[2,24,2048]{2,1,0:T(8,128)(2,1)S(1)} collective-permute-done((bf16[2,24,2048]{2,1,0:T(8,128)(2,1)S(1)}, bf16[2,24,2048]{2,1,0:T(8,128)(2,1)S(1)}, u32[]{:S(2)}, u32[]{:S(2)}) %collective-permute-start.14) | collective-permute-done | bytes 196640 | tf_op jit(solution)/shard_map/ppermute | solution.py:22
  139.2 5.2 %collective-permute-done.13 = bf16[2,24,2048]{2,1,0:T(8,128)(2,1)S(1)} collective-permute-done((bf16[2,24,2048]{2,1,0:T(8,128)(2,1)S(1)}, bf16[2,24,2048]{2,1,0:T(8,128)(2,1)S(1)}, u32[]{:S(2)}, u32[]{:S(2)}) %collective-permute-start.13) | collective-permute-done | bytes 196640 | tf_op jit(solution)/shard_map/ppermute | solution.py:22
  145.2 1.7 %convert_reduce_fusion = f32[32,384]{1,0:T(8,128)S(1)} fusion(bf16[64,32,384]{2,1,0:T(8,128)(2,1)} %all-to-all-done.2), kind=kLoop, calls=%fused_computation | loop fusion | flops 1560576 | bytes 1622016 | tf_op jit(solution)/shard_map/reduce_sum | solution.py:227
  (43 shorter events, 8.2 us)
Async XLA Ops:
  7.2 23.1 %copy-start.6 = (bf16[24,2048]{1,0:T(8,128)(2,1)S(1)}, bf16[24,2048]{1,0:T(8,128)(2,1)}, u32[]{:S(2)}) copy-start(bf16[24,2048]{1,0:T(8,128)(2,1)} %param.9) | copy-start | bytes 294916
  7.2 35.7 %copy-start.8 = (bf16[32,384]{1,0:T(8,128)(2,1)S(1)}, bf16[32,384]{1,0:T(8,128)(2,1)}, u32[]{:S(2)}) copy-start(bf16[32,384]{1,0:T(8,128)(2,1)} %param.12) | copy-start | bytes 73732
  7.2 84.9 %all-gather.2.cloned.1.call-start = ((), (), s32[]{:S(2)}) async-start(), calls=%async_computation.3 | async-start | bytes 3538944 | tf_op jit(solution)/shard_map/all_gather | solution.py:216
  30.9 22.7 %collective-permute-start.2 = (bf16[24,6144]{1,0:T(8,128)(2,1)}, bf16[24,6144]{1,0:T(8,128)(2,1)S(1)}, u32[]{:S(2)}, u32[]{:S(2)}) collective-permute-start(bf16[24,6144]{1,0:T(8,128)(2,1)} %get-tuple-element.18), channel_id=1, source_target_pairs={{0,4},{2,6},{4,0},{6,2},{1,5},{3,7},{5,1},{7,3},{8,12},{10,14},{12... | collective-permute-start | bytes 884744 | tf_op jit(solution)/shard_map/ppermute | solution.py:22
  37.6 16.0 %collective-permute-start.1 = (bf16[24,6144]{1,0:T(8,128)(2,1)}, bf16[24,6144]{1,0:T(8,128)(2,1)S(1)}, u32[]{:S(2)}, u32[]{:S(2)}) collective-permute-start(bf16[24,6144]{1,0:T(8,128)(2,1)} %get-tuple-element.18), channel_id=1, source_target_pairs={{0,6},{2,0},{4,2},{6,4},{1,7},{3,1},{5,3},{7,5},{8,14},{10,8},{12,... | collective-permute-start | bytes 884744 | tf_op jit(solution)/shard_map/ppermute | solution.py:22
  40.3 13.3 %collective-permute-start = (bf16[24,6144]{1,0:T(8,128)(2,1)}, bf16[24,6144]{1,0:T(8,128)(2,1)S(1)}, u32[]{:S(2)}, u32[]{:S(2)}) collective-permute-start(bf16[24,6144]{1,0:T(8,128)(2,1)} %get-tuple-element.18), channel_id=1, source_target_pairs={{0,2},{2,4},{4,6},{6,0},{1,3},{3,5},{5,7},{7,1},{8,10},{10,12},{12... | collective-permute-start | bytes 884744 | tf_op jit(solution)/shard_map/ppermute | solution.py:22
  43.6 21.4 %all-to-all-start.1 = ((bf16[8,32,384]{2,1,0:T(8,128)(2,1)}), bf16[8,32,384]{2,1,0:T(8,128)(2,1)S(1)}, u32[]{:S(2)}, u32[]{:S(2)}) async-start(bf16[8,32,384]{2,1,0:T(8,128)(2,1)} %broadcast_in_dim.11), calls=%async_computation.1 | async-start | bytes 393216 | tf_op jit(solution)/shard_map/all_to_all | solution.py:27
  53.6 7.3 %copy-start.5 = (bf16[24,6144]{1,0:T(8,128)(2,1)}, bf16[24,6144]{1,0:T(8,128)(2,1)S(1)}, u32[]{:S(2)}) copy-start(bf16[24,6144]{1,0:T(8,128)(2,1)S(1)} %collective-permute-done.1) | copy-start | bytes 884740
  55.8 34.9 %collective-permute-start.3 = (bf16[96,6144]{1,0:T(8,128)(2,1)}, bf16[96,6144]{1,0:T(8,128)(2,1)}, u32[]{:S(2)}, u32[]{:S(2)}) collective-permute-start(bf16[96,6144]{1,0:T(8,128)(2,1)} %pad_maximum_fusion), channel_id=1, source_target_pairs={{0,1},{1,0},{2,3},{3,2},{4,5},{5,4},{6,7},{7,6},{8,9},{9,8},{10,11... | collective-permute-start | bytes 3538952 | tf_op jit(solution)/shard_map/ppermute | solution.py:22
  65.0 8.0 %collective-permute-start.4 = (bf16[8,32,384]{2,1,0:T(8,128)(2,1)S(1)}, bf16[8,32,384]{2,1,0:T(8,128)(2,1)S(1)}, u32[]{:S(2)}, u32[]{:S(2)}) collective-permute-start(bf16[8,32,384]{2,1,0:T(8,128)(2,1)S(1)} %all-to-all-done.1.others_0_), channel_id=1, source_target_pairs={{0,8},{8,16},{16,24},{24,32},{32,40},{40,48},{48,56},{56,0},{1,9},... | collective-permute-start | bytes 589832 | tf_op jit(solution)/shard_map/ppermute | solution.py:22
  67.2 8.7 %collective-permute-start.5 = (bf16[8,32,384]{2,1,0:T(8,128)(2,1)S(1)}, bf16[8,32,384]{2,1,0:T(8,128)(2,1)S(1)}, u32[]{:S(2)}, u32[]{:S(2)}) collective-permute-start(bf16[8,32,384]{2,1,0:T(8,128)(2,1)S(1)} %all-to-all-done.1.others_0_), channel_id=1, source_target_pairs={{0,56},{8,0},{16,8},{24,16},{32,24},{40,32},{48,40},{56,48},{1,57}... | collective-permute-start | bytes 589832 | tf_op jit(solution)/shard_map/ppermute | solution.py:22
  73.0 8.0 %collective-permute-start.6 = (bf16[8,32,384]{2,1,0:T(8,128)(2,1)S(1)}, bf16[8,32,384]{2,1,0:T(8,128)(2,1)S(1)}, u32[]{:S(2)}, u32[]{:S(2)}) collective-permute-start(bf16[8,32,384]{2,1,0:T(8,128)(2,1)S(1)} %collective-permute-done.4.others_1_), channel_id=1, source_target_pairs={{0,8},{8,16},{16,24},{24,32},{32,40},{40,48},{48,56},{56,0},{1,9},... | collective-permute-start | bytes 589832 | tf_op jit(solution)/shard_map/ppermute | solution.py:22
  75.9 7.2 %collective-permute-start.7 = (bf16[8,32,384]{2,1,0:T(8,128)(2,1)S(1)}, bf16[8,32,384]{2,1,0:T(8,128)(2,1)}, u32[]{:S(2)}, u32[]{:S(2)}) collective-permute-start(bf16[8,32,384]{2,1,0:T(8,128)(2,1)S(1)} %collective-permute-done.5.others_2_), channel_id=1, source_target_pairs={{0,56},{8,0},{16,8},{24,16},{32,24},{40,32},{48,40},{56,48},{1,57}... | collective-permute-start | bytes 589832 | tf_op jit(solution)/shard_map/ppermute | solution.py:22
  81.0 11.0 %copy-start.3 = (bf16[8,32,384]{2,1,0:T(8,128)(2,1)}, bf16[8,32,384]{2,1,0:T(8,128)(2,1)S(1)}, u32[]{:S(2)}) copy-start(bf16[8,32,384]{2,1,0:T(8,128)(2,1)S(1)} %collective-permute-done.6.others_3_) | copy-start | bytes 589828
  81.0 7.7 %collective-permute-start.8 = (bf16[8,32,384]{2,1,0:T(8,128)(2,1)S(1)}, bf16[8,32,384]{2,1,0:T(8,128)(2,1)}, u32[]{:S(2)}, u32[]{:S(2)}) collective-permute-start(bf16[8,32,384]{2,1,0:T(8,128)(2,1)S(1)} %collective-permute-done.6.others_3_), channel_id=1, source_target_pairs={{0,8},{8,16},{16,24},{24,32},{32,40},{40,48},{48,56},{56,0},{1,9},... | collective-permute-start | bytes 589832 | tf_op jit(solution)/shard_map/ppermute | solution.py:22
  83.1 21.8 %collective-permute-start.9 = (bf16[8,32,384]{2,1,0:T(8,128)(2,1)}, bf16[8,32,384]{2,1,0:T(8,128)(2,1)}, u32[]{:S(2)}, u32[]{:S(2)}) collective-permute-start(bf16[8,32,384]{2,1,0:T(8,128)(2,1)} %collective-permute-done.7.others_4_), channel_id=1, source_target_pairs={{0,56},{8,0},{16,8},{24,16},{32,24},{40,32},{48,40},{56,48},{1,57}... | collective-permute-start | bytes 589832 | tf_op jit(solution)/shard_map/ppermute | solution.py:22
  88.7 16.1 %collective-permute-start.10 = (bf16[8,32,384]{2,1,0:T(8,128)(2,1)}, bf16[8,32,384]{2,1,0:T(8,128)(2,1)}, u32[]{:S(2)}, u32[]{:S(2)}) collective-permute-start(bf16[8,32,384]{2,1,0:T(8,128)(2,1)} %collective-permute-done.8.others_5_), channel_id=1, source_target_pairs={{0,8},{8,16},{16,24},{24,32},{32,40},{40,48},{48,56},{56,0},{1,9},... | collective-permute-start | bytes 589832 | tf_op jit(solution)/shard_map/ppermute | solution.py:22
  92.1 1.9 %copy-start = (bf16[2048,768]{1,0:T(8,128)(2,1)S(1)}, bf16[2048,768]{1,0:T(8,128)(2,1)}, u32[]{:S(2)}) copy-start(bf16[2048,768]{1,0:T(8,128)(2,1)} %all-gather.2.cloned.1.call-done.weight_ref) | copy-start | bytes 9437188
  97.2 1.2 copy-start.2
  98.4 46.8 %all-to-all-start.2 = ((bf16[64,32,384]{2,1,0:T(8,128)(2,1)}), bf16[64,32,384]{2,1,0:T(8,128)(2,1)}, u32[]{:S(2)}, u32[]{:S(2)}) async-start(bf16[64,32,384]{2,1,0:T(8,128)(2,1)} %bitcast.7), calls=%async_computation.2 | async-start | bytes 3145728 | tf_op jit(solution)/shard_map/all_to_all | solution.py:222
  104.9 1.9 %copy-start.1 = (bf16[2048,768]{1,0:T(8,128)(2,1)S(1)}, bf16[2048,768]{1,0:T(8,128)(2,1)}, u32[]{:S(2)}) copy-start(bf16[2048,768]{1,0:T(8,128)(2,1)} %all-gather.2.cloned.1.call-done.weight_ref) | copy-start | bytes 9437188
  106.8 0.9 copy-start.4
  114.1 11.5 %collective-permute-start.11 = (bf16[2,96,2048]{2,1,0:T(8,128)(2,1)S(1)}, bf16[2,96,2048]{2,1,0:T(8,128)(2,1)S(1)}, u32[]{:S(2)}, u32[]{:S(2)}) collective-permute-start(bf16[2,96,2048]{2,1,0:T(8,128)(2,1)S(1)} %get-tuple-element.11), channel_id=1, source_target_pairs={{0,1},{1,0},{2,3},{3,2},{4,5},{5,4},{6,7},{7,6},{8,9},{9,8},{10,11... | collective-permute-start | bytes 2359304 | tf_op jit(solution)/shard_map/ppermute | solution.py:22
  125.9 21.0 %copy-start.7 = (f32[32,384]{1,0:T(8,128)S(1)}, f32[32,384]{1,0:T(8,128)}, u32[]{:S(2)}) copy-start(f32[32,384]{1,0:T(8,128)} %param.13) | copy-start | bytes 147460
  125.9 8.4 %collective-permute-start.12 = (bf16[2,24,2048]{2,1,0:T(8,128)(2,1)S(1)}, bf16[2,24,2048]{2,1,0:T(8,128)(2,1)S(1)}, u32[]{:S(2)}, u32[]{:S(2)}) collective-permute-start(bf16[2,24,2048]{2,1,0:T(8,128)(2,1)S(1)} %get-tuple-element.13), channel_id=1, source_target_pairs={{0,6},{2,0},{4,2},{6,4},{1,7},{3,1},{5,3},{7,5},{8,14},{10,8},{12,... | collective-permute-start | bytes 589832 | tf_op jit(solution)/shard_map/ppermute | solution.py:22
  129.9 9.3 %collective-permute-start.14 = (bf16[2,24,2048]{2,1,0:T(8,128)(2,1)S(1)}, bf16[2,24,2048]{2,1,0:T(8,128)(2,1)S(1)}, u32[]{:S(2)}, u32[]{:S(2)}) collective-permute-start(bf16[2,24,2048]{2,1,0:T(8,128)(2,1)S(1)} %get-tuple-element.14), channel_id=1, source_target_pairs={{0,4},{2,6},{4,0},{6,2},{1,5},{3,7},{5,1},{7,3},{8,12},{10,14},{12... | collective-permute-start | bytes 589832 | tf_op jit(solution)/shard_map/ppermute | solution.py:22
  132.2 12.3 %collective-permute-start.13 = (bf16[2,24,2048]{2,1,0:T(8,128)(2,1)S(1)}, bf16[2,24,2048]{2,1,0:T(8,128)(2,1)S(1)}, u32[]{:S(2)}, u32[]{:S(2)}) collective-permute-start(bf16[2,24,2048]{2,1,0:T(8,128)(2,1)S(1)} %get-tuple-element.15), channel_id=1, source_target_pairs={{0,2},{2,4},{4,6},{6,0},{1,3},{3,5},{5,7},{7,1},{8,10},{10,12},{12... | collective-permute-start | bytes 589832 | tf_op jit(solution)/shard_map/ppermute | solution.py:22
Sparse Core Ops, SparseCore 0:
  27.3 55.1 all-gather.1

commit v5 on v4

--- a/solution.py
+++ b/solution.py
@@ -30,7 +30,7 @@
 def gather_down(down):
     line = spread(down, "z")
     chunks, ahead, behind = [line], line, line
-    for _ in range(3):
+    for _ in range(1, 4):
         ahead, behind = shift(ahead, "y", 1), shift(behind, "y", -1)
         chunks += [ahead, behind]
     return [*chunks, shift(ahead, "y", 1)]
@@ -105,7 +105,7 @@
         out_shape=[
             jax.ShapeDtypeStruct((rows, half), F32),
             jax.ShapeDtypeStruct((rows, half), F32),
-            jax.ShapeDtypeStruct((width, half), BF),
+            pltpu.HBM((width, half), BF),
         ],
         scratch_shapes=[pltpu.VMEM((rows, both), F32), pltpu.VMEM((rows, half), BF)],
         compiler_params=pltpu.CompilerParams(
@@ -214,6 +214,7 @@
     line = spread(jnp.concatenate([gate_w, up_w], axis=1), "y")
     line = line.reshape(-1, line.shape[-1])
     whole = lax.all_gather(line, "z", axis=0, tiled=True)
+    whole = pltpu.with_memory_space_constraint(whole, pltpu.HBM)
     tokens = jnp.concatenate([later, early, cotangent], axis=1)
     tokens = collect_tokens(tokens)
     chunks = gather_down(down_w)

time: 155 us -> 156 us (level)
  Pallas kernels: 9.64 us -> 14.6 us
  local copies, waits for them, and re-layouts: 13.5 us -> 8.62 us
    unnamed x23 -> x17, local copies, waits for them, and re-layouts: 10 us -> 5.11 us
    pallas_call x1, Pallas kernels: 3.21 us -> 6.29 us  [early_part(): pl.pallas_call(early_kernel, grid=(2 * BLOCKS,), in_specs=[pl.BlockSpec((...]
    pallas_call x1, Pallas kernels: 6.43 us -> 8.27 us  [rest_part(): pl.pallas_call(rest_kernel, grid=(2 * BLOCKS,), in_specs=[pl.BlockSpec(me...]
  transfers between devices with their start and end apart: 18 -> 18, of which waited for: 8 -> 8; matrix products, arithmetic and copies ran while one was open for 6% -> 7% of each run, Pallas kernels for 6% -> 9%
where the time goes in v5:
time: 156 us; the launch traced here: 154 us
  starting transfers between devices  73.5 us (47%)
  blocking collectives  19.1 us (12%)
  waiting for transfers between devices  18.7 us (12%)
  Pallas kernels  14.6 us (9%)
  between operations  14.4 us (9%)
  local copies, waits for them, and re-layouts  8.62 us (6%)
  other arithmetic  5.54 us (4%)
    ppermute x15, starting transfers between devices, shift(): lax.ppermute(value, axis, [(i, (i + step) % count) for i in range(count)])  56.9 us
    all_to_all x1, blocking collectives, spread(): lax.all_to_all(jnp.broadcast_to(value, (count, *value.shape)), axis, 0, 0)  19.1 us
    ppermute x15, waiting for transfers between devices, shift(): lax.ppermute(value, axis, [(i, (i + step) % count) for i in range(count)])  14.7 us
    all_to_all x1, starting transfers between devices, spread(): lax.all_to_all(jnp.broadcast_to(value, (count, *value.shape)), axis, 0, 0)  10 us
    pallas_call x1, Pallas kernels, rest_part(): pl.pallas_call(rest_kernel, grid=(2 * BLOCKS,), in_specs=[pl.BlockSpec(me...  8.27 us
    all_to_all x1, starting transfers between devices, shards(): received = lax.all_to_all(down_grad.reshape(-1, *gate_w.shape), FS, 0, 0)  6.55 us
    pallas_call x1, Pallas kernels, early_part(): pl.pallas_call(early_kernel, grid=(2 * BLOCKS,), in_specs=[pl.BlockSpec((...  6.29 us
    unnamed x17, local copies, waits for them, and re-layouts  5.11 us
  transfers between devices with their start and end apart: 18, of which 8 were waited for; matrix products, arithmetic and copies ran while one was open for 7% of the time, Pallas kernels for 9%

profile of v5, /device:TPU:1, one launch (start us, length us, event | category | flops | bytes accessed | tf_op | source)
XLA Modules:
  0.0 154.4 jit_solution(18173638506348830358)
XLA Ops:
  8.0 19.1 %all_to_all.15 = bf16[8,32,768]{2,1,0:T(8,128)(2,1)} all-to-all(bf16[8,32,768]{2,1,0:T(8,128)(2,1)S(1)} %broadcast_in_dim.10), channel_id=1, replica_groups=mesh['z'=8,'y'=8,'x'=4,'c'=2] {'y'}, dimensions={0} | all-to-all | bytes 786432 | tf_op jit(solution)/shard_map/all_to_all | solution.py:27
  27.2 1.6 %constant_dynamic-update-slice_fusion.2 = (bf16[24,6144]{1,0:T(8,128)(2,1)}, bf16[192,6144]{1,0:T(8,128)(2,1)S(1)}) fusion(bf16[24,2048]{1,0:T(8,128)(2,1)} %param.7), kind=kLoop, calls=%fused_computation.10 | loop fusion | bytes 294912
  28.8 1.6 %constant_dynamic-update-slice_fusion.1 = (bf16[24,6144]{1,0:T(8,128)(2,1)}, bf16[192,6144]{1,0:T(8,128)(2,1)S(1)}) fusion(bf16[24,6144]{1,0:T(8,128)(2,1)} %get-tuple-element.22, bf16[24,2048]{1,0:T(8,128)(2,1)} %param.8, bf16[192,6144]{1,0:T(8,128)(2,1)S(1)} %get-tuple-element.23), kind=kLoop, calls=%fused_computation.9 | loop fusion | bytes 294912
  31.0 6.6 %collective-permute-start.2 = (bf16[24,6144]{1,0:T(8,128)(2,1)}, bf16[24,6144]{1,0:T(8,128)(2,1)S(1)}, u32[]{:S(2)}, u32[]{:S(2)}) collective-permute-start(bf16[24,6144]{1,0:T(8,128)(2,1)} %get-tuple-element.18), channel_id=1, source_target_pairs={{0,4},{2,6},{4,0},{6,2},{1,5},{3,7},{5,1},{7,3},{8,12},{10,14},{12... | collective-permute-start | bytes 884744 | tf_op jit(solution)/shard_map/ppermute | solution.py:22
  37.6 2.8 %collective-permute-start.1 = (bf16[24,6144]{1,0:T(8,128)(2,1)}, bf16[24,6144]{1,0:T(8,128)(2,1)S(1)}, u32[]{:S(2)}, u32[]{:S(2)}) collective-permute-start(bf16[24,6144]{1,0:T(8,128)(2,1)} %get-tuple-element.18), channel_id=1, source_target_pairs={{0,6},{2,0},{4,2},{6,4},{1,7},{3,1},{5,3},{7,5},{8,14},{10,8},{12,... | collective-permute-start | bytes 884744 | tf_op jit(solution)/shard_map/ppermute | solution.py:22
  40.4 2.5 %collective-permute-start = (bf16[24,6144]{1,0:T(8,128)(2,1)}, bf16[24,6144]{1,0:T(8,128)(2,1)S(1)}, u32[]{:S(2)}, u32[]{:S(2)}) collective-permute-start(bf16[24,6144]{1,0:T(8,128)(2,1)} %get-tuple-element.18), channel_id=1, source_target_pairs={{0,2},{2,4},{4,6},{6,0},{1,3},{3,5},{5,7},{7,1},{8,10},{10,12},{12... | collective-permute-start | bytes 884744 | tf_op jit(solution)/shard_map/ppermute | solution.py:22
  43.7 10.0 %all-to-all-start.1 = ((bf16[8,32,384]{2,1,0:T(8,128)(2,1)}), bf16[8,32,384]{2,1,0:T(8,128)(2,1)S(1)}, u32[]{:S(2)}, u32[]{:S(2)}) async-start(bf16[8,32,384]{2,1,0:T(8,128)(2,1)} %broadcast_in_dim.11), calls=%async_computation.1 | async-start | bytes 393216 | tf_op jit(solution)/shard_map/all_to_all | solution.py:27
  53.7 2.2 %pad_maximum_fusion = bf16[96,6144]{1,0:T(8,128)(2,1)} fusion(bf16[24,6144]{1,0:T(8,128)(2,1)S(1)} %collective-permute-done.2, bf16[24,6144]{1,0:T(8,128)(2,1)S(1)} %collective-permute-done.1, bf16[24,6144]{1,0:T(8,128)(2,1)S(1)} %collective-permute-done, bf16[24,6144]{1,0:T(8,128)(2,1)} %get-tuple-element.18), kind=kLoop, calls=%fused_computation.2 | loop fusion | flops 4718592 | bytes 2359296 | tf_op jit(solution)/shard_map/concatenate | solution.py:41
  55.9 5.1 %collective-permute-start.3 = (bf16[96,6144]{1,0:T(8,128)(2,1)}, bf16[96,6144]{1,0:T(8,128)(2,1)}, u32[]{:S(2)}, u32[]{:S(2)}) collective-permute-start(bf16[96,6144]{1,0:T(8,128)(2,1)} %pad_maximum_fusion), channel_id=1, source_target_pairs={{0,1},{1,0},{2,3},{3,2},{4,5},{5,4},{6,7},{7,6},{8,9},{9,8},{10,11... | collective-permute-start | bytes 3538952 | tf_op jit(solution)/shard_map/ppermute | solution.py:22
  61.0 4.0 %all-to-all-done.1.others_0_ = bf16[8,32,384]{2,1,0:T(8,128)(2,1)S(1)} async-done(((bf16[8,32,384]{2,1,0:T(8,128)(2,1)}), bf16[8,32,384]{2,1,0:T(8,128)(2,1)S(1)}, u32[]{:S(2)}, u32[]{:S(2)}) %all-to-all-start.1) | async-done | bytes 196640 | tf_op jit(solution)/shard_map/all_to_all | solution.py:27
  65.1 2.3 %collective-permute-start.4 = (bf16[8,32,384]{2,1,0:T(8,128)(2,1)S(1)}, bf16[8,32,384]{2,1,0:T(8,128)(2,1)S(1)}, u32[]{:S(2)}, u32[]{:S(2)}) collective-permute-start(bf16[8,32,384]{2,1,0:T(8,128)(2,1)S(1)} %all-to-all-done.1.others_0_), channel_id=1, source_target_pairs={{0,8},{8,16},{16,24},{24,32},{32,40},{40,48},{48,56},{56,0},{1,9},... | collective-permute-start | bytes 589832 | tf_op jit(solution)/shard_map/ppermute | solution.py:22
  67.4 4.2 %collective-permute-start.5 = (bf16[8,32,384]{2,1,0:T(8,128)(2,1)S(1)}, bf16[8,32,384]{2,1,0:T(8,128)(2,1)S(1)}, u32[]{:S(2)}, u32[]{:S(2)}) collective-permute-start(bf16[8,32,384]{2,1,0:T(8,128)(2,1)S(1)} %all-to-all-done.1.others_0_), channel_id=1, source_target_pairs={{0,56},{8,0},{16,8},{24,16},{32,24},{40,32},{48,40},{56,48},{1,57}... | collective-permute-start | bytes 589832 | tf_op jit(solution)/shard_map/ppermute | solution.py:22
  71.6 1.5 collective-permute-done.4.others_1_
  73.1 1.9 %collective-permute-start.6 = (bf16[8,32,384]{2,1,0:T(8,128)(2,1)S(1)}, bf16[8,32,384]{2,1,0:T(8,128)(2,1)S(1)}, u32[]{:S(2)}, u32[]{:S(2)}) collective-permute-start(bf16[8,32,384]{2,1,0:T(8,128)(2,1)S(1)} %collective-permute-done.4.others_1_), channel_id=1, source_target_pairs={{0,8},{8,16},{16,24},{24,32},{32,40},{40,48},{48,56},{56,0},{1,9},... | collective-permute-start | bytes 589832 | tf_op jit(solution)/shard_map/ppermute | solution.py:22
  75.0 1.0 constant_dynamic-update-slice_fusion.5
  76.0 4.6 %collective-permute-start.7 = (bf16[8,32,384]{2,1,0:T(8,128)(2,1)S(1)}, bf16[8,32,384]{2,1,0:T(8,128)(2,1)}, u32[]{:S(2)}, u32[]{:S(2)}) collective-permute-start(bf16[8,32,384]{2,1,0:T(8,128)(2,1)S(1)} %collective-permute-done.5.others_2_), channel_id=1, source_target_pairs={{0,56},{8,0},{16,8},{24,16},{32,24},{40,32},{48,40},{56,48},{1,57}... | collective-permute-start | bytes 589832 | tf_op jit(solution)/shard_map/ppermute | solution.py:22
  81.1 1.9 %collective-permute-start.8 = (bf16[8,32,384]{2,1,0:T(8,128)(2,1)S(1)}, bf16[8,32,384]{2,1,0:T(8,128)(2,1)}, u32[]{:S(2)}, u32[]{:S(2)}) collective-permute-start(bf16[8,32,384]{2,1,0:T(8,128)(2,1)S(1)} %collective-permute-done.6.others_3_), channel_id=1, source_target_pairs={{0,8},{8,16},{16,24},{24,32},{32,40},{40,48},{48,56},{56,0},{1,9},... | collective-permute-start | bytes 589832 | tf_op jit(solution)/shard_map/ppermute | solution.py:22
  83.2 5.1 %collective-permute-start.9 = (bf16[8,32,384]{2,1,0:T(8,128)(2,1)}, bf16[8,32,384]{2,1,0:T(8,128)(2,1)}, u32[]{:S(2)}, u32[]{:S(2)}) collective-permute-start(bf16[8,32,384]{2,1,0:T(8,128)(2,1)} %collective-permute-done.7.others_4_), channel_id=1, source_target_pairs={{0,56},{8,0},{16,8},{24,16},{32,24},{40,32},{48,40},{56,48},{1,57}... | collective-permute-start | bytes 589832 | tf_op jit(solution)/shard_map/ppermute | solution.py:22
  88.8 1.9 %collective-permute-start.10 = (bf16[8,32,384]{2,1,0:T(8,128)(2,1)}, bf16[8,32,384]{2,1,0:T(8,128)(2,1)}, u32[]{:S(2)}, u32[]{:S(2)}) collective-permute-start(bf16[8,32,384]{2,1,0:T(8,128)(2,1)} %collective-permute-done.8.others_5_), channel_id=1, source_target_pairs={{0,8},{8,16},{16,24},{24,32},{32,40},{40,48},{48,56},{56,0},{1,9},... | collective-permute-start | bytes 589832 | tf_op jit(solution)/shard_map/ppermute | solution.py:22
  90.7 1.3 constant_dynamic-update-slice_fusion.3.token_ref.cot_ref.later_ref
  92.1 6.3 %shard_map.94 = (f32[192,384]{1,0:T(8,128)S(1)}, f32[192,384]{1,0:T(8,128)S(1)}, bf16[2048,384]{1,0:T(8,128)(2,1)}) custom-call(bf16[192,6144]{1,0:T(8,128)(2,1)S(1)} %constant_dynamic-update-slice_fusion.3.token_ref.cot_ref.later_ref, bf16[2048,768]{1,0:T(8,128)(2,1)} %all-gather.2.cloned.1.call-done.weight_ref, ...), custom_call_target="tpu_custom_call" | custom-call | flops 905969664 | bytes 8388608 | tf_op jit(solution)/shard_map/pallas_call | solution.py:92
  98.4 6.5 %all-to-all-start.2 = ((bf16[64,32,384]{2,1,0:T(8,128)(2,1)}), bf16[64,32,384]{2,1,0:T(8,128)(2,1)}, u32[]{:S(2)}, u32[]{:S(2)}) async-start(bf16[64,32,384]{2,1,0:T(8,128)(2,1)} %bitcast.7), calls=%async_computation.2 | async-start | bytes 3145728 | tf_op jit(solution)/shard_map/all_to_all | solution.py:223
  105.0 0.9 copy-done.1
  105.9 8.3 %shard_map.95 = (f32[2,96,2048]{2,1,0:T(8,128)S(1)}, bf16[2,96,2048]{2,1,0:T(8,128)(2,1)S(1)}) custom-call(s32[1]{0:T(128)} %bitcast.row_ref, bf16[192,6144]{1,0:T(8,128)(2,1)S(1)} %constant_dynamic-update-slice_fusion.3.token_ref.cot_ref.later_ref, bf16[192,6144]{1,0:T(8,128)(2,1)S(1)} %constant_dynamic-update-slice_fusion.3.token_ref.cot_ref.later_ref, ...), custom_call_target="tpu_custom_call" | custom-call | flops 1811939328 | bytes 16777216 | tf_op jit(solution)/shard_map/pallas_call | solution.py:170
  114.2 9.6 %collective-permute-start.11 = (bf16[2,96,2048]{2,1,0:T(8,128)(2,1)S(1)}, bf16[2,96,2048]{2,1,0:T(8,128)(2,1)S(1)}, u32[]{:S(2)}, u32[]{:S(2)}) collective-permute-start(bf16[2,96,2048]{2,1,0:T(8,128)(2,1)S(1)} %get-tuple-element.11), channel_id=1, source_target_pairs={{0,1},{1,0},{2,3},{3,2},{4,5},{5,4},{6,7},{7,6},{8,9},{9,8},{10,11... | collective-permute-start | bytes 2359304 | tf_op jit(solution)/shard_map/ppermute | solution.py:22
  123.8 1.9 %collective-permute-done.11 = bf16[2,96,2048]{2,1,0:T(8,128)(2,1)S(1)} collective-permute-done((bf16[2,96,2048]{2,1,0:T(8,128)(2,1)S(1)}, bf16[2,96,2048]{2,1,0:T(8,128)(2,1)S(1)}, u32[]{:S(2)}, u32[]{:S(2)}) %collective-permute-start.11) | collective-permute-done | bytes 786464 | tf_op jit(solution)/shard_map/ppermute | solution.py:22
  126.0 4.0 %collective-permute-start.12 = (bf16[2,24,2048]{2,1,0:T(8,128)(2,1)S(1)}, bf16[2,24,2048]{2,1,0:T(8,128)(2,1)S(1)}, u32[]{:S(2)}, u32[]{:S(2)}) collective-permute-start(bf16[2,24,2048]{2,1,0:T(8,128)(2,1)S(1)} %get-tuple-element.13), channel_id=1, source_target_pairs={{0,6},{2,0},{4,2},{6,4},{1,7},{3,1},{5,3},{7,5},{8,14},{10,8},{12,... | collective-permute-start | bytes 589832 | tf_op jit(solution)/shard_map/ppermute | solution.py:22
  129.9 2.1 %collective-permute-start.14 = (bf16[2,24,2048]{2,1,0:T(8,128)(2,1)S(1)}, bf16[2,24,2048]{2,1,0:T(8,128)(2,1)S(1)}, u32[]{:S(2)}, u32[]{:S(2)}) collective-permute-start(bf16[2,24,2048]{2,1,0:T(8,128)(2,1)S(1)} %get-tuple-element.14), channel_id=1, source_target_pairs={{0,4},{2,6},{4,0},{6,2},{1,5},{3,7},{5,1},{7,3},{8,12},{10,14},{12... | collective-permute-start | bytes 589832 | tf_op jit(solution)/shard_map/ppermute | solution.py:22
  132.1 2.3 %collective-permute-start.13 = (bf16[2,24,2048]{2,1,0:T(8,128)(2,1)S(1)}, bf16[2,24,2048]{2,1,0:T(8,128)(2,1)S(1)}, u32[]{:S(2)}, u32[]{:S(2)}) collective-permute-start(bf16[2,24,2048]{2,1,0:T(8,128)(2,1)S(1)} %get-tuple-element.15), channel_id=1, source_target_pairs={{0,2},{2,4},{4,6},{6,0},{1,3},{3,5},{5,7},{7,1},{8,10},{10,12},{12... | collective-permute-start | bytes 589832 | tf_op jit(solution)/shard_map/ppermute | solution.py:22
  134.4 4.9 %collective-permute-done.14 = bf16[2,24,2048]{2,1,0:T(8,128)(2,1)S(1)} collective-permute-done((bf16[2,24,2048]{2,1,0:T(8,128)(2,1)S(1)}, bf16[2,24,2048]{2,1,0:T(8,128)(2,1)S(1)}, u32[]{:S(2)}, u32[]{:S(2)}) %collective-permute-start.14) | collective-permute-done | bytes 196640 | tf_op jit(solution)/shard_map/ppermute | solution.py:22
  139.3 5.2 %collective-permute-done.13 = bf16[2,24,2048]{2,1,0:T(8,128)(2,1)S(1)} collective-permute-done((bf16[2,24,2048]{2,1,0:T(8,128)(2,1)S(1)}, bf16[2,24,2048]{2,1,0:T(8,128)(2,1)S(1)}, u32[]{:S(2)}, u32[]{:S(2)}) %collective-permute-start.13) | collective-permute-done | bytes 196640 | tf_op jit(solution)/shard_map/ppermute | solution.py:22
  145.3 1.7 %convert_reduce_fusion = f32[32,384]{1,0:T(8,128)S(1)} fusion(bf16[64,32,384]{2,1,0:T(8,128)(2,1)} %all-to-all-done.2), kind=kLoop, calls=%fused_computation | loop fusion | flops 1560576 | bytes 1622016 | tf_op jit(solution)/shard_map/reduce_sum | solution.py:228
  (37 shorter events, 5.2 us)
Async XLA Ops:
  7.2 23.2 %copy-start.3 = (bf16[24,2048]{1,0:T(8,128)(2,1)S(1)}, bf16[24,2048]{1,0:T(8,128)(2,1)}, u32[]{:S(2)}) copy-start(bf16[24,2048]{1,0:T(8,128)(2,1)} %param.9) | copy-start | bytes 294916
  7.2 35.8 %copy-start.5 = (bf16[32,384]{1,0:T(8,128)(2,1)S(1)}, bf16[32,384]{1,0:T(8,128)(2,1)}, u32[]{:S(2)}) copy-start(bf16[32,384]{1,0:T(8,128)(2,1)} %param.12) | copy-start | bytes 73732
  7.2 84.9 %all-gather.2.cloned.1.call-start = ((), (), s32[]{:S(2)}) async-start(), calls=%async_computation.3 | async-start | bytes 3538944 | tf_op jit(solution)/shard_map/all_gather | solution.py:216
  31.0 22.7 %collective-permute-start.2 = (bf16[24,6144]{1,0:T(8,128)(2,1)}, bf16[24,6144]{1,0:T(8,128)(2,1)S(1)}, u32[]{:S(2)}, u32[]{:S(2)}) collective-permute-start(bf16[24,6144]{1,0:T(8,128)(2,1)} %get-tuple-element.18), channel_id=1, source_target_pairs={{0,4},{2,6},{4,0},{6,2},{1,5},{3,7},{5,1},{7,3},{8,12},{10,14},{12... | collective-permute-start | bytes 884744 | tf_op jit(solution)/shard_map/ppermute | solution.py:22
  37.6 16.1 %collective-permute-start.1 = (bf16[24,6144]{1,0:T(8,128)(2,1)}, bf16[24,6144]{1,0:T(8,128)(2,1)S(1)}, u32[]{:S(2)}, u32[]{:S(2)}) collective-permute-start(bf16[24,6144]{1,0:T(8,128)(2,1)} %get-tuple-element.18), channel_id=1, source_target_pairs={{0,6},{2,0},{4,2},{6,4},{1,7},{3,1},{5,3},{7,5},{8,14},{10,8},{12,... | collective-permute-start | bytes 884744 | tf_op jit(solution)/shard_map/ppermute | solution.py:22
  40.4 13.3 %collective-permute-start = (bf16[24,6144]{1,0:T(8,128)(2,1)}, bf16[24,6144]{1,0:T(8,128)(2,1)S(1)}, u32[]{:S(2)}, u32[]{:S(2)}) collective-permute-start(bf16[24,6144]{1,0:T(8,128)(2,1)} %get-tuple-element.18), channel_id=1, source_target_pairs={{0,2},{2,4},{4,6},{6,0},{1,3},{3,5},{5,7},{7,1},{8,10},{10,12},{12... | collective-permute-start | bytes 884744 | tf_op jit(solution)/shard_map/ppermute | solution.py:22
  43.7 21.4 %all-to-all-start.1 = ((bf16[8,32,384]{2,1,0:T(8,128)(2,1)}), bf16[8,32,384]{2,1,0:T(8,128)(2,1)S(1)}, u32[]{:S(2)}, u32[]{:S(2)}) async-start(bf16[8,32,384]{2,1,0:T(8,128)(2,1)} %broadcast_in_dim.11), calls=%async_computation.1 | async-start | bytes 393216 | tf_op jit(solution)/shard_map/all_to_all | solution.py:27
  53.7 7.3 %copy-start.2 = (bf16[24,6144]{1,0:T(8,128)(2,1)}, bf16[24,6144]{1,0:T(8,128)(2,1)S(1)}, u32[]{:S(2)}) copy-start(bf16[24,6144]{1,0:T(8,128)(2,1)S(1)} %collective-permute-done.1) | copy-start | bytes 884740
  55.9 34.8 %collective-permute-start.3 = (bf16[96,6144]{1,0:T(8,128)(2,1)}, bf16[96,6144]{1,0:T(8,128)(2,1)}, u32[]{:S(2)}, u32[]{:S(2)}) collective-permute-start(bf16[96,6144]{1,0:T(8,128)(2,1)} %pad_maximum_fusion), channel_id=1, source_target_pairs={{0,1},{1,0},{2,3},{3,2},{4,5},{5,4},{6,7},{7,6},{8,9},{9,8},{10,11... | collective-permute-start | bytes 3538952 | tf_op jit(solution)/shard_map/ppermute | solution.py:22
  65.1 8.0 %collective-permute-start.4 = (bf16[8,32,384]{2,1,0:T(8,128)(2,1)S(1)}, bf16[8,32,384]{2,1,0:T(8,128)(2,1)S(1)}, u32[]{:S(2)}, u32[]{:S(2)}) collective-permute-start(bf16[8,32,384]{2,1,0:T(8,128)(2,1)S(1)} %all-to-all-done.1.others_0_), channel_id=1, source_target_pairs={{0,8},{8,16},{16,24},{24,32},{32,40},{40,48},{48,56},{56,0},{1,9},... | collective-permute-start | bytes 589832 | tf_op jit(solution)/shard_map/ppermute | solution.py:22
  67.4 8.6 %collective-permute-start.5 = (bf16[8,32,384]{2,1,0:T(8,128)(2,1)S(1)}, bf16[8,32,384]{2,1,0:T(8,128)(2,1)S(1)}, u32[]{:S(2)}, u32[]{:S(2)}) collective-permute-start(bf16[8,32,384]{2,1,0:T(8,128)(2,1)S(1)} %all-to-all-done.1.others_0_), channel_id=1, source_target_pairs={{0,56},{8,0},{16,8},{24,16},{32,24},{40,32},{48,40},{56,48},{1,57}... | collective-permute-start | bytes 589832 | tf_op jit(solution)/shard_map/ppermute | solution.py:22
  73.1 8.0 %collective-permute-start.6 = (bf16[8,32,384]{2,1,0:T(8,128)(2,1)S(1)}, bf16[8,32,384]{2,1,0:T(8,128)(2,1)S(1)}, u32[]{:S(2)}, u32[]{:S(2)}) collective-permute-start(bf16[8,32,384]{2,1,0:T(8,128)(2,1)S(1)} %collective-permute-done.4.others_1_), channel_id=1, source_target_pairs={{0,8},{8,16},{16,24},{24,32},{32,40},{40,48},{48,56},{56,0},{1,9},... | collective-permute-start | bytes 589832 | tf_op jit(solution)/shard_map/ppermute | solution.py:22
  76.0 7.2 %collective-permute-start.7 = (bf16[8,32,384]{2,1,0:T(8,128)(2,1)S(1)}, bf16[8,32,384]{2,1,0:T(8,128)(2,1)}, u32[]{:S(2)}, u32[]{:S(2)}) collective-permute-start(bf16[8,32,384]{2,1,0:T(8,128)(2,1)S(1)} %collective-permute-done.5.others_2_), channel_id=1, source_target_pairs={{0,56},{8,0},{16,8},{24,16},{32,24},{40,32},{48,40},{56,48},{1,57}... | collective-permute-start | bytes 589832 | tf_op jit(solution)/shard_map/ppermute | solution.py:22
  81.1 11.0 %copy-start = (bf16[8,32,384]{2,1,0:T(8,128)(2,1)}, bf16[8,32,384]{2,1,0:T(8,128)(2,1)S(1)}, u32[]{:S(2)}) copy-start(bf16[8,32,384]{2,1,0:T(8,128)(2,1)S(1)} %collective-permute-done.6.others_3_) | copy-start | bytes 589828
  81.1 7.7 %collective-permute-start.8 = (bf16[8,32,384]{2,1,0:T(8,128)(2,1)S(1)}, bf16[8,32,384]{2,1,0:T(8,128)(2,1)}, u32[]{:S(2)}, u32[]{:S(2)}) collective-permute-start(bf16[8,32,384]{2,1,0:T(8,128)(2,1)S(1)} %collective-permute-done.6.others_3_), channel_id=1, source_target_pairs={{0,8},{8,16},{16,24},{24,32},{32,40},{40,48},{48,56},{56,0},{1,9},... | collective-permute-start | bytes 589832 | tf_op jit(solution)/shard_map/ppermute | solution.py:22
  83.2 21.8 %collective-permute-start.9 = (bf16[8,32,384]{2,1,0:T(8,128)(2,1)}, bf16[8,32,384]{2,1,0:T(8,128)(2,1)}, u32[]{:S(2)}, u32[]{:S(2)}) collective-permute-start(bf16[8,32,384]{2,1,0:T(8,128)(2,1)} %collective-permute-done.7.others_4_), channel_id=1, source_target_pairs={{0,56},{8,0},{16,8},{24,16},{32,24},{40,32},{48,40},{56,48},{1,57}... | collective-permute-start | bytes 589832 | tf_op jit(solution)/shard_map/ppermute | solution.py:22
  88.8 16.2 %collective-permute-start.10 = (bf16[8,32,384]{2,1,0:T(8,128)(2,1)}, bf16[8,32,384]{2,1,0:T(8,128)(2,1)}, u32[]{:S(2)}, u32[]{:S(2)}) collective-permute-start(bf16[8,32,384]{2,1,0:T(8,128)(2,1)} %collective-permute-done.8.others_5_), channel_id=1, source_target_pairs={{0,8},{8,16},{16,24},{24,32},{32,40},{40,48},{48,56},{56,0},{1,9},... | collective-permute-start | bytes 589832 | tf_op jit(solution)/shard_map/ppermute | solution.py:22
  98.4 46.9 %all-to-all-start.2 = ((bf16[64,32,384]{2,1,0:T(8,128)(2,1)}), bf16[64,32,384]{2,1,0:T(8,128)(2,1)}, u32[]{:S(2)}, u32[]{:S(2)}) async-start(bf16[64,32,384]{2,1,0:T(8,128)(2,1)} %bitcast.7), calls=%async_computation.2 | async-start | bytes 3145728 | tf_op jit(solution)/shard_map/all_to_all | solution.py:223
  105.0 0.9 copy-start.1
  114.2 11.5 %collective-permute-start.11 = (bf16[2,96,2048]{2,1,0:T(8,128)(2,1)S(1)}, bf16[2,96,2048]{2,1,0:T(8,128)(2,1)S(1)}, u32[]{:S(2)}, u32[]{:S(2)}) collective-permute-start(bf16[2,96,2048]{2,1,0:T(8,128)(2,1)S(1)} %get-tuple-element.11), channel_id=1, source_target_pairs={{0,1},{1,0},{2,3},{3,2},{4,5},{5,4},{6,7},{7,6},{8,9},{9,8},{10,11... | collective-permute-start | bytes 2359304 | tf_op jit(solution)/shard_map/ppermute | solution.py:22
  125.9 21.0 %copy-start.4 = (f32[32,384]{1,0:T(8,128)S(1)}, f32[32,384]{1,0:T(8,128)}, u32[]{:S(2)}) copy-start(f32[32,384]{1,0:T(8,128)} %param.13) | copy-start | bytes 147460
  126.0 8.4 %collective-permute-start.12 = (bf16[2,24,2048]{2,1,0:T(8,128)(2,1)S(1)}, bf16[2,24,2048]{2,1,0:T(8,128)(2,1)S(1)}, u32[]{:S(2)}, u32[]{:S(2)}) collective-permute-start(bf16[2,24,2048]{2,1,0:T(8,128)(2,1)S(1)} %get-tuple-element.13), channel_id=1, source_target_pairs={{0,6},{2,0},{4,2},{6,4},{1,7},{3,1},{5,3},{7,5},{8,14},{10,8},{12,... | collective-permute-start | bytes 589832 | tf_op jit(solution)/shard_map/ppermute | solution.py:22
  129.9 9.3 %collective-permute-start.14 = (bf16[2,24,2048]{2,1,0:T(8,128)(2,1)S(1)}, bf16[2,24,2048]{2,1,0:T(8,128)(2,1)S(1)}, u32[]{:S(2)}, u32[]{:S(2)}) collective-permute-start(bf16[2,24,2048]{2,1,0:T(8,128)(2,1)S(1)} %get-tuple-element.14), channel_id=1, source_target_pairs={{0,4},{2,6},{4,0},{6,2},{1,5},{3,7},{5,1},{7,3},{8,12},{10,14},{12... | collective-permute-start | bytes 589832 | tf_op jit(solution)/shard_map/ppermute | solution.py:22
  132.1 12.4 %collective-permute-start.13 = (bf16[2,24,2048]{2,1,0:T(8,128)(2,1)S(1)}, bf16[2,24,2048]{2,1,0:T(8,128)(2,1)S(1)}, u32[]{:S(2)}, u32[]{:S(2)}) collective-permute-start(bf16[2,24,2048]{2,1,0:T(8,128)(2,1)S(1)} %get-tuple-element.15), channel_id=1, source_target_pairs={{0,2},{2,4},{4,6},{6,0},{1,3},{3,5},{5,7},{7,1},{8,10},{10,12},{12... | collective-permute-start | bytes 589832 | tf_op jit(solution)/shard_map/ppermute | solution.py:22
Sparse Core Ops, SparseCore 0:
  27.3 55.1 all-gather.1

commit v6 on v5

--- a/solution.py
+++ b/solution.py
@@ -22,13 +22,28 @@
     return lax.ppermute(value, axis, [(i, (i + step) % count) for i in range(count)])
 
 
-def spread(value, axis):
-    count = lax.axis_size(axis)
-    return lax.all_to_all(jnp.broadcast_to(value, (count, *value.shape)), axis, 0, 0)
+def copy_kernel(*refs):
+    *ins, out_ref = refs
+    at = 0
+    for ref in ins:
+        cols = ref.shape[1]
+        out_ref[:, :, at : at + cols] = jnp.broadcast_to(ref[...], (out_ref.shape[0], *ref.shape))
+        at += cols
+
+
+def copies(count, *arrays):
+    shape = (count, arrays[0].shape[0], sum(a.shape[1] for a in arrays))
+    return pl.pallas_call(
+        copy_kernel,
+        out_shape=jax.ShapeDtypeStruct(shape, arrays[0].dtype),
+        compiler_params=pltpu.CompilerParams(vmem_limit_bytes=8 << 20),
+        cost_estimate=pl.CostEstimate(flops=1 << 20, transcendentals=0, bytes_accessed=1 << 20),
+    )(*arrays)
 
 
 def gather_down(down):
-    line = spread(down, "z")
+    fan = copies(lax.axis_size("z"), down)
+    line = lax.all_to_all(fan, "z", 0, 0)
     chunks, ahead, behind = [line], line, line
     for _ in range(1, 4):
         ahead, behind = shift(ahead, "y", 1), shift(behind, "y", -1)
@@ -211,12 +226,14 @@
 
 def shards(later, early, cotangent, gate_w, up_w, down_w, down_grad_sum):
     rows, _ = later.shape
-    line = spread(jnp.concatenate([gate_w, up_w], axis=1), "y")
+    fan = copies(lax.axis_size("y"), gate_w, up_w)
+    line = lax.all_to_all(fan, "y", 0, 0)
     line = line.reshape(-1, line.shape[-1])
     whole = lax.all_gather(line, "z", axis=0, tiled=True)
     whole = pltpu.with_memory_space_constraint(whole, pltpu.HBM)
-    tokens = jnp.concatenate([later, early, cotangent], axis=1)
+    tokens = copies(1, later, early, cotangent)[0]
     tokens = collect_tokens(tokens)
+    tokens = pltpu.with_memory_space_constraint(tokens, pltpu.VMEM)
     chunks = gather_down(down_w)
 
     gate_early, up_early, down_grad = early_part(tokens, whole)

time: 156 us -> 156 us (level)
    unnamed x17 -> x24, local copies, waits for them, and re-layouts: 5.11 us -> 7.81 us
  transfers between devices with their start and end apart: 18 -> 18, of which waited for: 8 -> 8; matrix products, arithmetic and copies ran while one was open for 7% -> 4% of each run, Pallas kernels for 9% -> 10%
where the time goes in v6:
time: 156 us; the launch traced here: 155 us
  starting transfers between devices  73.5 us (47%)
  blocking collectives  19.1 us (12%)
  waiting for transfers between devices  17.7 us (11%)
  Pallas kernels  15.3 us (10%)
  between operations  14.4 us (9%)
  local copies, waits for them, and re-layouts  9.89 us (6%)
  other arithmetic  4.75 us (3%)
    ppermute x15, starting transfers between devices, shift(): lax.ppermute(value, axis, [(i, (i + step) % count) for i in range(count)])  56.9 us
    all_to_all x1, blocking collectives, shards(): line = lax.all_to_all(fan, 'y', 0, 0)  19.1 us
    ppermute x15, waiting for transfers between devices, shift(): lax.ppermute(value, axis, [(i, (i + step) % count) for i in range(count)])  13.7 us
    all_to_all x1, starting transfers between devices, gather_down(): line = lax.all_to_all(fan, 'z', 0, 0)  10 us
    pallas_call x1, Pallas kernels, rest_part(): pl.pallas_call(rest_kernel, grid=(2 * BLOCKS,), in_specs=[pl.BlockSpec(me...  8.27 us
    unnamed x24, local copies, waits for them, and re-layouts  7.81 us
    all_to_all x1, starting transfers between devices, shards(): received = lax.all_to_all(down_grad.reshape(-1, *gate_w.shape), FS, 0, 0)  6.55 us
    pallas_call x1, Pallas kernels, early_part(): pl.pallas_call(early_kernel, grid=(2 * BLOCKS,), in_specs=[pl.BlockSpec((...  6.3 us
  transfers between devices with their start and end apart: 18, of which 8 were waited for; matrix products, arithmetic and copies ran while one was open for 4% of the time, Pallas kernels for 10%

profile of v6, /device:TPU:1, one launch (start us, length us, event | category | flops | bytes accessed | tf_op | source)
XLA Modules:
  0.0 154.7 jit_solution(9734445674666198370)
XLA Ops:
  8.7 19.1 %all_to_all.15 = bf16[8,32,768]{2,1,0:T(8,128)(2,1)} all-to-all(bf16[8,32,768]{2,1,0:T(8,128)(2,1)S(1)} %shard_map.95), channel_id=1, replica_groups=mesh['z'=8,'y'=8,'x'=4,'c'=2] {'y'}, dimensions={0} | all-to-all | bytes 786432 | tf_op jit(solution)/shard_map/all_to_all | solution.py:230
  28.8 0.9 copy-done.3
  29.7 0.9 copy-done.4
  30.6 6.6 %collective-permute-start.2 = (bf16[24,6144]{1,0:T(8,128)(2,1)S(1)}, bf16[24,6144]{1,0:T(8,128)(2,1)S(1)}, u32[]{:S(2)}, u32[]{:S(2)}) collective-permute-start(bf16[24,6144]{1,0:T(8,128)(2,1)S(1)} %bitcast.9), channel_id=1, source_target_pairs={{0,4},{2,6},{4,0},{6,2},{1,5},{3,7},{5,1},{7,3},{8,12},{10,14},{12... | collective-permute-start | bytes 884744 | tf_op jit(solution)/shard_map/ppermute | solution.py:22
  37.2 2.8 %collective-permute-start.1 = (bf16[24,6144]{1,0:T(8,128)(2,1)S(1)}, bf16[24,6144]{1,0:T(8,128)(2,1)S(1)}, u32[]{:S(2)}, u32[]{:S(2)}) collective-permute-start(bf16[24,6144]{1,0:T(8,128)(2,1)S(1)} %bitcast.10), channel_id=1, source_target_pairs={{0,6},{2,0},{4,2},{6,4},{1,7},{3,1},{5,3},{7,5},{8,14},{10,8},{12,... | collective-permute-start | bytes 884744 | tf_op jit(solution)/shard_map/ppermute | solution.py:22
  40.0 2.5 %collective-permute-start = (bf16[24,6144]{1,0:T(8,128)(2,1)S(1)}, bf16[24,6144]{1,0:T(8,128)(2,1)}, u32[]{:S(2)}, u32[]{:S(2)}) collective-permute-start(bf16[24,6144]{1,0:T(8,128)(2,1)S(1)} %bitcast.11), channel_id=1, source_target_pairs={{0,2},{2,4},{4,6},{6,0},{1,3},{3,5},{5,7},{7,1},{8,10},{10,12},{12... | collective-permute-start | bytes 884744 | tf_op jit(solution)/shard_map/ppermute | solution.py:22
  44.0 10.0 %all-to-all-start.1 = ((bf16[8,32,384]{2,1,0:T(8,128)(2,1)}), bf16[8,32,384]{2,1,0:T(8,128)(2,1)S(1)}, u32[]{:S(2)}, u32[]{:S(2)}) async-start(bf16[8,32,384]{2,1,0:T(8,128)(2,1)} %shard_map.97), calls=%async_computation.1 | async-start | bytes 393216 | tf_op jit(solution)/shard_map/all_to_all | solution.py:46
  54.1 2.2 %pad_maximum_fusion = bf16[96,6144]{1,0:T(8,128)(2,1)} fusion(bf16[24,6144]{1,0:T(8,128)(2,1)S(1)} %collective-permute-done.2, bf16[24,6144]{1,0:T(8,128)(2,1)S(1)} %collective-permute-done.1, bf16[24,6144]{1,0:T(8,128)(2,1)} %collective-permute-done, bf16[24,6144]{1,0:T(8,128)(2,1)S(1)} %bitcast.12), kind=kLoop, calls=%fused_computation.2 | loop fusion | flops 4718592 | bytes 2359296 | tf_op jit(solution)/shard_map/concatenate | solution.py:56
  56.3 5.1 %collective-permute-start.3 = (bf16[96,6144]{1,0:T(8,128)(2,1)}, bf16[96,6144]{1,0:T(8,128)(2,1)}, u32[]{:S(2)}, u32[]{:S(2)}) collective-permute-start(bf16[96,6144]{1,0:T(8,128)(2,1)} %pad_maximum_fusion), channel_id=1, source_target_pairs={{0,1},{1,0},{2,3},{3,2},{4,5},{5,4},{6,7},{7,6},{8,9},{9,8},{10,11... | collective-permute-start | bytes 3538952 | tf_op jit(solution)/shard_map/ppermute | solution.py:22
  61.3 4.0 %all-to-all-done.1.others_0_ = bf16[8,32,384]{2,1,0:T(8,128)(2,1)S(1)} async-done(((bf16[8,32,384]{2,1,0:T(8,128)(2,1)}), bf16[8,32,384]{2,1,0:T(8,128)(2,1)S(1)}, u32[]{:S(2)}, u32[]{:S(2)}) %all-to-all-start.1) | async-done | bytes 196640 | tf_op jit(solution)/shard_map/all_to_all | solution.py:46
  65.4 2.2 %collective-permute-start.4 = (bf16[8,32,384]{2,1,0:T(8,128)(2,1)S(1)}, bf16[8,32,384]{2,1,0:T(8,128)(2,1)S(1)}, u32[]{:S(2)}, u32[]{:S(2)}) collective-permute-start(bf16[8,32,384]{2,1,0:T(8,128)(2,1)S(1)} %all-to-all-done.1.others_0_), channel_id=1, source_target_pairs={{0,8},{8,16},{16,24},{24,32},{32,40},{40,48},{48,56},{56,0},{1,9},... | collective-permute-start | bytes 589832 | tf_op jit(solution)/shard_map/ppermute | solution.py:22
  67.6 1.0 constant_dynamic-update-slice_fusion.3
  68.6 4.3 %collective-permute-start.5 = (bf16[8,32,384]{2,1,0:T(8,128)(2,1)S(1)}, bf16[8,32,384]{2,1,0:T(8,128)(2,1)S(1)}, u32[]{:S(2)}, u32[]{:S(2)}) collective-permute-start(bf16[8,32,384]{2,1,0:T(8,128)(2,1)S(1)} %all-to-all-done.1.others_0_), channel_id=1, source_target_pairs={{0,56},{8,0},{16,8},{24,16},{32,24},{40,32},{48,40},{56,48},{1,57}... | collective-permute-start | bytes 589832 | tf_op jit(solution)/shard_map/ppermute | solution.py:22
  73.4 1.9 %collective-permute-start.6 = (bf16[8,32,384]{2,1,0:T(8,128)(2,1)S(1)}, bf16[8,32,384]{2,1,0:T(8,128)(2,1)S(1)}, u32[]{:S(2)}, u32[]{:S(2)}) collective-permute-start(bf16[8,32,384]{2,1,0:T(8,128)(2,1)S(1)} %collective-permute-done.4.others_1_), channel_id=1, source_target_pairs={{0,8},{8,16},{16,24},{24,32},{32,40},{40,48},{48,56},{56,0},{1,9},... | collective-permute-start | bytes 589832 | tf_op jit(solution)/shard_map/ppermute | solution.py:22
  75.3 1.0 constant_dynamic-update-slice_fusion.2
  76.3 4.6 %collective-permute-start.7 = (bf16[8,32,384]{2,1,0:T(8,128)(2,1)S(1)}, bf16[8,32,384]{2,1,0:T(8,128)(2,1)}, u32[]{:S(2)}, u32[]{:S(2)}) collective-permute-start(bf16[8,32,384]{2,1,0:T(8,128)(2,1)S(1)} %collective-permute-done.5.others_2_), channel_id=1, source_target_pairs={{0,56},{8,0},{16,8},{24,16},{32,24},{40,32},{48,40},{56,48},{1,57}... | collective-permute-start | bytes 589832 | tf_op jit(solution)/shard_map/ppermute | solution.py:22
  81.4 1.9 %collective-permute-start.8 = (bf16[8,32,384]{2,1,0:T(8,128)(2,1)S(1)}, bf16[8,32,384]{2,1,0:T(8,128)(2,1)}, u32[]{:S(2)}, u32[]{:S(2)}) collective-permute-start(bf16[8,32,384]{2,1,0:T(8,128)(2,1)S(1)} %collective-permute-done.6.others_3_), channel_id=1, source_target_pairs={{0,8},{8,16},{16,24},{24,32},{32,40},{40,48},{48,56},{56,0},{1,9},... | collective-permute-start | bytes 589832 | tf_op jit(solution)/shard_map/ppermute | solution.py:22
  83.5 5.1 %collective-permute-start.9 = (bf16[8,32,384]{2,1,0:T(8,128)(2,1)}, bf16[8,32,384]{2,1,0:T(8,128)(2,1)}, u32[]{:S(2)}, u32[]{:S(2)}) collective-permute-start(bf16[8,32,384]{2,1,0:T(8,128)(2,1)} %collective-permute-done.7.others_4_), channel_id=1, source_target_pairs={{0,56},{8,0},{16,8},{24,16},{32,24},{40,32},{48,40},{56,48},{1,57}... | collective-permute-start | bytes 589832 | tf_op jit(solution)/shard_map/ppermute | solution.py:22
  89.1 1.9 %collective-permute-start.10 = (bf16[8,32,384]{2,1,0:T(8,128)(2,1)}, bf16[8,32,384]{2,1,0:T(8,128)(2,1)}, u32[]{:S(2)}, u32[]{:S(2)}) collective-permute-start(bf16[8,32,384]{2,1,0:T(8,128)(2,1)} %collective-permute-done.8.others_5_), channel_id=1, source_target_pairs={{0,8},{8,16},{16,24},{24,32},{32,40},{40,48},{48,56},{56,0},{1,9},... | collective-permute-start | bytes 589832 | tf_op jit(solution)/shard_map/ppermute | solution.py:22
  91.0 1.3 constant_dynamic-update-slice_fusion.token_ref.cot_ref.later_ref
  92.4 6.3 %shard_map.96 = (f32[192,384]{1,0:T(8,128)S(1)}, f32[192,384]{1,0:T(8,128)S(1)}, bf16[2048,384]{1,0:T(8,128)(2,1)}) custom-call(bf16[192,6144]{1,0:T(8,128)(2,1)S(1)} %constant_dynamic-update-slice_fusion.token_ref.cot_ref.later_ref, bf16[2048,768]{1,0:T(8,128)(2,1)} %all-gather.2.cloned.1.call-done.weight_ref, ...), custom_call_target="tpu_custom_call" | custom-call | flops 905969664 | bytes 8388608 | tf_op jit(solution)/shard_map/pallas_call | solution.py:107
  98.7 6.5 %all-to-all-start.2 = ((bf16[64,32,384]{2,1,0:T(8,128)(2,1)}), bf16[64,32,384]{2,1,0:T(8,128)(2,1)}, u32[]{:S(2)}, u32[]{:S(2)}) async-start(bf16[64,32,384]{2,1,0:T(8,128)(2,1)} %bitcast.13), calls=%async_computation.2 | async-start | bytes 3145728 | tf_op jit(solution)/shard_map/all_to_all | solution.py:240
  105.3 0.9 copy-done.1
  106.2 8.3 %shard_map.98 = (f32[2,96,2048]{2,1,0:T(8,128)S(1)}, bf16[2,96,2048]{2,1,0:T(8,128)(2,1)S(1)}) custom-call(s32[1]{0:T(128)} %bitcast.row_ref, bf16[192,6144]{1,0:T(8,128)(2,1)S(1)} %constant_dynamic-update-slice_fusion.token_ref.cot_ref.later_ref, bf16[192,6144]{1,0:T(8,128)(2,1)S(1)} %constant_dynamic-update-slice_fusion.token_ref.cot_ref.later_ref, ...), custom_call_target="tpu_custom_call" | custom-call | flops 1811939328 | bytes 16777216 | tf_op jit(solution)/shard_map/pallas_call | solution.py:185
  114.5 9.6 %collective-permute-start.11 = (bf16[2,96,2048]{2,1,0:T(8,128)(2,1)S(1)}, bf16[2,96,2048]{2,1,0:T(8,128)(2,1)S(1)}, u32[]{:S(2)}, u32[]{:S(2)}) collective-permute-start(bf16[2,96,2048]{2,1,0:T(8,128)(2,1)S(1)} %get-tuple-element.11), channel_id=1, source_target_pairs={{0,1},{1,0},{2,3},{3,2},{4,5},{5,4},{6,7},{7,6},{8,9},{9,8},{10,11... | collective-permute-start | bytes 2359304 | tf_op jit(solution)/shard_map/ppermute | solution.py:22
  124.1 1.9 %collective-permute-done.11 = bf16[2,96,2048]{2,1,0:T(8,128)(2,1)S(1)} collective-permute-done((bf16[2,96,2048]{2,1,0:T(8,128)(2,1)S(1)}, bf16[2,96,2048]{2,1,0:T(8,128)(2,1)S(1)}, u32[]{:S(2)}, u32[]{:S(2)}) %collective-permute-start.11) | collective-permute-done | bytes 786464 | tf_op jit(solution)/shard_map/ppermute | solution.py:22
  126.3 4.0 %collective-permute-start.12 = (bf16[2,24,2048]{2,1,0:T(8,128)(2,1)S(1)}, bf16[2,24,2048]{2,1,0:T(8,128)(2,1)S(1)}, u32[]{:S(2)}, u32[]{:S(2)}) collective-permute-start(bf16[2,24,2048]{2,1,0:T(8,128)(2,1)S(1)} %get-tuple-element.13), channel_id=1, source_target_pairs={{0,6},{2,0},{4,2},{6,4},{1,7},{3,1},{5,3},{7,5},{8,14},{10,8},{12,... | collective-permute-start | bytes 589832 | tf_op jit(solution)/shard_map/ppermute | solution.py:22
  130.2 2.3 %collective-permute-start.14 = (bf16[2,24,2048]{2,1,0:T(8,128)(2,1)S(1)}, bf16[2,24,2048]{2,1,0:T(8,128)(2,1)S(1)}, u32[]{:S(2)}, u32[]{:S(2)}) collective-permute-start(bf16[2,24,2048]{2,1,0:T(8,128)(2,1)S(1)} %get-tuple-element.14), channel_id=1, source_target_pairs={{0,4},{2,6},{4,0},{6,2},{1,5},{3,7},{5,1},{7,3},{8,12},{10,14},{12... | collective-permute-start | bytes 589832 | tf_op jit(solution)/shard_map/ppermute | solution.py:22
  132.5 2.1 %collective-permute-start.13 = (bf16[2,24,2048]{2,1,0:T(8,128)(2,1)S(1)}, bf16[2,24,2048]{2,1,0:T(8,128)(2,1)S(1)}, u32[]{:S(2)}, u32[]{:S(2)}) collective-permute-start(bf16[2,24,2048]{2,1,0:T(8,128)(2,1)S(1)} %get-tuple-element.15), channel_id=1, source_target_pairs={{0,2},{2,4},{4,6},{6,0},{1,3},{3,5},{5,7},{7,1},{8,10},{10,12},{12... | collective-permute-start | bytes 589832 | tf_op jit(solution)/shard_map/ppermute | solution.py:22
  134.7 4.9 %collective-permute-done.14 = bf16[2,24,2048]{2,1,0:T(8,128)(2,1)S(1)} collective-permute-done((bf16[2,24,2048]{2,1,0:T(8,128)(2,1)S(1)}, bf16[2,24,2048]{2,1,0:T(8,128)(2,1)S(1)}, u32[]{:S(2)}, u32[]{:S(2)}) %collective-permute-start.14) | collective-permute-done | bytes 196640 | tf_op jit(solution)/shard_map/ppermute | solution.py:22
  139.5 5.2 %collective-permute-done.13 = bf16[2,24,2048]{2,1,0:T(8,128)(2,1)S(1)} collective-permute-done((bf16[2,24,2048]{2,1,0:T(8,128)(2,1)S(1)}, bf16[2,24,2048]{2,1,0:T(8,128)(2,1)S(1)}, u32[]{:S(2)}, u32[]{:S(2)}) %collective-permute-start.13) | collective-permute-done | bytes 196640 | tf_op jit(solution)/shard_map/ppermute | solution.py:22
  145.5 1.7 %convert_reduce_fusion = f32[32,384]{1,0:T(8,128)S(1)} fusion(bf16[64,32,384]{2,1,0:T(8,128)(2,1)} %all-to-all-done.2), kind=kLoop, calls=%fused_computation | loop fusion | flops 1560576 | bytes 1622016 | tf_op jit(solution)/shard_map/reduce_sum | solution.py:245
  (43 shorter events, 7.3 us)
Async XLA Ops:
  7.2 85.2 %all-gather.2.cloned.1.call-start = ((), (), s32[]{:S(2)}) async-start(), calls=%async_computation.3 | async-start | bytes 3538944 | tf_op jit(solution)/shard_map/all_gather | solution.py:232
  7.2 0.7 copy-start.5
  7.9 0.7 copy-start.6
  27.9 0.9 copy-start.2
  28.8 0.9 copy-start.3
  29.7 0.9 copy-start.4
  30.6 23.4 %collective-permute-start.2 = (bf16[24,6144]{1,0:T(8,128)(2,1)S(1)}, bf16[24,6144]{1,0:T(8,128)(2,1)S(1)}, u32[]{:S(2)}, u32[]{:S(2)}) collective-permute-start(bf16[24,6144]{1,0:T(8,128)(2,1)S(1)} %bitcast.9), channel_id=1, source_target_pairs={{0,4},{2,6},{4,0},{6,2},{1,5},{3,7},{5,1},{7,3},{8,12},{10,14},{12... | collective-permute-start | bytes 884744 | tf_op jit(solution)/shard_map/ppermute | solution.py:22
  37.2 16.8 %collective-permute-start.1 = (bf16[24,6144]{1,0:T(8,128)(2,1)S(1)}, bf16[24,6144]{1,0:T(8,128)(2,1)S(1)}, u32[]{:S(2)}, u32[]{:S(2)}) collective-permute-start(bf16[24,6144]{1,0:T(8,128)(2,1)S(1)} %bitcast.10), channel_id=1, source_target_pairs={{0,6},{2,0},{4,2},{6,4},{1,7},{3,1},{5,3},{7,5},{8,14},{10,8},{12,... | collective-permute-start | bytes 884744 | tf_op jit(solution)/shard_map/ppermute | solution.py:22
  40.0 14.0 %collective-permute-start = (bf16[24,6144]{1,0:T(8,128)(2,1)S(1)}, bf16[24,6144]{1,0:T(8,128)(2,1)}, u32[]{:S(2)}, u32[]{:S(2)}) collective-permute-start(bf16[24,6144]{1,0:T(8,128)(2,1)S(1)} %bitcast.11), channel_id=1, source_target_pairs={{0,2},{2,4},{4,6},{6,0},{1,3},{3,5},{5,7},{7,1},{8,10},{10,12},{12... | collective-permute-start | bytes 884744 | tf_op jit(solution)/shard_map/ppermute | solution.py:22
  42.5 0.7 copy-start.7
  44.0 21.4 %all-to-all-start.1 = ((bf16[8,32,384]{2,1,0:T(8,128)(2,1)}), bf16[8,32,384]{2,1,0:T(8,128)(2,1)S(1)}, u32[]{:S(2)}, u32[]{:S(2)}) async-start(bf16[8,32,384]{2,1,0:T(8,128)(2,1)} %shard_map.97), calls=%async_computation.1 | async-start | bytes 393216 | tf_op jit(solution)/shard_map/all_to_all | solution.py:46
  54.0 18.8 %copy-start.8 = (bf16[24,6144]{1,0:T(8,128)(2,1)}, bf16[24,6144]{1,0:T(8,128)(2,1)S(1)}, u32[]{:S(2)}) copy-start(bf16[24,6144]{1,0:T(8,128)(2,1)S(1)} %collective-permute-done.1) | copy-start | bytes 884740
  56.3 34.8 %collective-permute-start.3 = (bf16[96,6144]{1,0:T(8,128)(2,1)}, bf16[96,6144]{1,0:T(8,128)(2,1)}, u32[]{:S(2)}, u32[]{:S(2)}) collective-permute-start(bf16[96,6144]{1,0:T(8,128)(2,1)} %pad_maximum_fusion), channel_id=1, source_target_pairs={{0,1},{1,0},{2,3},{3,2},{4,5},{5,4},{6,7},{7,6},{8,9},{9,8},{10,11... | collective-permute-start | bytes 3538952 | tf_op jit(solution)/shard_map/ppermute | solution.py:22
  65.4 8.0 %collective-permute-start.4 = (bf16[8,32,384]{2,1,0:T(8,128)(2,1)S(1)}, bf16[8,32,384]{2,1,0:T(8,128)(2,1)S(1)}, u32[]{:S(2)}, u32[]{:S(2)}) collective-permute-start(bf16[8,32,384]{2,1,0:T(8,128)(2,1)S(1)} %all-to-all-done.1.others_0_), channel_id=1, source_target_pairs={{0,8},{8,16},{16,24},{24,32},{32,40},{40,48},{48,56},{56,0},{1,9},... | collective-permute-start | bytes 589832 | tf_op jit(solution)/shard_map/ppermute | solution.py:22
  68.6 7.7 %collective-permute-start.5 = (bf16[8,32,384]{2,1,0:T(8,128)(2,1)S(1)}, bf16[8,32,384]{2,1,0:T(8,128)(2,1)S(1)}, u32[]{:S(2)}, u32[]{:S(2)}) collective-permute-start(bf16[8,32,384]{2,1,0:T(8,128)(2,1)S(1)} %all-to-all-done.1.others_0_), channel_id=1, source_target_pairs={{0,56},{8,0},{16,8},{24,16},{32,24},{40,32},{48,40},{56,48},{1,57}... | collective-permute-start | bytes 589832 | tf_op jit(solution)/shard_map/ppermute | solution.py:22
  73.4 8.0 %collective-permute-start.6 = (bf16[8,32,384]{2,1,0:T(8,128)(2,1)S(1)}, bf16[8,32,384]{2,1,0:T(8,128)(2,1)S(1)}, u32[]{:S(2)}, u32[]{:S(2)}) collective-permute-start(bf16[8,32,384]{2,1,0:T(8,128)(2,1)S(1)} %collective-permute-done.4.others_1_), channel_id=1, source_target_pairs={{0,8},{8,16},{16,24},{24,32},{32,40},{40,48},{48,56},{56,0},{1,9},... | collective-permute-start | bytes 589832 | tf_op jit(solution)/shard_map/ppermute | solution.py:22
  76.3 7.2 %collective-permute-start.7 = (bf16[8,32,384]{2,1,0:T(8,128)(2,1)S(1)}, bf16[8,32,384]{2,1,0:T(8,128)(2,1)}, u32[]{:S(2)}, u32[]{:S(2)}) collective-permute-start(bf16[8,32,384]{2,1,0:T(8,128)(2,1)S(1)} %collective-permute-done.5.others_2_), channel_id=1, source_target_pairs={{0,56},{8,0},{16,8},{24,16},{32,24},{40,32},{48,40},{56,48},{1,57}... | collective-permute-start | bytes 589832 | tf_op jit(solution)/shard_map/ppermute | solution.py:22
  81.4 11.0 %copy-start = (bf16[8,32,384]{2,1,0:T(8,128)(2,1)}, bf16[8,32,384]{2,1,0:T(8,128)(2,1)S(1)}, u32[]{:S(2)}) copy-start(bf16[8,32,384]{2,1,0:T(8,128)(2,1)S(1)} %collective-permute-done.6.others_3_) | copy-start | bytes 589828
  81.4 7.7 %collective-permute-start.8 = (bf16[8,32,384]{2,1,0:T(8,128)(2,1)S(1)}, bf16[8,32,384]{2,1,0:T(8,128)(2,1)}, u32[]{:S(2)}, u32[]{:S(2)}) collective-permute-start(bf16[8,32,384]{2,1,0:T(8,128)(2,1)S(1)} %collective-permute-done.6.others_3_), channel_id=1, source_target_pairs={{0,8},{8,16},{16,24},{24,32},{32,40},{40,48},{48,56},{56,0},{1,9},... | collective-permute-start | bytes 589832 | tf_op jit(solution)/shard_map/ppermute | solution.py:22
  83.5 21.8 %collective-permute-start.9 = (bf16[8,32,384]{2,1,0:T(8,128)(2,1)}, bf16[8,32,384]{2,1,0:T(8,128)(2,1)}, u32[]{:S(2)}, u32[]{:S(2)}) collective-permute-start(bf16[8,32,384]{2,1,0:T(8,128)(2,1)} %collective-permute-done.7.others_4_), channel_id=1, source_target_pairs={{0,56},{8,0},{16,8},{24,16},{32,24},{40,32},{48,40},{56,48},{1,57}... | collective-permute-start | bytes 589832 | tf_op jit(solution)/shard_map/ppermute | solution.py:22
  89.1 16.2 %collective-permute-start.10 = (bf16[8,32,384]{2,1,0:T(8,128)(2,1)}, bf16[8,32,384]{2,1,0:T(8,128)(2,1)}, u32[]{:S(2)}, u32[]{:S(2)}) collective-permute-start(bf16[8,32,384]{2,1,0:T(8,128)(2,1)} %collective-permute-done.8.others_5_), channel_id=1, source_target_pairs={{0,8},{8,16},{16,24},{24,32},{32,40},{40,48},{48,56},{56,0},{1,9},... | collective-permute-start | bytes 589832 | tf_op jit(solution)/shard_map/ppermute | solution.py:22
  98.7 46.8 %all-to-all-start.2 = ((bf16[64,32,384]{2,1,0:T(8,128)(2,1)}), bf16[64,32,384]{2,1,0:T(8,128)(2,1)}, u32[]{:S(2)}, u32[]{:S(2)}) async-start(bf16[64,32,384]{2,1,0:T(8,128)(2,1)} %bitcast.13), calls=%async_computation.2 | async-start | bytes 3145728 | tf_op jit(solution)/shard_map/all_to_all | solution.py:240
  105.3 0.9 copy-start.1
  114.5 11.5 %collective-permute-start.11 = (bf16[2,96,2048]{2,1,0:T(8,128)(2,1)S(1)}, bf16[2,96,2048]{2,1,0:T(8,128)(2,1)S(1)}, u32[]{:S(2)}, u32[]{:S(2)}) collective-permute-start(bf16[2,96,2048]{2,1,0:T(8,128)(2,1)S(1)} %get-tuple-element.11), channel_id=1, source_target_pairs={{0,1},{1,0},{2,3},{3,2},{4,5},{5,4},{6,7},{7,6},{8,9},{9,8},{10,11... | collective-permute-start | bytes 2359304 | tf_op jit(solution)/shard_map/ppermute | solution.py:22
  126.2 21.0 %copy-start.9 = (f32[32,384]{1,0:T(8,128)S(1)}, f32[32,384]{1,0:T(8,128)}, u32[]{:S(2)}) copy-start(f32[32,384]{1,0:T(8,128)} %param.13) | copy-start | bytes 147460
  126.3 8.4 %collective-permute-start.12 = (bf16[2,24,2048]{2,1,0:T(8,128)(2,1)S(1)}, bf16[2,24,2048]{2,1,0:T(8,128)(2,1)S(1)}, u32[]{:S(2)}, u32[]{:S(2)}) collective-permute-start(bf16[2,24,2048]{2,1,0:T(8,128)(2,1)S(1)} %get-tuple-element.13), channel_id=1, source_target_pairs={{0,6},{2,0},{4,2},{6,4},{1,7},{3,1},{5,3},{7,5},{8,14},{10,8},{12,... | collective-permute-start | bytes 589832 | tf_op jit(solution)/shard_map/ppermute | solution.py:22
  130.2 9.3 %collective-permute-start.14 = (bf16[2,24,2048]{2,1,0:T(8,128)(2,1)S(1)}, bf16[2,24,2048]{2,1,0:T(8,128)(2,1)S(1)}, u32[]{:S(2)}, u32[]{:S(2)}) collective-permute-start(bf16[2,24,2048]{2,1,0:T(8,128)(2,1)S(1)} %get-tuple-element.14), channel_id=1, source_target_pairs={{0,4},{2,6},{4,0},{6,2},{1,5},{3,7},{5,1},{7,3},{8,12},{10,14},{12... | collective-permute-start | bytes 589832 | tf_op jit(solution)/shard_map/ppermute | solution.py:22
  132.5 12.2 %collective-permute-start.13 = (bf16[2,24,2048]{2,1,0:T(8,128)(2,1)S(1)}, bf16[2,24,2048]{2,1,0:T(8,128)(2,1)S(1)}, u32[]{:S(2)}, u32[]{:S(2)}) collective-permute-start(bf16[2,24,2048]{2,1,0:T(8,128)(2,1)S(1)} %get-tuple-element.15), channel_id=1, source_target_pairs={{0,2},{2,4},{4,6},{6,0},{1,3},{3,5},{5,7},{7,1},{8,10},{10,12},{12... | collective-permute-start | bytes 589832 | tf_op jit(solution)/shard_map/ppermute | solution.py:22
Sparse Core Ops, SparseCore 0:
  28.0 55.1 all-gather.1

commit v7 on v6

--- a/solution.py
+++ b/solution.py
@@ -39,6 +39,23 @@
         compiler_params=pltpu.CompilerParams(vmem_limit_bytes=8 << 20),
         cost_estimate=pl.CostEstimate(flops=1 << 20, transcendentals=0, bytes_accessed=1 << 20),
     )(*arrays)
+
+
+def stack_kernel(*refs):
+    *ins, out_ref = refs
+    for at, ref in enumerate(ins):
+        rows = ref.shape[0]
+        out_ref[at * rows : (at + 1) * rows] = ref[...]
+
+
+def stacked(pieces):
+    rows, cols = pieces[0].shape
+    return pl.pallas_call(
+        stack_kernel,
+        out_shape=jax.ShapeDtypeStruct((len(pieces) * rows, cols), pieces[0].dtype),
+        compiler_params=pltpu.CompilerParams(vmem_limit_bytes=8 << 20),
+        cost_estimate=pl.CostEstimate(flops=1 << 20, transcendentals=0, bytes_accessed=1 << 20),
+    )(*pieces)
 
 
 def gather_down(down):
@@ -53,9 +70,9 @@
 
 def collect_tokens(own):
     pieces = [shift(own, "x", step) for step in STEPS]
-    line = jnp.concatenate(pieces, axis=0)
+    line = stacked(pieces)
     other = shift(line, "c", 1)
-    return jnp.concatenate([line, other], axis=0)
+    return line, other
 
 
 def give_rows(own, other, rows):
@@ -72,7 +89,13 @@
     )
 
 
-def early_kernel(token_ref, weight_ref, cot_ref, gate_ref, up_ref, grad_ref, sum_ref, hidden_ref):
+def rows_of(refs):
+    return jnp.concatenate([ref[...] for ref in refs], axis=0)
+
+
+def early_kernel(
+    own_ref, far_ref, weight_ref, cot_ref, cot_far_ref, gate_ref, up_ref, grad_ref, sum_ref, hidden_ref
+):
     step = pl.program_id(0)
     half = gate_ref.shape[1]
 
@@ -82,7 +105,8 @@
 
     @pl.when(step < BLOCKS)
     def _():
-        sum_ref[...] += jnp.dot(token_ref[...], weight_ref[...], preferred_element_type=F32)
+        block = rows_of((own_ref, far_ref))
+        sum_ref[...] += jnp.dot(block, weight_ref[...], preferred_element_type=F32)
 
     @pl.when(step == BLOCKS - 1)
     def _():
@@ -94,12 +118,13 @@
     @pl.when(step >= BLOCKS)
     def _():
         grad_ref[...] = lax.dot_general(
-            cot_ref[...], hidden_ref[...], (((0,), (0,)), ((), ())), preferred_element_type=F32
+            rows_of((cot_ref, cot_far_ref)), hidden_ref[...], (((0,), (0,)), ((), ())), preferred_element_type=F32
         ).astype(BF)
 
 
 def early_part(tokens, whole):
-    rows, width = tokens.shape[0], whole.shape[0]
+    mine, width = tokens[0].shape[0], whole.shape[0]
+    rows = 2 * mine
     both, block = whole.shape[1], width // BLOCKS
     half = both // 2
     first = lambda k: jnp.minimum(k, BLOCKS - 1)
@@ -108,9 +133,9 @@
         early_kernel,
         grid=(2 * BLOCKS,),
         in_specs=[
-            pl.BlockSpec((rows, block), lambda k: (0, BLOCKS + first(k))),
+            *[pl.BlockSpec((mine, block), lambda k: (0, BLOCKS + first(k)))] * 2,
             pl.BlockSpec((block, both), lambda k: (first(k), 0)),
-            pl.BlockSpec((rows, block), lambda k: (0, 2 * BLOCKS + then(k))),
+            *[pl.BlockSpec((mine, block), lambda k: (0, 2 * BLOCKS + then(k)))] * 2,
         ],
         out_specs=[
             pl.BlockSpec((rows, half), lambda k: (0, 0)),
@@ -129,11 +154,11 @@
         cost_estimate=pl.CostEstimate(
             flops=6 * rows * width * half, transcendentals=rows * half, bytes_accessed=8 << 20
         ),
-    )(tokens, whole, tokens)
+    )(*tokens, whole, *tokens)
 
 
 def rest_kernel(
-    row_ref, later_ref, cot_ref, weight_ref, gate_ref, up_ref, *others
+    row_ref, own_in_ref, far_in_ref, cot_ref, cot_far_ref, weight_ref, gate_ref, up_ref, *others
 ):
     chunk_refs, (own_ref, other_ref) = others[:8], others[8:10]
     down_ref, sum_ref, grad_ref, hidden_ref, to_gate_ref, to_up_ref = others[10:]
@@ -152,8 +177,10 @@
     @pl.when(step < BLOCKS)
     def _():
         down = down_ref[pl.ds(step * lines, lines)].reshape(-1, half)
-        sum_ref[...] += jnp.dot(later_ref[...], weight_ref[...], preferred_element_type=F32)
-        grad_ref[...] += jnp.dot(cot_ref[...], down, preferred_element_type=F32)
+        block = rows_of((own_in_ref, far_in_ref))
+        sum_ref[...] += jnp.dot(block, weight_ref[...], preferred_element_type=F32)
+        cot = rows_of((cot_ref, cot_far_ref))
+        grad_ref[...] += jnp.dot(cot, down, preferred_element_type=F32)
 
     @pl.when(step == BLOCKS - 1)
     def _():
@@ -175,7 +202,8 @@
 
 
 def rest_part(tokens, whole, gate_early, up_early, chunks):
-    rows, (width, both) = tokens.shape[0], whole.shape
+    mine, (width, both) = tokens[0].shape[0], whole.shape
+    rows = 2 * mine
     block, half = width // BLOCKS, both // 2
     lines = chunks[0].shape[0]
     first = lambda k: jnp.minimum(k, BLOCKS - 1)
@@ -187,8 +215,8 @@
         grid=(2 * BLOCKS,),
         in_specs=[
             pl.BlockSpec(memory_space=pltpu.SMEM),
-            pl.BlockSpec((rows, block), lambda k: (0, first(k))),
-            pl.BlockSpec((rows, block), lambda k: (0, 2 * BLOCKS + first(k))),
+            *[pl.BlockSpec((mine, block), lambda k: (0, first(k)))] * 2,
+            *[pl.BlockSpec((mine, block), lambda k: (0, 2 * BLOCKS + first(k)))] * 2,
             pl.BlockSpec((block, both), lambda k: (k % BLOCKS, 0)),
             whole_of(gate_early),
             whole_of(up_early),
@@ -215,8 +243,8 @@
         ),
     )(
         lax.axis_index("y").astype(jnp.int32)[None],
-        tokens,
-        tokens,
+        *tokens,
+        *tokens,
         whole,
         gate_early,
         up_early,
@@ -233,7 +261,7 @@
     whole = pltpu.with_memory_space_constraint(whole, pltpu.HBM)
     tokens = copies(1, later, early, cotangent)[0]
     tokens = collect_tokens(tokens)
-    tokens = pltpu.with_memory_space_constraint(tokens, pltpu.VMEM)
+    tokens = [pltpu.with_memory_space_constraint(t, pltpu.VMEM) for t in tokens]
     chunks = gather_down(down_w)
 
     gate_early, up_early, down_grad = early_part(tokens, whole)

time: 156 us -> 164 us (1.051)
  the two profiles are of different devices: /device:TPU:1 before, /device:TPU:8 now
where the time goes in v7:
time: 164 us; the launch traced here: 162 us
  starting transfers between devices  53.6 us (33%)
  blocking collectives  44.4 us (27%)
  waiting for transfers between devices  28.9 us (18%)
  Pallas kernels  14.8 us (9%)
  between operations  14.4 us (9%)
  local copies, waits for them, and re-layouts  3.88 us (2%)
  other arithmetic  2.57 us (2%)
    ppermute x15, starting transfers between devices, shift(): lax.ppermute(value, axis, [(i, (i + step) % count) for i in range(count)])  45.1 us
    ppermute x15, waiting for transfers between devices, shift(): lax.ppermute(value, axis, [(i, (i + step) % count) for i in range(count)])  24 us
    all_to_all x1, blocking collectives, gather_down(): line = lax.all_to_all(fan, 'z', 0, 0)  23.7 us
    all_to_all x1, blocking collectives, shards(): line = lax.all_to_all(fan, 'y', 0, 0)  20.7 us
    all_to_all x1, starting transfers between devices, shards(): received = lax.all_to_all(down_grad.reshape(-1, *gate_w.shape), FS, 0, 0)  8.44 us
    pallas_call x1, Pallas kernels, rest_part(): pl.pallas_call(rest_kernel, grid=(2 * BLOCKS,), in_specs=[pl.BlockSpec(me...  8.32 us
    pallas_call x1, Pallas kernels, early_part(): pl.pallas_call(early_kernel, grid=(2 * BLOCKS,), in_specs=[*[pl.BlockSpec...  6.33 us
    all_to_all x1, waiting for transfers between devices, shards(): received = lax.all_to_all(down_grad.reshape(-1, *gate_w.shape), FS, 0, 0)  4.85 us
  transfers between devices with their start and end apart: 17, of which 11 were waited for; matrix products, arithmetic and copies ran while one was open for 1% of the time, Pallas kernels for 9%

profile of v7, /device:TPU:8, one launch (start us, length us, event | category | flops | bytes accessed | tf_op | source)
XLA Modules:
  0.0 162.5 jit_solution(3268346433997167964)
XLA Ops:
  7.3 0.8 copy-done.5
  8.8 20.7 %all_to_all.15 = bf16[8,32,768]{2,1,0:T(8,128)(2,1)} all-to-all(bf16[8,32,768]{2,1,0:T(8,128)(2,1)S(1)} %shard_map.96), channel_id=1, replica_groups=mesh['z'=8,'y'=8,'x'=4,'c'=2] {'y'}, dimensions={0} | all-to-all | bytes 786432 | tf_op jit(solution)/shard_map/all_to_all | solution.py:258
  29.6 4.9 %collective-permute-start.2 = (bf16[24,6144]{1,0:T(8,128)(2,1)S(1)}, bf16[24,6144]{1,0:T(8,128)(2,1)S(1)}, u32[]{:S(2)}, u32[]{:S(2)}) collective-permute-start(bf16[24,6144]{1,0:T(8,128)(2,1)S(1)} %bitcast.8), channel_id=1, source_target_pairs={{0,4},{2,6},{4,0},{6,2},{1,5},{3,7},{5,1},{7,3},{8,12},{10,14},{12... | collective-permute-start | bytes 884744 | tf_op jit(solution)/shard_map/ppermute | solution.py:22
  34.5 3.0 %collective-permute-start.1 = (bf16[24,6144]{1,0:T(8,128)(2,1)S(1)}, bf16[24,6144]{1,0:T(8,128)(2,1)S(1)}, u32[]{:S(2)}, u32[]{:S(2)}) collective-permute-start(bf16[24,6144]{1,0:T(8,128)(2,1)S(1)} %bitcast.9), channel_id=1, source_target_pairs={{0,6},{2,0},{4,2},{6,4},{1,7},{3,1},{5,3},{7,5},{8,14},{10,8},{12,... | collective-permute-start | bytes 884744 | tf_op jit(solution)/shard_map/ppermute | solution.py:22
  37.6 2.8 %collective-permute-start = (bf16[24,6144]{1,0:T(8,128)(2,1)S(1)}, bf16[24,6144]{1,0:T(8,128)(2,1)S(1)}, u32[]{:S(2)}, u32[]{:S(2)}) collective-permute-start(bf16[24,6144]{1,0:T(8,128)(2,1)S(1)} %bitcast.10), channel_id=1, source_target_pairs={{0,2},{2,4},{4,6},{6,0},{1,3},{3,5},{5,7},{7,1},{8,10},{10,12},{12... | collective-permute-start | bytes 884744 | tf_op jit(solution)/shard_map/ppermute | solution.py:22
  40.6 6.2 %collective-permute-done.1.refs_2_ = bf16[24,6144]{1,0:T(8,128)(2,1)S(1)} collective-permute-done((bf16[24,6144]{1,0:T(8,128)(2,1)S(1)}, bf16[24,6144]{1,0:T(8,128)(2,1)S(1)}, u32[]{:S(2)}, u32[]{:S(2)}) %collective-permute-start.1) | collective-permute-done | bytes 294944 | tf_op jit(solution)/shard_map/ppermute | solution.py:22
  47.6 1.9 %collective-permute-start.3 = (bf16[96,6144]{1,0:T(8,128)(2,1)S(1)}, bf16[96,6144]{1,0:T(8,128)(2,1)S(1)}, u32[]{:S(2)}, u32[]{:S(2)}) collective-permute-start(bf16[96,6144]{1,0:T(8,128)(2,1)S(1)} %shard_map.95.own_ref.cot_ref.own_in_ref), channel_id=1, source_target_pairs={{0,1},{1,0},{2,3},{3,2},{4,5},{5,4},{6,7},{7,6},{8,9},{9,8},{10,11... | collective-permute-start | bytes 3538952 | tf_op jit(solution)/shard_map/ppermute | solution.py:22
  49.6 23.7 %all_to_all.16.others_0_ = bf16[8,32,384]{2,1,0:T(8,128)(2,1)S(1)} all-to-all(bf16[8,32,384]{2,1,0:T(8,128)(2,1)S(1)} %shard_map.98), channel_id=1, replica_groups=mesh['z'=8,'y'=8,'x'=4,'c'=2] {'z'}, dimensions={0} | all-to-all | bytes 393216 | tf_op jit(solution)/shard_map/all_to_all | solution.py:63
  73.3 1.9 %collective-permute-start.4 = (bf16[8,32,384]{2,1,0:T(8,128)(2,1)S(1)}, bf16[8,32,384]{2,1,0:T(8,128)(2,1)S(1)}, u32[]{:S(2)}, u32[]{:S(2)}) collective-permute-start(bf16[8,32,384]{2,1,0:T(8,128)(2,1)S(1)} %all_to_all.16.others_0_), channel_id=1, source_target_pairs={{0,8},{8,16},{16,24},{24,32},{32,40},{40,48},{48,56},{56,0},{1,9},... | collective-permute-start | bytes 589832 | tf_op jit(solution)/shard_map/ppermute | solution.py:22
  75.2 3.9 %collective-permute-start.5 = (bf16[8,32,384]{2,1,0:T(8,128)(2,1)S(1)}, bf16[8,32,384]{2,1,0:T(8,128)(2,1)S(1)}, u32[]{:S(2)}, u32[]{:S(2)}) collective-permute-start(bf16[8,32,384]{2,1,0:T(8,128)(2,1)S(1)} %all_to_all.16.others_0_), channel_id=1, source_target_pairs={{0,56},{8,0},{16,8},{24,16},{32,24},{40,32},{48,40},{56,48},{1,57}... | collective-permute-start | bytes 589832 | tf_op jit(solution)/shard_map/ppermute | solution.py:22
  79.1 2.6 %collective-permute-done.4.others_1_ = bf16[8,32,384]{2,1,0:T(8,128)(2,1)S(1)} collective-permute-done((bf16[8,32,384]{2,1,0:T(8,128)(2,1)S(1)}, bf16[8,32,384]{2,1,0:T(8,128)(2,1)S(1)}, u32[]{:S(2)}, u32[]{:S(2)}) %collective-permute-start.4) | collective-permute-done | bytes 196640 | tf_op jit(solution)/shard_map/ppermute | solution.py:22
  81.8 2.2 %collective-permute-start.6 = (bf16[8,32,384]{2,1,0:T(8,128)(2,1)S(1)}, bf16[8,32,384]{2,1,0:T(8,128)(2,1)S(1)}, u32[]{:S(2)}, u32[]{:S(2)}) collective-permute-start(bf16[8,32,384]{2,1,0:T(8,128)(2,1)S(1)} %collective-permute-done.4.others_1_), channel_id=1, source_target_pairs={{0,8},{8,16},{16,24},{24,32},{32,40},{40,48},{48,56},{56,0},{1,9},... | collective-permute-start | bytes 589832 | tf_op jit(solution)/shard_map/ppermute | solution.py:22
  84.0 4.3 %collective-permute-start.7 = (bf16[8,32,384]{2,1,0:T(8,128)(2,1)S(1)}, bf16[8,32,384]{2,1,0:T(8,128)(2,1)}, u32[]{:S(2)}, u32[]{:S(2)}) collective-permute-start(bf16[8,32,384]{2,1,0:T(8,128)(2,1)S(1)} %collective-permute-done.5.others_2_), channel_id=1, source_target_pairs={{0,56},{8,0},{16,8},{24,16},{32,24},{40,32},{48,40},{56,48},{1,57}... | collective-permute-start | bytes 589832 | tf_op jit(solution)/shard_map/ppermute | solution.py:22
  88.3 2.1 %collective-permute-done.6.others_3_ = bf16[8,32,384]{2,1,0:T(8,128)(2,1)S(1)} collective-permute-done((bf16[8,32,384]{2,1,0:T(8,128)(2,1)S(1)}, bf16[8,32,384]{2,1,0:T(8,128)(2,1)S(1)}, u32[]{:S(2)}, u32[]{:S(2)}) %collective-permute-start.6) | collective-permute-done | bytes 196640 | tf_op jit(solution)/shard_map/ppermute | solution.py:22
  90.3 1.9 %collective-permute-start.8 = (bf16[8,32,384]{2,1,0:T(8,128)(2,1)S(1)}, bf16[8,32,384]{2,1,0:T(8,128)(2,1)}, u32[]{:S(2)}, u32[]{:S(2)}) collective-permute-start(bf16[8,32,384]{2,1,0:T(8,128)(2,1)S(1)} %collective-permute-done.6.others_3_), channel_id=1, source_target_pairs={{0,8},{8,16},{16,24},{24,32},{32,40},{40,48},{48,56},{56,0},{1,9},... | collective-permute-start | bytes 589832 | tf_op jit(solution)/shard_map/ppermute | solution.py:22
  92.9 4.8 %collective-permute-start.9 = (bf16[8,32,384]{2,1,0:T(8,128)(2,1)}, bf16[8,32,384]{2,1,0:T(8,128)(2,1)}, u32[]{:S(2)}, u32[]{:S(2)}) collective-permute-start(bf16[8,32,384]{2,1,0:T(8,128)(2,1)} %collective-permute-done.7.others_4_), channel_id=1, source_target_pairs={{0,56},{8,0},{16,8},{24,16},{32,24},{40,32},{48,40},{56,48},{1,57}... | collective-permute-start | bytes 589832 | tf_op jit(solution)/shard_map/ppermute | solution.py:22
  97.8 1.1 collective-permute-done.8.others_5_
  98.9 1.9 %collective-permute-start.10 = (bf16[8,32,384]{2,1,0:T(8,128)(2,1)}, bf16[8,32,384]{2,1,0:T(8,128)(2,1)}, u32[]{:S(2)}, u32[]{:S(2)}) collective-permute-start(bf16[8,32,384]{2,1,0:T(8,128)(2,1)} %collective-permute-done.8.others_5_), channel_id=1, source_target_pairs={{0,8},{8,16},{16,24},{24,32},{32,40},{40,48},{48,56},{56,0},{1,9},... | collective-permute-start | bytes 589832 | tf_op jit(solution)/shard_map/ppermute | solution.py:22
  100.9 6.3 %shard_map.97 = (f32[192,384]{1,0:T(8,128)S(1)}, f32[192,384]{1,0:T(8,128)S(1)}, bf16[2048,384]{1,0:T(8,128)(2,1)}) custom-call(bf16[96,6144]{1,0:T(8,128)(2,1)S(1)} %shard_map.95.own_ref.cot_ref.own_in_ref, bf16[96,6144]{1,0:T(8,128)(2,1)S(1)} %collective-permute-done.3.far_ref.cot_far_ref.far_in_ref, ...), custom_call_target="tpu_custom_call" | custom-call | flops 905969664 | bytes 8388608 | tf_op jit(solution)/shard_map/pallas_call | solution.py:132
  107.2 8.4 %all-to-all-start.2 = ((bf16[64,32,384]{2,1,0:T(8,128)(2,1)}), bf16[64,32,384]{2,1,0:T(8,128)(2,1)}, u32[]{:S(2)}, u32[]{:S(2)}) async-start(bf16[64,32,384]{2,1,0:T(8,128)(2,1)} %bitcast.12), calls=%async_computation.2 | async-start | bytes 3145728 | tf_op jit(solution)/shard_map/all_to_all | solution.py:268
  115.7 0.9 copy-done.1
  116.6 8.3 %shard_map.99 = (f32[2,96,2048]{2,1,0:T(8,128)S(1)}, bf16[2,96,2048]{2,1,0:T(8,128)(2,1)S(1)}) custom-call(s32[1]{0:T(128)} %bitcast.row_ref, bf16[96,6144]{1,0:T(8,128)(2,1)S(1)} %shard_map.95.own_ref.cot_ref.own_in_ref, bf16[96,6144]{1,0:T(8,128)(2,1)S(1)} %collective-permute-done.3.far_ref.cot_far_ref.far_in_ref, ...), custom_call_target="tpu_custom_call" | custom-call | flops 1811939328 | bytes 16777216 | tf_op jit(solution)/shard_map/pallas_call | solution.py:213
  124.9 1.9 %collective-permute-start.11 = (bf16[2,96,2048]{2,1,0:T(8,128)(2,1)S(1)}, bf16[2,96,2048]{2,1,0:T(8,128)(2,1)S(1)}, u32[]{:S(2)}, u32[]{:S(2)}) collective-permute-start(bf16[2,96,2048]{2,1,0:T(8,128)(2,1)S(1)} %get-tuple-element.11), channel_id=1, source_target_pairs={{0,1},{1,0},{2,3},{3,2},{4,5},{5,4},{6,7},{7,6},{8,9},{9,8},{10,11... | collective-permute-start | bytes 2359304 | tf_op jit(solution)/shard_map/ppermute | solution.py:22
  126.9 2.3 %collective-permute-done.11 = bf16[2,96,2048]{2,1,0:T(8,128)(2,1)S(1)} collective-permute-done((bf16[2,96,2048]{2,1,0:T(8,128)(2,1)S(1)}, bf16[2,96,2048]{2,1,0:T(8,128)(2,1)S(1)}, u32[]{:S(2)}, u32[]{:S(2)}) %collective-permute-start.11) | collective-permute-done | bytes 786464 | tf_op jit(solution)/shard_map/ppermute | solution.py:22
  129.4 4.0 %collective-permute-start.12 = (bf16[2,24,2048]{2,1,0:T(8,128)(2,1)S(1)}, bf16[2,24,2048]{2,1,0:T(8,128)(2,1)S(1)}, u32[]{:S(2)}, u32[]{:S(2)}) collective-permute-start(bf16[2,24,2048]{2,1,0:T(8,128)(2,1)S(1)} %get-tuple-element.13), channel_id=1, source_target_pairs={{0,6},{2,0},{4,2},{6,4},{1,7},{3,1},{5,3},{7,5},{8,14},{10,8},{12,... | collective-permute-start | bytes 589832 | tf_op jit(solution)/shard_map/ppermute | solution.py:22
  133.4 2.7 %collective-permute-start.14 = (bf16[2,24,2048]{2,1,0:T(8,128)(2,1)S(1)}, bf16[2,24,2048]{2,1,0:T(8,128)(2,1)S(1)}, u32[]{:S(2)}, u32[]{:S(2)}) collective-permute-start(bf16[2,24,2048]{2,1,0:T(8,128)(2,1)S(1)} %get-tuple-element.14), channel_id=1, source_target_pairs={{0,4},{2,6},{4,0},{6,2},{1,5},{3,7},{5,1},{7,3},{8,12},{10,14},{12... | collective-permute-start | bytes 589832 | tf_op jit(solution)/shard_map/ppermute | solution.py:22
  136.1 2.8 %collective-permute-start.13 = (bf16[2,24,2048]{2,1,0:T(8,128)(2,1)S(1)}, bf16[2,24,2048]{2,1,0:T(8,128)(2,1)S(1)}, u32[]{:S(2)}, u32[]{:S(2)}) collective-permute-start(bf16[2,24,2048]{2,1,0:T(8,128)(2,1)S(1)} %get-tuple-element.15), channel_id=1, source_target_pairs={{0,2},{2,4},{4,6},{6,0},{1,3},{3,5},{5,7},{7,1},{8,10},{10,12},{12... | collective-permute-start | bytes 589832 | tf_op jit(solution)/shard_map/ppermute | solution.py:22
  138.9 3.2 %collective-permute-done.12 = bf16[2,24,2048]{2,1,0:T(8,128)(2,1)S(1)} collective-permute-done((bf16[2,24,2048]{2,1,0:T(8,128)(2,1)S(1)}, bf16[2,24,2048]{2,1,0:T(8,128)(2,1)S(1)}, u32[]{:S(2)}, u32[]{:S(2)}) %collective-permute-start.12) | collective-permute-done | bytes 196640 | tf_op jit(solution)/shard_map/ppermute | solution.py:22
  142.1 2.5 %collective-permute-done.14 = bf16[2,24,2048]{2,1,0:T(8,128)(2,1)S(1)} collective-permute-done((bf16[2,24,2048]{2,1,0:T(8,128)(2,1)S(1)}, bf16[2,24,2048]{2,1,0:T(8,128)(2,1)S(1)}, u32[]{:S(2)}, u32[]{:S(2)}) %collective-permute-start.14) | collective-permute-done | bytes 196640 | tf_op jit(solution)/shard_map/ppermute | solution.py:22
  144.6 3.1 %collective-permute-done.13 = bf16[2,24,2048]{2,1,0:T(8,128)(2,1)S(1)} collective-permute-done((bf16[2,24,2048]{2,1,0:T(8,128)(2,1)S(1)}, bf16[2,24,2048]{2,1,0:T(8,128)(2,1)S(1)}, u32[]{:S(2)}, u32[]{:S(2)}) %collective-permute-start.13) | collective-permute-done | bytes 196640 | tf_op jit(solution)/shard_map/ppermute | solution.py:22
  148.5 4.9 %all-to-all-done.2 = bf16[64,32,384]{2,1,0:T(8,128)(2,1)} async-done(((bf16[64,32,384]{2,1,0:T(8,128)(2,1)}), bf16[64,32,384]{2,1,0:T(8,128)(2,1)}, u32[]{:S(2)}, u32[]{:S(2)}) %all-to-all-start.2) | async-done | bytes 1572896 | tf_op jit(solution)/shard_map/all_to_all | solution.py:268
  153.3 1.7 %convert_reduce_fusion = f32[32,384]{1,0:T(8,128)S(1)} fusion(bf16[64,32,384]{2,1,0:T(8,128)(2,1)} %all-to-all-done.2), kind=kLoop, calls=%fused_computation | loop fusion | flops 1560576 | bytes 1622016 | tf_op jit(solution)/shard_map/reduce_sum | solution.py:273
  (35 shorter events, 4.2 us)
Async XLA Ops:
  7.2 22.4 %copy-start.4 = (bf16[24,2048]{1,0:T(8,128)(2,1)S(1)}, bf16[24,2048]{1,0:T(8,128)(2,1)}, u32[]{:S(2)}) copy-start(bf16[24,2048]{1,0:T(8,128)(2,1)} %refs_2_.1) | copy-start | bytes 294916
  7.2 22.4 %copy-start.3 = (bf16[24,2048]{1,0:T(8,128)(2,1)S(1)}, bf16[24,2048]{1,0:T(8,128)(2,1)}, u32[]{:S(2)}) copy-start(bf16[24,2048]{1,0:T(8,128)(2,1)} %refs_1_.2) | copy-start | bytes 294916
  7.2 22.4 %copy-start.2 = (bf16[24,2048]{1,0:T(8,128)(2,1)S(1)}, bf16[24,2048]{1,0:T(8,128)(2,1)}, u32[]{:S(2)}) copy-start(bf16[24,2048]{1,0:T(8,128)(2,1)} %refs_0_.3) | copy-start | bytes 294916
  7.2 93.7 %all-gather.2.cloned.1.call-start = ((), (), s32[]{:S(2)}) async-start(), calls=%async_computation.3 | async-start | bytes 3538944 | tf_op jit(solution)/shard_map/all_gather | solution.py:260
  7.2 0.8 copy-start.5
  8.0 0.7 copy-start.6
  29.6 20.0 %copy-start.7 = (bf16[32,384]{1,0:T(8,128)(2,1)S(1)}, bf16[32,384]{1,0:T(8,128)(2,1)}, u32[]{:S(2)}) copy-start(bf16[32,384]{1,0:T(8,128)(2,1)} %refs_0_.5) | copy-start | bytes 73732
  29.6 11.0 %collective-permute-start.2 = (bf16[24,6144]{1,0:T(8,128)(2,1)S(1)}, bf16[24,6144]{1,0:T(8,128)(2,1)S(1)}, u32[]{:S(2)}, u32[]{:S(2)}) collective-permute-start(bf16[24,6144]{1,0:T(8,128)(2,1)S(1)} %bitcast.8), channel_id=1, source_target_pairs={{0,4},{2,6},{4,0},{6,2},{1,5},{3,7},{5,1},{7,3},{8,12},{10,14},{12... | collective-permute-start | bytes 884744 | tf_op jit(solution)/shard_map/ppermute | solution.py:22
  34.5 12.3 %collective-permute-start.1 = (bf16[24,6144]{1,0:T(8,128)(2,1)S(1)}, bf16[24,6144]{1,0:T(8,128)(2,1)S(1)}, u32[]{:S(2)}, u32[]{:S(2)}) collective-permute-start(bf16[24,6144]{1,0:T(8,128)(2,1)S(1)} %bitcast.9), channel_id=1, source_target_pairs={{0,6},{2,0},{4,2},{6,4},{1,7},{3,1},{5,3},{7,5},{8,14},{10,8},{12,... | collective-permute-start | bytes 884744 | tf_op jit(solution)/shard_map/ppermute | solution.py:22
  37.6 10.0 %collective-permute-start = (bf16[24,6144]{1,0:T(8,128)(2,1)S(1)}, bf16[24,6144]{1,0:T(8,128)(2,1)S(1)}, u32[]{:S(2)}, u32[]{:S(2)}) collective-permute-start(bf16[24,6144]{1,0:T(8,128)(2,1)S(1)} %bitcast.10), channel_id=1, source_target_pairs={{0,2},{2,4},{4,6},{6,0},{1,3},{3,5},{5,7},{7,1},{8,10},{10,12},{12... | collective-permute-start | bytes 884744 | tf_op jit(solution)/shard_map/ppermute | solution.py:22
  47.6 53.2 %collective-permute-start.3 = (bf16[96,6144]{1,0:T(8,128)(2,1)S(1)}, bf16[96,6144]{1,0:T(8,128)(2,1)S(1)}, u32[]{:S(2)}, u32[]{:S(2)}) collective-permute-start(bf16[96,6144]{1,0:T(8,128)(2,1)S(1)} %shard_map.95.own_ref.cot_ref.own_in_ref), channel_id=1, source_target_pairs={{0,1},{1,0},{2,3},{3,2},{4,5},{5,4},{6,7},{7,6},{8,9},{9,8},{10,11... | collective-permute-start | bytes 3538952 | tf_op jit(solution)/shard_map/ppermute | solution.py:22
  73.3 8.5 %collective-permute-start.4 = (bf16[8,32,384]{2,1,0:T(8,128)(2,1)S(1)}, bf16[8,32,384]{2,1,0:T(8,128)(2,1)S(1)}, u32[]{:S(2)}, u32[]{:S(2)}) collective-permute-start(bf16[8,32,384]{2,1,0:T(8,128)(2,1)S(1)} %all_to_all.16.others_0_), channel_id=1, source_target_pairs={{0,8},{8,16},{16,24},{24,32},{32,40},{40,48},{48,56},{56,0},{1,9},... | collective-permute-start | bytes 589832 | tf_op jit(solution)/shard_map/ppermute | solution.py:22
  75.2 8.7 %collective-permute-start.5 = (bf16[8,32,384]{2,1,0:T(8,128)(2,1)S(1)}, bf16[8,32,384]{2,1,0:T(8,128)(2,1)S(1)}, u32[]{:S(2)}, u32[]{:S(2)}) collective-permute-start(bf16[8,32,384]{2,1,0:T(8,128)(2,1)S(1)} %all_to_all.16.others_0_), channel_id=1, source_target_pairs={{0,56},{8,0},{16,8},{24,16},{32,24},{40,32},{48,40},{56,48},{1,57}... | collective-permute-start | bytes 589832 | tf_op jit(solution)/shard_map/ppermute | solution.py:22
  81.8 8.5 %collective-permute-start.6 = (bf16[8,32,384]{2,1,0:T(8,128)(2,1)S(1)}, bf16[8,32,384]{2,1,0:T(8,128)(2,1)S(1)}, u32[]{:S(2)}, u32[]{:S(2)}) collective-permute-start(bf16[8,32,384]{2,1,0:T(8,128)(2,1)S(1)} %collective-permute-done.4.others_1_), channel_id=1, source_target_pairs={{0,8},{8,16},{16,24},{24,32},{32,40},{40,48},{48,56},{56,0},{1,9},... | collective-permute-start | bytes 589832 | tf_op jit(solution)/shard_map/ppermute | solution.py:22
  84.0 8.9 %collective-permute-start.7 = (bf16[8,32,384]{2,1,0:T(8,128)(2,1)S(1)}, bf16[8,32,384]{2,1,0:T(8,128)(2,1)}, u32[]{:S(2)}, u32[]{:S(2)}) collective-permute-start(bf16[8,32,384]{2,1,0:T(8,128)(2,1)S(1)} %collective-permute-done.5.others_2_), channel_id=1, source_target_pairs={{0,56},{8,0},{16,8},{24,16},{32,24},{40,32},{48,40},{56,48},{1,57}... | collective-permute-start | bytes 589832 | tf_op jit(solution)/shard_map/ppermute | solution.py:22
  90.3 8.6 %collective-permute-start.8 = (bf16[8,32,384]{2,1,0:T(8,128)(2,1)S(1)}, bf16[8,32,384]{2,1,0:T(8,128)(2,1)}, u32[]{:S(2)}, u32[]{:S(2)}) collective-permute-start(bf16[8,32,384]{2,1,0:T(8,128)(2,1)S(1)} %collective-permute-done.6.others_3_), channel_id=1, source_target_pairs={{0,8},{8,16},{16,24},{24,32},{32,40},{40,48},{48,56},{56,0},{1,9},... | collective-permute-start | bytes 589832 | tf_op jit(solution)/shard_map/ppermute | solution.py:22
  92.2 0.7 copy-start
  92.9 22.7 %collective-permute-start.9 = (bf16[8,32,384]{2,1,0:T(8,128)(2,1)}, bf16[8,32,384]{2,1,0:T(8,128)(2,1)}, u32[]{:S(2)}, u32[]{:S(2)}) collective-permute-start(bf16[8,32,384]{2,1,0:T(8,128)(2,1)} %collective-permute-done.7.others_4_), channel_id=1, source_target_pairs={{0,56},{8,0},{16,8},{24,16},{32,24},{40,32},{48,40},{56,48},{1,57}... | collective-permute-start | bytes 589832 | tf_op jit(solution)/shard_map/ppermute | solution.py:22
  98.9 16.8 %collective-permute-start.10 = (bf16[8,32,384]{2,1,0:T(8,128)(2,1)}, bf16[8,32,384]{2,1,0:T(8,128)(2,1)}, u32[]{:S(2)}, u32[]{:S(2)}) collective-permute-start(bf16[8,32,384]{2,1,0:T(8,128)(2,1)} %collective-permute-done.8.others_5_), channel_id=1, source_target_pairs={{0,8},{8,16},{16,24},{24,32},{32,40},{40,48},{48,56},{56,0},{1,9},... | collective-permute-start | bytes 589832 | tf_op jit(solution)/shard_map/ppermute | solution.py:22
  107.2 46.1 %all-to-all-start.2 = ((bf16[64,32,384]{2,1,0:T(8,128)(2,1)}), bf16[64,32,384]{2,1,0:T(8,128)(2,1)}, u32[]{:S(2)}, u32[]{:S(2)}) async-start(bf16[64,32,384]{2,1,0:T(8,128)(2,1)} %bitcast.12), calls=%async_computation.2 | async-start | bytes 3145728 | tf_op jit(solution)/shard_map/all_to_all | solution.py:268
  115.7 0.9 copy-start.1
  124.9 4.2 %collective-permute-start.11 = (bf16[2,96,2048]{2,1,0:T(8,128)(2,1)S(1)}, bf16[2,96,2048]{2,1,0:T(8,128)(2,1)S(1)}, u32[]{:S(2)}, u32[]{:S(2)}) collective-permute-start(bf16[2,96,2048]{2,1,0:T(8,128)(2,1)S(1)} %get-tuple-element.11), channel_id=1, source_target_pairs={{0,1},{1,0},{2,3},{3,2},{4,5},{5,4},{6,7},{7,6},{8,9},{9,8},{10,11... | collective-permute-start | bytes 2359304 | tf_op jit(solution)/shard_map/ppermute | solution.py:22
  129.4 25.6 %copy-start.8 = (f32[32,384]{1,0:T(8,128)S(1)}, f32[32,384]{1,0:T(8,128)}, u32[]{:S(2)}) copy-start(f32[32,384]{1,0:T(8,128)} %param.13) | copy-start | bytes 147460
  129.4 12.7 %collective-permute-start.12 = (bf16[2,24,2048]{2,1,0:T(8,128)(2,1)S(1)}, bf16[2,24,2048]{2,1,0:T(8,128)(2,1)S(1)}, u32[]{:S(2)}, u32[]{:S(2)}) collective-permute-start(bf16[2,24,2048]{2,1,0:T(8,128)(2,1)S(1)} %get-tuple-element.13), channel_id=1, source_target_pairs={{0,6},{2,0},{4,2},{6,4},{1,7},{3,1},{5,3},{7,5},{8,14},{10,8},{12,... | collective-permute-start | bytes 589832 | tf_op jit(solution)/shard_map/ppermute | solution.py:22
  133.4 11.2 %collective-permute-start.14 = (bf16[2,24,2048]{2,1,0:T(8,128)(2,1)S(1)}, bf16[2,24,2048]{2,1,0:T(8,128)(2,1)S(1)}, u32[]{:S(2)}, u32[]{:S(2)}) collective-permute-start(bf16[2,24,2048]{2,1,0:T(8,128)(2,1)S(1)} %get-tuple-element.14), channel_id=1, source_target_pairs={{0,4},{2,6},{4,0},{6,2},{1,5},{3,7},{5,1},{7,3},{8,12},{10,14},{12... | collective-permute-start | bytes 589832 | tf_op jit(solution)/shard_map/ppermute | solution.py:22
  136.1 11.5 %collective-permute-start.13 = (bf16[2,24,2048]{2,1,0:T(8,128)(2,1)S(1)}, bf16[2,24,2048]{2,1,0:T(8,128)(2,1)S(1)}, u32[]{:S(2)}, u32[]{:S(2)}) collective-permute-start(bf16[2,24,2048]{2,1,0:T(8,128)(2,1)S(1)} %get-tuple-element.15), channel_id=1, source_target_pairs={{0,2},{2,4},{4,6},{6,0},{1,3},{3,5},{5,7},{7,1},{8,10},{10,12},{12... | collective-permute-start | bytes 589832 | tf_op jit(solution)/shard_map/ppermute | solution.py:22
Sparse Core Ops, SparseCore 0:
  29.6 52.8 all-gather.1

commit v8 on v7

--- a/solution.py
+++ b/solution.py
@@ -38,7 +38,7 @@
         out_shape=jax.ShapeDtypeStruct(shape, arrays[0].dtype),
         compiler_params=pltpu.CompilerParams(vmem_limit_bytes=8 << 20),
         cost_estimate=pl.CostEstimate(flops=1 << 20, transcendentals=0, bytes_accessed=1 << 20),
-    )(*arrays)
+    )(*[pltpu.with_memory_space_constraint(a, pltpu.HBM) for a in arrays])
 
 
 def stack_kernel(*refs):
@@ -94,67 +94,69 @@
 
 
 def early_kernel(
-    own_ref, far_ref, weight_ref, cot_ref, cot_far_ref, gate_ref, up_ref, grad_ref, sum_ref, hidden_ref
+    own_ref, far_ref, whole_ref, gate_ref, up_ref, out_ref,
+    weight_ref, token_ref, cot_ref, grad_ref, in_sems, out_sems,
 ):
-    step = pl.program_id(0)
-    half = gate_ref.shape[1]
-
-    @pl.when(step == 0)
-    def _():
-        sum_ref[...] = jnp.zeros_like(sum_ref)
-
-    @pl.when(step < BLOCKS)
-    def _():
-        block = rows_of((own_ref, far_ref))
-        sum_ref[...] += jnp.dot(block, weight_ref[...], preferred_element_type=F32)
-
-    @pl.when(step == BLOCKS - 1)
-    def _():
-        gate, up = sum_ref[:, :half], sum_ref[:, half:]
-        gate_ref[...] = gate
-        up_ref[...] = up
-        hidden_ref[...] = (gate / (1.0 + jnp.exp(-gate)) * up).astype(BF)
-
-    @pl.when(step >= BLOCKS)
-    def _():
-        grad_ref[...] = lax.dot_general(
-            rows_of((cot_ref, cot_far_ref)), hidden_ref[...], (((0,), (0,)), ((), ())), preferred_element_type=F32
+    blocks, block, _ = weight_ref.shape
+    mine, half, width = own_ref.shape[0], gate_ref.shape[1], token_ref.shape[1]
+    rows = lambda k: pl.ds(k * block, block)
+    loads = [
+        pltpu.make_async_copy(whole_ref.at[rows(k)], weight_ref.at[k], in_sems.at[k])
+        for k in range(blocks)
+    ]
+    stores = [
+        pltpu.make_async_copy(grad_ref.at[k], out_ref.at[rows(k)], out_sems.at[k])
+        for k in range(blocks)
+    ]
+    for load in loads:
+        load.start()
+    for at, ref in ((0, own_ref), (mine, far_ref)):
+        token_ref[at : at + mine] = ref[:, width : 2 * width]
+        cot_ref[at : at + mine] = ref[:, 2 * width :]
+    both = 0.0
+    for k in range(blocks):
+        loads[k].wait()
+        both += jnp.dot(token_ref[:, rows(k)], weight_ref[k], preferred_element_type=F32)
+    gate, up = both[:, :half], both[:, half:]
+    gate_ref[...] = gate
+    up_ref[...] = up
+    hidden = (gate / (1.0 + jnp.exp(-gate)) * up).astype(BF)
+    for k in range(blocks):
+        grad_ref[k] = lax.dot_general(
+            cot_ref[:, rows(k)], hidden, (((0,), (0,)), ((), ())), preferred_element_type=F32
         ).astype(BF)
+        stores[k].start()
+    for store in stores:
+        store.wait()
 
 
 def early_part(tokens, whole):
-    mine, width = tokens[0].shape[0], whole.shape[0]
-    rows = 2 * mine
+    rows, width = 2 * tokens[0].shape[0], whole.shape[0]
     both, block = whole.shape[1], width // BLOCKS
     half = both // 2
-    first = lambda k: jnp.minimum(k, BLOCKS - 1)
-    then = lambda k: jnp.maximum(k - BLOCKS, 0)
+    vmem, hbm = pl.BlockSpec(memory_space=pltpu.VMEM), pl.BlockSpec(memory_space=pltpu.HBM)
     return pl.pallas_call(
         early_kernel,
-        grid=(2 * BLOCKS,),
-        in_specs=[
-            *[pl.BlockSpec((mine, block), lambda k: (0, BLOCKS + first(k)))] * 2,
-            pl.BlockSpec((block, both), lambda k: (first(k), 0)),
-            *[pl.BlockSpec((mine, block), lambda k: (0, 2 * BLOCKS + then(k)))] * 2,
-        ],
-        out_specs=[
-            pl.BlockSpec((rows, half), lambda k: (0, 0)),
-            pl.BlockSpec((rows, half), lambda k: (0, 0)),
-            pl.BlockSpec((block, half), lambda k: (then(k), 0)),
-        ],
+        in_specs=[vmem, vmem, hbm],
+        out_specs=[vmem, vmem, hbm],
         out_shape=[
             jax.ShapeDtypeStruct((rows, half), F32),
             jax.ShapeDtypeStruct((rows, half), F32),
             pltpu.HBM((width, half), BF),
         ],
-        scratch_shapes=[pltpu.VMEM((rows, both), F32), pltpu.VMEM((rows, half), BF)],
-        compiler_params=pltpu.CompilerParams(
-            dimension_semantics=("arbitrary",), vmem_limit_bytes=12 << 20
-        ),
+        scratch_shapes=[
+            pltpu.VMEM((BLOCKS, block, both), BF),
+            pltpu.VMEM((rows, width), BF),
+            pltpu.VMEM((rows, width), BF),
+            pltpu.VMEM((BLOCKS, block, half), BF),
+            pltpu.SemaphoreType.DMA((BLOCKS,)),
+            pltpu.SemaphoreType.DMA((BLOCKS,)),
+        ],
+        compiler_params=pltpu.CompilerParams(vmem_limit_bytes=16 << 20),
         cost_estimate=pl.CostEstimate(
             flops=6 * rows * width * half, transcendentals=rows * half, bytes_accessed=8 << 20
         ),
-    )(*tokens, whole, *tokens)
+    )(*tokens, whole)
 
 
 def rest_kernel(

time: 164 us -> 162 us (0.988)
    pallas_call x3, Pallas kernels: 0.08 us -> 2.56 us  [copies(): pl.pallas_call(copy_kernel, out_shape=jax.ShapeDtypeStruct(shape, arrays[...]
    pallas_call x1, Pallas kernels: 6.33 us -> 4.16 us  [early_part(): pl.pallas_call(early_kernel, in_specs=[vmem, vmem, hbm], out_specs=[vmem,...]
where the time goes in v8:
time: 162 us; the launch traced here: 161 us
  starting transfers between devices  53.5 us (33%)
  blocking collectives  44.4 us (27%)
  waiting for transfers between devices  29.1 us (18%)
  Pallas kernels  15.1 us (9%)
  between operations  14.3 us (9%)
  other arithmetic  2.57 us (2%)
  local copies, waits for them, and re-layouts  2.33 us (1%)
    ppermute x15, starting transfers between devices, shift(): lax.ppermute(value, axis, [(i, (i + step) % count) for i in range(count)])  45 us
    ppermute x15, waiting for transfers between devices, shift(): lax.ppermute(value, axis, [(i, (i + step) % count) for i in range(count)])  24 us
    all_to_all x1, blocking collectives, gather_down(): line = lax.all_to_all(fan, 'z', 0, 0)  23.7 us
    all_to_all x1, blocking collectives, shards(): line = lax.all_to_all(fan, 'y', 0, 0)  20.7 us
    all_to_all x1, starting transfers between devices, shards(): received = lax.all_to_all(down_grad.reshape(-1, *gate_w.shape), FS, 0, 0)  8.47 us
    pallas_call x1, Pallas kernels, rest_part(): pl.pallas_call(rest_kernel, grid=(2 * BLOCKS,), in_specs=[pl.BlockSpec(me...  8.32 us
    all_to_all x1, waiting for transfers between devices, shards(): received = lax.all_to_all(down_grad.reshape(-1, *gate_w.shape), FS, 0, 0)  4.99 us
    pallas_call x1, Pallas kernels, early_part(): pl.pallas_call(early_kernel, in_specs=[vmem, vmem, hbm], out_specs=[vmem,...  4.16 us
  transfers between devices with their start and end apart: 17, of which 11 were waited for; matrix products, arithmetic and copies ran while one was open for 1% of the time, Pallas kernels for 9%

profile of v8, /device:TPU:8, one launch (start us, length us, event | category | flops | bytes accessed | tf_op | source)
XLA Modules:
  0.0 161.2 jit_solution(13931833895815158893)
XLA Ops:
  8.0 20.7 %all_to_all.15 = bf16[8,32,768]{2,1,0:T(8,128)(2,1)} all-to-all(bf16[8,32,768]{2,1,0:T(8,128)(2,1)S(1)} %shard_map.96), channel_id=1, replica_groups=mesh['z'=8,'y'=8,'x'=4,'c'=2] {'y'}, dimensions={0} | all-to-all | bytes 786432 | tf_op jit(solution)/shard_map/all_to_all | solution.py:260
  28.7 1.0 shard_map.94
  29.7 4.9 %collective-permute-start.2 = (bf16[24,6144]{1,0:T(8,128)(2,1)S(1)}, bf16[24,6144]{1,0:T(8,128)(2,1)S(1)}, u32[]{:S(2)}, u32[]{:S(2)}) collective-permute-start(bf16[24,6144]{1,0:T(8,128)(2,1)S(1)} %bitcast.8), channel_id=1, source_target_pairs={{0,4},{2,6},{4,0},{6,2},{1,5},{3,7},{5,1},{7,3},{8,12},{10,14},{12... | collective-permute-start | bytes 884744 | tf_op jit(solution)/shard_map/ppermute | solution.py:22
  34.7 3.0 %collective-permute-start.1 = (bf16[24,6144]{1,0:T(8,128)(2,1)S(1)}, bf16[24,6144]{1,0:T(8,128)(2,1)S(1)}, u32[]{:S(2)}, u32[]{:S(2)}) collective-permute-start(bf16[24,6144]{1,0:T(8,128)(2,1)S(1)} %bitcast.9), channel_id=1, source_target_pairs={{0,6},{2,0},{4,2},{6,4},{1,7},{3,1},{5,3},{7,5},{8,14},{10,8},{12,... | collective-permute-start | bytes 884744 | tf_op jit(solution)/shard_map/ppermute | solution.py:22
  37.7 2.8 %collective-permute-start = (bf16[24,6144]{1,0:T(8,128)(2,1)S(1)}, bf16[24,6144]{1,0:T(8,128)(2,1)S(1)}, u32[]{:S(2)}, u32[]{:S(2)}) collective-permute-start(bf16[24,6144]{1,0:T(8,128)(2,1)S(1)} %bitcast.10), channel_id=1, source_target_pairs={{0,2},{2,4},{4,6},{6,0},{1,3},{3,5},{5,7},{7,1},{8,10},{10,12},{12... | collective-permute-start | bytes 884744 | tf_op jit(solution)/shard_map/ppermute | solution.py:22
  40.7 6.2 %collective-permute-done.1.refs_2_ = bf16[24,6144]{1,0:T(8,128)(2,1)S(1)} collective-permute-done((bf16[24,6144]{1,0:T(8,128)(2,1)S(1)}, bf16[24,6144]{1,0:T(8,128)(2,1)S(1)}, u32[]{:S(2)}, u32[]{:S(2)}) %collective-permute-start.1) | collective-permute-done | bytes 294944 | tf_op jit(solution)/shard_map/ppermute | solution.py:22
  47.8 1.9 %collective-permute-start.3 = (bf16[96,6144]{1,0:T(8,128)(2,1)S(1)}, bf16[96,6144]{1,0:T(8,128)(2,1)S(1)}, u32[]{:S(2)}, u32[]{:S(2)}) collective-permute-start(bf16[96,6144]{1,0:T(8,128)(2,1)S(1)} %shard_map.95.own_ref.own_in_ref.cot_ref), channel_id=1, source_target_pairs={{0,1},{1,0},{2,3},{3,2},{4,5},{5,4},{6,7},{7,6},{8,9},{9,8},{10,11... | collective-permute-start | bytes 3538952 | tf_op jit(solution)/shard_map/ppermute | solution.py:22
  50.5 23.7 %all_to_all.16.others_0_ = bf16[8,32,384]{2,1,0:T(8,128)(2,1)S(1)} all-to-all(bf16[8,32,384]{2,1,0:T(8,128)(2,1)S(1)} %shard_map.98), channel_id=1, replica_groups=mesh['z'=8,'y'=8,'x'=4,'c'=2] {'z'}, dimensions={0} | all-to-all | bytes 393216 | tf_op jit(solution)/shard_map/all_to_all | solution.py:63
  74.1 2.0 %collective-permute-start.4 = (bf16[8,32,384]{2,1,0:T(8,128)(2,1)S(1)}, bf16[8,32,384]{2,1,0:T(8,128)(2,1)S(1)}, u32[]{:S(2)}, u32[]{:S(2)}) collective-permute-start(bf16[8,32,384]{2,1,0:T(8,128)(2,1)S(1)} %all_to_all.16.others_0_), channel_id=1, source_target_pairs={{0,8},{8,16},{16,24},{24,32},{32,40},{40,48},{48,56},{56,0},{1,9},... | collective-permute-start | bytes 589832 | tf_op jit(solution)/shard_map/ppermute | solution.py:22
  76.1 3.9 %collective-permute-start.5 = (bf16[8,32,384]{2,1,0:T(8,128)(2,1)S(1)}, bf16[8,32,384]{2,1,0:T(8,128)(2,1)S(1)}, u32[]{:S(2)}, u32[]{:S(2)}) collective-permute-start(bf16[8,32,384]{2,1,0:T(8,128)(2,1)S(1)} %all_to_all.16.others_0_), channel_id=1, source_target_pairs={{0,56},{8,0},{16,8},{24,16},{32,24},{40,32},{48,40},{56,48},{1,57}... | collective-permute-start | bytes 589832 | tf_op jit(solution)/shard_map/ppermute | solution.py:22
  80.0 2.7 %collective-permute-done.4.others_1_ = bf16[8,32,384]{2,1,0:T(8,128)(2,1)S(1)} collective-permute-done((bf16[8,32,384]{2,1,0:T(8,128)(2,1)S(1)}, bf16[8,32,384]{2,1,0:T(8,128)(2,1)S(1)}, u32[]{:S(2)}, u32[]{:S(2)}) %collective-permute-start.4) | collective-permute-done | bytes 196640 | tf_op jit(solution)/shard_map/ppermute | solution.py:22
  82.6 2.2 %collective-permute-start.6 = (bf16[8,32,384]{2,1,0:T(8,128)(2,1)S(1)}, bf16[8,32,384]{2,1,0:T(8,128)(2,1)S(1)}, u32[]{:S(2)}, u32[]{:S(2)}) collective-permute-start(bf16[8,32,384]{2,1,0:T(8,128)(2,1)S(1)} %collective-permute-done.4.others_1_), channel_id=1, source_target_pairs={{0,8},{8,16},{16,24},{24,32},{32,40},{40,48},{48,56},{56,0},{1,9},... | collective-permute-start | bytes 589832 | tf_op jit(solution)/shard_map/ppermute | solution.py:22
  84.8 4.3 %collective-permute-start.7 = (bf16[8,32,384]{2,1,0:T(8,128)(2,1)S(1)}, bf16[8,32,384]{2,1,0:T(8,128)(2,1)}, u32[]{:S(2)}, u32[]{:S(2)}) collective-permute-start(bf16[8,32,384]{2,1,0:T(8,128)(2,1)S(1)} %collective-permute-done.5.others_2_), channel_id=1, source_target_pairs={{0,56},{8,0},{16,8},{24,16},{32,24},{40,32},{48,40},{56,48},{1,57}... | collective-permute-start | bytes 589832 | tf_op jit(solution)/shard_map/ppermute | solution.py:22
  89.1 2.1 %collective-permute-done.6.others_3_ = bf16[8,32,384]{2,1,0:T(8,128)(2,1)S(1)} collective-permute-done((bf16[8,32,384]{2,1,0:T(8,128)(2,1)S(1)}, bf16[8,32,384]{2,1,0:T(8,128)(2,1)S(1)}, u32[]{:S(2)}, u32[]{:S(2)}) %collective-permute-start.6) | collective-permute-done | bytes 196640 | tf_op jit(solution)/shard_map/ppermute | solution.py:22
  91.2 1.9 %collective-permute-start.8 = (bf16[8,32,384]{2,1,0:T(8,128)(2,1)S(1)}, bf16[8,32,384]{2,1,0:T(8,128)(2,1)}, u32[]{:S(2)}, u32[]{:S(2)}) collective-permute-start(bf16[8,32,384]{2,1,0:T(8,128)(2,1)S(1)} %collective-permute-done.6.others_3_), channel_id=1, source_target_pairs={{0,8},{8,16},{16,24},{24,32},{32,40},{40,48},{48,56},{56,0},{1,9},... | collective-permute-start | bytes 589832 | tf_op jit(solution)/shard_map/ppermute | solution.py:22
  93.8 4.8 %collective-permute-start.9 = (bf16[8,32,384]{2,1,0:T(8,128)(2,1)}, bf16[8,32,384]{2,1,0:T(8,128)(2,1)}, u32[]{:S(2)}, u32[]{:S(2)}) collective-permute-start(bf16[8,32,384]{2,1,0:T(8,128)(2,1)} %collective-permute-done.7.others_4_), channel_id=1, source_target_pairs={{0,56},{8,0},{16,8},{24,16},{32,24},{40,32},{48,40},{56,48},{1,57}... | collective-permute-start | bytes 589832 | tf_op jit(solution)/shard_map/ppermute | solution.py:22
  98.7 1.1 collective-permute-done.8.others_5_
  99.8 1.9 %collective-permute-start.10 = (bf16[8,32,384]{2,1,0:T(8,128)(2,1)}, bf16[8,32,384]{2,1,0:T(8,128)(2,1)}, u32[]{:S(2)}, u32[]{:S(2)}) collective-permute-start(bf16[8,32,384]{2,1,0:T(8,128)(2,1)} %collective-permute-done.8.others_5_), channel_id=1, source_target_pairs={{0,8},{8,16},{16,24},{24,32},{32,40},{40,48},{48,56},{56,0},{1,9},... | collective-permute-start | bytes 589832 | tf_op jit(solution)/shard_map/ppermute | solution.py:22
  101.8 4.2 %shard_map.97 = (f32[192,384]{1,0:T(8,128)S(1)}, f32[192,384]{1,0:T(8,128)S(1)}, bf16[2048,384]{1,0:T(8,128)(2,1)}) custom-call(bf16[96,6144]{1,0:T(8,128)(2,1)S(1)} %shard_map.95.own_ref.own_in_ref.cot_ref, bf16[96,6144]{1,0:T(8,128)(2,1)S(1)} %collective-permute-done.3.far_ref.far_in_ref.cot_far_ref, ...), custom_call_target="tpu_custom_call" | custom-call | flops 905969664 | bytes 8388608 | tf_op jit(solution)/shard_map/pallas_call | solution.py:138
  105.9 8.5 %all-to-all-start.2 = ((bf16[64,32,384]{2,1,0:T(8,128)(2,1)}), bf16[64,32,384]{2,1,0:T(8,128)(2,1)}, u32[]{:S(2)}, u32[]{:S(2)}) async-start(bf16[64,32,384]{2,1,0:T(8,128)(2,1)} %bitcast.12), calls=%async_computation.2 | async-start | bytes 3145728 | tf_op jit(solution)/shard_map/all_to_all | solution.py:270
  114.4 0.9 copy-done.1
  115.4 8.3 %shard_map.99 = (f32[2,96,2048]{2,1,0:T(8,128)S(1)}, bf16[2,96,2048]{2,1,0:T(8,128)(2,1)S(1)}) custom-call(s32[1]{0:T(128)} %bitcast.row_ref, bf16[96,6144]{1,0:T(8,128)(2,1)S(1)} %shard_map.95.own_ref.own_in_ref.cot_ref, bf16[96,6144]{1,0:T(8,128)(2,1)S(1)} %collective-permute-done.3.far_ref.far_in_ref.cot_far_ref, ...), custom_call_target="tpu_custom_call" | custom-call | flops 1811939328 | bytes 16777216 | tf_op jit(solution)/shard_map/pallas_call | solution.py:215
  123.7 1.9 %collective-permute-start.11 = (bf16[2,96,2048]{2,1,0:T(8,128)(2,1)S(1)}, bf16[2,96,2048]{2,1,0:T(8,128)(2,1)S(1)}, u32[]{:S(2)}, u32[]{:S(2)}) collective-permute-start(bf16[2,96,2048]{2,1,0:T(8,128)(2,1)S(1)} %get-tuple-element.11), channel_id=1, source_target_pairs={{0,1},{1,0},{2,3},{3,2},{4,5},{5,4},{6,7},{7,6},{8,9},{9,8},{10,11... | collective-permute-start | bytes 2359304 | tf_op jit(solution)/shard_map/ppermute | solution.py:22
  125.6 2.3 %collective-permute-done.11 = bf16[2,96,2048]{2,1,0:T(8,128)(2,1)S(1)} collective-permute-done((bf16[2,96,2048]{2,1,0:T(8,128)(2,1)S(1)}, bf16[2,96,2048]{2,1,0:T(8,128)(2,1)S(1)}, u32[]{:S(2)}, u32[]{:S(2)}) %collective-permute-start.11) | collective-permute-done | bytes 786464 | tf_op jit(solution)/shard_map/ppermute | solution.py:22
  128.1 3.9 %collective-permute-start.12 = (bf16[2,24,2048]{2,1,0:T(8,128)(2,1)S(1)}, bf16[2,24,2048]{2,1,0:T(8,128)(2,1)S(1)}, u32[]{:S(2)}, u32[]{:S(2)}) collective-permute-start(bf16[2,24,2048]{2,1,0:T(8,128)(2,1)S(1)} %get-tuple-element.13), channel_id=1, source_target_pairs={{0,6},{2,0},{4,2},{6,4},{1,7},{3,1},{5,3},{7,5},{8,14},{10,8},{12,... | collective-permute-start | bytes 589832 | tf_op jit(solution)/shard_map/ppermute | solution.py:22
  132.0 2.7 %collective-permute-start.14 = (bf16[2,24,2048]{2,1,0:T(8,128)(2,1)S(1)}, bf16[2,24,2048]{2,1,0:T(8,128)(2,1)S(1)}, u32[]{:S(2)}, u32[]{:S(2)}) collective-permute-start(bf16[2,24,2048]{2,1,0:T(8,128)(2,1)S(1)} %get-tuple-element.14), channel_id=1, source_target_pairs={{0,4},{2,6},{4,0},{6,2},{1,5},{3,7},{5,1},{7,3},{8,12},{10,14},{12... | collective-permute-start | bytes 589832 | tf_op jit(solution)/shard_map/ppermute | solution.py:22
  134.8 2.8 %collective-permute-start.13 = (bf16[2,24,2048]{2,1,0:T(8,128)(2,1)S(1)}, bf16[2,24,2048]{2,1,0:T(8,128)(2,1)S(1)}, u32[]{:S(2)}, u32[]{:S(2)}) collective-permute-start(bf16[2,24,2048]{2,1,0:T(8,128)(2,1)S(1)} %get-tuple-element.15), channel_id=1, source_target_pairs={{0,2},{2,4},{4,6},{6,0},{1,3},{3,5},{5,7},{7,1},{8,10},{10,12},{12... | collective-permute-start | bytes 589832 | tf_op jit(solution)/shard_map/ppermute | solution.py:22
  137.6 3.1 %collective-permute-done.12 = bf16[2,24,2048]{2,1,0:T(8,128)(2,1)S(1)} collective-permute-done((bf16[2,24,2048]{2,1,0:T(8,128)(2,1)S(1)}, bf16[2,24,2048]{2,1,0:T(8,128)(2,1)S(1)}, u32[]{:S(2)}, u32[]{:S(2)}) %collective-permute-start.12) | collective-permute-done | bytes 196640 | tf_op jit(solution)/shard_map/ppermute | solution.py:22
  140.7 2.5 %collective-permute-done.14 = bf16[2,24,2048]{2,1,0:T(8,128)(2,1)S(1)} collective-permute-done((bf16[2,24,2048]{2,1,0:T(8,128)(2,1)S(1)}, bf16[2,24,2048]{2,1,0:T(8,128)(2,1)S(1)}, u32[]{:S(2)}, u32[]{:S(2)}) %collective-permute-start.14) | collective-permute-done | bytes 196640 | tf_op jit(solution)/shard_map/ppermute | solution.py:22
  143.2 3.1 %collective-permute-done.13 = bf16[2,24,2048]{2,1,0:T(8,128)(2,1)S(1)} collective-permute-done((bf16[2,24,2048]{2,1,0:T(8,128)(2,1)S(1)}, bf16[2,24,2048]{2,1,0:T(8,128)(2,1)S(1)}, u32[]{:S(2)}, u32[]{:S(2)}) %collective-permute-start.13) | collective-permute-done | bytes 196640 | tf_op jit(solution)/shard_map/ppermute | solution.py:22
  147.1 5.0 %all-to-all-done.2 = bf16[64,32,384]{2,1,0:T(8,128)(2,1)} async-done(((bf16[64,32,384]{2,1,0:T(8,128)(2,1)}), bf16[64,32,384]{2,1,0:T(8,128)(2,1)}, u32[]{:S(2)}, u32[]{:S(2)}) %all-to-all-start.2) | async-done | bytes 1572896 | tf_op jit(solution)/shard_map/all_to_all | solution.py:270
  152.1 1.7 %convert_reduce_fusion = f32[32,384]{1,0:T(8,128)S(1)} fusion(bf16[64,32,384]{2,1,0:T(8,128)(2,1)} %all-to-all-done.2), kind=kLoop, calls=%fused_computation | loop fusion | flops 1560576 | bytes 1622016 | tf_op jit(solution)/shard_map/reduce_sum | solution.py:275
  (23 shorter events, 5.0 us)
Async XLA Ops:
  7.2 94.6 %all-gather.2.cloned.1.call-start = ((), (), s32[]{:S(2)}) async-start(), calls=%async_computation.3 | async-start | bytes 3538944 | tf_op jit(solution)/shard_map/all_gather | solution.py:262
  29.7 11.0 %collective-permute-start.2 = (bf16[24,6144]{1,0:T(8,128)(2,1)S(1)}, bf16[24,6144]{1,0:T(8,128)(2,1)S(1)}, u32[]{:S(2)}, u32[]{:S(2)}) collective-permute-start(bf16[24,6144]{1,0:T(8,128)(2,1)S(1)} %bitcast.8), channel_id=1, source_target_pairs={{0,4},{2,6},{4,0},{6,2},{1,5},{3,7},{5,1},{7,3},{8,12},{10,14},{12... | collective-permute-start | bytes 884744 | tf_op jit(solution)/shard_map/ppermute | solution.py:22
  34.7 12.3 %collective-permute-start.1 = (bf16[24,6144]{1,0:T(8,128)(2,1)S(1)}, bf16[24,6144]{1,0:T(8,128)(2,1)S(1)}, u32[]{:S(2)}, u32[]{:S(2)}) collective-permute-start(bf16[24,6144]{1,0:T(8,128)(2,1)S(1)} %bitcast.9), channel_id=1, source_target_pairs={{0,6},{2,0},{4,2},{6,4},{1,7},{3,1},{5,3},{7,5},{8,14},{10,8},{12,... | collective-permute-start | bytes 884744 | tf_op jit(solution)/shard_map/ppermute | solution.py:22
  37.7 10.0 %collective-permute-start = (bf16[24,6144]{1,0:T(8,128)(2,1)S(1)}, bf16[24,6144]{1,0:T(8,128)(2,1)S(1)}, u32[]{:S(2)}, u32[]{:S(2)}) collective-permute-start(bf16[24,6144]{1,0:T(8,128)(2,1)S(1)} %bitcast.10), channel_id=1, source_target_pairs={{0,2},{2,4},{4,6},{6,0},{1,3},{3,5},{5,7},{7,1},{8,10},{10,12},{12... | collective-permute-start | bytes 884744 | tf_op jit(solution)/shard_map/ppermute | solution.py:22
  47.8 54.0 %collective-permute-start.3 = (bf16[96,6144]{1,0:T(8,128)(2,1)S(1)}, bf16[96,6144]{1,0:T(8,128)(2,1)S(1)}, u32[]{:S(2)}, u32[]{:S(2)}) collective-permute-start(bf16[96,6144]{1,0:T(8,128)(2,1)S(1)} %shard_map.95.own_ref.own_in_ref.cot_ref), channel_id=1, source_target_pairs={{0,1},{1,0},{2,3},{3,2},{4,5},{5,4},{6,7},{7,6},{8,9},{9,8},{10,11... | collective-permute-start | bytes 3538952 | tf_op jit(solution)/shard_map/ppermute | solution.py:22
  74.1 8.5 %collective-permute-start.4 = (bf16[8,32,384]{2,1,0:T(8,128)(2,1)S(1)}, bf16[8,32,384]{2,1,0:T(8,128)(2,1)S(1)}, u32[]{:S(2)}, u32[]{:S(2)}) collective-permute-start(bf16[8,32,384]{2,1,0:T(8,128)(2,1)S(1)} %all_to_all.16.others_0_), channel_id=1, source_target_pairs={{0,8},{8,16},{16,24},{24,32},{32,40},{40,48},{48,56},{56,0},{1,9},... | collective-permute-start | bytes 589832 | tf_op jit(solution)/shard_map/ppermute | solution.py:22
  76.1 8.7 %collective-permute-start.5 = (bf16[8,32,384]{2,1,0:T(8,128)(2,1)S(1)}, bf16[8,32,384]{2,1,0:T(8,128)(2,1)S(1)}, u32[]{:S(2)}, u32[]{:S(2)}) collective-permute-start(bf16[8,32,384]{2,1,0:T(8,128)(2,1)S(1)} %all_to_all.16.others_0_), channel_id=1, source_target_pairs={{0,56},{8,0},{16,8},{24,16},{32,24},{40,32},{48,40},{56,48},{1,57}... | collective-permute-start | bytes 589832 | tf_op jit(solution)/shard_map/ppermute | solution.py:22
  82.6 8.6 %collective-permute-start.6 = (bf16[8,32,384]{2,1,0:T(8,128)(2,1)S(1)}, bf16[8,32,384]{2,1,0:T(8,128)(2,1)S(1)}, u32[]{:S(2)}, u32[]{:S(2)}) collective-permute-start(bf16[8,32,384]{2,1,0:T(8,128)(2,1)S(1)} %collective-permute-done.4.others_1_), channel_id=1, source_target_pairs={{0,8},{8,16},{16,24},{24,32},{32,40},{40,48},{48,56},{56,0},{1,9},... | collective-permute-start | bytes 589832 | tf_op jit(solution)/shard_map/ppermute | solution.py:22
  84.8 9.0 %collective-permute-start.7 = (bf16[8,32,384]{2,1,0:T(8,128)(2,1)S(1)}, bf16[8,32,384]{2,1,0:T(8,128)(2,1)}, u32[]{:S(2)}, u32[]{:S(2)}) collective-permute-start(bf16[8,32,384]{2,1,0:T(8,128)(2,1)S(1)} %collective-permute-done.5.others_2_), channel_id=1, source_target_pairs={{0,56},{8,0},{16,8},{24,16},{32,24},{40,32},{48,40},{56,48},{1,57}... | collective-permute-start | bytes 589832 | tf_op jit(solution)/shard_map/ppermute | solution.py:22
  91.2 8.6 %collective-permute-start.8 = (bf16[8,32,384]{2,1,0:T(8,128)(2,1)S(1)}, bf16[8,32,384]{2,1,0:T(8,128)(2,1)}, u32[]{:S(2)}, u32[]{:S(2)}) collective-permute-start(bf16[8,32,384]{2,1,0:T(8,128)(2,1)S(1)} %collective-permute-done.6.others_3_), channel_id=1, source_target_pairs={{0,8},{8,16},{16,24},{24,32},{32,40},{40,48},{48,56},{56,0},{1,9},... | collective-permute-start | bytes 589832 | tf_op jit(solution)/shard_map/ppermute | solution.py:22
  93.1 0.7 copy-start
  93.8 20.6 %collective-permute-start.9 = (bf16[8,32,384]{2,1,0:T(8,128)(2,1)}, bf16[8,32,384]{2,1,0:T(8,128)(2,1)}, u32[]{:S(2)}, u32[]{:S(2)}) collective-permute-start(bf16[8,32,384]{2,1,0:T(8,128)(2,1)} %collective-permute-done.7.others_4_), channel_id=1, source_target_pairs={{0,56},{8,0},{16,8},{24,16},{32,24},{40,32},{48,40},{56,48},{1,57}... | collective-permute-start | bytes 589832 | tf_op jit(solution)/shard_map/ppermute | solution.py:22
  99.8 14.6 %collective-permute-start.10 = (bf16[8,32,384]{2,1,0:T(8,128)(2,1)}, bf16[8,32,384]{2,1,0:T(8,128)(2,1)}, u32[]{:S(2)}, u32[]{:S(2)}) collective-permute-start(bf16[8,32,384]{2,1,0:T(8,128)(2,1)} %collective-permute-done.8.others_5_), channel_id=1, source_target_pairs={{0,8},{8,16},{16,24},{24,32},{32,40},{40,48},{48,56},{56,0},{1,9},... | collective-permute-start | bytes 589832 | tf_op jit(solution)/shard_map/ppermute | solution.py:22
  105.9 46.2 %all-to-all-start.2 = ((bf16[64,32,384]{2,1,0:T(8,128)(2,1)}), bf16[64,32,384]{2,1,0:T(8,128)(2,1)}, u32[]{:S(2)}, u32[]{:S(2)}) async-start(bf16[64,32,384]{2,1,0:T(8,128)(2,1)} %bitcast.12), calls=%async_computation.2 | async-start | bytes 3145728 | tf_op jit(solution)/shard_map/all_to_all | solution.py:270
  114.4 0.9 copy-start.1
  123.7 4.2 %collective-permute-start.11 = (bf16[2,96,2048]{2,1,0:T(8,128)(2,1)S(1)}, bf16[2,96,2048]{2,1,0:T(8,128)(2,1)S(1)}, u32[]{:S(2)}, u32[]{:S(2)}) collective-permute-start(bf16[2,96,2048]{2,1,0:T(8,128)(2,1)S(1)} %get-tuple-element.11), channel_id=1, source_target_pairs={{0,1},{1,0},{2,3},{3,2},{4,5},{5,4},{6,7},{7,6},{8,9},{9,8},{10,11... | collective-permute-start | bytes 2359304 | tf_op jit(solution)/shard_map/ppermute | solution.py:22
  128.1 25.7 %copy-start.2 = (f32[32,384]{1,0:T(8,128)S(1)}, f32[32,384]{1,0:T(8,128)}, u32[]{:S(2)}) copy-start(f32[32,384]{1,0:T(8,128)} %param.13) | copy-start | bytes 147460
  128.1 12.6 %collective-permute-start.12 = (bf16[2,24,2048]{2,1,0:T(8,128)(2,1)S(1)}, bf16[2,24,2048]{2,1,0:T(8,128)(2,1)S(1)}, u32[]{:S(2)}, u32[]{:S(2)}) collective-permute-start(bf16[2,24,2048]{2,1,0:T(8,128)(2,1)S(1)} %get-tuple-element.13), channel_id=1, source_target_pairs={{0,6},{2,0},{4,2},{6,4},{1,7},{3,1},{5,3},{7,5},{8,14},{10,8},{12,... | collective-permute-start | bytes 589832 | tf_op jit(solution)/shard_map/ppermute | solution.py:22
  132.0 11.2 %collective-permute-start.14 = (bf16[2,24,2048]{2,1,0:T(8,128)(2,1)S(1)}, bf16[2,24,2048]{2,1,0:T(8,128)(2,1)S(1)}, u32[]{:S(2)}, u32[]{:S(2)}) collective-permute-start(bf16[2,24,2048]{2,1,0:T(8,128)(2,1)S(1)} %get-tuple-element.14), channel_id=1, source_target_pairs={{0,4},{2,6},{4,0},{6,2},{1,5},{3,7},{5,1},{7,3},{8,12},{10,14},{12... | collective-permute-start | bytes 589832 | tf_op jit(solution)/shard_map/ppermute | solution.py:22
  134.8 11.5 %collective-permute-start.13 = (bf16[2,24,2048]{2,1,0:T(8,128)(2,1)S(1)}, bf16[2,24,2048]{2,1,0:T(8,128)(2,1)S(1)}, u32[]{:S(2)}, u32[]{:S(2)}) collective-permute-start(bf16[2,24,2048]{2,1,0:T(8,128)(2,1)S(1)} %get-tuple-element.15), channel_id=1, source_target_pairs={{0,2},{2,4},{4,6},{6,0},{1,3},{3,5},{5,7},{7,1},{8,10},{10,12},{12... | collective-permute-start | bytes 589832 | tf_op jit(solution)/shard_map/ppermute | solution.py:22
Sparse Core Ops, SparseCore 0:
  28.8 52.8 all-gather.1

commit v9 on v8

--- a/solution.py
+++ b/solution.py
@@ -1,3 +1,5 @@
+import functools
+
 import jax
 import jax.numpy as jnp
 from jax import lax
@@ -41,6 +43,35 @@
     )(*[pltpu.with_memory_space_constraint(a, pltpu.HBM) for a in arrays])
 
 
+def fan_kernel(*refs):
+    *ins, out_ref, sems = refs
+    moves, at = [], 0
+    for ref in ins:
+        cols = ref.shape[1]
+        for k in range(out_ref.shape[0]):
+            place = out_ref.at[k, :, pl.ds(at, cols)]
+            moves.append(pltpu.make_async_copy(ref, place, sems.at[len(moves)]))
+        at += cols
+    for move in moves:
+        move.start()
+    for move in moves:
+        move.wait()
+
+
+def fanned(count, *arrays):
+    shape = (count, arrays[0].shape[0], sum(a.shape[1] for a in arrays))
+    hbm = pl.BlockSpec(memory_space=pltpu.HBM)
+    return pl.pallas_call(
+        fan_kernel,
+        in_specs=[hbm] * len(arrays),
+        out_specs=hbm,
+        out_shape=pltpu.HBM(shape, arrays[0].dtype),
+        scratch_shapes=[pltpu.SemaphoreType.DMA((count * len(arrays),))],
+        compiler_params=pltpu.CompilerParams(vmem_limit_bytes=1 << 20),
+        cost_estimate=pl.CostEstimate(flops=1 << 20, transcendentals=0, bytes_accessed=1 << 20),
+    )(*[pltpu.with_memory_space_constraint(a, pltpu.HBM) for a in arrays])
+
+
 def stack_kernel(*refs):
     *ins, out_ref = refs
     for at, ref in enumerate(ins):
@@ -59,7 +90,7 @@
 
 
 def gather_down(down):
-    fan = copies(lax.axis_size("z"), down)
+    fan = fanned(lax.axis_size("z"), down)
     line = lax.all_to_all(fan, "z", 0, 0)
     chunks, ahead, behind = [line], line, line
     for _ in range(1, 4):
@@ -254,9 +285,39 @@
     )
 
 
+def final_kernel(parts_ref, sum_ref, out_ref, load_ref, sems, *, factor):
+    count, size = load_ref.shape[:2]
+    loads = [
+        pltpu.make_async_copy(parts_ref.at[pl.ds(k * size, size)], load_ref.at[k], sems.at[k])
+        for k in range(count)
+    ]
+    for load in loads:
+        load.start()
+    total = 0.0
+    for k, load in enumerate(loads):
+        load.wait()
+        total += jnp.sum(load_ref[k].astype(F32), axis=0)
+    out_ref[...] = sum_ref[...] + total * factor
+
+
+def final_part(parts, running, factor):
+    vmem, count = pl.BlockSpec(memory_space=pltpu.VMEM), 8
+    return pl.pallas_call(
+        functools.partial(final_kernel, factor=factor),
+        in_specs=[pl.BlockSpec(memory_space=pltpu.HBM), vmem],
+        out_specs=vmem,
+        out_shape=jax.ShapeDtypeStruct(running.shape, F32),
+        scratch_shapes=[
+            pltpu.VMEM((count, parts.shape[0] // count, *parts.shape[1:]), BF),
+            pltpu.SemaphoreType.DMA((count,)),
+        ],
+        compiler_params=pltpu.CompilerParams(vmem_limit_bytes=6 << 20),
+    )(parts, running)
+
+
 def shards(later, early, cotangent, gate_w, up_w, down_w, down_grad_sum):
     rows, _ = later.shape
-    fan = copies(lax.axis_size("y"), gate_w, up_w)
+    fan = fanned(lax.axis_size("y"), gate_w, up_w)
     line = lax.all_to_all(fan, "y", 0, 0)
     line = line.reshape(-1, line.shape[-1])
     whole = lax.all_gather(line, "z", axis=0, tiled=True)
@@ -272,9 +333,8 @@
     own, other = rest_part(tokens, whole, gate_early, up_early, chunks)
     later_output, earlier_grad_input = give_rows(own, other, rows)
 
-    summed = jnp.sum(received.astype(F32), axis=0)
     factor = (rows * lax.axis_size(AXES)) ** (-0.5)
-    return later_output, earlier_grad_input, down_grad_sum + summed * factor
+    return later_output, earlier_grad_input, final_part(received, down_grad_sum, factor)
 
 
 def solution(mesh):

time: 162 us -> 184 us (1.14)
  the two profiles are of different devices: /device:TPU:8 before, /device:TPU:2 now
where the time goes in v9:
time: 184 us; the launch traced here: 183 us
  starting transfers between devices  55.8 us (30%)
  blocking collectives  42.6 us (23%)
  Pallas kernels  40.4 us (22%)
  waiting for transfers between devices  26.8 us (15%)
  between operations  14.3 us (8%)
  local copies, waits for them, and re-layouts  2.32 us (1%)
    ppermute x15, starting transfers between devices, shift(): lax.ppermute(value, axis, [(i, (i + step) % count) for i in range(count)])  47.2 us
    pallas_call x2, Pallas kernels, fanned(): pl.pallas_call(fan_kernel, in_specs=[hbm] * len(arrays), out_specs=hbm, o...  24.6 us
    all_to_all x1, blocking collectives, shards(): line = lax.all_to_all(fan, 'y', 0, 0)  21.9 us
    ppermute x15, waiting for transfers between devices, shift(): lax.ppermute(value, axis, [(i, (i + step) % count) for i in range(count)])  21 us
    all_to_all x1, blocking collectives, gather_down(): line = lax.all_to_all(fan, 'z', 0, 0)  20.7 us
    all_to_all x1, starting transfers between devices, shards(): received = lax.all_to_all(down_grad.reshape(-1, *gate_w.shape), FS, 0, 0)  8.54 us
    pallas_call x1, Pallas kernels, rest_part(): pl.pallas_call(rest_kernel, grid=(2 * BLOCKS,), in_specs=[pl.BlockSpec(me...  8.32 us
    all_to_all x1, waiting for transfers between devices, shards(): received = lax.all_to_all(down_grad.reshape(-1, *gate_w.shape), FS, 0, 0)  5.82 us
  transfers between devices with their start and end apart: 17, of which 9 were waited for; matrix products, arithmetic and copies ran while one was open for 1% of the time, Pallas kernels for 14%

profile of v9, /device:TPU:2, one launch (start us, length us, event | category | flops | bytes accessed | tf_op | source)
XLA Modules:
  0.0 182.5 jit_solution(2943452869376279143)
XLA Ops:
  7.2 13.2 %shard_map.96 = bf16[8,32,768]{2,1,0:T(8,128)(2,1)} custom-call(bf16[32,384]{1,0:T(8,128)(2,1)} %refs_0_.4, bf16[32,384]{1,0:T(8,128)(2,1)} %refs_1_.3), custom_call_target="tpu_custom_call" | custom-call | flops 1048576 | bytes 1048576 | tf_op jit(solution)/shard_map/pallas_call | solution.py:64
  20.4 21.9 %all_to_all.15 = bf16[8,32,768]{2,1,0:T(8,128)(2,1)} all-to-all(bf16[8,32,768]{2,1,0:T(8,128)(2,1)} %shard_map.96), channel_id=1, replica_groups=mesh['z'=8,'y'=8,'x'=4,'c'=2] {'y'}, dimensions={0} | all-to-all | bytes 786432 | tf_op jit(solution)/shard_map/all_to_all | solution.py:321
  43.3 4.0 %collective-permute-start.2 = (bf16[24,6144]{1,0:T(8,128)(2,1)S(1)}, bf16[24,6144]{1,0:T(8,128)(2,1)S(1)}, u32[]{:S(2)}, u32[]{:S(2)}) collective-permute-start(bf16[24,6144]{1,0:T(8,128)(2,1)S(1)} %bitcast.8), channel_id=1, source_target_pairs={{0,4},{2,6},{4,0},{6,2},{1,5},{3,7},{5,1},{7,3},{8,12},{10,14},{12... | collective-permute-start | bytes 884744 | tf_op jit(solution)/shard_map/ppermute | solution.py:24
  47.4 3.3 %collective-permute-start.1 = (bf16[24,6144]{1,0:T(8,128)(2,1)S(1)}, bf16[24,6144]{1,0:T(8,128)(2,1)S(1)}, u32[]{:S(2)}, u32[]{:S(2)}) collective-permute-start(bf16[24,6144]{1,0:T(8,128)(2,1)S(1)} %bitcast.9), channel_id=1, source_target_pairs={{0,6},{2,0},{4,2},{6,4},{1,7},{3,1},{5,3},{7,5},{8,14},{10,8},{12,... | collective-permute-start | bytes 884744 | tf_op jit(solution)/shard_map/ppermute | solution.py:24
  50.7 2.5 %collective-permute-start = (bf16[24,6144]{1,0:T(8,128)(2,1)S(1)}, bf16[24,6144]{1,0:T(8,128)(2,1)S(1)}, u32[]{:S(2)}, u32[]{:S(2)}) collective-permute-start(bf16[24,6144]{1,0:T(8,128)(2,1)S(1)} %bitcast.10), channel_id=1, source_target_pairs={{0,2},{2,4},{4,6},{6,0},{1,3},{3,5},{5,7},{7,1},{8,10},{10,12},{12... | collective-permute-start | bytes 884744 | tf_op jit(solution)/shard_map/ppermute | solution.py:24
  53.2 3.4 %collective-permute-done.2.refs_3_ = bf16[24,6144]{1,0:T(8,128)(2,1)S(1)} collective-permute-done((bf16[24,6144]{1,0:T(8,128)(2,1)S(1)}, bf16[24,6144]{1,0:T(8,128)(2,1)S(1)}, u32[]{:S(2)}, u32[]{:S(2)}) %collective-permute-start.2) | collective-permute-done | bytes 294944 | tf_op jit(solution)/shard_map/ppermute | solution.py:24
  56.6 3.8 %collective-permute-done.1.refs_2_ = bf16[24,6144]{1,0:T(8,128)(2,1)S(1)} collective-permute-done((bf16[24,6144]{1,0:T(8,128)(2,1)S(1)}, bf16[24,6144]{1,0:T(8,128)(2,1)S(1)}, u32[]{:S(2)}, u32[]{:S(2)}) %collective-permute-start.1) | collective-permute-done | bytes 294944 | tf_op jit(solution)/shard_map/ppermute | solution.py:24
  60.5 1.9 %collective-permute-start.3 = (bf16[96,6144]{1,0:T(8,128)(2,1)S(1)}, bf16[96,6144]{1,0:T(8,128)(2,1)S(1)}, u32[]{:S(2)}, u32[]{:S(2)}) collective-permute-start(bf16[96,6144]{1,0:T(8,128)(2,1)S(1)} %shard_map.95.own_ref.own_in_ref.cot_ref), channel_id=1, source_target_pairs={{0,1},{1,0},{2,3},{3,2},{4,5},{5,4},{6,7},{7,6},{8,9},{9,8},{10,11... | collective-permute-start | bytes 3538952 | tf_op jit(solution)/shard_map/ppermute | solution.py:24
  62.4 11.5 %shard_map.98 = bf16[8,32,384]{2,1,0:T(8,128)(2,1)} custom-call(bf16[32,384]{1,0:T(8,128)(2,1)} %refs_0_.5), custom_call_target="tpu_custom_call" | custom-call | flops 1048576 | bytes 1048576 | tf_op jit(solution)/shard_map/pallas_call | solution.py:64
  73.9 20.7 %all_to_all.16.others_0_ = bf16[8,32,384]{2,1,0:T(8,128)(2,1)S(1)} all-to-all(bf16[8,32,384]{2,1,0:T(8,128)(2,1)} %shard_map.98), channel_id=1, replica_groups=mesh['z'=8,'y'=8,'x'=4,'c'=2] {'z'}, dimensions={0} | all-to-all | bytes 393216 | tf_op jit(solution)/shard_map/all_to_all | solution.py:94
  94.7 3.4 %collective-permute-start.4 = (bf16[8,32,384]{2,1,0:T(8,128)(2,1)S(1)}, bf16[8,32,384]{2,1,0:T(8,128)(2,1)S(1)}, u32[]{:S(2)}, u32[]{:S(2)}) collective-permute-start(bf16[8,32,384]{2,1,0:T(8,128)(2,1)S(1)} %all_to_all.16.others_0_), channel_id=1, source_target_pairs={{0,8},{8,16},{16,24},{24,32},{32,40},{40,48},{48,56},{56,0},{1,9},... | collective-permute-start | bytes 589832 | tf_op jit(solution)/shard_map/ppermute | solution.py:24
  98.0 3.7 %collective-permute-start.5 = (bf16[8,32,384]{2,1,0:T(8,128)(2,1)S(1)}, bf16[8,32,384]{2,1,0:T(8,128)(2,1)S(1)}, u32[]{:S(2)}, u32[]{:S(2)}) collective-permute-start(bf16[8,32,384]{2,1,0:T(8,128)(2,1)S(1)} %all_to_all.16.others_0_), channel_id=1, source_target_pairs={{0,56},{8,0},{16,8},{24,16},{32,24},{40,32},{48,40},{56,48},{1,57}... | collective-permute-start | bytes 589832 | tf_op jit(solution)/shard_map/ppermute | solution.py:24
  101.7 2.4 %collective-permute-done.4.others_1_ = bf16[8,32,384]{2,1,0:T(8,128)(2,1)S(1)} collective-permute-done((bf16[8,32,384]{2,1,0:T(8,128)(2,1)S(1)}, bf16[8,32,384]{2,1,0:T(8,128)(2,1)S(1)}, u32[]{:S(2)}, u32[]{:S(2)}) %collective-permute-start.4) | collective-permute-done | bytes 196640 | tf_op jit(solution)/shard_map/ppermute | solution.py:24
  104.1 2.2 %collective-permute-start.6 = (bf16[8,32,384]{2,1,0:T(8,128)(2,1)S(1)}, bf16[8,32,384]{2,1,0:T(8,128)(2,1)S(1)}, u32[]{:S(2)}, u32[]{:S(2)}) collective-permute-start(bf16[8,32,384]{2,1,0:T(8,128)(2,1)S(1)} %collective-permute-done.4.others_1_), channel_id=1, source_target_pairs={{0,8},{8,16},{16,24},{24,32},{32,40},{40,48},{48,56},{56,0},{1,9},... | collective-permute-start | bytes 589832 | tf_op jit(solution)/shard_map/ppermute | solution.py:24
  106.3 4.9 %collective-permute-start.7 = (bf16[8,32,384]{2,1,0:T(8,128)(2,1)S(1)}, bf16[8,32,384]{2,1,0:T(8,128)(2,1)}, u32[]{:S(2)}, u32[]{:S(2)}) collective-permute-start(bf16[8,32,384]{2,1,0:T(8,128)(2,1)S(1)} %collective-permute-done.5.others_2_), channel_id=1, source_target_pairs={{0,56},{8,0},{16,8},{24,16},{32,24},{40,32},{48,40},{56,48},{1,57}... | collective-permute-start | bytes 589832 | tf_op jit(solution)/shard_map/ppermute | solution.py:24
  111.1 1.7 collective-permute-done.6.others_3_
  112.8 1.9 %collective-permute-start.8 = (bf16[8,32,384]{2,1,0:T(8,128)(2,1)S(1)}, bf16[8,32,384]{2,1,0:T(8,128)(2,1)}, u32[]{:S(2)}, u32[]{:S(2)}) collective-permute-start(bf16[8,32,384]{2,1,0:T(8,128)(2,1)S(1)} %collective-permute-done.6.others_3_), channel_id=1, source_target_pairs={{0,8},{8,16},{16,24},{24,32},{32,40},{40,48},{48,56},{56,0},{1,9},... | collective-permute-start | bytes 589832 | tf_op jit(solution)/shard_map/ppermute | solution.py:24
  115.4 5.1 %collective-permute-start.9 = (bf16[8,32,384]{2,1,0:T(8,128)(2,1)}, bf16[8,32,384]{2,1,0:T(8,128)(2,1)}, u32[]{:S(2)}, u32[]{:S(2)}) collective-permute-start(bf16[8,32,384]{2,1,0:T(8,128)(2,1)} %collective-permute-done.7.others_4_), channel_id=1, source_target_pairs={{0,56},{8,0},{16,8},{24,16},{32,24},{40,32},{48,40},{56,48},{1,57}... | collective-permute-start | bytes 589832 | tf_op jit(solution)/shard_map/ppermute | solution.py:24
  120.6 1.1 collective-permute-done.8.others_5_
  121.7 1.9 %collective-permute-start.10 = (bf16[8,32,384]{2,1,0:T(8,128)(2,1)}, bf16[8,32,384]{2,1,0:T(8,128)(2,1)}, u32[]{:S(2)}, u32[]{:S(2)}) collective-permute-start(bf16[8,32,384]{2,1,0:T(8,128)(2,1)} %collective-permute-done.8.others_5_), channel_id=1, source_target_pairs={{0,8},{8,16},{16,24},{24,32},{32,40},{40,48},{48,56},{56,0},{1,9},... | collective-permute-start | bytes 589832 | tf_op jit(solution)/shard_map/ppermute | solution.py:24
  123.7 4.2 %shard_map.97 = (f32[192,384]{1,0:T(8,128)S(1)}, f32[192,384]{1,0:T(8,128)S(1)}, bf16[2048,384]{1,0:T(8,128)(2,1)}) custom-call(bf16[96,6144]{1,0:T(8,128)(2,1)S(1)} %shard_map.95.own_ref.own_in_ref.cot_ref, bf16[96,6144]{1,0:T(8,128)(2,1)S(1)} %collective-permute-done.3.far_ref.far_in_ref.cot_far_ref, ...), custom_call_target="tpu_custom_call" | custom-call | flops 905969664 | bytes 8388608 | tf_op jit(solution)/shard_map/pallas_call | solution.py:169
  127.8 8.5 %all-to-all-start.2 = ((bf16[64,32,384]{2,1,0:T(8,128)(2,1)}), bf16[64,32,384]{2,1,0:T(8,128)(2,1)}, u32[]{:S(2)}, u32[]{:S(2)}) async-start(bf16[64,32,384]{2,1,0:T(8,128)(2,1)} %bitcast.12), calls=%async_computation.2 | async-start | bytes 3145728 | tf_op jit(solution)/shard_map/all_to_all | solution.py:331
  137.3 8.3 %shard_map.99 = (f32[2,96,2048]{2,1,0:T(8,128)S(1)}, bf16[2,96,2048]{2,1,0:T(8,128)(2,1)S(1)}) custom-call(s32[1]{0:T(128)} %bitcast.row_ref, bf16[96,6144]{1,0:T(8,128)(2,1)S(1)} %shard_map.95.own_ref.own_in_ref.cot_ref, bf16[96,6144]{1,0:T(8,128)(2,1)S(1)} %collective-permute-done.3.far_ref.far_in_ref.cot_far_ref, ...), custom_call_target="tpu_custom_call" | custom-call | flops 1811939328 | bytes 16777216 | tf_op jit(solution)/shard_map/pallas_call | solution.py:246
  145.7 1.9 %collective-permute-start.11 = (bf16[2,96,2048]{2,1,0:T(8,128)(2,1)S(1)}, bf16[2,96,2048]{2,1,0:T(8,128)(2,1)S(1)}, u32[]{:S(2)}, u32[]{:S(2)}) collective-permute-start(bf16[2,96,2048]{2,1,0:T(8,128)(2,1)S(1)} %get-tuple-element.11), channel_id=1, source_target_pairs={{0,1},{1,0},{2,3},{3,2},{4,5},{5,4},{6,7},{7,6},{8,9},{9,8},{10,11... | collective-permute-start | bytes 2359304 | tf_op jit(solution)/shard_map/ppermute | solution.py:24
  147.6 2.3 %collective-permute-done.11 = bf16[2,96,2048]{2,1,0:T(8,128)(2,1)S(1)} collective-permute-done((bf16[2,96,2048]{2,1,0:T(8,128)(2,1)S(1)}, bf16[2,96,2048]{2,1,0:T(8,128)(2,1)S(1)}, u32[]{:S(2)}, u32[]{:S(2)}) %collective-permute-start.11) | collective-permute-done | bytes 786464 | tf_op jit(solution)/shard_map/ppermute | solution.py:24
  150.1 2.5 %collective-permute-start.12 = (bf16[2,24,2048]{2,1,0:T(8,128)(2,1)S(1)}, bf16[2,24,2048]{2,1,0:T(8,128)(2,1)S(1)}, u32[]{:S(2)}, u32[]{:S(2)}) collective-permute-start(bf16[2,24,2048]{2,1,0:T(8,128)(2,1)S(1)} %get-tuple-element.13), channel_id=1, source_target_pairs={{0,6},{2,0},{4,2},{6,4},{1,7},{3,1},{5,3},{7,5},{8,14},{10,8},{12,... | collective-permute-start | bytes 589832 | tf_op jit(solution)/shard_map/ppermute | solution.py:24
  152.6 4.3 %collective-permute-start.14 = (bf16[2,24,2048]{2,1,0:T(8,128)(2,1)S(1)}, bf16[2,24,2048]{2,1,0:T(8,128)(2,1)S(1)}, u32[]{:S(2)}, u32[]{:S(2)}) collective-permute-start(bf16[2,24,2048]{2,1,0:T(8,128)(2,1)S(1)} %get-tuple-element.14), channel_id=1, source_target_pairs={{0,4},{2,6},{4,0},{6,2},{1,5},{3,7},{5,1},{7,3},{8,12},{10,14},{12... | collective-permute-start | bytes 589832 | tf_op jit(solution)/shard_map/ppermute | solution.py:24
  156.9 3.7 %collective-permute-start.13 = (bf16[2,24,2048]{2,1,0:T(8,128)(2,1)S(1)}, bf16[2,24,2048]{2,1,0:T(8,128)(2,1)S(1)}, u32[]{:S(2)}, u32[]{:S(2)}) collective-permute-start(bf16[2,24,2048]{2,1,0:T(8,128)(2,1)S(1)} %get-tuple-element.15), channel_id=1, source_target_pairs={{0,2},{2,4},{4,6},{6,0},{1,3},{3,5},{5,7},{7,1},{8,10},{10,12},{12... | collective-permute-start | bytes 589832 | tf_op jit(solution)/shard_map/ppermute | solution.py:24
  160.6 3.5 %collective-permute-done.14 = bf16[2,24,2048]{2,1,0:T(8,128)(2,1)S(1)} collective-permute-done((bf16[2,24,2048]{2,1,0:T(8,128)(2,1)S(1)}, bf16[2,24,2048]{2,1,0:T(8,128)(2,1)S(1)}, u32[]{:S(2)}, u32[]{:S(2)}) %collective-permute-start.14) | collective-permute-done | bytes 196640 | tf_op jit(solution)/shard_map/ppermute | solution.py:24
  164.1 2.8 %collective-permute-done.13 = bf16[2,24,2048]{2,1,0:T(8,128)(2,1)S(1)} collective-permute-done((bf16[2,24,2048]{2,1,0:T(8,128)(2,1)S(1)}, bf16[2,24,2048]{2,1,0:T(8,128)(2,1)S(1)}, u32[]{:S(2)}, u32[]{:S(2)}) %collective-permute-start.13) | collective-permute-done | bytes 196640 | tf_op jit(solution)/shard_map/ppermute | solution.py:24
  167.6 5.8 %all-to-all-done.2.parts_ref = bf16[64,32,384]{2,1,0:T(8,128)(2,1)} async-done(((bf16[64,32,384]{2,1,0:T(8,128)(2,1)}), bf16[64,32,384]{2,1,0:T(8,128)(2,1)}, u32[]{:S(2)}, u32[]{:S(2)}) %all-to-all-start.2) | async-done | bytes 1572896 | tf_op jit(solution)/shard_map/all_to_all | solution.py:331
  173.5 2.2 %shard_map.100 = f32[32,384]{1,0:T(8,128)} custom-call(bf16[64,32,384]{2,1,0:T(8,128)(2,1)} %all-to-all-done.2.parts_ref, f32[32,384]{1,0:T(8,128)S(1)} %copy-done.2), custom_call_target="tpu_custom_call" | custom-call | tf_op jit(solution)/shard_map/pallas_call | solution.py:305
  (22 shorter events, 3.8 us)
Async XLA Ops:
  7.2 116.5 %all-gather.2.cloned.1.call-start = ((), (), s32[]{:S(2)}) async-start(), calls=%async_computation.3 | async-start | bytes 3538944 | tf_op jit(solution)/shard_map/all_gather | solution.py:323
  43.3 13.3 %collective-permute-start.2 = (bf16[24,6144]{1,0:T(8,128)(2,1)S(1)}, bf16[24,6144]{1,0:T(8,128)(2,1)S(1)}, u32[]{:S(2)}, u32[]{:S(2)}) collective-permute-start(bf16[24,6144]{1,0:T(8,128)(2,1)S(1)} %bitcast.8), channel_id=1, source_target_pairs={{0,4},{2,6},{4,0},{6,2},{1,5},{3,7},{5,1},{7,3},{8,12},{10,14},{12... | collective-permute-start | bytes 884744 | tf_op jit(solution)/shard_map/ppermute | solution.py:24
  47.4 13.0 %collective-permute-start.1 = (bf16[24,6144]{1,0:T(8,128)(2,1)S(1)}, bf16[24,6144]{1,0:T(8,128)(2,1)S(1)}, u32[]{:S(2)}, u32[]{:S(2)}) collective-permute-start(bf16[24,6144]{1,0:T(8,128)(2,1)S(1)} %bitcast.9), channel_id=1, source_target_pairs={{0,6},{2,0},{4,2},{6,4},{1,7},{3,1},{5,3},{7,5},{8,14},{10,8},{12,... | collective-permute-start | bytes 884744 | tf_op jit(solution)/shard_map/ppermute | solution.py:24
  50.7 9.7 %collective-permute-start = (bf16[24,6144]{1,0:T(8,128)(2,1)S(1)}, bf16[24,6144]{1,0:T(8,128)(2,1)S(1)}, u32[]{:S(2)}, u32[]{:S(2)}) collective-permute-start(bf16[24,6144]{1,0:T(8,128)(2,1)S(1)} %bitcast.10), channel_id=1, source_target_pairs={{0,2},{2,4},{4,6},{6,0},{1,3},{3,5},{5,7},{7,1},{8,10},{10,12},{12... | collective-permute-start | bytes 884744 | tf_op jit(solution)/shard_map/ppermute | solution.py:24
  60.5 63.1 %collective-permute-start.3 = (bf16[96,6144]{1,0:T(8,128)(2,1)S(1)}, bf16[96,6144]{1,0:T(8,128)(2,1)S(1)}, u32[]{:S(2)}, u32[]{:S(2)}) collective-permute-start(bf16[96,6144]{1,0:T(8,128)(2,1)S(1)} %shard_map.95.own_ref.own_in_ref.cot_ref), channel_id=1, source_target_pairs={{0,1},{1,0},{2,3},{3,2},{4,5},{5,4},{6,7},{7,6},{8,9},{9,8},{10,11... | collective-permute-start | bytes 3538952 | tf_op jit(solution)/shard_map/ppermute | solution.py:24
  94.7 9.4 %collective-permute-start.4 = (bf16[8,32,384]{2,1,0:T(8,128)(2,1)S(1)}, bf16[8,32,384]{2,1,0:T(8,128)(2,1)S(1)}, u32[]{:S(2)}, u32[]{:S(2)}) collective-permute-start(bf16[8,32,384]{2,1,0:T(8,128)(2,1)S(1)} %all_to_all.16.others_0_), channel_id=1, source_target_pairs={{0,8},{8,16},{16,24},{24,32},{32,40},{40,48},{48,56},{56,0},{1,9},... | collective-permute-start | bytes 589832 | tf_op jit(solution)/shard_map/ppermute | solution.py:24
  98.0 8.2 %collective-permute-start.5 = (bf16[8,32,384]{2,1,0:T(8,128)(2,1)S(1)}, bf16[8,32,384]{2,1,0:T(8,128)(2,1)S(1)}, u32[]{:S(2)}, u32[]{:S(2)}) collective-permute-start(bf16[8,32,384]{2,1,0:T(8,128)(2,1)S(1)} %all_to_all.16.others_0_), channel_id=1, source_target_pairs={{0,56},{8,0},{16,8},{24,16},{32,24},{40,32},{48,40},{56,48},{1,57}... | collective-permute-start | bytes 589832 | tf_op jit(solution)/shard_map/ppermute | solution.py:24
  104.1 8.8 %collective-permute-start.6 = (bf16[8,32,384]{2,1,0:T(8,128)(2,1)S(1)}, bf16[8,32,384]{2,1,0:T(8,128)(2,1)S(1)}, u32[]{:S(2)}, u32[]{:S(2)}) collective-permute-start(bf16[8,32,384]{2,1,0:T(8,128)(2,1)S(1)} %collective-permute-done.4.others_1_), channel_id=1, source_target_pairs={{0,8},{8,16},{16,24},{24,32},{32,40},{40,48},{48,56},{56,0},{1,9},... | collective-permute-start | bytes 589832 | tf_op jit(solution)/shard_map/ppermute | solution.py:24
  106.3 9.2 %collective-permute-start.7 = (bf16[8,32,384]{2,1,0:T(8,128)(2,1)S(1)}, bf16[8,32,384]{2,1,0:T(8,128)(2,1)}, u32[]{:S(2)}, u32[]{:S(2)}) collective-permute-start(bf16[8,32,384]{2,1,0:T(8,128)(2,1)S(1)} %collective-permute-done.5.others_2_), channel_id=1, source_target_pairs={{0,56},{8,0},{16,8},{24,16},{32,24},{40,32},{48,40},{56,48},{1,57}... | collective-permute-start | bytes 589832 | tf_op jit(solution)/shard_map/ppermute | solution.py:24
  112.8 8.9 %collective-permute-start.8 = (bf16[8,32,384]{2,1,0:T(8,128)(2,1)S(1)}, bf16[8,32,384]{2,1,0:T(8,128)(2,1)}, u32[]{:S(2)}, u32[]{:S(2)}) collective-permute-start(bf16[8,32,384]{2,1,0:T(8,128)(2,1)S(1)} %collective-permute-done.6.others_3_), channel_id=1, source_target_pairs={{0,8},{8,16},{16,24},{24,32},{32,40},{40,48},{48,56},{56,0},{1,9},... | collective-permute-start | bytes 589832 | tf_op jit(solution)/shard_map/ppermute | solution.py:24
  114.8 0.7 copy-start
  115.4 21.0 %collective-permute-start.9 = (bf16[8,32,384]{2,1,0:T(8,128)(2,1)}, bf16[8,32,384]{2,1,0:T(8,128)(2,1)}, u32[]{:S(2)}, u32[]{:S(2)}) collective-permute-start(bf16[8,32,384]{2,1,0:T(8,128)(2,1)} %collective-permute-done.7.others_4_), channel_id=1, source_target_pairs={{0,56},{8,0},{16,8},{24,16},{32,24},{40,32},{48,40},{56,48},{1,57}... | collective-permute-start | bytes 589832 | tf_op jit(solution)/shard_map/ppermute | solution.py:24
  121.7 14.7 %collective-permute-start.10 = (bf16[8,32,384]{2,1,0:T(8,128)(2,1)}, bf16[8,32,384]{2,1,0:T(8,128)(2,1)}, u32[]{:S(2)}, u32[]{:S(2)}) collective-permute-start(bf16[8,32,384]{2,1,0:T(8,128)(2,1)} %collective-permute-done.8.others_5_), channel_id=1, source_target_pairs={{0,8},{8,16},{16,24},{24,32},{32,40},{40,48},{48,56},{56,0},{1,9},... | collective-permute-start | bytes 589832 | tf_op jit(solution)/shard_map/ppermute | solution.py:24
  127.8 45.6 %all-to-all-start.2 = ((bf16[64,32,384]{2,1,0:T(8,128)(2,1)}), bf16[64,32,384]{2,1,0:T(8,128)(2,1)}, u32[]{:S(2)}, u32[]{:S(2)}) async-start(bf16[64,32,384]{2,1,0:T(8,128)(2,1)} %bitcast.12), calls=%async_computation.2 | async-start | bytes 3145728 | tf_op jit(solution)/shard_map/all_to_all | solution.py:331
  136.4 0.9 copy-start.1
  145.7 4.2 %collective-permute-start.11 = (bf16[2,96,2048]{2,1,0:T(8,128)(2,1)S(1)}, bf16[2,96,2048]{2,1,0:T(8,128)(2,1)S(1)}, u32[]{:S(2)}, u32[]{:S(2)}) collective-permute-start(bf16[2,96,2048]{2,1,0:T(8,128)(2,1)S(1)} %get-tuple-element.11), channel_id=1, source_target_pairs={{0,1},{1,0},{2,3},{3,2},{4,5},{5,4},{6,7},{7,6},{8,9},{9,8},{10,11... | collective-permute-start | bytes 2359304 | tf_op jit(solution)/shard_map/ppermute | solution.py:24
  150.0 23.4 %copy-start.2 = (f32[32,384]{1,0:T(8,128)S(1)}, f32[32,384]{1,0:T(8,128)}, u32[]{:S(2)}) copy-start(f32[32,384]{1,0:T(8,128)} %sum_ref.1) | copy-start | bytes 147460
  150.1 10.5 %collective-permute-start.12 = (bf16[2,24,2048]{2,1,0:T(8,128)(2,1)S(1)}, bf16[2,24,2048]{2,1,0:T(8,128)(2,1)S(1)}, u32[]{:S(2)}, u32[]{:S(2)}) collective-permute-start(bf16[2,24,2048]{2,1,0:T(8,128)(2,1)S(1)} %get-tuple-element.13), channel_id=1, source_target_pairs={{0,6},{2,0},{4,2},{6,4},{1,7},{3,1},{5,3},{7,5},{8,14},{10,8},{12,... | collective-permute-start | bytes 589832 | tf_op jit(solution)/shard_map/ppermute | solution.py:24
  152.6 11.5 %collective-permute-start.14 = (bf16[2,24,2048]{2,1,0:T(8,128)(2,1)S(1)}, bf16[2,24,2048]{2,1,0:T(8,128)(2,1)S(1)}, u32[]{:S(2)}, u32[]{:S(2)}) collective-permute-start(bf16[2,24,2048]{2,1,0:T(8,128)(2,1)S(1)} %get-tuple-element.14), channel_id=1, source_target_pairs={{0,4},{2,6},{4,0},{6,2},{1,5},{3,7},{5,1},{7,3},{8,12},{10,14},{12... | collective-permute-start | bytes 589832 | tf_op jit(solution)/shard_map/ppermute | solution.py:24
  156.9 10.0 %collective-permute-start.13 = (bf16[2,24,2048]{2,1,0:T(8,128)(2,1)S(1)}, bf16[2,24,2048]{2,1,0:T(8,128)(2,1)S(1)}, u32[]{:S(2)}, u32[]{:S(2)}) collective-permute-start(bf16[2,24,2048]{2,1,0:T(8,128)(2,1)S(1)} %get-tuple-element.15), channel_id=1, source_target_pairs={{0,2},{2,4},{4,6},{6,0},{1,3},{3,5},{5,7},{7,1},{8,10},{10,12},{12... | collective-permute-start | bytes 589832 | tf_op jit(solution)/shard_map/ppermute | solution.py:24
Sparse Core Ops, SparseCore 0:
  42.4 51.5 all-gather.1

commit v10 on v8

--- a/solution.py
+++ b/solution.py
@@ -41,6 +41,42 @@
     )(*[pltpu.with_memory_space_constraint(a, pltpu.HBM) for a in arrays])
 
 
+def fan_kernel(*refs):
+    *ins, out_ref, side_ref, sems = refs
+    at, loads = 0, []
+    for ref in ins:
+        cols = ref.shape[1]
+        place = side_ref.at[:, pl.ds(at, cols)]
+        loads.append(pltpu.make_async_copy(ref, place, sems.at[len(loads)]))
+        at += cols
+    stores = [
+        pltpu.make_async_copy(side_ref, out_ref.at[k], sems.at[len(loads) + k])
+        for k in range(out_ref.shape[0])
+    ]
+    for group in (loads, stores):
+        for move in group:
+            move.start()
+        for move in group:
+            move.wait()
+
+
+def fanned(count, *arrays):
+    side = (arrays[0].shape[0], sum(a.shape[1] for a in arrays))
+    hbm = pl.BlockSpec(memory_space=pltpu.HBM)
+    return pl.pallas_call(
+        fan_kernel,
+        in_specs=[hbm] * len(arrays),
+        out_specs=hbm,
+        out_shape=pltpu.HBM((count, *side), arrays[0].dtype),
+        scratch_shapes=[
+            pltpu.VMEM(side, arrays[0].dtype),
+            pltpu.SemaphoreType.DMA((count + len(arrays),)),
+        ],
+        compiler_params=pltpu.CompilerParams(vmem_limit_bytes=4 << 20),
+        cost_estimate=pl.CostEstimate(flops=1 << 20, transcendentals=0, bytes_accessed=1 << 20),
+    )(*[pltpu.with_memory_space_constraint(a, pltpu.HBM) for a in arrays])
+
+
 def stack_kernel(*refs):
     *ins, out_ref = refs
     for at, ref in enumerate(ins):
@@ -59,7 +95,7 @@
 
 
 def gather_down(down):
-    fan = copies(lax.axis_size("z"), down)
+    fan = fanned(lax.axis_size("z"), down)
     line = lax.all_to_all(fan, "z", 0, 0)
     chunks, ahead, behind = [line], line, line
     for _ in range(1, 4):
@@ -256,7 +292,7 @@
 
 def shards(later, early, cotangent, gate_w, up_w, down_w, down_grad_sum):
     rows, _ = later.shape
-    fan = copies(lax.axis_size("y"), gate_w, up_w)
+    fan = fanned(lax.axis_size("y"), gate_w, up_w)
     line = lax.all_to_all(fan, "y", 0, 0)
     line = line.reshape(-1, line.shape[-1])
     whole = lax.all_gather(line, "z", axis=0, tiled=True)

time: 162 us -> 164 us (1.012)
    pallas_call x0 -> x2, Pallas kernels: none -> 3.1 us  [fanned(): pl.pallas_call(fan_kernel, in_specs=[hbm] * len(arrays), out_specs=hbm, o...]
where the time goes in v10:
time: 164 us; the launch traced here: 163 us
  starting transfers between devices  53.5 us (33%)
  blocking collectives  44.8 us (27%)
  waiting for transfers between devices  29 us (18%)
  Pallas kernels  16.7 us (10%)
  between operations  14.3 us (9%)
  other arithmetic  2.57 us (2%)
  local copies, waits for them, and re-layouts  2.33 us (1%)
    ppermute x15, starting transfers between devices, shift(): lax.ppermute(value, axis, [(i, (i + step) % count) for i in range(count)])  45 us
    ppermute x15, waiting for transfers between devices, shift(): lax.ppermute(value, axis, [(i, (i + step) % count) for i in range(count)])  24.1 us
    all_to_all x1, blocking collectives, gather_down(): line = lax.all_to_all(fan, 'z', 0, 0)  23.9 us
    all_to_all x1, blocking collectives, shards(): line = lax.all_to_all(fan, 'y', 0, 0)  20.9 us
    all_to_all x1, starting transfers between devices, shards(): received = lax.all_to_all(down_grad.reshape(-1, *gate_w.shape), FS, 0, 0)  8.48 us
    pallas_call x1, Pallas kernels, rest_part(): pl.pallas_call(rest_kernel, grid=(2 * BLOCKS,), in_specs=[pl.BlockSpec(me...  8.31 us
    all_to_all x1, waiting for transfers between devices, shards(): received = lax.all_to_all(down_grad.reshape(-1, *gate_w.shape), FS, 0, 0)  4.93 us
    pallas_call x1, Pallas kernels, early_part(): pl.pallas_call(early_kernel, in_specs=[vmem, vmem, hbm], out_specs=[vmem,...  4.16 us
  transfers between devices with their start and end apart: 17, of which 11 were waited for; matrix products, arithmetic and copies ran while one was open for 1% of the time, Pallas kernels for 9%

profile of v10, /device:TPU:8, one launch (start us, length us, event | category | flops | bytes accessed | tf_op | source)
XLA Modules:
  0.0 163.2 jit_solution(5437015309788333484)
XLA Ops:
  7.2 1.6 shard_map.96
  8.8 20.9 %all_to_all.15 = bf16[8,32,768]{2,1,0:T(8,128)(2,1)} all-to-all(bf16[8,32,768]{2,1,0:T(8,128)(2,1)} %shard_map.96), channel_id=1, replica_groups=mesh['z'=8,'y'=8,'x'=4,'c'=2] {'y'}, dimensions={0} | all-to-all | bytes 786432 | tf_op jit(solution)/shard_map/all_to_all | solution.py:296
  30.7 4.9 %collective-permute-start.2 = (bf16[24,6144]{1,0:T(8,128)(2,1)S(1)}, bf16[24,6144]{1,0:T(8,128)(2,1)S(1)}, u32[]{:S(2)}, u32[]{:S(2)}) collective-permute-start(bf16[24,6144]{1,0:T(8,128)(2,1)S(1)} %bitcast.8), channel_id=1, source_target_pairs={{0,4},{2,6},{4,0},{6,2},{1,5},{3,7},{5,1},{7,3},{8,12},{10,14},{12... | collective-permute-start | bytes 884744 | tf_op jit(solution)/shard_map/ppermute | solution.py:22
  35.7 3.0 %collective-permute-start.1 = (bf16[24,6144]{1,0:T(8,128)(2,1)S(1)}, bf16[24,6144]{1,0:T(8,128)(2,1)S(1)}, u32[]{:S(2)}, u32[]{:S(2)}) collective-permute-start(bf16[24,6144]{1,0:T(8,128)(2,1)S(1)} %bitcast.9), channel_id=1, source_target_pairs={{0,6},{2,0},{4,2},{6,4},{1,7},{3,1},{5,3},{7,5},{8,14},{10,8},{12,... | collective-permute-start | bytes 884744 | tf_op jit(solution)/shard_map/ppermute | solution.py:22
  38.7 2.8 %collective-permute-start = (bf16[24,6144]{1,0:T(8,128)(2,1)S(1)}, bf16[24,6144]{1,0:T(8,128)(2,1)S(1)}, u32[]{:S(2)}, u32[]{:S(2)}) collective-permute-start(bf16[24,6144]{1,0:T(8,128)(2,1)S(1)} %bitcast.10), channel_id=1, source_target_pairs={{0,2},{2,4},{4,6},{6,0},{1,3},{3,5},{5,7},{7,1},{8,10},{10,12},{12... | collective-permute-start | bytes 884744 | tf_op jit(solution)/shard_map/ppermute | solution.py:22
  41.7 6.2 %collective-permute-done.1.refs_2_ = bf16[24,6144]{1,0:T(8,128)(2,1)S(1)} collective-permute-done((bf16[24,6144]{1,0:T(8,128)(2,1)S(1)}, bf16[24,6144]{1,0:T(8,128)(2,1)S(1)}, u32[]{:S(2)}, u32[]{:S(2)}) %collective-permute-start.1) | collective-permute-done | bytes 294944 | tf_op jit(solution)/shard_map/ppermute | solution.py:22
  48.8 1.9 %collective-permute-start.3 = (bf16[96,6144]{1,0:T(8,128)(2,1)S(1)}, bf16[96,6144]{1,0:T(8,128)(2,1)S(1)}, u32[]{:S(2)}, u32[]{:S(2)}) collective-permute-start(bf16[96,6144]{1,0:T(8,128)(2,1)S(1)} %shard_map.95.own_ref.own_in_ref.cot_ref), channel_id=1, source_target_pairs={{0,1},{1,0},{2,3},{3,2},{4,5},{5,4},{6,7},{7,6},{8,9},{9,8},{10,11... | collective-permute-start | bytes 3538952 | tf_op jit(solution)/shard_map/ppermute | solution.py:22
  50.7 1.5 shard_map.98
  52.2 23.9 %all_to_all.16.others_0_ = bf16[8,32,384]{2,1,0:T(8,128)(2,1)S(1)} all-to-all(bf16[8,32,384]{2,1,0:T(8,128)(2,1)} %shard_map.98), channel_id=1, replica_groups=mesh['z'=8,'y'=8,'x'=4,'c'=2] {'z'}, dimensions={0} | all-to-all | bytes 393216 | tf_op jit(solution)/shard_map/all_to_all | solution.py:99
  76.1 2.0 %collective-permute-start.4 = (bf16[8,32,384]{2,1,0:T(8,128)(2,1)S(1)}, bf16[8,32,384]{2,1,0:T(8,128)(2,1)S(1)}, u32[]{:S(2)}, u32[]{:S(2)}) collective-permute-start(bf16[8,32,384]{2,1,0:T(8,128)(2,1)S(1)} %all_to_all.16.others_0_), channel_id=1, source_target_pairs={{0,8},{8,16},{16,24},{24,32},{32,40},{40,48},{48,56},{56,0},{1,9},... | collective-permute-start | bytes 589832 | tf_op jit(solution)/shard_map/ppermute | solution.py:22
  78.1 3.9 %collective-permute-start.5 = (bf16[8,32,384]{2,1,0:T(8,128)(2,1)S(1)}, bf16[8,32,384]{2,1,0:T(8,128)(2,1)S(1)}, u32[]{:S(2)}, u32[]{:S(2)}) collective-permute-start(bf16[8,32,384]{2,1,0:T(8,128)(2,1)S(1)} %all_to_all.16.others_0_), channel_id=1, source_target_pairs={{0,56},{8,0},{16,8},{24,16},{32,24},{40,32},{48,40},{56,48},{1,57}... | collective-permute-start | bytes 589832 | tf_op jit(solution)/shard_map/ppermute | solution.py:22
  82.0 2.7 %collective-permute-done.4.others_1_ = bf16[8,32,384]{2,1,0:T(8,128)(2,1)S(1)} collective-permute-done((bf16[8,32,384]{2,1,0:T(8,128)(2,1)S(1)}, bf16[8,32,384]{2,1,0:T(8,128)(2,1)S(1)}, u32[]{:S(2)}, u32[]{:S(2)}) %collective-permute-start.4) | collective-permute-done | bytes 196640 | tf_op jit(solution)/shard_map/ppermute | solution.py:22
  84.6 2.2 %collective-permute-start.6 = (bf16[8,32,384]{2,1,0:T(8,128)(2,1)S(1)}, bf16[8,32,384]{2,1,0:T(8,128)(2,1)S(1)}, u32[]{:S(2)}, u32[]{:S(2)}) collective-permute-start(bf16[8,32,384]{2,1,0:T(8,128)(2,1)S(1)} %collective-permute-done.4.others_1_), channel_id=1, source_target_pairs={{0,8},{8,16},{16,24},{24,32},{32,40},{40,48},{48,56},{56,0},{1,9},... | collective-permute-start | bytes 589832 | tf_op jit(solution)/shard_map/ppermute | solution.py:22
  86.8 4.2 %collective-permute-start.7 = (bf16[8,32,384]{2,1,0:T(8,128)(2,1)S(1)}, bf16[8,32,384]{2,1,0:T(8,128)(2,1)}, u32[]{:S(2)}, u32[]{:S(2)}) collective-permute-start(bf16[8,32,384]{2,1,0:T(8,128)(2,1)S(1)} %collective-permute-done.5.others_2_), channel_id=1, source_target_pairs={{0,56},{8,0},{16,8},{24,16},{32,24},{40,32},{48,40},{56,48},{1,57}... | collective-permute-start | bytes 589832 | tf_op jit(solution)/shard_map/ppermute | solution.py:22
  91.1 2.1 %collective-permute-done.6.others_3_ = bf16[8,32,384]{2,1,0:T(8,128)(2,1)S(1)} collective-permute-done((bf16[8,32,384]{2,1,0:T(8,128)(2,1)S(1)}, bf16[8,32,384]{2,1,0:T(8,128)(2,1)S(1)}, u32[]{:S(2)}, u32[]{:S(2)}) %collective-permute-start.6) | collective-permute-done | bytes 196640 | tf_op jit(solution)/shard_map/ppermute | solution.py:22
  93.2 1.9 %collective-permute-start.8 = (bf16[8,32,384]{2,1,0:T(8,128)(2,1)S(1)}, bf16[8,32,384]{2,1,0:T(8,128)(2,1)}, u32[]{:S(2)}, u32[]{:S(2)}) collective-permute-start(bf16[8,32,384]{2,1,0:T(8,128)(2,1)S(1)} %collective-permute-done.6.others_3_), channel_id=1, source_target_pairs={{0,8},{8,16},{16,24},{24,32},{32,40},{40,48},{48,56},{56,0},{1,9},... | collective-permute-start | bytes 589832 | tf_op jit(solution)/shard_map/ppermute | solution.py:22
  95.8 4.8 %collective-permute-start.9 = (bf16[8,32,384]{2,1,0:T(8,128)(2,1)}, bf16[8,32,384]{2,1,0:T(8,128)(2,1)}, u32[]{:S(2)}, u32[]{:S(2)}) collective-permute-start(bf16[8,32,384]{2,1,0:T(8,128)(2,1)} %collective-permute-done.7.others_4_), channel_id=1, source_target_pairs={{0,56},{8,0},{16,8},{24,16},{32,24},{40,32},{48,40},{56,48},{1,57}... | collective-permute-start | bytes 589832 | tf_op jit(solution)/shard_map/ppermute | solution.py:22
  100.6 1.1 collective-permute-done.8.others_5_
  101.7 1.9 %collective-permute-start.10 = (bf16[8,32,384]{2,1,0:T(8,128)(2,1)}, bf16[8,32,384]{2,1,0:T(8,128)(2,1)}, u32[]{:S(2)}, u32[]{:S(2)}) collective-permute-start(bf16[8,32,384]{2,1,0:T(8,128)(2,1)} %collective-permute-done.8.others_5_), channel_id=1, source_target_pairs={{0,8},{8,16},{16,24},{24,32},{32,40},{40,48},{48,56},{56,0},{1,9},... | collective-permute-start | bytes 589832 | tf_op jit(solution)/shard_map/ppermute | solution.py:22
  103.7 4.2 %shard_map.97 = (f32[192,384]{1,0:T(8,128)S(1)}, f32[192,384]{1,0:T(8,128)S(1)}, bf16[2048,384]{1,0:T(8,128)(2,1)}) custom-call(bf16[96,6144]{1,0:T(8,128)(2,1)S(1)} %shard_map.95.own_ref.own_in_ref.cot_ref, bf16[96,6144]{1,0:T(8,128)(2,1)S(1)} %collective-permute-done.3.far_ref.far_in_ref.cot_far_ref, ...), custom_call_target="tpu_custom_call" | custom-call | flops 905969664 | bytes 8388608 | tf_op jit(solution)/shard_map/pallas_call | solution.py:174
  107.9 8.5 %all-to-all-start.2 = ((bf16[64,32,384]{2,1,0:T(8,128)(2,1)}), bf16[64,32,384]{2,1,0:T(8,128)(2,1)}, u32[]{:S(2)}, u32[]{:S(2)}) async-start(bf16[64,32,384]{2,1,0:T(8,128)(2,1)} %bitcast.12), calls=%async_computation.2 | async-start | bytes 3145728 | tf_op jit(solution)/shard_map/all_to_all | solution.py:306
  117.3 8.3 %shard_map.99 = (f32[2,96,2048]{2,1,0:T(8,128)S(1)}, bf16[2,96,2048]{2,1,0:T(8,128)(2,1)S(1)}) custom-call(s32[1]{0:T(128)} %bitcast.row_ref, bf16[96,6144]{1,0:T(8,128)(2,1)S(1)} %shard_map.95.own_ref.own_in_ref.cot_ref, bf16[96,6144]{1,0:T(8,128)(2,1)S(1)} %collective-permute-done.3.far_ref.far_in_ref.cot_far_ref, ...), custom_call_target="tpu_custom_call" | custom-call | flops 1811939328 | bytes 16777216 | tf_op jit(solution)/shard_map/pallas_call | solution.py:251
  125.6 1.9 %collective-permute-start.11 = (bf16[2,96,2048]{2,1,0:T(8,128)(2,1)S(1)}, bf16[2,96,2048]{2,1,0:T(8,128)(2,1)S(1)}, u32[]{:S(2)}, u32[]{:S(2)}) collective-permute-start(bf16[2,96,2048]{2,1,0:T(8,128)(2,1)S(1)} %get-tuple-element.11), channel_id=1, source_target_pairs={{0,1},{1,0},{2,3},{3,2},{4,5},{5,4},{6,7},{7,6},{8,9},{9,8},{10,11... | collective-permute-start | bytes 2359304 | tf_op jit(solution)/shard_map/ppermute | solution.py:22
  127.6 2.3 %collective-permute-done.11 = bf16[2,96,2048]{2,1,0:T(8,128)(2,1)S(1)} collective-permute-done((bf16[2,96,2048]{2,1,0:T(8,128)(2,1)S(1)}, bf16[2,96,2048]{2,1,0:T(8,128)(2,1)S(1)}, u32[]{:S(2)}, u32[]{:S(2)}) %collective-permute-start.11) | collective-permute-done | bytes 786464 | tf_op jit(solution)/shard_map/ppermute | solution.py:22
  130.1 4.0 %collective-permute-start.12 = (bf16[2,24,2048]{2,1,0:T(8,128)(2,1)S(1)}, bf16[2,24,2048]{2,1,0:T(8,128)(2,1)S(1)}, u32[]{:S(2)}, u32[]{:S(2)}) collective-permute-start(bf16[2,24,2048]{2,1,0:T(8,128)(2,1)S(1)} %get-tuple-element.13), channel_id=1, source_target_pairs={{0,6},{2,0},{4,2},{6,4},{1,7},{3,1},{5,3},{7,5},{8,14},{10,8},{12,... | collective-permute-start | bytes 589832 | tf_op jit(solution)/shard_map/ppermute | solution.py:22
  134.0 2.7 %collective-permute-start.14 = (bf16[2,24,2048]{2,1,0:T(8,128)(2,1)S(1)}, bf16[2,24,2048]{2,1,0:T(8,128)(2,1)S(1)}, u32[]{:S(2)}, u32[]{:S(2)}) collective-permute-start(bf16[2,24,2048]{2,1,0:T(8,128)(2,1)S(1)} %get-tuple-element.14), channel_id=1, source_target_pairs={{0,4},{2,6},{4,0},{6,2},{1,5},{3,7},{5,1},{7,3},{8,12},{10,14},{12... | collective-permute-start | bytes 589832 | tf_op jit(solution)/shard_map/ppermute | solution.py:22
  136.8 2.8 %collective-permute-start.13 = (bf16[2,24,2048]{2,1,0:T(8,128)(2,1)S(1)}, bf16[2,24,2048]{2,1,0:T(8,128)(2,1)S(1)}, u32[]{:S(2)}, u32[]{:S(2)}) collective-permute-start(bf16[2,24,2048]{2,1,0:T(8,128)(2,1)S(1)} %get-tuple-element.15), channel_id=1, source_target_pairs={{0,2},{2,4},{4,6},{6,0},{1,3},{3,5},{5,7},{7,1},{8,10},{10,12},{12... | collective-permute-start | bytes 589832 | tf_op jit(solution)/shard_map/ppermute | solution.py:22
  139.5 3.2 %collective-permute-done.12 = bf16[2,24,2048]{2,1,0:T(8,128)(2,1)S(1)} collective-permute-done((bf16[2,24,2048]{2,1,0:T(8,128)(2,1)S(1)}, bf16[2,24,2048]{2,1,0:T(8,128)(2,1)S(1)}, u32[]{:S(2)}, u32[]{:S(2)}) %collective-permute-start.12) | collective-permute-done | bytes 196640 | tf_op jit(solution)/shard_map/ppermute | solution.py:22
  142.7 2.5 %collective-permute-done.14 = bf16[2,24,2048]{2,1,0:T(8,128)(2,1)S(1)} collective-permute-done((bf16[2,24,2048]{2,1,0:T(8,128)(2,1)S(1)}, bf16[2,24,2048]{2,1,0:T(8,128)(2,1)S(1)}, u32[]{:S(2)}, u32[]{:S(2)}) %collective-permute-start.14) | collective-permute-done | bytes 196640 | tf_op jit(solution)/shard_map/ppermute | solution.py:22
  145.2 3.1 %collective-permute-done.13 = bf16[2,24,2048]{2,1,0:T(8,128)(2,1)S(1)} collective-permute-done((bf16[2,24,2048]{2,1,0:T(8,128)(2,1)S(1)}, bf16[2,24,2048]{2,1,0:T(8,128)(2,1)S(1)}, u32[]{:S(2)}, u32[]{:S(2)}) %collective-permute-start.13) | collective-permute-done | bytes 196640 | tf_op jit(solution)/shard_map/ppermute | solution.py:22
  149.1 4.9 %all-to-all-done.2 = bf16[64,32,384]{2,1,0:T(8,128)(2,1)} async-done(((bf16[64,32,384]{2,1,0:T(8,128)(2,1)}), bf16[64,32,384]{2,1,0:T(8,128)(2,1)}, u32[]{:S(2)}, u32[]{:S(2)}) %all-to-all-start.2) | async-done | bytes 1572896 | tf_op jit(solution)/shard_map/all_to_all | solution.py:306
  154.0 1.7 %convert_reduce_fusion = f32[32,384]{1,0:T(8,128)S(1)} fusion(bf16[64,32,384]{2,1,0:T(8,128)(2,1)} %all-to-all-done.2), kind=kLoop, calls=%fused_computation | loop fusion | flops 1560576 | bytes 1622016 | tf_op jit(solution)/shard_map/reduce_sum | solution.py:311
  (23 shorter events, 5.3 us)
Async XLA Ops:
  7.2 96.5 %all-gather.2.cloned.1.call-start = ((), (), s32[]{:S(2)}) async-start(), calls=%async_computation.3 | async-start | bytes 3538944 | tf_op jit(solution)/shard_map/all_gather | solution.py:298
  30.7 11.0 %collective-permute-start.2 = (bf16[24,6144]{1,0:T(8,128)(2,1)S(1)}, bf16[24,6144]{1,0:T(8,128)(2,1)S(1)}, u32[]{:S(2)}, u32[]{:S(2)}) collective-permute-start(bf16[24,6144]{1,0:T(8,128)(2,1)S(1)} %bitcast.8), channel_id=1, source_target_pairs={{0,4},{2,6},{4,0},{6,2},{1,5},{3,7},{5,1},{7,3},{8,12},{10,14},{12... | collective-permute-start | bytes 884744 | tf_op jit(solution)/shard_map/ppermute | solution.py:22
  35.7 12.3 %collective-permute-start.1 = (bf16[24,6144]{1,0:T(8,128)(2,1)S(1)}, bf16[24,6144]{1,0:T(8,128)(2,1)S(1)}, u32[]{:S(2)}, u32[]{:S(2)}) collective-permute-start(bf16[24,6144]{1,0:T(8,128)(2,1)S(1)} %bitcast.9), channel_id=1, source_target_pairs={{0,6},{2,0},{4,2},{6,4},{1,7},{3,1},{5,3},{7,5},{8,14},{10,8},{12,... | collective-permute-start | bytes 884744 | tf_op jit(solution)/shard_map/ppermute | solution.py:22
  38.7 10.0 %collective-permute-start = (bf16[24,6144]{1,0:T(8,128)(2,1)S(1)}, bf16[24,6144]{1,0:T(8,128)(2,1)S(1)}, u32[]{:S(2)}, u32[]{:S(2)}) collective-permute-start(bf16[24,6144]{1,0:T(8,128)(2,1)S(1)} %bitcast.10), channel_id=1, source_target_pairs={{0,2},{2,4},{4,6},{6,0},{1,3},{3,5},{5,7},{7,1},{8,10},{10,12},{12... | collective-permute-start | bytes 884744 | tf_op jit(solution)/shard_map/ppermute | solution.py:22
  48.8 54.9 %collective-permute-start.3 = (bf16[96,6144]{1,0:T(8,128)(2,1)S(1)}, bf16[96,6144]{1,0:T(8,128)(2,1)S(1)}, u32[]{:S(2)}, u32[]{:S(2)}) collective-permute-start(bf16[96,6144]{1,0:T(8,128)(2,1)S(1)} %shard_map.95.own_ref.own_in_ref.cot_ref), channel_id=1, source_target_pairs={{0,1},{1,0},{2,3},{3,2},{4,5},{5,4},{6,7},{7,6},{8,9},{9,8},{10,11... | collective-permute-start | bytes 3538952 | tf_op jit(solution)/shard_map/ppermute | solution.py:22
  76.1 8.5 %collective-permute-start.4 = (bf16[8,32,384]{2,1,0:T(8,128)(2,1)S(1)}, bf16[8,32,384]{2,1,0:T(8,128)(2,1)S(1)}, u32[]{:S(2)}, u32[]{:S(2)}) collective-permute-start(bf16[8,32,384]{2,1,0:T(8,128)(2,1)S(1)} %all_to_all.16.others_0_), channel_id=1, source_target_pairs={{0,8},{8,16},{16,24},{24,32},{32,40},{40,48},{48,56},{56,0},{1,9},... | collective-permute-start | bytes 589832 | tf_op jit(solution)/shard_map/ppermute | solution.py:22
  78.1 8.7 %collective-permute-start.5 = (bf16[8,32,384]{2,1,0:T(8,128)(2,1)S(1)}, bf16[8,32,384]{2,1,0:T(8,128)(2,1)S(1)}, u32[]{:S(2)}, u32[]{:S(2)}) collective-permute-start(bf16[8,32,384]{2,1,0:T(8,128)(2,1)S(1)} %all_to_all.16.others_0_), channel_id=1, source_target_pairs={{0,56},{8,0},{16,8},{24,16},{32,24},{40,32},{48,40},{56,48},{1,57}... | collective-permute-start | bytes 589832 | tf_op jit(solution)/shard_map/ppermute | solution.py:22
  84.6 8.5 %collective-permute-start.6 = (bf16[8,32,384]{2,1,0:T(8,128)(2,1)S(1)}, bf16[8,32,384]{2,1,0:T(8,128)(2,1)S(1)}, u32[]{:S(2)}, u32[]{:S(2)}) collective-permute-start(bf16[8,32,384]{2,1,0:T(8,128)(2,1)S(1)} %collective-permute-done.4.others_1_), channel_id=1, source_target_pairs={{0,8},{8,16},{16,24},{24,32},{32,40},{40,48},{48,56},{56,0},{1,9},... | collective-permute-start | bytes 589832 | tf_op jit(solution)/shard_map/ppermute | solution.py:22
  86.8 8.9 %collective-permute-start.7 = (bf16[8,32,384]{2,1,0:T(8,128)(2,1)S(1)}, bf16[8,32,384]{2,1,0:T(8,128)(2,1)}, u32[]{:S(2)}, u32[]{:S(2)}) collective-permute-start(bf16[8,32,384]{2,1,0:T(8,128)(2,1)S(1)} %collective-permute-done.5.others_2_), channel_id=1, source_target_pairs={{0,56},{8,0},{16,8},{24,16},{32,24},{40,32},{48,40},{56,48},{1,57}... | collective-permute-start | bytes 589832 | tf_op jit(solution)/shard_map/ppermute | solution.py:22
  93.2 8.6 %collective-permute-start.8 = (bf16[8,32,384]{2,1,0:T(8,128)(2,1)S(1)}, bf16[8,32,384]{2,1,0:T(8,128)(2,1)}, u32[]{:S(2)}, u32[]{:S(2)}) collective-permute-start(bf16[8,32,384]{2,1,0:T(8,128)(2,1)S(1)} %collective-permute-done.6.others_3_), channel_id=1, source_target_pairs={{0,8},{8,16},{16,24},{24,32},{32,40},{40,48},{48,56},{56,0},{1,9},... | collective-permute-start | bytes 589832 | tf_op jit(solution)/shard_map/ppermute | solution.py:22
  95.1 0.7 copy-start
  95.8 20.6 %collective-permute-start.9 = (bf16[8,32,384]{2,1,0:T(8,128)(2,1)}, bf16[8,32,384]{2,1,0:T(8,128)(2,1)}, u32[]{:S(2)}, u32[]{:S(2)}) collective-permute-start(bf16[8,32,384]{2,1,0:T(8,128)(2,1)} %collective-permute-done.7.others_4_), channel_id=1, source_target_pairs={{0,56},{8,0},{16,8},{24,16},{32,24},{40,32},{48,40},{56,48},{1,57}... | collective-permute-start | bytes 589832 | tf_op jit(solution)/shard_map/ppermute | solution.py:22
  101.7 14.6 %collective-permute-start.10 = (bf16[8,32,384]{2,1,0:T(8,128)(2,1)}, bf16[8,32,384]{2,1,0:T(8,128)(2,1)}, u32[]{:S(2)}, u32[]{:S(2)}) collective-permute-start(bf16[8,32,384]{2,1,0:T(8,128)(2,1)} %collective-permute-done.8.others_5_), channel_id=1, source_target_pairs={{0,8},{8,16},{16,24},{24,32},{32,40},{40,48},{48,56},{56,0},{1,9},... | collective-permute-start | bytes 589832 | tf_op jit(solution)/shard_map/ppermute | solution.py:22
  107.9 46.2 %all-to-all-start.2 = ((bf16[64,32,384]{2,1,0:T(8,128)(2,1)}), bf16[64,32,384]{2,1,0:T(8,128)(2,1)}, u32[]{:S(2)}, u32[]{:S(2)}) async-start(bf16[64,32,384]{2,1,0:T(8,128)(2,1)} %bitcast.12), calls=%async_computation.2 | async-start | bytes 3145728 | tf_op jit(solution)/shard_map/all_to_all | solution.py:306
  116.4 0.9 copy-start.1
  125.6 4.2 %collective-permute-start.11 = (bf16[2,96,2048]{2,1,0:T(8,128)(2,1)S(1)}, bf16[2,96,2048]{2,1,0:T(8,128)(2,1)S(1)}, u32[]{:S(2)}, u32[]{:S(2)}) collective-permute-start(bf16[2,96,2048]{2,1,0:T(8,128)(2,1)S(1)} %get-tuple-element.11), channel_id=1, source_target_pairs={{0,1},{1,0},{2,3},{3,2},{4,5},{5,4},{6,7},{7,6},{8,9},{9,8},{10,11... | collective-permute-start | bytes 2359304 | tf_op jit(solution)/shard_map/ppermute | solution.py:22
  130.0 25.6 %copy-start.2 = (f32[32,384]{1,0:T(8,128)S(1)}, f32[32,384]{1,0:T(8,128)}, u32[]{:S(2)}) copy-start(f32[32,384]{1,0:T(8,128)} %param.13) | copy-start | bytes 147460
  130.1 12.7 %collective-permute-start.12 = (bf16[2,24,2048]{2,1,0:T(8,128)(2,1)S(1)}, bf16[2,24,2048]{2,1,0:T(8,128)(2,1)S(1)}, u32[]{:S(2)}, u32[]{:S(2)}) collective-permute-start(bf16[2,24,2048]{2,1,0:T(8,128)(2,1)S(1)} %get-tuple-element.13), channel_id=1, source_target_pairs={{0,6},{2,0},{4,2},{6,4},{1,7},{3,1},{5,3},{7,5},{8,14},{10,8},{12,... | collective-permute-start | bytes 589832 | tf_op jit(solution)/shard_map/ppermute | solution.py:22
  134.0 11.2 %collective-permute-start.14 = (bf16[2,24,2048]{2,1,0:T(8,128)(2,1)S(1)}, bf16[2,24,2048]{2,1,0:T(8,128)(2,1)S(1)}, u32[]{:S(2)}, u32[]{:S(2)}) collective-permute-start(bf16[2,24,2048]{2,1,0:T(8,128)(2,1)S(1)} %get-tuple-element.14), channel_id=1, source_target_pairs={{0,4},{2,6},{4,0},{6,2},{1,5},{3,7},{5,1},{7,3},{8,12},{10,14},{12... | collective-permute-start | bytes 589832 | tf_op jit(solution)/shard_map/ppermute | solution.py:22
  136.8 11.6 %collective-permute-start.13 = (bf16[2,24,2048]{2,1,0:T(8,128)(2,1)S(1)}, bf16[2,24,2048]{2,1,0:T(8,128)(2,1)S(1)}, u32[]{:S(2)}, u32[]{:S(2)}) collective-permute-start(bf16[2,24,2048]{2,1,0:T(8,128)(2,1)S(1)} %get-tuple-element.15), channel_id=1, source_target_pairs={{0,2},{2,4},{4,6},{6,0},{1,3},{3,5},{5,7},{7,1},{8,10},{10,12},{12... | collective-permute-start | bytes 589832 | tf_op jit(solution)/shard_map/ppermute | solution.py:22
Sparse Core Ops, SparseCore 0:
  29.8 52.8 all-gather.1
